TPU v7x, 512 devices: a whole 4x4x16 slice. The times are simulated.
512 devices in a mesh: dp: 4 (over x), kv: 64 (over z, y), tp: 2 (over core).
Axes of the slice: x: 4, y: 4, z: 16, core: 2. Of those that a mesh axis runs over, the one named last changes fastest.
Arguments:
- tokens: bfloat16 [65536, 4096], P(('dp', 'kv')), parts along dimension 0, may hold values from -16 to 16
- query_weight: bfloat16 [4096, 1024], P('kv', 'tp'), may hold values from -0.09375 to 0.09375
- key_weight: bfloat16 [4096, 256], P('kv', 'tp'), may hold values from -0.09375 to 0.09375
- value_weight: bfloat16 [4096, 256], P('kv', 'tp'), may hold values from -0.09375 to 0.09375
- out_weight: bfloat16 [1024, 4096], P('kv', 'tp'), may hold values from -1.5 to 1.5
- chosen: int32 [2048, 16], P(('dp', 'kv')), parts along dimension 0, may hold values from -1 to 511, as said below
- live_length: int32 [4], P('dp'), parts along dimension 0, may hold values from 2048 to 16384
Outputs:
- mixed: bfloat16 [65536, 4096], P(('dp', 'kv'), 'tp'), parts along dimension 0
There are 4 independent parts, one for each index of `dp`. A program takes and returns all parts, laid end to end along the dimension named above; an argument that names none is the same for every part. Nothing has to cross between parts.
Inputs may be any that keep to these rules, and one draw needn't show every extreme that they name: `chosen`: row j lists 16 entries: entry 0 is j itself, the others are distinct blocks before j, or -1 for unused entries. The query blocks of one device together read at most 2 distinct blocks held by any one other device, and some device reads 2 of another's in every draw.
All inputs are finite; a program needn't handle non-finite values.
Results may differ from a plain program's by a relative error of at most 0.0085.
Values may be sent and summed in bfloat16 or wider, within the bound.
No kernel may reach another device: no remote copies, remote signals or barrier semaphores. Data moves between devices by JAX's collectives and lax.ppermute only.
A program may use at most 64 MiB of HBM per device.

v0:
```python
import jax
import jax.numpy as jnp
from jax import lax
from jax.experimental import pallas as pl
from jax.experimental.pallas import tpu as pltpu
from jax.sharding import Mesh
from jax.sharding import PartitionSpec as P


HD = 128
BLOCK = 32
CAP = 2
NEVER = 1 << 30
KV = ("kv_0", "kv_1")
DP_KV = ("dp", "kv_0", "kv_1")
F32 = jnp.float32
BF16 = jnp.bfloat16


def call(kernel, out_shape, *args, scratch=(), flops=0):
    spaces = [
        pl.BlockSpec(memory_space=pltpu.SMEM if a.dtype == jnp.int32 and a.ndim < 3 else pltpu.VMEM)
        for a in args
    ]
    return pl.pallas_call(
        kernel,
        out_shape=out_shape,
        in_specs=spaces,
        out_specs=pl.BlockSpec(memory_space=pltpu.VMEM),
        scratch_shapes=list(scratch),
        compiler_params=pltpu.CompilerParams(vmem_limit_bytes=40 << 20),
        cost_estimate=pl.CostEstimate(flops=flops, bytes_accessed=0, transcendentals=0),
    )(*args)


def copy_for_each(shard, axis):
    count = lax.axis_size(axis)
    return lax.all_to_all(
        jnp.broadcast_to(shard[None], (count, *shard.shape)), axis, 0, 0, tiled=True
    )


def from_ahead(x, axis, step):
    n = lax.axis_size(axis)
    return lax.ppermute(x, axis, [((i + step) % n, i) for i in range(n)])


def spread(x, axis):
    steps = range(1, lax.axis_size(axis))
    return [x, *(from_ahead(x, axis, s) for s in steps)]


def after(*values):
    return lax.optimization_barrier(values)


def slots_wanted(chosen, owners, per_dev, me):
    ids = owners[:, None] * per_dev + jnp.arange(per_dev, dtype=jnp.int32)[None, :]
    hits = chosen.reshape(-1)[:, None, None] == ids[None]
    needed = jnp.any(hits, axis=0) & (owners != me)[:, None]
    ranks = jnp.cumsum(needed.astype(jnp.int32), axis=1)
    local_ids = jnp.arange(per_dev, dtype=jnp.int32)[None, :]
    lists = []
    for slot in range(CAP):
        marked = needed & (ranks == slot + 1)
        found = jnp.any(marked, axis=1)
        lists.append(jnp.where(found, jnp.sum(jnp.where(marked, local_ids, 0), axis=1), -1))
    return jnp.stack(lists, axis=1)


def project_pair(tokens, every):
    planes, wide, tall, both, _ = every.shape
    small = both // 2
    deep = planes * wide * small

    def kernel(t_ref, w_ref, o_ref):
        total = jnp.zeros(o_ref.shape, F32)
        for z in range(tall):
            lines = [(x, y) for y in range(wide) for x in range(planes)]
            keys = jnp.concatenate([w_ref[x, y, z, :small] for x, y in lines], axis=0)
            values = jnp.concatenate([w_ref[x, y, z, small:] for x, y in lines], axis=0)
            total += jnp.dot(
                t_ref[:, z * deep : (z + 1) * deep],
                jnp.concatenate([keys, values], axis=1),
                preferred_element_type=F32,
            )
        o_ref[...] = total.astype(BF16)

    out = jax.ShapeDtypeStruct((tokens.shape[0], 2 * HD), BF16)
    flops = 2 * tokens.size * 2 * HD
    return call(kernel, out, tokens, every, flops=flops)


def project_queries(tokens, pieces, tile):
    def kernel(t_ref, *refs):
        o_ref = refs[-1]
        for i in range(0, len(pieces), 2):
            w = jnp.concatenate([refs[i][...], refs[i + 1][...]], axis=1)
            o_ref[:, i * HD : (i + 2) * HD] = jnp.dot(
                t_ref[...], w, preferred_element_type=F32
            ).astype(BF16)

    width = len(pieces) * HD
    out = jax.ShapeDtypeStruct((tokens.shape[0], width), BF16)
    flops = 2 * tokens.size * width
    return call(kernel, out, tokens, *pieces, tile, flops=flops)


def turned(pieces, at):
    n = len(pieces)
    tall, rows, width = pieces[0].shape

    def kernel(at_ref, *refs):
        for s in range(n):
            refs[-1][:, (at_ref[0] + s) % n] = refs[s][...]

    out = jax.ShapeDtypeStruct((tall, n, rows, width), BF16)
    return call(kernel, out, at[None], *pieces)


def turned_columns(pieces, at):
    n = len(pieces)
    tall, rows, width = pieces[0].shape

    def kernel(at_ref, *refs):
        for s in range(n):
            first = pl.multiple_of(((at_ref[0] + s) % n) * width, width)
            refs[-1][:, :, pl.ds(first, width)] = refs[s][...]

    out = jax.ShapeDtypeStruct((tall, rows, n * width), BF16)
    return call(kernel, out, at[None], *pieces)


def pick_blocks(pieces, asked):
    wide, count = asked.shape

    def kernel(asked_ref, *refs):
        for y in range(wide):
            for i in range(count):
                refs[-1][y, i] = refs[i // CAP][asked_ref[y, i]]

    out = jax.ShapeDtypeStruct((wide, count, *pieces[0].shape[1:]), BF16)
    return call(kernel, out, asked, *pieces)


def attend(queries, incoming, local_blocks, position, key_pos, facts):
    rows, width = queries.shape
    heads = width // HD
    far = incoming.shape[0]
    per_dev, nsel = position.shape
    keys = nsel * BLOCK

    def kernel(f_ref, p_ref, q_ref, in_ref, own_ref, kp_ref, o_ref, tab, k_s, v_s):
        tab[:far] = in_ref[...]
        tab[far:] = own_ref[...]
        for j in range(per_dev):
            for n in range(nsel):
                block = tab[p_ref[j, n]]
                k_s[j % 2, n * BLOCK : (n + 1) * BLOCK] = block[:, :HD]
                v_s[j % 2, n * BLOCK : (n + 1) * BLOCK] = block[:, HD:]
            mine = slice(j * BLOCK, (j + 1) * BLOCK)
            q = jnp.concatenate(
                [q_ref[mine, h * HD : (h + 1) * HD] for h in range(heads)], axis=0
            )
            scores = lax.dot_general(
                q, k_s[j % 2], (((1,), (1,)), ((), ())), preferred_element_type=F32
            ) * HD ** (-0.5)
            line = lax.broadcasted_iota(jnp.int32, (heads * BLOCK, 1), 0) % BLOCK
            at = f_ref[0] + j * BLOCK + line
            masked = jnp.where(kp_ref[j] <= at, scores, -jnp.inf)
            top = jnp.max(masked, axis=1, keepdims=True)
            weights = jnp.exp(masked - top)
            total = jnp.sum(weights, axis=1, keepdims=True)
            summed = jnp.dot(weights.astype(BF16), v_s[j % 2], preferred_element_type=F32)
            result = jnp.where(at < f_ref[1], summed / total, 0.0).astype(BF16)
            for h in range(heads):
                first = pl.multiple_of(((f_ref[2] + h) % heads) * HD, HD)
                o_ref[mine, pl.ds(first, HD)] = result[h * BLOCK : (h + 1) * BLOCK]

    return call(
        kernel,
        jax.ShapeDtypeStruct((rows, width), BF16),
        facts,
        position,
        queries,
        incoming,
        local_blocks,
        key_pos,
        scratch=(
            pltpu.VMEM((far + per_dev, BLOCK, 2 * HD), BF16),
            pltpu.VMEM((2, keys, HD), BF16),
            pltpu.VMEM((2, keys, HD), BF16),
        ),
        flops=4 * rows * keys * width,
    )


def mix(mine, other, pieces, places):
    n = len(pieces)
    tall, lines, width = pieces[0].shape
    half = tall // 2

    def kernel(p_ref, m_ref, t_ref, *refs):
        o_ref, w_s = refs[n], refs[n + 1]
        for s in range(n):
            w_s[:, (p_ref[0] + s) % n] = refs[s][...]
        first = w_s[pl.ds(p_ref[1] * half, half)].reshape(half * n * lines, width)
        second = w_s[pl.ds((1 - p_ref[1]) * half, half)].reshape(half * n * lines, width)
        o_ref[...] = (
            jnp.dot(m_ref[...], first, preferred_element_type=F32)
            + jnp.dot(t_ref[...], second, preferred_element_type=F32)
        ).astype(BF16)

    out = jax.ShapeDtypeStruct((mine.shape[0], width), BF16)
    scratch = (pltpu.VMEM((tall, n, lines, width), BF16),)
    flops = 4 * mine.size * width
    return call(kernel, out, places, mine, other, *pieces, scratch=scratch, flops=flops)


def body(tokens, query_weight, key_weight, value_weight, out_weight, chosen, live_length):
    rows = tokens.shape[0]
    per_dev = rows // BLOCK
    planes, tall, wide = (lax.axis_size(a) for a in ("dp", "kv_0", "kv_1"))
    x_at, z_at, y_at = (lax.axis_index(a) for a in ("dp", "kv_0", "kv_1"))
    owners = tall * wide
    me = z_at * wide + y_at

    def part(w, dim):
        size = w.shape[dim] // planes
        return lax.dynamic_slice_in_dim(w, x_at * size, size, axis=dim)

    pair_rows = 2 * (key_weight.shape[0] // planes)
    cargo = jnp.concatenate(
        [part(key_weight, 0), part(value_weight, 0), part(query_weight, 1)], axis=0
    )
    column = copy_for_each(cargo, "kv_0")
    every = copy_for_each(column[:, :pair_rows], ("dp", "kv_1"))
    every = every.reshape(planes, wide, tall, pair_rows, HD)
    q_small = column[:, pair_rows:]
    o_part = part(out_weight, 1)

    mates = spread(chosen, "kv_1")
    back = jnp.arange(tall, dtype=jnp.int32)
    column_owners = ((z_at - back) % tall) * wide + y_at
    asked = jnp.stack(
        [
            slots_wanted(mates[s], column_owners, per_dev, z_at * wide + (y_at + s) % wide)
            for s in range(wide)
        ]
    )
    asked = jnp.roll(jnp.maximum(asked, 0).reshape(wide, tall * CAP), y_at, axis=0)
    valid = chosen >= 0
    safe = jnp.maximum(chosen, 0)
    wanted = slots_wanted(chosen, jnp.arange(owners, dtype=jnp.int32), per_dev, me)
    holder = safe // per_dev
    local_of = safe % per_dev
    match = (wanted[None, None, :, :] == local_of[:, :, None, None]) & (
        jnp.arange(owners, dtype=jnp.int32)[None, None, :, None] == holder[:, :, None, None]
    )
    slot = jnp.sum(
        jnp.where(match, jnp.arange(CAP, dtype=jnp.int32)[None, None, None], 0), axis=(2, 3)
    )
    step = (z_at - holder // wide) % tall
    far = wide * tall * CAP
    remote_at = ((holder % wide) * tall + step) * CAP + slot
    position = jnp.where(holder == me, far + local_of, remote_at)
    key_pos = safe[:, :, None] * BLOCK + jnp.arange(BLOCK, dtype=jnp.int32)[None, None, :]
    key_pos = jnp.where(valid[:, :, None], key_pos, NEVER).reshape(per_dev, 1, -1)
    facts = jnp.stack([me * rows, live_length[0], x_at]).astype(jnp.int32)

    paired = project_pair(tokens, every)
    local_blocks = paired.reshape(per_dev, BLOCK, paired.shape[1])

    pieces = [None] * tall
    pieces[0] = up = down = local_blocks
    for s in range(1, tall // 2 + 1):
        up = from_ahead(up, "kv_0", -1)
        if s < tall - s:
            down = from_ahead(down, "kv_0", 1)
        if s == 1:
            up, down, q_small, o_part = after(up, down, q_small, o_part)
            q_pieces = spread(q_small, "kv_1")
            o_small = copy_for_each(o_part, "kv_0")
        if s == 3:
            up, down, *q_pieces = after(up, down, *q_pieces)
            q_tall = turned(q_pieces, y_at).reshape(-1, HD)
            q_pieces = spread(q_tall, "dp")
        if s == 4:
            up, down, o_small = after(up, down, o_small)
            o_pieces = spread(o_small, "dp")
        if s == 6:
            up, down, *o_pieces = after(up, down, *o_pieces)
            o_full = turned_columns(o_pieces, x_at)
            o_pieces = spread(o_full, "kv_1")
        pieces[s] = up
        if s < tall - s:
            pieces[tall - s] = down
    outgoing = pick_blocks(pieces, asked)
    incoming = lax.all_to_all(outgoing, "kv_1", split_axis=0, concat_axis=0, tiled=True)
    queries = project_queries(tokens, q_pieces, outgoing[0, 0, :16, :HD])
    attended = attend(
        queries,
        incoming.reshape(far, BLOCK, paired.shape[1]),
        local_blocks,
        position,
        key_pos,
        facts,
    )
    other = from_ahead(attended, "tp", 1)
    places = jnp.stack([y_at, lax.axis_index("tp")]).astype(jnp.int32)
    return mix(attended, other, o_pieces, places)


def solution(mesh):
    split = Mesh(
        mesh.devices.reshape(mesh.shape["dp"], 16, 4, mesh.shape["tp"]),
        ("dp", "kv_0", "kv_1", "tp"),
    )
    placed = (
        P(DP_KV, None),
        P(KV, "tp"),
        P(KV, "tp"),
        P(KV, "tp"),
        P(KV, "tp"),
        P(DP_KV, None),
        P("dp"),
    )

    return jax.shard_map(
        body, mesh=split, in_specs=placed, out_specs=P(DP_KV, "tp"), check_vma=False
    )
```

profile of v0, /device:TPU:2, one launch (start us, length us, event | category | flops | bytes accessed | tf_op | source)
XLA Modules:
  0.0 271.2 jit_solution(8161885814276115808)
XLA Ops:
  0.0 5.0 %collective-permute-start.12 = (s32[8,16]{1,0:T(8,128)}, s32[8,16]{1,0:T(8,128)S(1)}, u32[]{:S(2)}, u32[]{:S(2)}) collective-permute-start(s32[8,16]{1,0:T(8,128)} %param.12), channel_id=1, source_target_pairs={{2,0},{4,2},{6,4},{0,6},{3,1},{5,3},{7,5},{1,7},{10,8},{12,10},{14... | collective-permute-start | bytes 1544 | tf_op jit(solution)/shard_map/ppermute | solution.py:45
  12.1 15.2 %all-to-all-start = ((bf16[16,96,128]{2,1,0:T(8,128)(2,1)}), bf16[16,96,128]{2,1,0:T(8,128)(2,1)S(1)}, u32[]{:S(2)}, u32[]{:S(2)}) async-start(bf16[16,96,128]{2,1,0:T(8,128)(2,1)} %broadcast_in_dim.151), calls=%async_computation | async-start | bytes 786432 | tf_op jit(solution)/shard_map/all_to_all | solution.py:38
  30.7 19.1 %all-to-all-done = bf16[16,96,128]{2,1,0:T(8,128)(2,1)S(1)} async-done(((bf16[16,96,128]{2,1,0:T(8,128)(2,1)}), bf16[16,96,128]{2,1,0:T(8,128)(2,1)S(1)}, u32[]{:S(2)}, u32[]{:S(2)}) %all-to-all-start) | async-done | bytes 393248 | tf_op jit(solution)/shard_map/all_to_all | solution.py:38
  51.5 6.5 %all-to-all-start.1 = ((bf16[16,16,32,128]{3,2,1,0:T(8,128)(2,1)}), bf16[16,16,32,128]{3,2,1,0:T(8,128)(2,1)S(1)}, u32[]{:S(2)}, u32[]{:S(2)}) async-start(bf16[16,16,32,128]{3,2,1,0:T(8,128)(2,1)} %broadcast_in_dim.152), calls=%async_computation.1 | async-start | bytes 4194304 | tf_op jit(solution)/shard_map/all_to_all | solution.py:38
  62.3 16.4 %all-to-all-done.1 = bf16[16,16,32,128]{3,2,1,0:T(8,128)(2,1)S(1)} async-done(((bf16[16,16,32,128]{3,2,1,0:T(8,128)(2,1)}), bf16[16,16,32,128]{3,2,1,0:T(8,128)(2,1)S(1)}, u32[]{:S(2)}, u32[]{:S(2)}) %all-to-all-start.1) | async-done | bytes 2097184 | tf_op jit(solution)/shard_map/all_to_all | solution.py:38
  81.0 7.6 %collective-permute-start = (bf16[8,32,256]{2,1,0:T(8,128)(2,1)S(1)}, bf16[8,32,256]{2,1,0:T(8,128)(2,1)S(1)}, u32[]{:S(2)}, u32[]{:S(2)}) collective-permute-start(bf16[8,32,256]{2,1,0:T(8,128)(2,1)S(1)} %bitcast.36), channel_id=1, source_target_pairs={{120,0},{0,8},{8,16},{16,24},{24,32},{32,40},{40,48},{48,56},{56,6... | collective-permute-start | bytes 393224 | tf_op jit(solution)/shard_map/ppermute | solution.py:45
  88.7 4.6 %collective-permute-start.1 = (bf16[8,32,256]{2,1,0:T(8,128)(2,1)S(1)}, bf16[8,32,256]{2,1,0:T(8,128)(2,1)S(1)}, u32[]{:S(2)}, u32[]{:S(2)}) collective-permute-start(bf16[8,32,256]{2,1,0:T(8,128)(2,1)S(1)} %bitcast.37), channel_id=1, source_target_pairs={{8,0},{16,8},{24,16},{32,24},{40,32},{48,40},{56,48},{64,56},{72,6... | collective-permute-start | bytes 393224 | tf_op jit(solution)/shard_map/ppermute | solution.py:45
  96.5 8.4 %all-to-all-start.2 = ((bf16[16,16,512]{2,1,0:T(8,128)(2,1)}), bf16[16,16,512]{2,1,0:T(8,128)(2,1)S(1)}, u32[]{:S(2)}, u32[]{:S(2)}) async-start(bf16[16,16,512]{2,1,0:T(8,128)(2,1)} %broadcast_in_dim.155), calls=%async_computation.2 | async-start | bytes 524288 | tf_op jit(solution)/shard_map/all_to_all | solution.py:38
  105.4 3.3 %collective-permute-start.6 = (bf16[16,64,128]{2,1,0:T(8,128)(2,1)S(1)}, bf16[16,64,128]{2,1,0:T(8,128)(2,1)S(1)}, u32[]{:S(2)}, u32[]{:S(2)}) collective-permute-start(bf16[16,64,128]{2,1,0:T(8,128)(2,1)S(1)} %slice.13.refs_0_), channel_id=1, source_target_pairs={{2,0},{4,2},{6,4},{0,6},{3,1},{5,3},{7,5},{1,7},{10,8},{12,10},{14... | collective-permute-start | bytes 786440 | tf_op jit(solution)/shard_map/ppermute | solution.py:45
  108.8 3.1 %collective-permute-start.7 = (bf16[16,64,128]{2,1,0:T(8,128)(2,1)S(1)}, bf16[16,64,128]{2,1,0:T(8,128)(2,1)S(1)}, u32[]{:S(2)}, u32[]{:S(2)}) collective-permute-start(bf16[16,64,128]{2,1,0:T(8,128)(2,1)S(1)} %slice.13.refs_0_), channel_id=1, source_target_pairs={{4,0},{6,2},{0,4},{2,6},{5,1},{7,3},{1,5},{3,7},{12,8},{14,10},{8,... | collective-permute-start | bytes 786440 | tf_op jit(solution)/shard_map/ppermute | solution.py:45
  114.6 3.8 %collective-permute-start.2 = (bf16[8,32,256]{2,1,0:T(8,128)(2,1)S(1)}, bf16[8,32,256]{2,1,0:T(8,128)(2,1)S(1)}, u32[]{:S(2)}, u32[]{:S(2)}) collective-permute-start(bf16[8,32,256]{2,1,0:T(8,128)(2,1)S(1)} %collective-permute-done.refs_1_), channel_id=1, source_target_pairs={{120,0},{0,8},{8,16},{16,24},{24,32},{32,40},{40,48},{48,56},{56,6... | collective-permute-start | bytes 393224 | tf_op jit(solution)/shard_map/ppermute | solution.py:45
  118.4 3.2 %collective-permute-start.4 = (bf16[8,32,256]{2,1,0:T(8,128)(2,1)S(1)}, bf16[8,32,256]{2,1,0:T(8,128)(2,1)S(1)}, u32[]{:S(2)}, u32[]{:S(2)}) collective-permute-start(bf16[8,32,256]{2,1,0:T(8,128)(2,1)S(1)} %collective-permute-done.1.refs_15_), channel_id=1, source_target_pairs={{8,0},{16,8},{24,16},{32,24},{40,32},{48,40},{56,48},{64,56},{72,6... | collective-permute-start | bytes 393224 | tf_op jit(solution)/shard_map/ppermute | solution.py:45
  125.9 4.4 %collective-permute-start.5 = (bf16[8,32,256]{2,1,0:T(8,128)(2,1)S(1)}, bf16[8,32,256]{2,1,0:T(8,128)(2,1)S(1)}, u32[]{:S(2)}, u32[]{:S(2)}) collective-permute-start(bf16[8,32,256]{2,1,0:T(8,128)(2,1)S(1)} %collective-permute-done.4.refs_14_), channel_id=1, source_target_pairs={{8,0},{16,8},{24,16},{32,24},{40,32},{48,40},{56,48},{64,56},{72,6... | collective-permute-start | bytes 393224 | tf_op jit(solution)/shard_map/ppermute | solution.py:45
  132.9 3.3 %collective-permute-start.15 = (bf16[8,32,256]{2,1,0:T(8,128)(2,1)S(1)}, bf16[8,32,256]{2,1,0:T(8,128)(2,1)S(1)}, u32[]{:S(2)}, u32[]{:S(2)}) collective-permute-start(bf16[8,32,256]{2,1,0:T(8,128)(2,1)S(1)} %collective-permute-done.3.refs_3_), channel_id=1, source_target_pairs={{120,0},{0,8},{8,16},{16,24},{24,32},{32,40},{40,48},{48,56},{56,6... | collective-permute-start | bytes 393224 | tf_op jit(solution)/shard_map/ppermute | solution.py:45
  136.8 4.2 %collective-permute-start.16 = (bf16[8,32,256]{2,1,0:T(8,128)(2,1)S(1)}, bf16[8,32,256]{2,1,0:T(8,128)(2,1)S(1)}, u32[]{:S(2)}, u32[]{:S(2)}) collective-permute-start(bf16[8,32,256]{2,1,0:T(8,128)(2,1)S(1)} %collective-permute-done.5.refs_13_), channel_id=1, source_target_pairs={{8,0},{16,8},{24,16},{32,24},{40,32},{48,40},{56,48},{64,56},{72,6... | collective-permute-start | bytes 393224 | tf_op jit(solution)/shard_map/ppermute | solution.py:45
  141.7 3.3 %collective-permute-done.16.refs_12_ = bf16[8,32,256]{2,1,0:T(8,128)(2,1)S(1)} collective-permute-done((bf16[8,32,256]{2,1,0:T(8,128)(2,1)S(1)}, bf16[8,32,256]{2,1,0:T(8,128)(2,1)S(1)}, u32[]{:S(2)}, u32[]{:S(2)}) %collective-permute-start.16) | collective-permute-done | bytes 131104 | tf_op jit(solution)/shard_map/ppermute | solution.py:45
  145.0 5.1 %collective-permute-start.17 = (bf16[8,32,256]{2,1,0:T(8,128)(2,1)S(1)}, bf16[8,32,256]{2,1,0:T(8,128)(2,1)S(1)}, u32[]{:S(2)}, u32[]{:S(2)}) collective-permute-start(bf16[8,32,256]{2,1,0:T(8,128)(2,1)S(1)} %collective-permute-done.15.refs_4_), channel_id=1, source_target_pairs={{120,0},{0,8},{8,16},{16,24},{24,32},{32,40},{40,48},{48,56},{56,6... | collective-permute-start | bytes 393224 | tf_op jit(solution)/shard_map/ppermute | solution.py:45
  153.4 6.9 %collective-permute-start.21 = (bf16[16,16,512]{2,1,0:T(8,128)(2,1)S(1)}, bf16[16,16,512]{2,1,0:T(8,128)(2,1)S(1)}, u32[]{:S(2)}, u32[]{:S(2)}) collective-permute-start(bf16[16,16,512]{2,1,0:T(8,128)(2,1)S(1)} %all-to-all-done.2.refs_0_), channel_id=1, source_target_pairs={{128,0},{256,128},{384,256},{0,384},{129,1},{257,129},{385,257},{1... | collective-permute-start | bytes 786440 | tf_op jit(solution)/shard_map/ppermute | solution.py:45
  162.2 3.4 %collective-permute-start.23 = (bf16[16,16,512]{2,1,0:T(8,128)(2,1)S(1)}, bf16[16,16,512]{2,1,0:T(8,128)(2,1)S(1)}, u32[]{:S(2)}, u32[]{:S(2)}) collective-permute-start(bf16[16,16,512]{2,1,0:T(8,128)(2,1)S(1)} %all-to-all-done.2.refs_0_), channel_id=1, source_target_pairs={{384,0},{0,128},{128,256},{256,384},{385,1},{1,129},{129,257},{257... | collective-permute-start | bytes 786440 | tf_op jit(solution)/shard_map/ppermute | solution.py:45
  165.6 3.9 %collective-permute-start.18 = (bf16[8,32,256]{2,1,0:T(8,128)(2,1)S(1)}, bf16[8,32,256]{2,1,0:T(8,128)(2,1)}, u32[]{:S(2)}, u32[]{:S(2)}) collective-permute-start(bf16[8,32,256]{2,1,0:T(8,128)(2,1)S(1)} %collective-permute-done.17.refs_5_), channel_id=1, source_target_pairs={{120,0},{0,8},{8,16},{16,24},{24,32},{32,40},{40,48},{48,56},{56,6... | collective-permute-start | bytes 393224 | tf_op jit(solution)/shard_map/ppermute | solution.py:45
  170.2 3.1 %collective-permute-start.20 = (bf16[8,32,256]{2,1,0:T(8,128)(2,1)S(1)}, bf16[8,32,256]{2,1,0:T(8,128)(2,1)S(1)}, u32[]{:S(2)}, u32[]{:S(2)}) collective-permute-start(bf16[8,32,256]{2,1,0:T(8,128)(2,1)S(1)} %collective-permute-done.19.refs_11_), channel_id=1, source_target_pairs={{8,0},{16,8},{24,16},{32,24},{40,32},{48,40},{56,48},{64,56},{72,6... | collective-permute-start | bytes 393224 | tf_op jit(solution)/shard_map/ppermute | solution.py:45
  174.0 3.9 %collective-permute-done.20.refs_10_ = bf16[8,32,256]{2,1,0:T(8,128)(2,1)S(1)} collective-permute-done((bf16[8,32,256]{2,1,0:T(8,128)(2,1)S(1)}, bf16[8,32,256]{2,1,0:T(8,128)(2,1)S(1)}, u32[]{:S(2)}, u32[]{:S(2)}) %collective-permute-start.20) | collective-permute-done | bytes 131104 | tf_op jit(solution)/shard_map/ppermute | solution.py:45
  184.6 3.3 %collective-permute-start.26 = (bf16[8,32,256]{2,1,0:T(8,128)(2,1)S(1)}, bf16[8,32,256]{2,1,0:T(8,128)(2,1)S(1)}, u32[]{:S(2)}, u32[]{:S(2)}) collective-permute-start(bf16[8,32,256]{2,1,0:T(8,128)(2,1)S(1)} %copy-done.32), channel_id=1, source_target_pairs={{8,0},{16,8},{24,16},{32,24},{40,32},{48,40},{56,48},{64,56},{72,6... | collective-permute-start | bytes 393224 | tf_op jit(solution)/shard_map/ppermute | solution.py:45
  191.5 4.8 %collective-permute-done.25.refs_8_ = bf16[8,32,256]{2,1,0:T(8,128)(2,1)S(1)} collective-permute-done((bf16[8,32,256]{2,1,0:T(8,128)(2,1)}, bf16[8,32,256]{2,1,0:T(8,128)(2,1)S(1)}, u32[]{:S(2)}, u32[]{:S(2)}) %collective-permute-start.25) | collective-permute-done | bytes 131104 | tf_op jit(solution)/shard_map/ppermute | solution.py:45
  198.9 6.3 %all-to-all-start.3 = ((bf16[4,32,32,256]{3,2,1,0:T(8,128)(2,1)}), bf16[4,32,32,256]{3,2,1,0:T(8,128)(2,1)S(1)}, u32[]{:S(2)}, u32[]{:S(2)}) async-start(bf16[4,32,32,256]{3,2,1,0:T(8,128)(2,1)} %shard_map.75), calls=%async_computation.3 | async-start | bytes 4194304 | tf_op jit(solution)/shard_map/all_to_all | solution.py:299
  205.3 3.3 %collective-permute-start.10 = (bf16[4096,128]{1,0:T(8,128)(2,1)S(1)}, bf16[4096,128]{1,0:T(8,128)(2,1)}, u32[]{:S(2)}, u32[]{:S(2)}) collective-permute-start(bf16[4096,128]{1,0:T(8,128)(2,1)S(1)} %bitcast.33), channel_id=1, source_target_pairs={{256,0},{384,128},{0,256},{128,384},{257,1},{385,129},{1,257},{129... | collective-permute-start | bytes 3145736 | tf_op jit(solution)/shard_map/ppermute | solution.py:45
  208.7 3.9 %collective-permute-start.11 = (bf16[4096,128]{1,0:T(8,128)(2,1)S(1)}, bf16[4096,128]{1,0:T(8,128)(2,1)}, u32[]{:S(2)}, u32[]{:S(2)}) collective-permute-start(bf16[4096,128]{1,0:T(8,128)(2,1)S(1)} %bitcast.34), channel_id=1, source_target_pairs={{384,0},{0,128},{128,256},{256,384},{385,1},{1,129},{129,257},{257... | collective-permute-start | bytes 3145736 | tf_op jit(solution)/shard_map/ppermute | solution.py:45
  217.8 5.1 %collective-permute-start.28 = (bf16[16,16,2048]{2,1,0:T(8,128)(2,1)}, bf16[16,16,2048]{2,1,0:T(8,128)(2,1)}, u32[]{:S(2)}, u32[]{:S(2)}) collective-permute-start(bf16[16,16,2048]{2,1,0:T(8,128)(2,1)} %shard_map.78.refs_0_), channel_id=1, source_target_pairs={{2,0},{4,2},{6,4},{0,6},{3,1},{5,3},{7,5},{1,7},{10,8},{12,10},{14... | collective-permute-start | bytes 3145736 | tf_op jit(solution)/shard_map/ppermute | solution.py:45
  230.5 8.8 %collective-permute-done.11.refs_3_ = bf16[4096,128]{1,0:T(8,128)(2,1)} collective-permute-done((bf16[4096,128]{1,0:T(8,128)(2,1)S(1)}, bf16[4096,128]{1,0:T(8,128)(2,1)}, u32[]{:S(2)}, u32[]{:S(2)}) %collective-permute-start.11) | collective-permute-done | bytes 1048608 | tf_op jit(solution)/shard_map/ppermute | solution.py:45
  250.7 12.0 %collective-permute-done.28.refs_1_ = bf16[16,16,2048]{2,1,0:T(8,128)(2,1)} collective-permute-done((bf16[16,16,2048]{2,1,0:T(8,128)(2,1)}, bf16[16,16,2048]{2,1,0:T(8,128)(2,1)}, u32[]{:S(2)}, u32[]{:S(2)}) %collective-permute-start.28) | collective-permute-done | bytes 1048608 | tf_op jit(solution)/shard_map/ppermute | solution.py:45
  262.7 3.8 %collective-permute-done.30.refs_3_ = bf16[16,16,2048]{2,1,0:T(8,128)(2,1)} collective-permute-done((bf16[16,16,2048]{2,1,0:T(8,128)(2,1)}, bf16[16,16,2048]{2,1,0:T(8,128)(2,1)}, u32[]{:S(2)}, u32[]{:S(2)}) %collective-permute-start.30) | collective-permute-done | bytes 1048608 | tf_op jit(solution)/shard_map/ppermute | solution.py:45
  266.5 4.7 %shard_map.79 = bf16[256,2048]{1,0:T(8,128)(2,1)} custom-call(s32[2]{0:T(128)S(1)} %pad_add_fusion.6.p_ref, bf16[256,512]{1,0:T(8,128)(2,1)S(1)} %shard_map.77.m_ref, bf16[256,512]{1,0:T(8,128)(2,1)S(1)} %collective-permute-done.27.t_ref, bf16[16,16,2048]{2,1,0:T(8,128)(2,1)} %shard_map.78.refs_0_, bf16[16,16,2048]{2,1,0:T(8,128)(2,1)} %collective-permute-done.28.refs_1_, ...), custom_call_target="tpu_custom_call" | custom-call | flops 1073741824 | tf_op jit(solution)/shard_map/pallas_call | solution.py:25
  (198 shorter events, 75.4 us)
Async XLA Ops:
  0.0 59.0 %collective-permute-start.12 = (s32[8,16]{1,0:T(8,128)}, s32[8,16]{1,0:T(8,128)S(1)}, u32[]{:S(2)}, u32[]{:S(2)}) collective-permute-start(s32[8,16]{1,0:T(8,128)} %param.12), channel_id=1, source_target_pairs={{2,0},{4,2},{6,4},{0,6},{3,1},{5,3},{7,5},{1,7},{10,8},{12,10},{14... | collective-permute-start | bytes 1544 | tf_op jit(solution)/shard_map/ppermute | solution.py:45
  5.1 54.1 %collective-permute-start.13 = (s32[8,16]{1,0:T(8,128)}, s32[8,16]{1,0:T(8,128)S(1)}, u32[]{:S(2)}, u32[]{:S(2)}) collective-permute-start(s32[8,16]{1,0:T(8,128)} %param.12), channel_id=1, source_target_pairs={{4,0},{6,2},{0,4},{2,6},{5,1},{7,3},{1,5},{3,7},{12,8},{14,10},{8,... | collective-permute-start | bytes 1544 | tf_op jit(solution)/shard_map/ppermute | solution.py:45
  7.6 51.6 %collective-permute-start.14 = (s32[8,16]{1,0:T(8,128)}, s32[8,16]{1,0:T(8,128)S(1)}, u32[]{:S(2)}, u32[]{:S(2)}) collective-permute-start(s32[8,16]{1,0:T(8,128)} %param.12), channel_id=1, source_target_pairs={{6,0},{0,2},{2,4},{4,6},{7,1},{1,3},{3,5},{5,7},{14,8},{8,10},{10,... | collective-permute-start | bytes 1544 | tf_op jit(solution)/shard_map/ppermute | solution.py:45
  12.1 37.7 %all-to-all-start = ((bf16[16,96,128]{2,1,0:T(8,128)(2,1)}), bf16[16,96,128]{2,1,0:T(8,128)(2,1)S(1)}, u32[]{:S(2)}, u32[]{:S(2)}) async-start(bf16[16,96,128]{2,1,0:T(8,128)(2,1)} %broadcast_in_dim.151), calls=%async_computation | async-start | bytes 786432 | tf_op jit(solution)/shard_map/all_to_all | solution.py:38
  51.5 27.2 %all-to-all-start.1 = ((bf16[16,16,32,128]{3,2,1,0:T(8,128)(2,1)}), bf16[16,16,32,128]{3,2,1,0:T(8,128)(2,1)S(1)}, u32[]{:S(2)}, u32[]{:S(2)}) async-start(bf16[16,16,32,128]{3,2,1,0:T(8,128)(2,1)} %broadcast_in_dim.152), calls=%async_computation.1 | async-start | bytes 4194304 | tf_op jit(solution)/shard_map/all_to_all | solution.py:38
  81.0 13.2 %collective-permute-start = (bf16[8,32,256]{2,1,0:T(8,128)(2,1)S(1)}, bf16[8,32,256]{2,1,0:T(8,128)(2,1)S(1)}, u32[]{:S(2)}, u32[]{:S(2)}) collective-permute-start(bf16[8,32,256]{2,1,0:T(8,128)(2,1)S(1)} %bitcast.36), channel_id=1, source_target_pairs={{120,0},{0,8},{8,16},{16,24},{24,32},{32,40},{40,48},{48,56},{56,6... | collective-permute-start | bytes 393224 | tf_op jit(solution)/shard_map/ppermute | solution.py:45
  96.5 48.5 %all-to-all-start.2 = ((bf16[16,16,512]{2,1,0:T(8,128)(2,1)}), bf16[16,16,512]{2,1,0:T(8,128)(2,1)S(1)}, u32[]{:S(2)}, u32[]{:S(2)}) async-start(bf16[16,16,512]{2,1,0:T(8,128)(2,1)} %broadcast_in_dim.155), calls=%async_computation.2 | async-start | bytes 524288 | tf_op jit(solution)/shard_map/all_to_all | solution.py:38
  105.4 27.5 %collective-permute-start.6 = (bf16[16,64,128]{2,1,0:T(8,128)(2,1)S(1)}, bf16[16,64,128]{2,1,0:T(8,128)(2,1)S(1)}, u32[]{:S(2)}, u32[]{:S(2)}) collective-permute-start(bf16[16,64,128]{2,1,0:T(8,128)(2,1)S(1)} %slice.13.refs_0_), channel_id=1, source_target_pairs={{2,0},{4,2},{6,4},{0,6},{3,1},{5,3},{7,5},{1,7},{10,8},{12,10},{14... | collective-permute-start | bytes 786440 | tf_op jit(solution)/shard_map/ppermute | solution.py:45
  108.8 24.1 %collective-permute-start.7 = (bf16[16,64,128]{2,1,0:T(8,128)(2,1)S(1)}, bf16[16,64,128]{2,1,0:T(8,128)(2,1)S(1)}, u32[]{:S(2)}, u32[]{:S(2)}) collective-permute-start(bf16[16,64,128]{2,1,0:T(8,128)(2,1)S(1)} %slice.13.refs_0_), channel_id=1, source_target_pairs={{4,0},{6,2},{0,4},{2,6},{5,1},{7,3},{1,5},{3,7},{12,8},{14,10},{8,... | collective-permute-start | bytes 786440 | tf_op jit(solution)/shard_map/ppermute | solution.py:45
  111.9 21.0 %collective-permute-start.8 = (bf16[16,64,128]{2,1,0:T(8,128)(2,1)S(1)}, bf16[16,64,128]{2,1,0:T(8,128)(2,1)S(1)}, u32[]{:S(2)}, u32[]{:S(2)}) collective-permute-start(bf16[16,64,128]{2,1,0:T(8,128)(2,1)S(1)} %slice.13.refs_0_), channel_id=1, source_target_pairs={{6,0},{0,2},{2,4},{4,6},{7,1},{1,3},{3,5},{5,7},{14,8},{8,10},{10,... | collective-permute-start | bytes 786440 | tf_op jit(solution)/shard_map/ppermute | solution.py:45
  114.6 8.1 %collective-permute-start.2 = (bf16[8,32,256]{2,1,0:T(8,128)(2,1)S(1)}, bf16[8,32,256]{2,1,0:T(8,128)(2,1)S(1)}, u32[]{:S(2)}, u32[]{:S(2)}) collective-permute-start(bf16[8,32,256]{2,1,0:T(8,128)(2,1)S(1)} %collective-permute-done.refs_1_), channel_id=1, source_target_pairs={{120,0},{0,8},{8,16},{16,24},{24,32},{32,40},{40,48},{48,56},{56,6... | collective-permute-start | bytes 393224 | tf_op jit(solution)/shard_map/ppermute | solution.py:45
  118.4 7.5 %collective-permute-start.4 = (bf16[8,32,256]{2,1,0:T(8,128)(2,1)S(1)}, bf16[8,32,256]{2,1,0:T(8,128)(2,1)S(1)}, u32[]{:S(2)}, u32[]{:S(2)}) collective-permute-start(bf16[8,32,256]{2,1,0:T(8,128)(2,1)S(1)} %collective-permute-done.1.refs_15_), channel_id=1, source_target_pairs={{8,0},{16,8},{24,16},{32,24},{40,32},{48,40},{56,48},{64,56},{72,6... | collective-permute-start | bytes 393224 | tf_op jit(solution)/shard_map/ppermute | solution.py:45
  122.7 8.3 %collective-permute-start.3 = (bf16[8,32,256]{2,1,0:T(8,128)(2,1)S(1)}, bf16[8,32,256]{2,1,0:T(8,128)(2,1)S(1)}, u32[]{:S(2)}, u32[]{:S(2)}) collective-permute-start(bf16[8,32,256]{2,1,0:T(8,128)(2,1)S(1)} %collective-permute-done.2.refs_2_), channel_id=1, source_target_pairs={{120,0},{0,8},{8,16},{16,24},{24,32},{32,40},{40,48},{48,56},{56,6... | collective-permute-start | bytes 393224 | tf_op jit(solution)/shard_map/ppermute | solution.py:45
  132.9 8.8 %collective-permute-start.15 = (bf16[8,32,256]{2,1,0:T(8,128)(2,1)S(1)}, bf16[8,32,256]{2,1,0:T(8,128)(2,1)S(1)}, u32[]{:S(2)}, u32[]{:S(2)}) collective-permute-start(bf16[8,32,256]{2,1,0:T(8,128)(2,1)S(1)} %collective-permute-done.3.refs_3_), channel_id=1, source_target_pairs={{120,0},{0,8},{8,16},{16,24},{24,32},{32,40},{40,48},{48,56},{56,6... | collective-permute-start | bytes 393224 | tf_op jit(solution)/shard_map/ppermute | solution.py:45
  136.8 8.2 %collective-permute-start.16 = (bf16[8,32,256]{2,1,0:T(8,128)(2,1)S(1)}, bf16[8,32,256]{2,1,0:T(8,128)(2,1)S(1)}, u32[]{:S(2)}, u32[]{:S(2)}) collective-permute-start(bf16[8,32,256]{2,1,0:T(8,128)(2,1)S(1)} %collective-permute-done.5.refs_13_), channel_id=1, source_target_pairs={{8,0},{16,8},{24,16},{32,24},{40,32},{48,40},{56,48},{64,56},{72,6... | collective-permute-start | bytes 393224 | tf_op jit(solution)/shard_map/ppermute | solution.py:45
  145.0 20.6 %collective-permute-start.17 = (bf16[8,32,256]{2,1,0:T(8,128)(2,1)S(1)}, bf16[8,32,256]{2,1,0:T(8,128)(2,1)S(1)}, u32[]{:S(2)}, u32[]{:S(2)}) collective-permute-start(bf16[8,32,256]{2,1,0:T(8,128)(2,1)S(1)} %collective-permute-done.15.refs_4_), channel_id=1, source_target_pairs={{120,0},{0,8},{8,16},{16,24},{24,32},{32,40},{40,48},{48,56},{56,6... | collective-permute-start | bytes 393224 | tf_op jit(solution)/shard_map/ppermute | solution.py:45
  150.8 19.4 %collective-permute-start.19 = (bf16[8,32,256]{2,1,0:T(8,128)(2,1)S(1)}, bf16[8,32,256]{2,1,0:T(8,128)(2,1)S(1)}, u32[]{:S(2)}, u32[]{:S(2)}) collective-permute-start(bf16[8,32,256]{2,1,0:T(8,128)(2,1)S(1)} %collective-permute-done.16.refs_12_), channel_id=1, source_target_pairs={{8,0},{16,8},{24,16},{32,24},{40,32},{48,40},{56,48},{64,56},{72,6... | collective-permute-start | bytes 393224 | tf_op jit(solution)/shard_map/ppermute | solution.py:45
  153.4 24.5 %collective-permute-start.21 = (bf16[16,16,512]{2,1,0:T(8,128)(2,1)S(1)}, bf16[16,16,512]{2,1,0:T(8,128)(2,1)S(1)}, u32[]{:S(2)}, u32[]{:S(2)}) collective-permute-start(bf16[16,16,512]{2,1,0:T(8,128)(2,1)S(1)} %all-to-all-done.2.refs_0_), channel_id=1, source_target_pairs={{128,0},{256,128},{384,256},{0,384},{129,1},{257,129},{385,257},{1... | collective-permute-start | bytes 786440 | tf_op jit(solution)/shard_map/ppermute | solution.py:45
  160.3 17.6 %collective-permute-start.22 = (bf16[16,16,512]{2,1,0:T(8,128)(2,1)S(1)}, bf16[16,16,512]{2,1,0:T(8,128)(2,1)S(1)}, u32[]{:S(2)}, u32[]{:S(2)}) collective-permute-start(bf16[16,16,512]{2,1,0:T(8,128)(2,1)S(1)} %all-to-all-done.2.refs_0_), channel_id=1, source_target_pairs={{256,0},{384,128},{0,256},{128,384},{257,1},{385,129},{1,257},{129... | collective-permute-start | bytes 786440 | tf_op jit(solution)/shard_map/ppermute | solution.py:45
  162.2 15.7 %collective-permute-start.23 = (bf16[16,16,512]{2,1,0:T(8,128)(2,1)S(1)}, bf16[16,16,512]{2,1,0:T(8,128)(2,1)S(1)}, u32[]{:S(2)}, u32[]{:S(2)}) collective-permute-start(bf16[16,16,512]{2,1,0:T(8,128)(2,1)S(1)} %all-to-all-done.2.refs_0_), channel_id=1, source_target_pairs={{384,0},{0,128},{128,256},{256,384},{385,1},{1,129},{129,257},{257... | collective-permute-start | bytes 786440 | tf_op jit(solution)/shard_map/ppermute | solution.py:45
  165.6 8.4 %collective-permute-start.18 = (bf16[8,32,256]{2,1,0:T(8,128)(2,1)S(1)}, bf16[8,32,256]{2,1,0:T(8,128)(2,1)}, u32[]{:S(2)}, u32[]{:S(2)}) collective-permute-start(bf16[8,32,256]{2,1,0:T(8,128)(2,1)S(1)} %collective-permute-done.17.refs_5_), channel_id=1, source_target_pairs={{120,0},{0,8},{8,16},{16,24},{24,32},{32,40},{40,48},{48,56},{56,6... | collective-permute-start | bytes 393224 | tf_op jit(solution)/shard_map/ppermute | solution.py:45
  170.2 7.7 %collective-permute-start.20 = (bf16[8,32,256]{2,1,0:T(8,128)(2,1)S(1)}, bf16[8,32,256]{2,1,0:T(8,128)(2,1)S(1)}, u32[]{:S(2)}, u32[]{:S(2)}) collective-permute-start(bf16[8,32,256]{2,1,0:T(8,128)(2,1)S(1)} %collective-permute-done.19.refs_11_), channel_id=1, source_target_pairs={{8,0},{16,8},{24,16},{32,24},{40,32},{48,40},{56,48},{64,56},{72,6... | collective-permute-start | bytes 393224 | tf_op jit(solution)/shard_map/ppermute | solution.py:45
  177.9 10.1 %collective-permute-start.24 = (bf16[8,32,256]{2,1,0:T(8,128)(2,1)}, bf16[8,32,256]{2,1,0:T(8,128)(2,1)}, u32[]{:S(2)}, u32[]{:S(2)}) collective-permute-start(bf16[8,32,256]{2,1,0:T(8,128)(2,1)} %collective-permute-done.18.refs_6_), channel_id=1, source_target_pairs={{120,0},{0,8},{8,16},{16,24},{24,32},{32,40},{40,48},{48,56},{56,6... | collective-permute-start | bytes 393224 | tf_op jit(solution)/shard_map/ppermute | solution.py:45
  181.7 44.1 %collective-permute-start.9 = (bf16[4096,128]{1,0:T(8,128)(2,1)S(1)}, bf16[4096,128]{1,0:T(8,128)(2,1)}, u32[]{:S(2)}, u32[]{:S(2)}) collective-permute-start(bf16[4096,128]{1,0:T(8,128)(2,1)S(1)} %bitcast.32), channel_id=1, source_target_pairs={{128,0},{256,128},{384,256},{0,384},{129,1},{257,129},{385,257},{1... | collective-permute-start | bytes 3145736 | tf_op jit(solution)/shard_map/ppermute | solution.py:45
  188.0 8.3 %collective-permute-start.25 = (bf16[8,32,256]{2,1,0:T(8,128)(2,1)}, bf16[8,32,256]{2,1,0:T(8,128)(2,1)S(1)}, u32[]{:S(2)}, u32[]{:S(2)}) collective-permute-start(bf16[8,32,256]{2,1,0:T(8,128)(2,1)} %collective-permute-done.24.refs_7_), channel_id=1, source_target_pairs={{120,0},{0,8},{8,16},{16,24},{24,32},{32,40},{40,48},{48,56},{56,6... | collective-permute-start | bytes 393224 | tf_op jit(solution)/shard_map/ppermute | solution.py:45
  198.9 45.8 %all-to-all-start.3 = ((bf16[4,32,32,256]{3,2,1,0:T(8,128)(2,1)}), bf16[4,32,32,256]{3,2,1,0:T(8,128)(2,1)S(1)}, u32[]{:S(2)}, u32[]{:S(2)}) async-start(bf16[4,32,32,256]{3,2,1,0:T(8,128)(2,1)} %shard_map.75), calls=%async_computation.3 | async-start | bytes 4194304 | tf_op jit(solution)/shard_map/all_to_all | solution.py:299
  205.3 25.1 %collective-permute-start.10 = (bf16[4096,128]{1,0:T(8,128)(2,1)S(1)}, bf16[4096,128]{1,0:T(8,128)(2,1)}, u32[]{:S(2)}, u32[]{:S(2)}) collective-permute-start(bf16[4096,128]{1,0:T(8,128)(2,1)S(1)} %bitcast.33), channel_id=1, source_target_pairs={{256,0},{384,128},{0,256},{128,384},{257,1},{385,129},{1,257},{129... | collective-permute-start | bytes 3145736 | tf_op jit(solution)/shard_map/ppermute | solution.py:45
  208.7 30.6 %collective-permute-start.11 = (bf16[4096,128]{1,0:T(8,128)(2,1)S(1)}, bf16[4096,128]{1,0:T(8,128)(2,1)}, u32[]{:S(2)}, u32[]{:S(2)}) collective-permute-start(bf16[4096,128]{1,0:T(8,128)(2,1)S(1)} %bitcast.34), channel_id=1, source_target_pairs={{384,0},{0,128},{128,256},{256,384},{385,1},{1,129},{129,257},{257... | collective-permute-start | bytes 3145736 | tf_op jit(solution)/shard_map/ppermute | solution.py:45
  217.8 44.9 %collective-permute-start.28 = (bf16[16,16,2048]{2,1,0:T(8,128)(2,1)}, bf16[16,16,2048]{2,1,0:T(8,128)(2,1)}, u32[]{:S(2)}, u32[]{:S(2)}) collective-permute-start(bf16[16,16,2048]{2,1,0:T(8,128)(2,1)} %shard_map.78.refs_0_), channel_id=1, source_target_pairs={{2,0},{4,2},{6,4},{0,6},{3,1},{5,3},{7,5},{1,7},{10,8},{12,10},{14... | collective-permute-start | bytes 3145736 | tf_op jit(solution)/shard_map/ppermute | solution.py:45
  223.0 39.7 %collective-permute-start.29 = (bf16[16,16,2048]{2,1,0:T(8,128)(2,1)}, bf16[16,16,2048]{2,1,0:T(8,128)(2,1)}, u32[]{:S(2)}, u32[]{:S(2)}) collective-permute-start(bf16[16,16,2048]{2,1,0:T(8,128)(2,1)} %shard_map.78.refs_0_), channel_id=1, source_target_pairs={{4,0},{6,2},{0,4},{2,6},{5,1},{7,3},{1,5},{3,7},{12,8},{14,10},{8,... | collective-permute-start | bytes 3145736 | tf_op jit(solution)/shard_map/ppermute | solution.py:45
  225.8 40.7 %collective-permute-start.30 = (bf16[16,16,2048]{2,1,0:T(8,128)(2,1)}, bf16[16,16,2048]{2,1,0:T(8,128)(2,1)}, u32[]{:S(2)}, u32[]{:S(2)}) collective-permute-start(bf16[16,16,2048]{2,1,0:T(8,128)(2,1)} %shard_map.78.refs_0_), channel_id=1, source_target_pairs={{6,0},{0,2},{2,4},{4,6},{7,1},{1,3},{3,5},{5,7},{14,8},{8,10},{10,... | collective-permute-start | bytes 3145736 | tf_op jit(solution)/shard_map/ppermute | solution.py:45
  248.7 17.8 %collective-permute-start.27 = (bf16[256,512]{1,0:T(8,128)(2,1)S(1)}, bf16[256,512]{1,0:T(8,128)(2,1)S(1)}, u32[]{:S(2)}, u32[]{:S(2)}) collective-permute-start(bf16[256,512]{1,0:T(8,128)(2,1)S(1)} %shard_map.77.m_ref), channel_id=1, source_target_pairs={{1,0},{0,1},{3,2},{2,3},{5,4},{4,5},{7,6},{6,7},{9,8},{8,9},{11,10... | collective-permute-start | bytes 786440 | tf_op jit(solution)/shard_map/ppermute | solution.py:45
  (37 other events, 373.6 us)
where the time goes:
time: 273 us; the launch traced here: 271 us
  starting transfers between devices  148 us (54%)
  waiting for transfers between devices  77.9 us (29%)
  local copies, waits for them, and re-layouts  21.4 us (8%)
  Pallas kernels  15.2 us (6%)
  other arithmetic  7.37 us (3%)
    ppermute x31, starting transfers between devices, from_ahead(): return lax.ppermute(x, axis, [((i + step) % n, i) for i in range(n)])  111 us
    ppermute x31, waiting for transfers between devices, from_ahead(): return lax.ppermute(x, axis, [((i + step) % n, i) for i in range(n)])  42.4 us
    all_to_all x3, waiting for transfers between devices, copy_for_each(): lax.all_to_all(jnp.broadcast_to(shard[None], (count, *shard.shape)), axis...  35.5 us
    all_to_all x3, starting transfers between devices, copy_for_each(): lax.all_to_all(jnp.broadcast_to(shard[None], (count, *shard.shape)), axis...  30.2 us
    pallas_call x7, Pallas kernels, call(): pl.pallas_call(kernel, out_shape=out_shape, in_specs=spaces, out_specs=pl...  15.2 us
    unnamed x68, local copies, waits for them, and re-layouts  13.8 us
    all_to_all x1, starting transfers between devices, body(): lax.all_to_all(outgoing, 'kv_1', split_axis=0, concat_axis=0, tiled=True)  6.35 us
  transfers between devices with their start and end apart: 35, of which 13 were waited for; matrix products, arithmetic and copies ran while one was open for 5% of the time, Pallas kernels for 4%

commit v1 on v0

--- a/solution.py
+++ b/solution.py
@@ -108,39 +108,66 @@
 
 def turned(pieces, at):
     n = len(pieces)
-    tall, rows, width = pieces[0].shape
+    tall, lines, _ = pieces[0].shape
+    columns = 2
+    rows = lines // columns
 
     def kernel(at_ref, *refs):
         for s in range(n):
-            refs[-1][:, (at_ref[0] + s) % n] = refs[s][...]
-
-    out = jax.ShapeDtypeStruct((tall, n, rows, width), BF16)
+            y = (at_ref[0] + s) % n
+            for i in range(columns):
+                refs[-1][i, :, y] = refs[s][:, i * rows : (i + 1) * rows]
+
+    out = jax.ShapeDtypeStruct((columns, tall, n, rows, HD), BF16)
     return call(kernel, out, at[None], *pieces)
 
 
-def turned_columns(pieces, at):
-    n = len(pieces)
-    tall, rows, width = pieces[0].shape
-
-    def kernel(at_ref, *refs):
-        for s in range(n):
-            first = pl.multiple_of(((at_ref[0] + s) % n) * width, width)
-            refs[-1][:, :, pl.ds(first, width)] = refs[s][...]
-
-    out = jax.ShapeDtypeStruct((tall, rows, n * width), BF16)
-    return call(kernel, out, at[None], *pieces)
-
-
-def pick_blocks(pieces, asked):
+def full_columns(own, ahead, behind, lines, parity):
+    tall, held, _ = own.shape
+    groups = held // lines
+
+    def kernel(p_ref, own_ref, ahead_ref, behind_ref, o_ref):
+        def put(half, i, value):
+            first = pl.multiple_of((half * groups + i) * HD, HD)
+            o_ref[:, :, pl.ds(first, HD)] = value
+
+        for i in range(groups):
+            put(p_ref[0], i, own_ref[:, i * lines : (i + 1) * lines])
+        for i in range(groups // 2):
+            cut = slice(i * lines, (i + 1) * lines)
+            put(1 - p_ref[0], i, ahead_ref[:, cut])
+            put(1 - p_ref[0], i + groups // 2, behind_ref[:, cut])
+
+    out = jax.ShapeDtypeStruct((tall, lines, 2 * groups * HD), BF16)
+    return call(kernel, out, parity[None], own, ahead, behind)
+
+
+def key_positions(chosen):
+    per_dev, nsel = chosen.shape
+
+    def kernel(c_ref, o_ref):
+        lane = lax.broadcasted_iota(jnp.int32, (1, nsel * BLOCK), 1)
+        for j in range(per_dev):
+            row = jnp.zeros((1, nsel * BLOCK), jnp.int32)
+            for n in range(nsel):
+                first = jnp.where(c_ref[j, n] >= 0, c_ref[j, n] * BLOCK, NEVER)
+                row = jnp.where(lane // BLOCK == n, first, row)
+            o_ref[j] = row + lane % BLOCK
+
+    out = jax.ShapeDtypeStruct((per_dev, 1, nsel * BLOCK), jnp.int32)
+    return call(kernel, out, chosen)
+
+
+def pick_blocks(blocks, asked):
     wide, count = asked.shape
 
-    def kernel(asked_ref, *refs):
+    def kernel(asked_ref, b_ref, o_ref):
         for y in range(wide):
             for i in range(count):
-                refs[-1][y, i] = refs[i // CAP][asked_ref[y, i]]
-
-    out = jax.ShapeDtypeStruct((wide, count, *pieces[0].shape[1:]), BF16)
-    return call(kernel, out, asked, *pieces)
+                o_ref[y, i] = b_ref[asked_ref[y, i]]
+
+    out = jax.ShapeDtypeStruct((wide, count, *blocks.shape[1:]), BF16)
+    return call(kernel, out, asked, blocks)
 
 
 def attend(queries, incoming, local_blocks, position, key_pos, facts):
@@ -225,33 +252,60 @@
     owners = tall * wide
     me = z_at * wide + y_at
 
+    def stacked(w):
+        return jnp.concatenate(
+            [w[:, i * HD : (i + 1) * HD] for i in range(w.shape[1] // HD)], axis=0
+        )
+
     def part(w, dim):
         size = w.shape[dim] // planes
         return lax.dynamic_slice_in_dim(w, x_at * size, size, axis=dim)
 
+    parity = x_at % 2
+    lines = out_weight.shape[0]
+    q_half = lax.dynamic_slice_in_dim(
+        query_weight, parity * (query_weight.shape[1] // 2), query_weight.shape[1] // 2, axis=1
+    )
+    o_half = lax.dynamic_slice_in_dim(
+        out_weight, parity * (out_weight.shape[1] // 2), out_weight.shape[1] // 2, axis=1
+    )
+    halves = jnp.concatenate([stacked(q_half), stacked(o_half)], axis=0)
+    halves = lax.all_gather(halves, "kv_0", axis=0, tiled=False)
+
     pair_rows = 2 * (key_weight.shape[0] // planes)
-    cargo = jnp.concatenate(
-        [part(key_weight, 0), part(value_weight, 0), part(query_weight, 1)], axis=0
-    )
+    cargo = jnp.concatenate([part(key_weight, 0), part(value_weight, 0)], axis=0)
     column = copy_for_each(cargo, "kv_0")
-    every = copy_for_each(column[:, :pair_rows], ("dp", "kv_1"))
+    every = copy_for_each(column, ("dp", "kv_1"))
     every = every.reshape(planes, wide, tall, pair_rows, HD)
-    q_small = column[:, pair_rows:]
-    o_part = part(out_weight, 1)
-
-    mates = spread(chosen, "kv_1")
-    back = jnp.arange(tall, dtype=jnp.int32)
-    column_owners = ((z_at - back) % tall) * wide + y_at
+    paired = project_pair(tokens, every)
+    paired, halves, late_chosen = after(paired, halves, chosen)
+    local_blocks = paired.reshape(per_dev, BLOCK, paired.shape[1])
+    column_blocks = lax.all_gather(local_blocks, "kv_0", axis=0, tiled=True)
+
+    q_lines = halves.shape[1] // 2
+    q_pieces = spread(halves[:, :q_lines], "kv_1")
+    o_own = halves[:, q_lines:]
+    cut = o_own.shape[1] // 2
+    o_ahead = from_ahead(o_own[:, :cut], "dp", 1)
+    o_behind = from_ahead(o_own[:, cut:], "dp", -1)
+    q_tall = turned(q_pieces, y_at).reshape(2, -1, HD)
+    q_pieces = [
+        q_tall[0], q_tall[1], from_ahead(q_tall[0], "dp", 1), from_ahead(q_tall[1], "dp", -1)
+    ]
+    o_pieces = spread(full_columns(o_own, o_ahead, o_behind, lines, parity), "kv_1")
+
+    mates = spread(late_chosen, "kv_1")
+    column_owners = jnp.arange(tall, dtype=jnp.int32) * wide + y_at
     asked = jnp.stack(
         [
             slots_wanted(mates[s], column_owners, per_dev, z_at * wide + (y_at + s) % wide)
             for s in range(wide)
         ]
     )
-    asked = jnp.roll(jnp.maximum(asked, 0).reshape(wide, tall * CAP), y_at, axis=0)
-    valid = chosen >= 0
-    safe = jnp.maximum(chosen, 0)
-    wanted = slots_wanted(chosen, jnp.arange(owners, dtype=jnp.int32), per_dev, me)
+    asked = jnp.maximum(asked, 0) + (jnp.arange(tall, dtype=jnp.int32) * per_dev)[None, :, None]
+    asked = jnp.roll(asked.reshape(wide, tall * CAP), y_at, axis=0)
+    safe = jnp.maximum(late_chosen, 0)
+    wanted = slots_wanted(late_chosen, jnp.arange(owners, dtype=jnp.int32), per_dev, me)
     holder = safe // per_dev
     local_of = safe % per_dev
     match = (wanted[None, None, :, :] == local_of[:, :, None, None]) & (
@@ -260,42 +314,13 @@
     slot = jnp.sum(
         jnp.where(match, jnp.arange(CAP, dtype=jnp.int32)[None, None, None], 0), axis=(2, 3)
     )
-    step = (z_at - holder // wide) % tall
     far = wide * tall * CAP
-    remote_at = ((holder % wide) * tall + step) * CAP + slot
+    remote_at = ((holder % wide) * tall + holder // wide) * CAP + slot
     position = jnp.where(holder == me, far + local_of, remote_at)
-    key_pos = safe[:, :, None] * BLOCK + jnp.arange(BLOCK, dtype=jnp.int32)[None, None, :]
-    key_pos = jnp.where(valid[:, :, None], key_pos, NEVER).reshape(per_dev, 1, -1)
-    facts = jnp.stack([me * rows, live_length[0], x_at]).astype(jnp.int32)
-
-    paired = project_pair(tokens, every)
-    local_blocks = paired.reshape(per_dev, BLOCK, paired.shape[1])
-
-    pieces = [None] * tall
-    pieces[0] = up = down = local_blocks
-    for s in range(1, tall // 2 + 1):
-        up = from_ahead(up, "kv_0", -1)
-        if s < tall - s:
-            down = from_ahead(down, "kv_0", 1)
-        if s == 1:
-            up, down, q_small, o_part = after(up, down, q_small, o_part)
-            q_pieces = spread(q_small, "kv_1")
-            o_small = copy_for_each(o_part, "kv_0")
-        if s == 3:
-            up, down, *q_pieces = after(up, down, *q_pieces)
-            q_tall = turned(q_pieces, y_at).reshape(-1, HD)
-            q_pieces = spread(q_tall, "dp")
-        if s == 4:
-            up, down, o_small = after(up, down, o_small)
-            o_pieces = spread(o_small, "dp")
-        if s == 6:
-            up, down, *o_pieces = after(up, down, *o_pieces)
-            o_full = turned_columns(o_pieces, x_at)
-            o_pieces = spread(o_full, "kv_1")
-        pieces[s] = up
-        if s < tall - s:
-            pieces[tall - s] = down
-    outgoing = pick_blocks(pieces, asked)
+    key_pos = key_positions(late_chosen)
+    facts = jnp.stack([me * rows, live_length[0], 2 * parity]).astype(jnp.int32)
+
+    outgoing = pick_blocks(column_blocks, asked)
     incoming = lax.all_to_all(outgoing, "kv_1", split_axis=0, concat_axis=0, tiled=True)
     queries = project_queries(tokens, q_pieces, outgoing[0, 0, :16, :HD])
     attended = attend(

time: 273 us -> 287 us (1.051)
  waiting for transfers between devices: 77.9 us -> 154 us
  starting transfers between devices: 148 us -> 73 us
  between operations: 1.57 us -> 14.6 us
    all_gather x0 -> x2, waiting for transfers between devices: none -> 97.7 us  [the longest x1 59.1 us: body(): column_blocks = lax.all_gather(local_blocks, 'kv_0', axis=0, tiled=True)]
    ppermute x31 -> x14, starting transfers between devices: 111 us -> 46 us  [from_ahead(): return lax.ppermute(x, axis, [((i + step) % n, i) for i in range(n)])]
    ppermute x31 -> x14, waiting for transfers between devices: 42.4 us -> 26 us  [from_ahead(): return lax.ppermute(x, axis, [((i + step) % n, i) for i in range(n)])]
    all_to_all x3 -> x2, starting transfers between devices: 30.2 us -> 22.7 us  [copy_for_each(): lax.all_to_all(jnp.broadcast_to(shard[None], (count, *shard.shape)), axis...]
    all_to_all x3 -> x2, waiting for transfers between devices: 35.5 us -> 30.6 us  [copy_for_each(): lax.all_to_all(jnp.broadcast_to(shard[None], (count, *shard.shape)), axis...]
    slice x2 -> x3, local copies, waits for them, and re-layouts: 0.03 us -> 4.24 us  [the longest x1 2.11 us: body(): o_own = halves[:, q_lines:]]
    unnamed x68 -> x27, local copies, waits for them, and re-layouts: 13.8 us -> 12.5 us
    pallas_call x7 -> x8, Pallas kernels: 15.2 us -> 14.8 us  [call(): pl.pallas_call(kernel, out_shape=out_shape, in_specs=spaces, out_specs=pl...]
  transfers between devices with their start and end apart: 35 -> 19, of which waited for: 13 -> 8; matrix products, arithmetic and copies ran while one was open for 5% -> 7% of each run, Pallas kernels for 4% -> 4%
where the time goes in v1:
time: 287 us; the launch traced here: 286 us
  waiting for transfers between devices  154 us (54%)
  starting transfers between devices  73 us (25%)
  local copies, waits for them, and re-layouts  22.4 us (8%)
  Pallas kernels  14.8 us (5%)
  between operations  14.6 us (5%)
  other arithmetic  6.69 us (2%)
    all_gather x1, waiting for transfers between devices, body(): column_blocks = lax.all_gather(local_blocks, 'kv_0', axis=0, tiled=True)  59.1 us
    ppermute x14, starting transfers between devices, from_ahead(): return lax.ppermute(x, axis, [((i + step) % n, i) for i in range(n)])  46 us
    all_gather x1, waiting for transfers between devices, body(): halves = lax.all_gather(halves, 'kv_0', axis=0, tiled=False)  38.7 us
    all_to_all x2, waiting for transfers between devices, copy_for_each(): lax.all_to_all(jnp.broadcast_to(shard[None], (count, *shard.shape)), axis...  30.6 us
    ppermute x14, waiting for transfers between devices, from_ahead(): return lax.ppermute(x, axis, [((i + step) % n, i) for i in range(n)])  26 us
    all_to_all x2, starting transfers between devices, copy_for_each(): lax.all_to_all(jnp.broadcast_to(shard[None], (count, *shard.shape)), axis...  22.7 us
    pallas_call x8, Pallas kernels, call(): pl.pallas_call(kernel, out_shape=out_shape, in_specs=spaces, out_specs=pl...  14.8 us
    unnamed x27, local copies, waits for them, and re-layouts  12.5 us
  transfers between devices with their start and end apart: 19, of which 8 were waited for; matrix products, arithmetic and copies ran while one was open for 7% of the time, Pallas kernels for 4%

profile of v1, /device:TPU:2, one launch (start us, length us, event | category | flops | bytes accessed | tf_op | source)
XLA Modules:
  0.0 285.9 jit_solution(2123348235831694663)
XLA Ops:
  8.6 15.2 %all-to-all-start = ((bf16[16,32,128]{2,1,0:T(8,128)(2,1)}), bf16[16,32,128]{2,1,0:T(8,128)(2,1)S(1)}, u32[]{:S(2)}, u32[]{:S(2)}) async-start(bf16[16,32,128]{2,1,0:T(8,128)(2,1)} %broadcast_in_dim.127), calls=%async_computation | async-start | bytes 262144 | tf_op jit(solution)/shard_map/all_to_all | solution.py:38
  30.2 8.4 %all-to-all-done = bf16[16,32,128]{2,1,0:T(8,128)(2,1)S(1)} async-done(((bf16[16,32,128]{2,1,0:T(8,128)(2,1)}), bf16[16,32,128]{2,1,0:T(8,128)(2,1)S(1)}, u32[]{:S(2)}, u32[]{:S(2)}) %all-to-all-start) | async-done | bytes 131104 | tf_op jit(solution)/shard_map/all_to_all | solution.py:38
  38.6 1.8 broadcast_in_dim.128
  40.4 7.5 %all-to-all-start.1 = ((bf16[16,16,32,128]{3,2,1,0:T(8,128)(2,1)}), bf16[16,16,32,128]{3,2,1,0:T(8,128)(2,1)S(1)}, u32[]{:S(2)}, u32[]{:S(2)}) async-start(bf16[16,16,32,128]{3,2,1,0:T(8,128)(2,1)} %broadcast_in_dim.128), calls=%async_computation.1 | async-start | bytes 4194304 | tf_op jit(solution)/shard_map/all_to_all | solution.py:38
  50.5 22.2 %all-to-all-done.1 = bf16[16,16,32,128]{3,2,1,0:T(8,128)(2,1)S(1)} async-done(((bf16[16,16,32,128]{3,2,1,0:T(8,128)(2,1)}), bf16[16,16,32,128]{3,2,1,0:T(8,128)(2,1)S(1)}, u32[]{:S(2)}, u32[]{:S(2)}) %all-to-all-start.1) | async-done | bytes 2097184 | tf_op jit(solution)/shard_map/all_to_all | solution.py:38
  72.7 1.6 copy-done.1
  75.7 38.7 %all-gather.6.cloned.1.call-done = bf16[4096,128]{1,0:T(8,128)(2,1)} async-done(((bf16[256,128]{1,0:T(8,128)(2,1)}), bf16[4096,128]{1,0:T(8,128)(2,1)}) %all-gather.6.cloned.1.call-update) | async-done | bytes 1048592 | tf_op jit(solution)/shard_map/all_gather | solution.py:273
  114.4 3.4 %collective-permute-start.7 = (s32[8,16]{1,0:T(8,128)S(1)}, s32[8,16]{1,0:T(8,128)S(1)}, u32[]{:S(2)}, u32[]{:S(2)}) collective-permute-start(s32[8,16]{1,0:T(8,128)S(1)} %copy-done.7), channel_id=1, source_target_pairs={{6,0},{0,2},{2,4},{4,6},{7,1},{1,3},{3,5},{5,7},{14,8},{8,10},{10,... | collective-permute-start | bytes 1544 | tf_op jit(solution)/shard_map/ppermute | solution.py:45
  117.8 4.6 %collective-permute-start.6 = (s32[8,16]{1,0:T(8,128)S(1)}, s32[8,16]{1,0:T(8,128)S(1)}, u32[]{:S(2)}, u32[]{:S(2)}) collective-permute-start(s32[8,16]{1,0:T(8,128)S(1)} %copy-done.7), channel_id=1, source_target_pairs={{4,0},{6,2},{0,4},{2,6},{5,1},{7,3},{1,5},{3,7},{12,8},{14,10},{8,... | collective-permute-start | bytes 1544 | tf_op jit(solution)/shard_map/ppermute | solution.py:45
  122.4 3.3 %collective-permute-start.5 = (s32[8,16]{1,0:T(8,128)S(1)}, s32[8,16]{1,0:T(8,128)S(1)}, u32[]{:S(2)}, u32[]{:S(2)}) collective-permute-start(s32[8,16]{1,0:T(8,128)S(1)} %copy-done.7), channel_id=1, source_target_pairs={{2,0},{4,2},{6,4},{0,6},{3,1},{5,3},{7,5},{1,7},{10,8},{12,10},{14... | collective-permute-start | bytes 1544 | tf_op jit(solution)/shard_map/ppermute | solution.py:45
  125.8 1.9 fusion.12
  127.6 2.1 fusion.13
  129.7 2.5 collective-permute-start.2
  132.2 2.8 collective-permute-start.1
  136.8 3.7 %collective-permute-start = (bf16[16,128,128]{2,1,0:T(8,128)(2,1)S(1)}, bf16[16,128,128]{2,1,0:T(8,128)(2,1)}, u32[]{:S(2)}, u32[]{:S(2)}) collective-permute-start(bf16[16,128,128]{2,1,0:T(8,128)(2,1)S(1)} %get-tuple-element.40.refs_0_), channel_id=1, source_target_pairs={{2,0},{4,2},{6,4},{0,6},{3,1},{5,3},{7,5},{1,7},{10,8},{12,10},{14... | collective-permute-start | bytes 1572872 | tf_op jit(solution)/shard_map/ppermute | solution.py:45
  145.5 59.1 %all-gather.4.cloned.1.call-done.b_ref = bf16[128,32,256]{2,1,0:T(8,128)(2,1)} async-done(((bf16[8,32,256]{2,1,0:T(8,128)(2,1)}), bf16[128,32,256]{2,1,0:T(8,128)(2,1)}) %all-gather.4.cloned.1.call-update) | async-done | bytes 2097168 | tf_op jit(solution)/shard_map/all_gather | solution.py:283
  204.6 1.6 copy-done.4
  206.2 2.1 shard_map.75
  208.3 4.3 %all-to-all-start.2 = ((bf16[4,32,32,256]{3,2,1,0:T(8,128)(2,1)}), bf16[4,32,32,256]{3,2,1,0:T(8,128)(2,1)S(1)}, u32[]{:S(2)}, u32[]{:S(2)}) async-start(bf16[4,32,32,256]{3,2,1,0:T(8,128)(2,1)} %shard_map.75), calls=%async_computation.2 | async-start | bytes 4194304 | tf_op jit(solution)/shard_map/all_to_all | solution.py:324
  212.8 3.4 %collective-permute-start.10 = (bf16[16,64,128]{2,1,0:T(8,128)(2,1)}, bf16[16,64,128]{2,1,0:T(8,128)(2,1)S(1)}, u32[]{:S(2)}, u32[]{:S(2)}) collective-permute-start(bf16[16,64,128]{2,1,0:T(8,128)(2,1)} %get-tuple-element.37), channel_id=1, source_target_pairs={{384,0},{0,128},{128,256},{256,384},{385,1},{1,129},{129,257},{257... | collective-permute-start | bytes 786440 | tf_op jit(solution)/shard_map/ppermute | solution.py:45
  216.2 2.5 collective-permute-start.9
  220.3 3.8 %collective-permute-start.3 = (bf16[4096,128]{1,0:T(8,128)(2,1)S(1)}, bf16[4096,128]{1,0:T(8,128)(2,1)S(1)}, u32[]{:S(2)}, u32[]{:S(2)}) collective-permute-start(bf16[4096,128]{1,0:T(8,128)(2,1)S(1)} %bitcast.37), channel_id=1, source_target_pairs={{128,0},{256,128},{384,256},{0,384},{129,1},{257,129},{385,257},{1... | collective-permute-start | bytes 3145736 | tf_op jit(solution)/shard_map/ppermute | solution.py:45
  224.1 2.2 collective-permute-start.4
  227.7 3.9 %collective-permute-start.13 = (bf16[16,16,2048]{2,1,0:T(8,128)(2,1)S(1)}, bf16[16,16,2048]{2,1,0:T(8,128)(2,1)}, u32[]{:S(2)}, u32[]{:S(2)}) collective-permute-start(bf16[16,16,2048]{2,1,0:T(8,128)(2,1)S(1)} %shard_map.79.refs_0_), channel_id=1, source_target_pairs={{6,0},{0,2},{2,4},{4,6},{7,1},{1,3},{3,5},{5,7},{14,8},{8,10},{10,... | collective-permute-start | bytes 3145736 | tf_op jit(solution)/shard_map/ppermute | solution.py:45
  231.7 4.6 %collective-permute-start.12 = (bf16[16,16,2048]{2,1,0:T(8,128)(2,1)S(1)}, bf16[16,16,2048]{2,1,0:T(8,128)(2,1)}, u32[]{:S(2)}, u32[]{:S(2)}) collective-permute-start(bf16[16,16,2048]{2,1,0:T(8,128)(2,1)S(1)} %shard_map.79.refs_0_), channel_id=1, source_target_pairs={{4,0},{6,2},{0,4},{2,6},{5,1},{7,3},{1,5},{3,7},{12,8},{14,10},{8,... | collective-permute-start | bytes 3145736 | tf_op jit(solution)/shard_map/ppermute | solution.py:45
  236.3 3.4 %collective-permute-start.11 = (bf16[16,16,2048]{2,1,0:T(8,128)(2,1)S(1)}, bf16[16,16,2048]{2,1,0:T(8,128)(2,1)}, u32[]{:S(2)}, u32[]{:S(2)}) collective-permute-start(bf16[16,16,2048]{2,1,0:T(8,128)(2,1)S(1)} %shard_map.79.refs_0_), channel_id=1, source_target_pairs={{2,0},{4,2},{6,4},{0,6},{3,1},{5,3},{7,5},{1,7},{10,8},{12,10},{14... | collective-permute-start | bytes 3145736 | tf_op jit(solution)/shard_map/ppermute | solution.py:45
  240.7 2.7 collective-permute-done.4.refs_3_
  246.3 3.4 %shard_map.78.m_ref = bf16[256,512]{1,0:T(8,128)(2,1)S(1)} custom-call(s32[3]{0:T(128)S(1)} %pad_add_fusion.7.f_ref, s32[8,16]{1,0:T(8,128)S(1)} %fusion.4.p_ref, bf16[256,512]{1,0:T(8,128)(2,1)S(1)} %copy-done.6, bf16[128,32,256]{2,1,0:T(8,128)(2,1)S(1)} %bitcast.34, bf16[8,32,256]{2,1,0:T(8,128)(2,1)} %bitcast.18.own_ref, s32[8,1,512]{2,1,0:T(1,128)S(1)} %shard_map.77.kp_ref), custom_call_target="tpu_custom_call" | custom-call | flops 268435456 | tf_op jit(solution)/shard_map/pallas_call | solution.py:25
  249.7 1.9 collective-permute-start.8
  251.7 6.7 %collective-permute-done.13.refs_3_ = bf16[16,16,2048]{2,1,0:T(8,128)(2,1)} collective-permute-done((bf16[16,16,2048]{2,1,0:T(8,128)(2,1)S(1)}, bf16[16,16,2048]{2,1,0:T(8,128)(2,1)}, u32[]{:S(2)}, u32[]{:S(2)}) %collective-permute-start.13) | collective-permute-done | bytes 1048608 | tf_op jit(solution)/shard_map/ppermute | solution.py:45
  258.4 16.3 %collective-permute-done.12.refs_2_ = bf16[16,16,2048]{2,1,0:T(8,128)(2,1)} collective-permute-done((bf16[16,16,2048]{2,1,0:T(8,128)(2,1)S(1)}, bf16[16,16,2048]{2,1,0:T(8,128)(2,1)}, u32[]{:S(2)}, u32[]{:S(2)}) %collective-permute-start.12) | collective-permute-done | bytes 1048608 | tf_op jit(solution)/shard_map/ppermute | solution.py:45
  274.7 4.4 %shard_map.80 = bf16[256,2048]{1,0:T(8,128)(2,1)} custom-call(s32[2]{0:T(128)S(1)} %pad_add_fusion.6.p_ref, bf16[256,512]{1,0:T(8,128)(2,1)S(1)} %shard_map.78.m_ref, bf16[256,512]{1,0:T(8,128)(2,1)S(1)} %collective-permute-done.8.t_ref, bf16[16,16,2048]{2,1,0:T(8,128)(2,1)S(1)} %shard_map.79.refs_0_, bf16[16,16,2048]{2,1,0:T(8,128)(2,1)} %collective-permute-done.11.refs_1_, ...), custom_call_target="tpu_custom_call" | custom-call | flops 1073741824 | tf_op jit(solution)/shard_map/pallas_call | solution.py:25
  (125 shorter events, 25.6 us)
Async XLA Ops:
  6.5 0.7 copy-start
  8.6 30.0 %all-to-all-start = ((bf16[16,32,128]{2,1,0:T(8,128)(2,1)}), bf16[16,32,128]{2,1,0:T(8,128)(2,1)S(1)}, u32[]{:S(2)}, u32[]{:S(2)}) async-start(bf16[16,32,128]{2,1,0:T(8,128)(2,1)} %broadcast_in_dim.127), calls=%async_computation | async-start | bytes 262144 | tf_op jit(solution)/shard_map/all_to_all | solution.py:38
  40.4 32.3 %all-to-all-start.1 = ((bf16[16,16,32,128]{3,2,1,0:T(8,128)(2,1)}), bf16[16,16,32,128]{3,2,1,0:T(8,128)(2,1)S(1)}, u32[]{:S(2)}, u32[]{:S(2)}) async-start(bf16[16,16,32,128]{3,2,1,0:T(8,128)(2,1)} %broadcast_in_dim.128), calls=%async_computation.1 | async-start | bytes 4194304 | tf_op jit(solution)/shard_map/all_to_all | solution.py:38
  47.8 66.5 %all-gather.6.cloned.1.call-start = ((), (), s32[]{:S(2)}) async-start(), calls=%async_computation.4 | async-start | bytes 1114112 | tf_op jit(solution)/shard_map/all_gather | solution.py:273
  48.6 0.6 copy-start.8
  49.2 155.4 %all-gather.4.cloned.1.call-start = ((), (), s32[]{:S(2)}) async-start(), calls=%async_computation.3 | async-start | bytes 2228224 | tf_op jit(solution)/shard_map/all_gather | solution.py:283
  72.7 1.6 copy-start.1
  74.3 40.0 %copy-start.7 = (s32[8,16]{1,0:T(8,128)S(1)}, s32[8,16]{1,0:T(8,128)}, u32[]{:S(2)}) copy-start(s32[8,16]{1,0:T(8,128)} %c_ref) | copy-start | bytes 1540
  114.4 22.4 %collective-permute-start.7 = (s32[8,16]{1,0:T(8,128)S(1)}, s32[8,16]{1,0:T(8,128)S(1)}, u32[]{:S(2)}, u32[]{:S(2)}) collective-permute-start(s32[8,16]{1,0:T(8,128)S(1)} %copy-done.7), channel_id=1, source_target_pairs={{6,0},{0,2},{2,4},{4,6},{7,1},{1,3},{3,5},{5,7},{14,8},{8,10},{10,... | collective-permute-start | bytes 1544 | tf_op jit(solution)/shard_map/ppermute | solution.py:45
  117.8 22.8 %collective-permute-start.6 = (s32[8,16]{1,0:T(8,128)S(1)}, s32[8,16]{1,0:T(8,128)S(1)}, u32[]{:S(2)}, u32[]{:S(2)}) collective-permute-start(s32[8,16]{1,0:T(8,128)S(1)} %copy-done.7), channel_id=1, source_target_pairs={{4,0},{6,2},{0,4},{2,6},{5,1},{7,3},{1,5},{3,7},{12,8},{14,10},{8,... | collective-permute-start | bytes 1544 | tf_op jit(solution)/shard_map/ppermute | solution.py:45
  122.4 18.2 %collective-permute-start.5 = (s32[8,16]{1,0:T(8,128)S(1)}, s32[8,16]{1,0:T(8,128)S(1)}, u32[]{:S(2)}, u32[]{:S(2)}) collective-permute-start(s32[8,16]{1,0:T(8,128)S(1)} %copy-done.7), channel_id=1, source_target_pairs={{2,0},{4,2},{6,4},{0,6},{3,1},{5,3},{7,5},{1,7},{10,8},{12,10},{14... | collective-permute-start | bytes 1544 | tf_op jit(solution)/shard_map/ppermute | solution.py:45
  129.7 88.9 %collective-permute-start.2 = (bf16[16,128,128]{2,1,0:T(8,128)(2,1)S(1)}, bf16[16,128,128]{2,1,0:T(8,128)(2,1)S(1)}, u32[]{:S(2)}, u32[]{:S(2)}) collective-permute-start(bf16[16,128,128]{2,1,0:T(8,128)(2,1)S(1)} %get-tuple-element.40.refs_0_), channel_id=1, source_target_pairs={{6,0},{0,2},{2,4},{4,6},{7,1},{1,3},{3,5},{5,7},{14,8},{8,10},{10,... | collective-permute-start | bytes 1572872 | tf_op jit(solution)/shard_map/ppermute | solution.py:45
  132.2 86.4 %collective-permute-start.1 = (bf16[16,128,128]{2,1,0:T(8,128)(2,1)S(1)}, bf16[16,128,128]{2,1,0:T(8,128)(2,1)}, u32[]{:S(2)}, u32[]{:S(2)}) collective-permute-start(bf16[16,128,128]{2,1,0:T(8,128)(2,1)S(1)} %get-tuple-element.40.refs_0_), channel_id=1, source_target_pairs={{4,0},{6,2},{0,4},{2,6},{5,1},{7,3},{1,5},{3,7},{12,8},{14,10},{8,... | collective-permute-start | bytes 1572872 | tf_op jit(solution)/shard_map/ppermute | solution.py:45
  136.8 81.9 %collective-permute-start = (bf16[16,128,128]{2,1,0:T(8,128)(2,1)S(1)}, bf16[16,128,128]{2,1,0:T(8,128)(2,1)}, u32[]{:S(2)}, u32[]{:S(2)}) collective-permute-start(bf16[16,128,128]{2,1,0:T(8,128)(2,1)S(1)} %get-tuple-element.40.refs_0_), channel_id=1, source_target_pairs={{2,0},{4,2},{6,4},{0,6},{3,1},{5,3},{7,5},{1,7},{10,8},{12,10},{14... | collective-permute-start | bytes 1572872 | tf_op jit(solution)/shard_map/ppermute | solution.py:45
  204.6 1.6 copy-start.4
  208.3 37.1 %all-to-all-start.2 = ((bf16[4,32,32,256]{3,2,1,0:T(8,128)(2,1)}), bf16[4,32,32,256]{3,2,1,0:T(8,128)(2,1)S(1)}, u32[]{:S(2)}, u32[]{:S(2)}) async-start(bf16[4,32,32,256]{3,2,1,0:T(8,128)(2,1)} %shard_map.75), calls=%async_computation.2 | async-start | bytes 4194304 | tf_op jit(solution)/shard_map/all_to_all | solution.py:324
  212.8 14.4 %collective-permute-start.10 = (bf16[16,64,128]{2,1,0:T(8,128)(2,1)}, bf16[16,64,128]{2,1,0:T(8,128)(2,1)S(1)}, u32[]{:S(2)}, u32[]{:S(2)}) collective-permute-start(bf16[16,64,128]{2,1,0:T(8,128)(2,1)} %get-tuple-element.37), channel_id=1, source_target_pairs={{384,0},{0,128},{128,256},{256,384},{385,1},{1,129},{129,257},{257... | collective-permute-start | bytes 786440 | tf_op jit(solution)/shard_map/ppermute | solution.py:45
  216.2 11.3 %collective-permute-start.9 = (bf16[16,64,128]{2,1,0:T(8,128)(2,1)}, bf16[16,64,128]{2,1,0:T(8,128)(2,1)S(1)}, u32[]{:S(2)}, u32[]{:S(2)}) collective-permute-start(bf16[16,64,128]{2,1,0:T(8,128)(2,1)} %get-tuple-element.38), channel_id=1, source_target_pairs={{128,0},{256,128},{384,256},{0,384},{129,1},{257,129},{385,257},{1... | collective-permute-start | bytes 786440 | tf_op jit(solution)/shard_map/ppermute | solution.py:45
  220.0 7.4 %copy-start.3 = (bf16[16,128,128]{2,1,0:T(8,128)(2,1)S(1)}, bf16[16,128,128]{2,1,0:T(8,128)(2,1)}, u32[]{:S(2)}) copy-start(bf16[16,128,128]{2,1,0:T(8,128)(2,1)} %get-tuple-element.39.own_ref) | copy-start | bytes 1572868
  220.3 23.1 %copy-start.2 = (bf16[256,4096]{1,0:T(8,128)(2,1)S(1)}, bf16[256,4096]{1,0:T(8,128)(2,1)}, u32[]{:S(2)}) copy-start(bf16[256,4096]{1,0:T(8,128)(2,1)} %t_ref.3) | copy-start | bytes 6291460
  220.3 20.4 %collective-permute-start.3 = (bf16[4096,128]{1,0:T(8,128)(2,1)S(1)}, bf16[4096,128]{1,0:T(8,128)(2,1)S(1)}, u32[]{:S(2)}, u32[]{:S(2)}) collective-permute-start(bf16[4096,128]{1,0:T(8,128)(2,1)S(1)} %bitcast.37), channel_id=1, source_target_pairs={{128,0},{256,128},{384,256},{0,384},{129,1},{257,129},{385,257},{1... | collective-permute-start | bytes 3145736 | tf_op jit(solution)/shard_map/ppermute | solution.py:45
  224.1 19.3 %collective-permute-start.4 = (bf16[4096,128]{1,0:T(8,128)(2,1)S(1)}, bf16[4096,128]{1,0:T(8,128)(2,1)S(1)}, u32[]{:S(2)}, u32[]{:S(2)}) collective-permute-start(bf16[4096,128]{1,0:T(8,128)(2,1)S(1)} %bitcast.35), channel_id=1, source_target_pairs={{384,0},{0,128},{128,256},{256,384},{385,1},{1,129},{129,257},{257... | collective-permute-start | bytes 3145736 | tf_op jit(solution)/shard_map/ppermute | solution.py:45
  227.7 30.7 %collective-permute-start.13 = (bf16[16,16,2048]{2,1,0:T(8,128)(2,1)S(1)}, bf16[16,16,2048]{2,1,0:T(8,128)(2,1)}, u32[]{:S(2)}, u32[]{:S(2)}) collective-permute-start(bf16[16,16,2048]{2,1,0:T(8,128)(2,1)S(1)} %shard_map.79.refs_0_), channel_id=1, source_target_pairs={{6,0},{0,2},{2,4},{4,6},{7,1},{1,3},{3,5},{5,7},{14,8},{8,10},{10,... | collective-permute-start | bytes 3145736 | tf_op jit(solution)/shard_map/ppermute | solution.py:45
  231.7 43.0 %collective-permute-start.12 = (bf16[16,16,2048]{2,1,0:T(8,128)(2,1)S(1)}, bf16[16,16,2048]{2,1,0:T(8,128)(2,1)}, u32[]{:S(2)}, u32[]{:S(2)}) collective-permute-start(bf16[16,16,2048]{2,1,0:T(8,128)(2,1)S(1)} %shard_map.79.refs_0_), channel_id=1, source_target_pairs={{4,0},{6,2},{0,4},{2,6},{5,1},{7,3},{1,5},{3,7},{12,8},{14,10},{8,... | collective-permute-start | bytes 3145736 | tf_op jit(solution)/shard_map/ppermute | solution.py:45
  236.3 38.4 %collective-permute-start.11 = (bf16[16,16,2048]{2,1,0:T(8,128)(2,1)S(1)}, bf16[16,16,2048]{2,1,0:T(8,128)(2,1)}, u32[]{:S(2)}, u32[]{:S(2)}) collective-permute-start(bf16[16,16,2048]{2,1,0:T(8,128)(2,1)S(1)} %shard_map.79.refs_0_), channel_id=1, source_target_pairs={{2,0},{4,2},{6,4},{0,6},{3,1},{5,3},{7,5},{1,7},{10,8},{12,10},{14... | collective-permute-start | bytes 3145736 | tf_op jit(solution)/shard_map/ppermute | solution.py:45
  244.7 0.7 copy-start.5
  245.4 1.0 copy-start.6
  249.7 25.0 %collective-permute-start.8 = (bf16[256,512]{1,0:T(8,128)(2,1)S(1)}, bf16[256,512]{1,0:T(8,128)(2,1)S(1)}, u32[]{:S(2)}, u32[]{:S(2)}) collective-permute-start(bf16[256,512]{1,0:T(8,128)(2,1)S(1)} %shard_map.78.m_ref), channel_id=1, source_target_pairs={{1,0},{0,1},{3,2},{2,3},{5,4},{4,5},{7,6},{6,7},{9,8},{8,9},{11,10... | collective-permute-start | bytes 786440 | tf_op jit(solution)/shard_map/ppermute | solution.py:45
Sparse Core Ops, SparseCore 0:
  50.7 63.5 all-gather.5
  135.2 69.3 all-gather.3

commit v2 on v1

--- a/solution.py
+++ b/solution.py
@@ -26,7 +26,7 @@
         kernel,
         out_shape=out_shape,
         in_specs=spaces,
-        out_specs=pl.BlockSpec(memory_space=pltpu.VMEM),
+        out_specs=jax.tree.map(lambda _: pl.BlockSpec(memory_space=pltpu.VMEM), out_shape),
         scratch_shapes=list(scratch),
         compiler_params=pltpu.CompilerParams(vmem_limit_bytes=40 << 20),
         cost_estimate=pl.CostEstimate(flops=flops, bytes_accessed=0, transcendentals=0),
@@ -66,6 +66,36 @@
         found = jnp.any(marked, axis=1)
         lists.append(jnp.where(found, jnp.sum(jnp.where(marked, local_ids, 0), axis=1), -1))
     return jnp.stack(lists, axis=1)
+
+
+def pack(query_weight, key_weight, value_weight, out_weight, x_at, planes, tall):
+    rows = key_weight.shape[0]
+    lines, wide_out = out_weight.shape
+    small = rows // planes
+    q_groups = query_weight.shape[1] // 2 // HD
+    o_groups = wide_out // 2 // HD
+
+    def kernel(x_ref, q_ref, k_ref, v_ref, o_ref, half_ref, cargo_ref):
+        parity = x_ref[0] % 2
+        for i in range(q_groups):
+            first = pl.multiple_of((parity * q_groups + i) * HD, HD)
+            half_ref[i * rows : (i + 1) * rows] = q_ref[:, pl.ds(first, HD)]
+        base = q_groups * rows
+        for i in range(o_groups):
+            first = pl.multiple_of((parity * o_groups + i) * HD, HD)
+            half_ref[base + i * lines : base + (i + 1) * lines] = o_ref[:, pl.ds(first, HD)]
+        first = pl.multiple_of(x_ref[0] * small, small)
+        keys = k_ref[pl.ds(first, small)]
+        values = v_ref[pl.ds(first, small)]
+        for z in range(tall):
+            cargo_ref[z, :small] = keys
+            cargo_ref[z, small:] = values
+
+    outs = (
+        jax.ShapeDtypeStruct((q_groups * rows + o_groups * lines, HD), BF16),
+        jax.ShapeDtypeStruct((tall, 2 * small, HD), BF16),
+    )
+    return call(kernel, outs, x_at[None], query_weight, key_weight, value_weight, out_weight)
 
 
 def project_pair(tokens, every):
@@ -252,29 +282,13 @@
     owners = tall * wide
     me = z_at * wide + y_at
 
-    def stacked(w):
-        return jnp.concatenate(
-            [w[:, i * HD : (i + 1) * HD] for i in range(w.shape[1] // HD)], axis=0
-        )
-
-    def part(w, dim):
-        size = w.shape[dim] // planes
-        return lax.dynamic_slice_in_dim(w, x_at * size, size, axis=dim)
-
     parity = x_at % 2
     lines = out_weight.shape[0]
-    q_half = lax.dynamic_slice_in_dim(
-        query_weight, parity * (query_weight.shape[1] // 2), query_weight.shape[1] // 2, axis=1
-    )
-    o_half = lax.dynamic_slice_in_dim(
-        out_weight, parity * (out_weight.shape[1] // 2), out_weight.shape[1] // 2, axis=1
-    )
-    halves = jnp.concatenate([stacked(q_half), stacked(o_half)], axis=0)
+    halves, cargo = pack(query_weight, key_weight, value_weight, out_weight, x_at, planes, tall)
     halves = lax.all_gather(halves, "kv_0", axis=0, tiled=False)
 
-    pair_rows = 2 * (key_weight.shape[0] // planes)
-    cargo = jnp.concatenate([part(key_weight, 0), part(value_weight, 0)], axis=0)
-    column = copy_for_each(cargo, "kv_0")
+    pair_rows = cargo.shape[1]
+    column = lax.all_to_all(cargo, "kv_0", 0, 0, tiled=True)
     every = copy_for_each(column, ("dp", "kv_1"))
     every = every.reshape(planes, wide, tall, pair_rows, HD)
     paired = project_pair(tokens, every)

time: 287 us -> 288 us (level)
  blocking collectives: 0 us -> 29.8 us
  starting transfers between devices: 73 us -> 57.8 us
  waiting for transfers between devices: 154 us -> 147 us
  local copies, waits for them, and re-layouts: 22.4 us -> 15.8 us
    all_to_all x0 -> x1, blocking collectives: none -> 29.8 us  [body(): column = lax.all_to_all(cargo, 'kv_0', 0, 0, tiled=True)]
    all_to_all x2 -> x1, starting transfers between devices: 22.7 us -> 7.48 us  [copy_for_each(): lax.all_to_all(jnp.broadcast_to(shard[None], (count, *shard.shape)), axis...]
    all_to_all x2 -> x1, waiting for transfers between devices: 30.6 us -> 22.9 us  [copy_for_each(): lax.all_to_all(jnp.broadcast_to(shard[None], (count, *shard.shape)), axis...]
    unnamed x27 -> x22, local copies, waits for them, and re-layouts: 12.5 us -> 7.96 us
    pallas_call x8 -> x9, Pallas kernels: 14.8 us -> 15.4 us  [call(): pl.pallas_call(kernel, out_shape=out_shape, in_specs=spaces, out_specs=ja...]
  transfers between devices with their start and end apart: 19 -> 18, of which waited for: 8 -> 7; matrix products, arithmetic and copies ran while one was open for 7% -> 4% of each run, Pallas kernels for 4% -> 4%
where the time goes in v2:
time: 288 us; the launch traced here: 287 us
  waiting for transfers between devices  147 us (51%)
  starting transfers between devices  57.8 us (20%)
  blocking collectives  29.8 us (10%)
  local copies, waits for them, and re-layouts  15.8 us (5%)
  Pallas kernels  15.4 us (5%)
  between operations  14.6 us (5%)
  other arithmetic  6.67 us (2%)
    all_gather x1, waiting for transfers between devices, body(): column_blocks = lax.all_gather(local_blocks, 'kv_0', axis=0, tiled=True)  59.1 us
    ppermute x14, starting transfers between devices, from_ahead(): return lax.ppermute(x, axis, [((i + step) % n, i) for i in range(n)])  46 us
    all_gather x1, waiting for transfers between devices, body(): halves = lax.all_gather(halves, 'kv_0', axis=0, tiled=False)  38.7 us
    all_to_all x1, blocking collectives, body(): column = lax.all_to_all(cargo, 'kv_0', 0, 0, tiled=True)  29.8 us
    ppermute x14, waiting for transfers between devices, from_ahead(): return lax.ppermute(x, axis, [((i + step) % n, i) for i in range(n)])  26 us
    all_to_all x1, waiting for transfers between devices, copy_for_each(): lax.all_to_all(jnp.broadcast_to(shard[None], (count, *shard.shape)), axis...  22.9 us
    pallas_call x9, Pallas kernels, call(): pl.pallas_call(kernel, out_shape=out_shape, in_specs=spaces, out_specs=ja...  15.4 us
    unnamed x22, local copies, waits for them, and re-layouts  7.96 us
  transfers between devices with their start and end apart: 18, of which 7 were waited for; matrix products, arithmetic and copies ran while one was open for 4% of the time, Pallas kernels for 4%

profile of v2, /device:TPU:2, one launch (start us, length us, event | category | flops | bytes accessed | tf_op | source)
XLA Modules:
  0.0 287.4 jit_solution(14435556738401183726)
XLA Ops:
  10.3 29.8 %all_to_all.15 = bf16[16,32,128]{2,1,0:T(8,128)(2,1)S(1)} all-to-all(bf16[16,32,128]{2,1,0:T(8,128)(2,1)S(1)} %get-tuple-element.10), channel_id=1, replica_groups=mesh['dp'=4,'kv_0'=16,'kv_1'=4,'tp'=2] {'kv_0'}, dimensions={0} | all-to-all | bytes 262144 | tf_op jit(solution)/shard_map/all_to_all | solution.py:291
  40.1 1.8 broadcast_in_dim.125
  41.8 7.5 %all-to-all-start.1 = ((bf16[16,16,32,128]{3,2,1,0:T(8,128)(2,1)}), bf16[16,16,32,128]{3,2,1,0:T(8,128)(2,1)S(1)}, u32[]{:S(2)}, u32[]{:S(2)}) async-start(bf16[16,16,32,128]{3,2,1,0:T(8,128)(2,1)} %broadcast_in_dim.125), calls=%async_computation.1 | async-start | bytes 4194304 | tf_op jit(solution)/shard_map/all_to_all | solution.py:38
  51.3 22.9 %all-to-all-done.1 = bf16[16,16,32,128]{3,2,1,0:T(8,128)(2,1)S(1)} async-done(((bf16[16,16,32,128]{3,2,1,0:T(8,128)(2,1)}), bf16[16,16,32,128]{3,2,1,0:T(8,128)(2,1)S(1)}, u32[]{:S(2)}, u32[]{:S(2)}) %all-to-all-start.1) | async-done | bytes 2097184 | tf_op jit(solution)/shard_map/all_to_all | solution.py:38
  74.2 1.6 copy-done
  75.8 1.4 shard_map.74
  77.1 38.7 %all-gather.6.cloned.1.call-done = bf16[4096,128]{1,0:T(8,128)(2,1)} async-done(((bf16[256,128]{1,0:T(8,128)(2,1)}), bf16[4096,128]{1,0:T(8,128)(2,1)}) %all-gather.6.cloned.1.call-update) | async-done | bytes 1048592 | tf_op jit(solution)/shard_map/all_gather | solution.py:288
  115.8 3.4 %collective-permute-start.7 = (s32[8,16]{1,0:T(8,128)S(1)}, s32[8,16]{1,0:T(8,128)S(1)}, u32[]{:S(2)}, u32[]{:S(2)}) collective-permute-start(s32[8,16]{1,0:T(8,128)S(1)} %copy-done.6), channel_id=1, source_target_pairs={{6,0},{0,2},{2,4},{4,6},{7,1},{1,3},{3,5},{5,7},{14,8},{8,10},{10,... | collective-permute-start | bytes 1544 | tf_op jit(solution)/shard_map/ppermute | solution.py:45
  119.2 4.6 %collective-permute-start.6 = (s32[8,16]{1,0:T(8,128)S(1)}, s32[8,16]{1,0:T(8,128)S(1)}, u32[]{:S(2)}, u32[]{:S(2)}) collective-permute-start(s32[8,16]{1,0:T(8,128)S(1)} %copy-done.6), channel_id=1, source_target_pairs={{4,0},{6,2},{0,4},{2,6},{5,1},{7,3},{1,5},{3,7},{12,8},{14,10},{8,... | collective-permute-start | bytes 1544 | tf_op jit(solution)/shard_map/ppermute | solution.py:45
  123.9 3.3 %collective-permute-start.5 = (s32[8,16]{1,0:T(8,128)S(1)}, s32[8,16]{1,0:T(8,128)S(1)}, u32[]{:S(2)}, u32[]{:S(2)}) collective-permute-start(s32[8,16]{1,0:T(8,128)S(1)} %copy-done.6), channel_id=1, source_target_pairs={{2,0},{4,2},{6,4},{0,6},{3,1},{5,3},{7,5},{1,7},{10,8},{12,10},{14... | collective-permute-start | bytes 1544 | tf_op jit(solution)/shard_map/ppermute | solution.py:45
  127.2 1.9 fusion.12
  129.1 2.1 fusion.13
  131.2 2.5 collective-permute-start.2
  133.7 2.8 collective-permute-start.1
  138.2 3.7 %collective-permute-start = (bf16[16,128,128]{2,1,0:T(8,128)(2,1)S(1)}, bf16[16,128,128]{2,1,0:T(8,128)(2,1)}, u32[]{:S(2)}, u32[]{:S(2)}) collective-permute-start(bf16[16,128,128]{2,1,0:T(8,128)(2,1)S(1)} %get-tuple-element.44.refs_0_), channel_id=1, source_target_pairs={{2,0},{4,2},{6,4},{0,6},{3,1},{5,3},{7,5},{1,7},{10,8},{12,10},{14... | collective-permute-start | bytes 1572872 | tf_op jit(solution)/shard_map/ppermute | solution.py:45
  147.0 59.1 %all-gather.4.cloned.1.call-done.b_ref = bf16[128,32,256]{2,1,0:T(8,128)(2,1)} async-done(((bf16[8,32,256]{2,1,0:T(8,128)(2,1)}), bf16[128,32,256]{2,1,0:T(8,128)(2,1)}) %all-gather.4.cloned.1.call-update) | async-done | bytes 2097168 | tf_op jit(solution)/shard_map/all_gather | solution.py:297
  206.1 1.6 copy-done.3
  207.6 2.1 shard_map.76
  209.7 4.3 %all-to-all-start.2 = ((bf16[4,32,32,256]{3,2,1,0:T(8,128)(2,1)}), bf16[4,32,32,256]{3,2,1,0:T(8,128)(2,1)S(1)}, u32[]{:S(2)}, u32[]{:S(2)}) async-start(bf16[4,32,32,256]{3,2,1,0:T(8,128)(2,1)} %shard_map.76), calls=%async_computation.2 | async-start | bytes 4194304 | tf_op jit(solution)/shard_map/all_to_all | solution.py:338
  214.2 3.4 %collective-permute-start.10 = (bf16[16,64,128]{2,1,0:T(8,128)(2,1)}, bf16[16,64,128]{2,1,0:T(8,128)(2,1)S(1)}, u32[]{:S(2)}, u32[]{:S(2)}) collective-permute-start(bf16[16,64,128]{2,1,0:T(8,128)(2,1)} %get-tuple-element.41), channel_id=1, source_target_pairs={{384,0},{0,128},{128,256},{256,384},{385,1},{1,129},{129,257},{257... | collective-permute-start | bytes 786440 | tf_op jit(solution)/shard_map/ppermute | solution.py:45
  217.6 2.5 collective-permute-start.9
  221.8 3.8 %collective-permute-start.3 = (bf16[4096,128]{1,0:T(8,128)(2,1)S(1)}, bf16[4096,128]{1,0:T(8,128)(2,1)S(1)}, u32[]{:S(2)}, u32[]{:S(2)}) collective-permute-start(bf16[4096,128]{1,0:T(8,128)(2,1)S(1)} %bitcast.38), channel_id=1, source_target_pairs={{128,0},{256,128},{384,256},{0,384},{129,1},{257,129},{385,257},{1... | collective-permute-start | bytes 3145736 | tf_op jit(solution)/shard_map/ppermute | solution.py:45
  225.6 2.2 collective-permute-start.4
  229.2 3.9 %collective-permute-start.13 = (bf16[16,16,2048]{2,1,0:T(8,128)(2,1)S(1)}, bf16[16,16,2048]{2,1,0:T(8,128)(2,1)}, u32[]{:S(2)}, u32[]{:S(2)}) collective-permute-start(bf16[16,16,2048]{2,1,0:T(8,128)(2,1)S(1)} %shard_map.80.refs_0_), channel_id=1, source_target_pairs={{6,0},{0,2},{2,4},{4,6},{7,1},{1,3},{3,5},{5,7},{14,8},{8,10},{10,... | collective-permute-start | bytes 3145736 | tf_op jit(solution)/shard_map/ppermute | solution.py:45
  233.1 4.6 %collective-permute-start.12 = (bf16[16,16,2048]{2,1,0:T(8,128)(2,1)S(1)}, bf16[16,16,2048]{2,1,0:T(8,128)(2,1)}, u32[]{:S(2)}, u32[]{:S(2)}) collective-permute-start(bf16[16,16,2048]{2,1,0:T(8,128)(2,1)S(1)} %shard_map.80.refs_0_), channel_id=1, source_target_pairs={{4,0},{6,2},{0,4},{2,6},{5,1},{7,3},{1,5},{3,7},{12,8},{14,10},{8,... | collective-permute-start | bytes 3145736 | tf_op jit(solution)/shard_map/ppermute | solution.py:45
  237.7 3.4 %collective-permute-start.11 = (bf16[16,16,2048]{2,1,0:T(8,128)(2,1)S(1)}, bf16[16,16,2048]{2,1,0:T(8,128)(2,1)}, u32[]{:S(2)}, u32[]{:S(2)}) collective-permute-start(bf16[16,16,2048]{2,1,0:T(8,128)(2,1)S(1)} %shard_map.80.refs_0_), channel_id=1, source_target_pairs={{2,0},{4,2},{6,4},{0,6},{3,1},{5,3},{7,5},{1,7},{10,8},{12,10},{14... | collective-permute-start | bytes 3145736 | tf_op jit(solution)/shard_map/ppermute | solution.py:45
  242.1 2.7 collective-permute-done.4.refs_3_
  247.8 3.4 %shard_map.79.m_ref = bf16[256,512]{1,0:T(8,128)(2,1)S(1)} custom-call(s32[3]{0:T(128)S(1)} %pad_add_fusion.7.f_ref, s32[8,16]{1,0:T(8,128)S(1)} %fusion.4.p_ref, bf16[256,512]{1,0:T(8,128)(2,1)S(1)} %copy-done.5, bf16[128,32,256]{2,1,0:T(8,128)(2,1)S(1)} %bitcast.35, bf16[8,32,256]{2,1,0:T(8,128)(2,1)} %bitcast.19.own_ref, s32[8,1,512]{2,1,0:T(1,128)S(1)} %shard_map.78.kp_ref), custom_call_target="tpu_custom_call" | custom-call | flops 268435456 | tf_op jit(solution)/shard_map/pallas_call | solution.py:25
  251.2 1.9 collective-permute-start.8
  253.2 6.7 %collective-permute-done.13.refs_3_ = bf16[16,16,2048]{2,1,0:T(8,128)(2,1)} collective-permute-done((bf16[16,16,2048]{2,1,0:T(8,128)(2,1)S(1)}, bf16[16,16,2048]{2,1,0:T(8,128)(2,1)}, u32[]{:S(2)}, u32[]{:S(2)}) %collective-permute-start.13) | collective-permute-done | bytes 1048608 | tf_op jit(solution)/shard_map/ppermute | solution.py:45
  259.9 16.3 %collective-permute-done.12.refs_2_ = bf16[16,16,2048]{2,1,0:T(8,128)(2,1)} collective-permute-done((bf16[16,16,2048]{2,1,0:T(8,128)(2,1)S(1)}, bf16[16,16,2048]{2,1,0:T(8,128)(2,1)}, u32[]{:S(2)}, u32[]{:S(2)}) %collective-permute-start.12) | collective-permute-done | bytes 1048608 | tf_op jit(solution)/shard_map/ppermute | solution.py:45
  276.2 4.4 %shard_map.81 = bf16[256,2048]{1,0:T(8,128)(2,1)} custom-call(s32[2]{0:T(128)S(1)} %pad_add_fusion.6.p_ref, bf16[256,512]{1,0:T(8,128)(2,1)S(1)} %shard_map.79.m_ref, bf16[256,512]{1,0:T(8,128)(2,1)S(1)} %collective-permute-done.8.t_ref, bf16[16,16,2048]{2,1,0:T(8,128)(2,1)S(1)} %shard_map.80.refs_0_, bf16[16,16,2048]{2,1,0:T(8,128)(2,1)} %collective-permute-done.11.refs_1_, ...), custom_call_target="tpu_custom_call" | custom-call | flops 1073741824 | tf_op jit(solution)/shard_map/pallas_call | solution.py:25
  (115 shorter events, 18.9 us)
Async XLA Ops:
  6.5 0.8 copy-start.7
  7.4 0.8 copy-start.8
  8.2 0.7 copy-start.9
  8.9 0.7 copy-start.10
  41.8 32.3 %all-to-all-start.1 = ((bf16[16,16,32,128]{3,2,1,0:T(8,128)(2,1)}), bf16[16,16,32,128]{3,2,1,0:T(8,128)(2,1)S(1)}, u32[]{:S(2)}, u32[]{:S(2)}) async-start(bf16[16,16,32,128]{3,2,1,0:T(8,128)(2,1)} %broadcast_in_dim.125), calls=%async_computation.1 | async-start | bytes 4194304 | tf_op jit(solution)/shard_map/all_to_all | solution.py:38
  49.3 66.5 %all-gather.6.cloned.1.call-start = ((), (), s32[]{:S(2)}) async-start(), calls=%async_computation.4 | async-start | bytes 1114112 | tf_op jit(solution)/shard_map/all_gather | solution.py:288
  50.0 156.0 %all-gather.4.cloned.1.call-start = ((), (), s32[]{:S(2)}) async-start(), calls=%async_computation.3 | async-start | bytes 2228224 | tf_op jit(solution)/shard_map/all_gather | solution.py:297
  74.2 1.6 copy-start
  75.8 40.0 %copy-start.6 = (s32[8,16]{1,0:T(8,128)S(1)}, s32[8,16]{1,0:T(8,128)}, u32[]{:S(2)}) copy-start(s32[8,16]{1,0:T(8,128)} %c_ref) | copy-start | bytes 1540
  115.8 22.4 %collective-permute-start.7 = (s32[8,16]{1,0:T(8,128)S(1)}, s32[8,16]{1,0:T(8,128)S(1)}, u32[]{:S(2)}, u32[]{:S(2)}) collective-permute-start(s32[8,16]{1,0:T(8,128)S(1)} %copy-done.6), channel_id=1, source_target_pairs={{6,0},{0,2},{2,4},{4,6},{7,1},{1,3},{3,5},{5,7},{14,8},{8,10},{10,... | collective-permute-start | bytes 1544 | tf_op jit(solution)/shard_map/ppermute | solution.py:45
  119.2 22.8 %collective-permute-start.6 = (s32[8,16]{1,0:T(8,128)S(1)}, s32[8,16]{1,0:T(8,128)S(1)}, u32[]{:S(2)}, u32[]{:S(2)}) collective-permute-start(s32[8,16]{1,0:T(8,128)S(1)} %copy-done.6), channel_id=1, source_target_pairs={{4,0},{6,2},{0,4},{2,6},{5,1},{7,3},{1,5},{3,7},{12,8},{14,10},{8,... | collective-permute-start | bytes 1544 | tf_op jit(solution)/shard_map/ppermute | solution.py:45
  123.9 18.2 %collective-permute-start.5 = (s32[8,16]{1,0:T(8,128)S(1)}, s32[8,16]{1,0:T(8,128)S(1)}, u32[]{:S(2)}, u32[]{:S(2)}) collective-permute-start(s32[8,16]{1,0:T(8,128)S(1)} %copy-done.6), channel_id=1, source_target_pairs={{2,0},{4,2},{6,4},{0,6},{3,1},{5,3},{7,5},{1,7},{10,8},{12,10},{14... | collective-permute-start | bytes 1544 | tf_op jit(solution)/shard_map/ppermute | solution.py:45
  131.2 88.9 %collective-permute-start.2 = (bf16[16,128,128]{2,1,0:T(8,128)(2,1)S(1)}, bf16[16,128,128]{2,1,0:T(8,128)(2,1)S(1)}, u32[]{:S(2)}, u32[]{:S(2)}) collective-permute-start(bf16[16,128,128]{2,1,0:T(8,128)(2,1)S(1)} %get-tuple-element.44.refs_0_), channel_id=1, source_target_pairs={{6,0},{0,2},{2,4},{4,6},{7,1},{1,3},{3,5},{5,7},{14,8},{8,10},{10,... | collective-permute-start | bytes 1572872 | tf_op jit(solution)/shard_map/ppermute | solution.py:45
  133.7 86.4 %collective-permute-start.1 = (bf16[16,128,128]{2,1,0:T(8,128)(2,1)S(1)}, bf16[16,128,128]{2,1,0:T(8,128)(2,1)}, u32[]{:S(2)}, u32[]{:S(2)}) collective-permute-start(bf16[16,128,128]{2,1,0:T(8,128)(2,1)S(1)} %get-tuple-element.44.refs_0_), channel_id=1, source_target_pairs={{4,0},{6,2},{0,4},{2,6},{5,1},{7,3},{1,5},{3,7},{12,8},{14,10},{8,... | collective-permute-start | bytes 1572872 | tf_op jit(solution)/shard_map/ppermute | solution.py:45
  138.2 81.9 %collective-permute-start = (bf16[16,128,128]{2,1,0:T(8,128)(2,1)S(1)}, bf16[16,128,128]{2,1,0:T(8,128)(2,1)}, u32[]{:S(2)}, u32[]{:S(2)}) collective-permute-start(bf16[16,128,128]{2,1,0:T(8,128)(2,1)S(1)} %get-tuple-element.44.refs_0_), channel_id=1, source_target_pairs={{2,0},{4,2},{6,4},{0,6},{3,1},{5,3},{7,5},{1,7},{10,8},{12,10},{14... | collective-permute-start | bytes 1572872 | tf_op jit(solution)/shard_map/ppermute | solution.py:45
  206.1 1.6 copy-start.3
  209.7 37.1 %all-to-all-start.2 = ((bf16[4,32,32,256]{3,2,1,0:T(8,128)(2,1)}), bf16[4,32,32,256]{3,2,1,0:T(8,128)(2,1)S(1)}, u32[]{:S(2)}, u32[]{:S(2)}) async-start(bf16[4,32,32,256]{3,2,1,0:T(8,128)(2,1)} %shard_map.76), calls=%async_computation.2 | async-start | bytes 4194304 | tf_op jit(solution)/shard_map/all_to_all | solution.py:338
  214.2 14.4 %collective-permute-start.10 = (bf16[16,64,128]{2,1,0:T(8,128)(2,1)}, bf16[16,64,128]{2,1,0:T(8,128)(2,1)S(1)}, u32[]{:S(2)}, u32[]{:S(2)}) collective-permute-start(bf16[16,64,128]{2,1,0:T(8,128)(2,1)} %get-tuple-element.41), channel_id=1, source_target_pairs={{384,0},{0,128},{128,256},{256,384},{385,1},{1,129},{129,257},{257... | collective-permute-start | bytes 786440 | tf_op jit(solution)/shard_map/ppermute | solution.py:45
  217.6 11.3 %collective-permute-start.9 = (bf16[16,64,128]{2,1,0:T(8,128)(2,1)}, bf16[16,64,128]{2,1,0:T(8,128)(2,1)S(1)}, u32[]{:S(2)}, u32[]{:S(2)}) collective-permute-start(bf16[16,64,128]{2,1,0:T(8,128)(2,1)} %get-tuple-element.42), channel_id=1, source_target_pairs={{128,0},{256,128},{384,256},{0,384},{129,1},{257,129},{385,257},{1... | collective-permute-start | bytes 786440 | tf_op jit(solution)/shard_map/ppermute | solution.py:45
  221.5 7.4 %copy-start.2 = (bf16[16,128,128]{2,1,0:T(8,128)(2,1)S(1)}, bf16[16,128,128]{2,1,0:T(8,128)(2,1)}, u32[]{:S(2)}) copy-start(bf16[16,128,128]{2,1,0:T(8,128)(2,1)} %get-tuple-element.43.own_ref) | copy-start | bytes 1572868
  221.7 23.1 %copy-start.1 = (bf16[256,4096]{1,0:T(8,128)(2,1)S(1)}, bf16[256,4096]{1,0:T(8,128)(2,1)}, u32[]{:S(2)}) copy-start(bf16[256,4096]{1,0:T(8,128)(2,1)} %t_ref.3) | copy-start | bytes 6291460
  221.8 20.4 %collective-permute-start.3 = (bf16[4096,128]{1,0:T(8,128)(2,1)S(1)}, bf16[4096,128]{1,0:T(8,128)(2,1)S(1)}, u32[]{:S(2)}, u32[]{:S(2)}) collective-permute-start(bf16[4096,128]{1,0:T(8,128)(2,1)S(1)} %bitcast.38), channel_id=1, source_target_pairs={{128,0},{256,128},{384,256},{0,384},{129,1},{257,129},{385,257},{1... | collective-permute-start | bytes 3145736 | tf_op jit(solution)/shard_map/ppermute | solution.py:45
  225.6 19.3 %collective-permute-start.4 = (bf16[4096,128]{1,0:T(8,128)(2,1)S(1)}, bf16[4096,128]{1,0:T(8,128)(2,1)S(1)}, u32[]{:S(2)}, u32[]{:S(2)}) collective-permute-start(bf16[4096,128]{1,0:T(8,128)(2,1)S(1)} %bitcast.36), channel_id=1, source_target_pairs={{384,0},{0,128},{128,256},{256,384},{385,1},{1,129},{129,257},{257... | collective-permute-start | bytes 3145736 | tf_op jit(solution)/shard_map/ppermute | solution.py:45
  229.2 30.7 %collective-permute-start.13 = (bf16[16,16,2048]{2,1,0:T(8,128)(2,1)S(1)}, bf16[16,16,2048]{2,1,0:T(8,128)(2,1)}, u32[]{:S(2)}, u32[]{:S(2)}) collective-permute-start(bf16[16,16,2048]{2,1,0:T(8,128)(2,1)S(1)} %shard_map.80.refs_0_), channel_id=1, source_target_pairs={{6,0},{0,2},{2,4},{4,6},{7,1},{1,3},{3,5},{5,7},{14,8},{8,10},{10,... | collective-permute-start | bytes 3145736 | tf_op jit(solution)/shard_map/ppermute | solution.py:45
  233.1 43.0 %collective-permute-start.12 = (bf16[16,16,2048]{2,1,0:T(8,128)(2,1)S(1)}, bf16[16,16,2048]{2,1,0:T(8,128)(2,1)}, u32[]{:S(2)}, u32[]{:S(2)}) collective-permute-start(bf16[16,16,2048]{2,1,0:T(8,128)(2,1)S(1)} %shard_map.80.refs_0_), channel_id=1, source_target_pairs={{4,0},{6,2},{0,4},{2,6},{5,1},{7,3},{1,5},{3,7},{12,8},{14,10},{8,... | collective-permute-start | bytes 3145736 | tf_op jit(solution)/shard_map/ppermute | solution.py:45
  237.7 38.5 %collective-permute-start.11 = (bf16[16,16,2048]{2,1,0:T(8,128)(2,1)S(1)}, bf16[16,16,2048]{2,1,0:T(8,128)(2,1)}, u32[]{:S(2)}, u32[]{:S(2)}) collective-permute-start(bf16[16,16,2048]{2,1,0:T(8,128)(2,1)S(1)} %shard_map.80.refs_0_), channel_id=1, source_target_pairs={{2,0},{4,2},{6,4},{0,6},{3,1},{5,3},{7,5},{1,7},{10,8},{12,10},{14... | collective-permute-start | bytes 3145736 | tf_op jit(solution)/shard_map/ppermute | solution.py:45
  246.1 0.7 copy-start.4
  246.8 1.0 copy-start.5
  251.2 25.0 %collective-permute-start.8 = (bf16[256,512]{1,0:T(8,128)(2,1)S(1)}, bf16[256,512]{1,0:T(8,128)(2,1)S(1)}, u32[]{:S(2)}, u32[]{:S(2)}) collective-permute-start(bf16[256,512]{1,0:T(8,128)(2,1)S(1)} %shard_map.79.m_ref), channel_id=1, source_target_pairs={{1,0},{0,1},{3,2},{2,3},{5,4},{4,5},{7,6},{6,7},{9,8},{8,9},{11,10... | collective-permute-start | bytes 786440 | tf_op jit(solution)/shard_map/ppermute | solution.py:45
Sparse Core Ops, SparseCore 0:
  52.2 63.5 all-gather.5
  136.6 69.3 all-gather.3

commit v3 on v2

--- a/solution.py
+++ b/solution.py
@@ -11,8 +11,10 @@
 BLOCK = 32
 CAP = 2
 NEVER = 1 << 30
-KV = ("kv_0", "kv_1")
-DP_KV = ("dp", "kv_0", "kv_1")
+TALL = ("zh", "zl")
+NEAR = ("zl", "y")
+KV = ("zh", "zl", "y")
+DP_KV = ("dp", "zh", "zl", "y")
 F32 = jnp.float32
 BF16 = jnp.bfloat16
 
@@ -50,40 +52,31 @@
     return [x, *(from_ahead(x, axis, s) for s in steps)]
 
 
-def after(*values):
-    return lax.optimization_barrier(values)
-
-
-def slots_wanted(chosen, owners, per_dev, me):
+def slots_wanted(chosen, owners, per_dev, readers):
     ids = owners[:, None] * per_dev + jnp.arange(per_dev, dtype=jnp.int32)[None, :]
-    hits = chosen.reshape(-1)[:, None, None] == ids[None]
-    needed = jnp.any(hits, axis=0) & (owners != me)[:, None]
-    ranks = jnp.cumsum(needed.astype(jnp.int32), axis=1)
-    local_ids = jnp.arange(per_dev, dtype=jnp.int32)[None, :]
+    hits = chosen[:, :, None, None] == ids[None, None]
+    needed = jnp.any(hits, axis=1) & (owners[None, :] != readers[:, None])[:, :, None]
+    ranks = jnp.cumsum(needed.astype(jnp.int32), axis=2)
+    local_ids = jnp.arange(per_dev, dtype=jnp.int32)
     lists = []
     for slot in range(CAP):
         marked = needed & (ranks == slot + 1)
-        found = jnp.any(marked, axis=1)
-        lists.append(jnp.where(found, jnp.sum(jnp.where(marked, local_ids, 0), axis=1), -1))
-    return jnp.stack(lists, axis=1)
+        found = jnp.any(marked, axis=2)
+        lists.append(jnp.where(found, jnp.sum(jnp.where(marked, local_ids, 0), axis=2), -1))
+    return jnp.stack(lists, axis=2)
 
 
 def pack(query_weight, key_weight, value_weight, out_weight, x_at, planes, tall):
     rows = key_weight.shape[0]
     lines, wide_out = out_weight.shape
     small = rows // planes
-    q_groups = query_weight.shape[1] // 2 // HD
-    o_groups = wide_out // 2 // HD
-
-    def kernel(x_ref, q_ref, k_ref, v_ref, o_ref, half_ref, cargo_ref):
-        parity = x_ref[0] % 2
-        for i in range(q_groups):
-            first = pl.multiple_of((parity * q_groups + i) * HD, HD)
-            half_ref[i * rows : (i + 1) * rows] = q_ref[:, pl.ds(first, HD)]
-        base = q_groups * rows
-        for i in range(o_groups):
-            first = pl.multiple_of((parity * o_groups + i) * HD, HD)
-            half_ref[base + i * lines : base + (i + 1) * lines] = o_ref[:, pl.ds(first, HD)]
+    groups = wide_out // planes // HD
+
+    def kernel(x_ref, q_ref, k_ref, v_ref, o_ref, part_ref, cargo_ref):
+        part_ref[:rows] = q_ref[:, pl.ds(pl.multiple_of(x_ref[0] * HD, HD), HD)]
+        for i in range(groups):
+            first = pl.multiple_of((x_ref[0] * groups + i) * HD, HD)
+            part_ref[rows + i * lines : rows + (i + 1) * lines] = o_ref[:, pl.ds(first, HD)]
         first = pl.multiple_of(x_ref[0] * small, small)
         keys = k_ref[pl.ds(first, small)]
         values = v_ref[pl.ds(first, small)]
@@ -92,10 +85,39 @@
             cargo_ref[z, small:] = values
 
     outs = (
-        jax.ShapeDtypeStruct((q_groups * rows + o_groups * lines, HD), BF16),
+        jax.ShapeDtypeStruct((rows + groups * lines, HD), BF16),
         jax.ShapeDtypeStruct((tall, 2 * small, HD), BF16),
     )
     return call(kernel, outs, x_at[None], query_weight, key_weight, value_weight, out_weight)
+
+
+def joined(pieces, at):
+    n = len(pieces)
+
+    def kernel(at_ref, *refs):
+        for s in range(n):
+            refs[-1][(at_ref[0] + s) % n] = refs[s][...]
+
+    out = jax.ShapeDtypeStruct((n, *pieces[0].shape), BF16)
+    return call(kernel, out, at[None], *pieces)
+
+
+def columns_of(pieces, at, rows):
+    n = len(pieces)
+    high, both, _ = pieces[0].shape
+
+    def kernel(at_ref, *refs):
+        for s in range(n):
+            for h in range(high):
+                z = h * n + (at_ref[0] + s) % n
+                refs[n][z] = refs[s][h, :rows]
+                refs[n + 1][z] = refs[s][h, rows:]
+
+    outs = (
+        jax.ShapeDtypeStruct((high * n, rows, HD), BF16),
+        jax.ShapeDtypeStruct((high * n, both - rows, HD), BF16),
+    )
+    return call(kernel, outs, at[None], *pieces)
 
 
 def project_pair(tokens, every):
@@ -138,38 +160,29 @@
 
 def turned(pieces, at):
     n = len(pieces)
-    tall, lines, _ = pieces[0].shape
-    columns = 2
-    rows = lines // columns
+    tall, rows, _ = pieces[0].shape
 
     def kernel(at_ref, *refs):
         for s in range(n):
-            y = (at_ref[0] + s) % n
-            for i in range(columns):
-                refs[-1][i, :, y] = refs[s][:, i * rows : (i + 1) * rows]
-
-    out = jax.ShapeDtypeStruct((columns, tall, n, rows, HD), BF16)
+            refs[-1][:, (at_ref[0] + s) % n] = refs[s][...]
+
+    out = jax.ShapeDtypeStruct((tall, n, rows, HD), BF16)
     return call(kernel, out, at[None], *pieces)
 
 
-def full_columns(own, ahead, behind, lines, parity):
-    tall, held, _ = own.shape
+def full_columns(pieces, at, lines):
+    n = len(pieces)
+    tall, held, _ = pieces[0].shape
     groups = held // lines
 
-    def kernel(p_ref, own_ref, ahead_ref, behind_ref, o_ref):
-        def put(half, i, value):
-            first = pl.multiple_of((half * groups + i) * HD, HD)
-            o_ref[:, :, pl.ds(first, HD)] = value
-
-        for i in range(groups):
-            put(p_ref[0], i, own_ref[:, i * lines : (i + 1) * lines])
-        for i in range(groups // 2):
-            cut = slice(i * lines, (i + 1) * lines)
-            put(1 - p_ref[0], i, ahead_ref[:, cut])
-            put(1 - p_ref[0], i + groups // 2, behind_ref[:, cut])
-
-    out = jax.ShapeDtypeStruct((tall, lines, 2 * groups * HD), BF16)
-    return call(kernel, out, parity[None], own, ahead, behind)
+    def kernel(at_ref, *refs):
+        for s in range(n):
+            for i in range(groups):
+                first = pl.multiple_of((((at_ref[0] + s) % n) * groups + i) * HD, HD)
+                refs[n][:, :, pl.ds(first, HD)] = refs[s][:, i * lines : (i + 1) * lines]
+
+    out = jax.ShapeDtypeStruct((tall, lines, n * groups * HD), BF16)
+    return call(kernel, out, at[None], *pieces)
 
 
 def key_positions(chosen):
@@ -188,16 +201,19 @@
     return call(kernel, out, chosen)
 
 
-def pick_blocks(blocks, asked):
-    wide, count = asked.shape
-
-    def kernel(asked_ref, b_ref, o_ref):
-        for y in range(wide):
-            for i in range(count):
-                o_ref[y, i] = b_ref[asked_ref[y, i]]
-
-    out = jax.ShapeDtypeStruct((wide, count, *blocks.shape[1:]), BF16)
-    return call(kernel, out, asked, blocks)
+def pick_blocks(blocks, asked, places):
+    low, wide, count = asked.shape
+
+    def kernel(asked_ref, p_ref, b_ref, o_ref):
+        for t in range(low):
+            for s in range(wide):
+                to = ((p_ref[0] + t) % low) * wide + (p_ref[1] + s) % wide
+                for i in range(count):
+                    o_ref[to, i] = b_ref[asked_ref[t * wide + s, i]]
+
+    out = jax.ShapeDtypeStruct((low * wide, count, *blocks.shape[1:]), BF16)
+    flat = asked.reshape(low * wide, count)
+    return call(kernel, out, flat, places, blocks)
 
 
 def attend(queries, incoming, local_blocks, position, key_pos, facts):
@@ -277,49 +293,52 @@
 def body(tokens, query_weight, key_weight, value_weight, out_weight, chosen, live_length):
     rows = tokens.shape[0]
     per_dev = rows // BLOCK
-    planes, tall, wide = (lax.axis_size(a) for a in ("dp", "kv_0", "kv_1"))
-    x_at, z_at, y_at = (lax.axis_index(a) for a in ("dp", "kv_0", "kv_1"))
+    planes, high, low, wide = (lax.axis_size(a) for a in ("dp", "zh", "zl", "y"))
+    x_at, h_at, l_at, y_at = (lax.axis_index(a) for a in ("dp", "zh", "zl", "y"))
+    tall = high * low
     owners = tall * wide
-    me = z_at * wide + y_at
-
-    parity = x_at % 2
-    lines = out_weight.shape[0]
-    halves, cargo = pack(query_weight, key_weight, value_weight, out_weight, x_at, planes, tall)
-    halves = lax.all_gather(halves, "kv_0", axis=0, tiled=False)
-
-    pair_rows = cargo.shape[1]
-    column = lax.all_to_all(cargo, "kv_0", 0, 0, tiled=True)
-    every = copy_for_each(column, ("dp", "kv_1"))
-    every = every.reshape(planes, wide, tall, pair_rows, HD)
+    me = lax.axis_index(KV)
+    places = jnp.stack([l_at, y_at])
+
+    part, cargo = pack(query_weight, key_weight, value_weight, out_weight, x_at, planes, tall)
+    column = lax.all_to_all(cargo, TALL, 0, 0, tiled=True)
+    parts = spread(part, "zh")
+    every = copy_for_each(column, ("dp", "y"))
+    every = every.reshape(planes, wide, tall, cargo.shape[1], HD)
+    parts = spread(joined(parts, h_at), "zl")
     paired = project_pair(tokens, every)
-    paired, halves, late_chosen = after(paired, halves, chosen)
     local_blocks = paired.reshape(per_dev, BLOCK, paired.shape[1])
-    column_blocks = lax.all_gather(local_blocks, "kv_0", axis=0, tiled=True)
-
-    q_lines = halves.shape[1] // 2
-    q_pieces = spread(halves[:, :q_lines], "kv_1")
-    o_own = halves[:, q_lines:]
-    cut = o_own.shape[1] // 2
-    o_ahead = from_ahead(o_own[:, :cut], "dp", 1)
-    o_behind = from_ahead(o_own[:, cut:], "dp", -1)
-    q_tall = turned(q_pieces, y_at).reshape(2, -1, HD)
-    q_pieces = [
-        q_tall[0], q_tall[1], from_ahead(q_tall[0], "dp", 1), from_ahead(q_tall[1], "dp", -1)
-    ]
-    o_pieces = spread(full_columns(o_own, o_ahead, o_behind, lines, parity), "kv_1")
-
-    mates = spread(late_chosen, "kv_1")
-    column_owners = jnp.arange(tall, dtype=jnp.int32) * wide + y_at
-    asked = jnp.stack(
-        [
-            slots_wanted(mates[s], column_owners, per_dev, z_at * wide + (y_at + s) % wide)
-            for s in range(wide)
-        ]
-    )
-    asked = jnp.maximum(asked, 0) + (jnp.arange(tall, dtype=jnp.int32) * per_dev)[None, :, None]
-    asked = jnp.roll(asked.reshape(wide, tall * CAP), y_at, axis=0)
-    safe = jnp.maximum(late_chosen, 0)
-    wanted = slots_wanted(late_chosen, jnp.arange(owners, dtype=jnp.int32), per_dev, me)
+    class_blocks = copy_for_each(local_blocks, "zh")
+
+    q_small, o_small = columns_of(parts, l_at, query_weight.shape[0])
+    q_pieces = spread(q_small, "y")
+    o_pieces = spread(o_small, "dp")
+    q_pieces = spread(turned(q_pieces, y_at).reshape(-1, HD), "dp")
+    o_pieces = spread(full_columns(o_pieces, x_at, out_weight.shape[0]), "y")
+
+    mates = jnp.stack(spread(chosen.reshape(-1), "y"))
+    mates = jnp.stack(spread(mates, "zl"))
+    ahead = jnp.arange(low, dtype=jnp.int32)[:, None], jnp.arange(wide, dtype=jnp.int32)[None, :]
+    readers = (h_at * low + (l_at + ahead[0]) % low) * wide + (y_at + ahead[1]) % wide
+    highs = jnp.arange(high, dtype=jnp.int32)
+    asked = slots_wanted(
+        mates.reshape(low * wide, -1),
+        (highs * low + l_at) * wide + y_at,
+        per_dev,
+        readers.reshape(-1),
+    )
+    asked = jnp.maximum(asked, 0) + (highs * per_dev)[None, :, None]
+    outgoing = pick_blocks(
+        class_blocks.reshape(high * per_dev, BLOCK, paired.shape[1]),
+        asked.reshape(low, wide, high * CAP),
+        places,
+    )
+    incoming = lax.all_to_all(outgoing, NEAR, split_axis=0, concat_axis=0, tiled=True)
+
+    safe = jnp.maximum(chosen, 0)
+    wanted = slots_wanted(
+        chosen.reshape(1, -1), jnp.arange(owners, dtype=jnp.int32), per_dev, me[None]
+    )[0]
     holder = safe // per_dev
     local_of = safe % per_dev
     match = (wanted[None, None, :, :] == local_of[:, :, None, None]) & (
@@ -328,14 +347,12 @@
     slot = jnp.sum(
         jnp.where(match, jnp.arange(CAP, dtype=jnp.int32)[None, None, None], 0), axis=(2, 3)
     )
-    far = wide * tall * CAP
-    remote_at = ((holder % wide) * tall + holder // wide) * CAP + slot
+    far = owners * CAP
+    remote_at = ((holder % (low * wide)) * high + holder // (low * wide)) * CAP + slot
     position = jnp.where(holder == me, far + local_of, remote_at)
-    key_pos = key_positions(late_chosen)
-    facts = jnp.stack([me * rows, live_length[0], 2 * parity]).astype(jnp.int32)
-
-    outgoing = pick_blocks(column_blocks, asked)
-    incoming = lax.all_to_all(outgoing, "kv_1", split_axis=0, concat_axis=0, tiled=True)
+    key_pos = key_positions(chosen)
+    facts = jnp.stack([me * rows, live_length[0], x_at]).astype(jnp.int32)
+
     queries = project_queries(tokens, q_pieces, outgoing[0, 0, :16, :HD])
     attended = attend(
         queries,
@@ -346,14 +363,14 @@
         facts,
     )
     other = from_ahead(attended, "tp", 1)
-    places = jnp.stack([y_at, lax.axis_index("tp")]).astype(jnp.int32)
-    return mix(attended, other, o_pieces, places)
+    cores = jnp.stack([y_at, lax.axis_index("tp")])
+    return mix(attended, other, o_pieces, cores)
 
 
 def solution(mesh):
     split = Mesh(
-        mesh.devices.reshape(mesh.shape["dp"], 16, 4, mesh.shape["tp"]),
-        ("dp", "kv_0", "kv_1", "tp"),
+        mesh.devices.reshape(mesh.shape["dp"], 4, 4, 4, mesh.shape["tp"]),
+        ("dp", "zh", "zl", "y", "tp"),
     )
     placed = (
         P(DP_KV, None),

time: 288 us -> 337 us (1.17)
  the two profiles are of different devices: /device:TPU:2 before, /device:TPU:67 now
where the time goes in v3:
time: 337 us; the launch traced here: 335 us
  waiting for transfers between devices  154 us (46%)
  starting transfers between devices  104 us (31%)
  blocking collectives  25.6 us (8%)
  Pallas kernels  18.1 us (5%)
  other arithmetic  16.8 us (5%)
  local copies, waits for them, and re-layouts  15.7 us (5%)
    ppermute x25, waiting for transfers between devices, from_ahead(): return lax.ppermute(x, axis, [((i + step) % n, i) for i in range(n)])  132 us
    ppermute x25, starting transfers between devices, from_ahead(): return lax.ppermute(x, axis, [((i + step) % n, i) for i in range(n)])  83.7 us
    all_to_all x1, blocking collectives, body(): column = lax.all_to_all(cargo, TALL, 0, 0, tiled=True)  25.6 us
    all_to_all x2, waiting for transfers between devices, copy_for_each(): lax.all_to_all(jnp.broadcast_to(shard[None], (count, *shard.shape)), axis...  21.9 us
    pallas_call x11, Pallas kernels, call(): pl.pallas_call(kernel, out_shape=out_shape, in_specs=spaces, out_specs=ja...  18.1 us
    unnamed x40, local copies, waits for them, and re-layouts  11.9 us
    all_to_all x2, starting transfers between devices, copy_for_each(): lax.all_to_all(jnp.broadcast_to(shard[None], (count, *shard.shape)), axis...  11.4 us
    all_to_all x1, starting transfers between devices, body(): lax.all_to_all(outgoing, NEAR, split_axis=0, concat_axis=0, tiled=True)  8.51 us
  transfers between devices with their start and end apart: 28, of which 14 were waited for; matrix products, arithmetic and copies ran while one was open for 6% of the time, Pallas kernels for 3%

profile of v3, /device:TPU:67, one launch (start us, length us, event | category | flops | bytes accessed | tf_op | source)
XLA Modules:
  0.0 335.0 jit_solution(14379861586643657840)
XLA Ops:
  3.1 25.6 %all_to_all.20 = bf16[16,32,128]{2,1,0:T(8,128)(2,1)S(1)} all-to-all(bf16[16,32,128]{2,1,0:T(8,128)(2,1)S(1)} %get-tuple-element.11), channel_id=1, replica_groups=mesh['dp'=4,'zh'=4,'zl'=4,'y'=4,'tp'=2] {'zh','zl'}, dimensions={0} | all-to-all | bytes 262144 | tf_op jit(solution)/shard_map/all_to_all | solution.py:304
  30.5 7.0 %all-to-all-start.1 = ((bf16[16,16,32,128]{3,2,1,0:T(8,128)(2,1)}), bf16[16,16,32,128]{3,2,1,0:T(8,128)(2,1)S(1)}, u32[]{:S(2)}, u32[]{:S(2)}) async-start(bf16[16,16,32,128]{3,2,1,0:T(8,128)(2,1)} %broadcast_in_dim.97), calls=%async_computation.1 | async-start | bytes 4194304 | tf_op jit(solution)/shard_map/all_to_all | solution.py:40
  37.6 4.3 %collective-permute-start.12 = (s32[128]{0:T(128)S(1)}, s32[128]{0:T(128)S(1)}, u32[]{:S(2)}, u32[]{:S(2)}) collective-permute-start(s32[128]{0:T(128)S(1)} %eq.126), channel_id=1, source_target_pairs={{2,0},{4,2},{6,4},{0,6},{3,1},{5,3},{7,5},{1,7},{10,8},{12,10},{14... | collective-permute-start | bytes 1544 | tf_op jit(solution)/shard_map/ppermute | solution.py:47
  47.3 8.1 %collective-permute-done.12 = s32[128]{0:T(128)S(1)} collective-permute-done((s32[128]{0:T(128)S(1)}, s32[128]{0:T(128)S(1)}, u32[]{:S(2)}, u32[]{:S(2)}) %collective-permute-start.12) | collective-permute-done | bytes 544 | tf_op jit(solution)/shard_map/ppermute | solution.py:47
  57.5 4.5 %collective-permute-done.14 = s32[128]{0:T(128)S(1)} collective-permute-done((s32[128]{0:T(128)S(1)}, s32[128]{0:T(128)S(1)}, u32[]{:S(2)}, u32[]{:S(2)}) %collective-permute-start.14) | collective-permute-done | bytes 544 | tf_op jit(solution)/shard_map/ppermute | solution.py:47
  64.0 5.3 %collective-permute-start.16 = (s32[4,128]{1,0:T(4,128)S(1)}, s32[4,128]{1,0:T(4,128)S(1)}, u32[]{:S(2)}, u32[]{:S(2)}) collective-permute-start(s32[4,128]{1,0:T(4,128)S(1)} %get-tuple-element.30), channel_id=1, source_target_pairs={{16,0},{24,8},{0,16},{8,24},{17,1},{25,9},{1,17},{9,25},{18,2},{26... | collective-permute-start | bytes 6152 | tf_op jit(solution)/shard_map/ppermute | solution.py:47
  74.4 4.4 %all-to-all-start.2 = ((bf16[4,8,32,256]{3,2,1,0:T(8,128)(2,1)}), bf16[4,8,32,256]{3,2,1,0:T(8,128)(2,1)S(1)}, u32[]{:S(2)}, u32[]{:S(2)}) async-start(bf16[4,8,32,256]{3,2,1,0:T(8,128)(2,1)} %broadcast_in_dim.99), calls=%async_computation.2 | async-start | bytes 1048576 | tf_op jit(solution)/shard_map/all_to_all | solution.py:40
  80.4 2.8 reduce_window_sum.23
  85.1 21.9 %all-to-all-done.2 = bf16[4,8,32,256]{3,2,1,0:T(8,128)(2,1)S(1)} async-done(((bf16[4,8,32,256]{3,2,1,0:T(8,128)(2,1)}), bf16[4,8,32,256]{3,2,1,0:T(8,128)(2,1)S(1)}, u32[]{:S(2)}, u32[]{:S(2)}) %all-to-all-start.2) | async-done | bytes 524320 | tf_op jit(solution)/shard_map/all_to_all | solution.py:40
  109.2 8.5 %all-to-all-start.3 = ((bf16[16,8,32,256]{3,2,1,0:T(8,128)(2,1)}), bf16[16,8,32,256]{3,2,1,0:T(8,128)(2,1)S(1)}, u32[]{:S(2)}, u32[]{:S(2)}) async-start(bf16[16,8,32,256]{3,2,1,0:T(8,128)(2,1)} %shard_map.78), calls=%async_computation.3 | async-start | bytes 4194304 | tf_op jit(solution)/shard_map/all_to_all | solution.py:336
  117.7 6.1 %collective-permute-start = (bf16[128,128]{1,0:T(8,128)(2,1)S(1)}, bf16[128,128]{1,0:T(8,128)(2,1)S(1)}, u32[]{:S(2)}, u32[]{:S(2)}) collective-permute-start(bf16[128,128]{1,0:T(8,128)(2,1)S(1)} %get-tuple-element.9.refs_0_), channel_id=1, source_target_pairs={{32,0},{64,32},{96,64},{0,96},{33,1},{65,33},{97,65},{1,97},{34,2}... | collective-permute-start | bytes 98312 | tf_op jit(solution)/shard_map/ppermute | solution.py:47
  123.8 4.7 %collective-permute-start.1 = (bf16[128,128]{1,0:T(8,128)(2,1)S(1)}, bf16[128,128]{1,0:T(8,128)(2,1)S(1)}, u32[]{:S(2)}, u32[]{:S(2)}) collective-permute-start(bf16[128,128]{1,0:T(8,128)(2,1)S(1)} %get-tuple-element.9.refs_0_), channel_id=1, source_target_pairs={{64,0},{96,32},{0,64},{32,96},{65,1},{97,33},{1,65},{33,97},{66,2}... | collective-permute-start | bytes 98312 | tf_op jit(solution)/shard_map/ppermute | solution.py:47
  128.5 4.5 %collective-permute-start.2 = (bf16[128,128]{1,0:T(8,128)(2,1)S(1)}, bf16[128,128]{1,0:T(8,128)(2,1)S(1)}, u32[]{:S(2)}, u32[]{:S(2)}) collective-permute-start(bf16[128,128]{1,0:T(8,128)(2,1)S(1)} %get-tuple-element.9.refs_0_), channel_id=1, source_target_pairs={{96,0},{0,32},{32,64},{64,96},{97,1},{1,33},{33,65},{65,97},{98,2}... | collective-permute-start | bytes 98312 | tf_op jit(solution)/shard_map/ppermute | solution.py:47
  133.0 37.4 %collective-permute-done.refs_1_ = bf16[128,128]{1,0:T(8,128)(2,1)S(1)} collective-permute-done((bf16[128,128]{1,0:T(8,128)(2,1)S(1)}, bf16[128,128]{1,0:T(8,128)(2,1)S(1)}, u32[]{:S(2)}, u32[]{:S(2)}) %collective-permute-start) | collective-permute-done | bytes 32800 | tf_op jit(solution)/shard_map/ppermute | solution.py:47
  170.5 7.0 %collective-permute-start.3 = (bf16[4,128,128]{2,1,0:T(8,128)(2,1)S(1)}, bf16[4,128,128]{2,1,0:T(8,128)(2,1)S(1)}, u32[]{:S(2)}, u32[]{:S(2)}) collective-permute-start(bf16[4,128,128]{2,1,0:T(8,128)(2,1)S(1)} %shard_map.74.refs_0_), channel_id=1, source_target_pairs={{8,0},{16,8},{24,16},{0,24},{9,1},{17,9},{25,17},{1,25},{10,2},{18... | collective-permute-start | bytes 393224 | tf_op jit(solution)/shard_map/ppermute | solution.py:47
  179.4 3.1 collective-permute-start.5
  184.9 3.8 %collective-permute-done.5.refs_3_ = bf16[4,128,128]{2,1,0:T(8,128)(2,1)S(1)} collective-permute-done((bf16[4,128,128]{2,1,0:T(8,128)(2,1)S(1)}, bf16[4,128,128]{2,1,0:T(8,128)(2,1)S(1)}, u32[]{:S(2)}, u32[]{:S(2)}) %collective-permute-start.5) | collective-permute-done | bytes 131104 | tf_op jit(solution)/shard_map/ppermute | solution.py:47
  188.7 4.3 %collective-permute-start.6 = (bf16[16,64,128]{2,1,0:T(8,128)(2,1)S(1)}, bf16[16,64,128]{2,1,0:T(8,128)(2,1)S(1)}, u32[]{:S(2)}, u32[]{:S(2)}) collective-permute-start(bf16[16,64,128]{2,1,0:T(8,128)(2,1)S(1)} %get-tuple-element.10.refs_0_), channel_id=1, source_target_pairs={{2,0},{4,2},{6,4},{0,6},{3,1},{5,3},{7,5},{1,7},{10,8},{12,10},{14... | collective-permute-start | bytes 786440 | tf_op jit(solution)/shard_map/ppermute | solution.py:47
  203.3 6.6 %collective-permute-done.8.refs_3_ = bf16[16,64,128]{2,1,0:T(8,128)(2,1)} collective-permute-done((bf16[16,64,128]{2,1,0:T(8,128)(2,1)S(1)}, bf16[16,64,128]{2,1,0:T(8,128)(2,1)}, u32[]{:S(2)}, u32[]{:S(2)}) %collective-permute-start.8) | collective-permute-done | bytes 262176 | tf_op jit(solution)/shard_map/ppermute | solution.py:47
  213.7 3.6 %collective-permute-start.10 = (bf16[4096,128]{1,0:T(8,128)(2,1)S(1)}, bf16[4096,128]{1,0:T(8,128)(2,1)}, u32[]{:S(2)}, u32[]{:S(2)}) collective-permute-start(bf16[4096,128]{1,0:T(8,128)(2,1)S(1)} %bitcast.35), channel_id=1, source_target_pairs={{256,0},{384,128},{0,256},{128,384},{257,1},{385,129},{1,257},{129... | collective-permute-start | bytes 3145736 | tf_op jit(solution)/shard_map/ppermute | solution.py:47
  226.4 3.4 %collective-permute-start.11 = (bf16[4096,128]{1,0:T(8,128)(2,1)S(1)}, bf16[4096,128]{1,0:T(8,128)(2,1)}, u32[]{:S(2)}, u32[]{:S(2)}) collective-permute-start(bf16[4096,128]{1,0:T(8,128)(2,1)S(1)} %bitcast.36), channel_id=1, source_target_pairs={{384,0},{0,128},{128,256},{256,384},{385,1},{1,129},{129,257},{257... | collective-permute-start | bytes 3145736 | tf_op jit(solution)/shard_map/ppermute | solution.py:47
  233.1 3.7 %collective-permute-start.20 = (bf16[16,64,128]{2,1,0:T(8,128)(2,1)S(1)}, bf16[16,64,128]{2,1,0:T(8,128)(2,1)}, u32[]{:S(2)}, u32[]{:S(2)}) collective-permute-start(bf16[16,64,128]{2,1,0:T(8,128)(2,1)S(1)} %get-tuple-element.12.refs_0_), channel_id=1, source_target_pairs={{256,0},{384,128},{0,256},{128,384},{257,1},{385,129},{1,257},{129... | collective-permute-start | bytes 786440 | tf_op jit(solution)/shard_map/ppermute | solution.py:47
  236.8 11.2 %collective-permute-done.19.refs_1_ = bf16[16,64,128]{2,1,0:T(8,128)(2,1)} collective-permute-done((bf16[16,64,128]{2,1,0:T(8,128)(2,1)S(1)}, bf16[16,64,128]{2,1,0:T(8,128)(2,1)}, u32[]{:S(2)}, u32[]{:S(2)}) %collective-permute-start.19) | collective-permute-done | bytes 262176 | tf_op jit(solution)/shard_map/ppermute | solution.py:47
  252.1 22.5 %collective-permute-done.20.refs_2_ = bf16[16,64,128]{2,1,0:T(8,128)(2,1)} collective-permute-done((bf16[16,64,128]{2,1,0:T(8,128)(2,1)S(1)}, bf16[16,64,128]{2,1,0:T(8,128)(2,1)}, u32[]{:S(2)}, u32[]{:S(2)}) %collective-permute-start.20) | collective-permute-done | bytes 262176 | tf_op jit(solution)/shard_map/ppermute | solution.py:47
  281.0 3.4 %collective-permute-start.24 = (bf16[16,16,2048]{2,1,0:T(8,128)(2,1)}, bf16[16,16,2048]{2,1,0:T(8,128)(2,1)}, u32[]{:S(2)}, u32[]{:S(2)}) collective-permute-start(bf16[16,16,2048]{2,1,0:T(8,128)(2,1)} %shard_map.82.refs_0_), channel_id=1, source_target_pairs={{6,0},{0,2},{2,4},{4,6},{7,1},{1,3},{3,5},{5,7},{14,8},{8,10},{10,... | collective-permute-start | bytes 3145736 | tf_op jit(solution)/shard_map/ppermute | solution.py:47
  286.6 3.1 shard_map.79.q_ref
  291.0 3.1 shard_map.81.m_ref
  294.1 4.4 %collective-permute-start.18 = (bf16[256,512]{1,0:T(8,128)(2,1)S(1)}, bf16[256,512]{1,0:T(8,128)(2,1)S(1)}, u32[]{:S(2)}, u32[]{:S(2)}) collective-permute-start(bf16[256,512]{1,0:T(8,128)(2,1)S(1)} %shard_map.81.m_ref), channel_id=1, source_target_pairs={{1,0},{0,1},{3,2},{2,3},{5,4},{4,5},{7,6},{6,7},{9,8},{8,9},{11,10... | collective-permute-start | bytes 786440 | tf_op jit(solution)/shard_map/ppermute | solution.py:47
  298.6 3.5 %collective-permute-done.22.refs_1_ = bf16[16,16,2048]{2,1,0:T(8,128)(2,1)} collective-permute-done((bf16[16,16,2048]{2,1,0:T(8,128)(2,1)}, bf16[16,16,2048]{2,1,0:T(8,128)(2,1)}, u32[]{:S(2)}, u32[]{:S(2)}) %collective-permute-start.22) | collective-permute-done | bytes 1048608 | tf_op jit(solution)/shard_map/ppermute | solution.py:47
  302.1 3.5 %collective-permute-done.23.refs_2_ = bf16[16,16,2048]{2,1,0:T(8,128)(2,1)} collective-permute-done((bf16[16,16,2048]{2,1,0:T(8,128)(2,1)}, bf16[16,16,2048]{2,1,0:T(8,128)(2,1)}, u32[]{:S(2)}, u32[]{:S(2)}) %collective-permute-start.23) | collective-permute-done | bytes 1048608 | tf_op jit(solution)/shard_map/ppermute | solution.py:47
  305.6 24.7 %collective-permute-done.24.refs_3_ = bf16[16,16,2048]{2,1,0:T(8,128)(2,1)} collective-permute-done((bf16[16,16,2048]{2,1,0:T(8,128)(2,1)}, bf16[16,16,2048]{2,1,0:T(8,128)(2,1)}, u32[]{:S(2)}, u32[]{:S(2)}) %collective-permute-start.24) | collective-permute-done | bytes 1048608 | tf_op jit(solution)/shard_map/ppermute | solution.py:47
  330.3 4.7 %shard_map.83 = bf16[256,2048]{1,0:T(8,128)(2,1)} custom-call(s32[2]{0:T(128)S(1)} %pad_add_fusion.2.p_ref, bf16[256,512]{1,0:T(8,128)(2,1)S(1)} %shard_map.81.m_ref, bf16[256,512]{1,0:T(8,128)(2,1)S(1)} %collective-permute-done.18.t_ref, bf16[16,16,2048]{2,1,0:T(8,128)(2,1)} %shard_map.82.refs_0_, bf16[16,16,2048]{2,1,0:T(8,128)(2,1)} %collective-permute-done.22.refs_1_, ...), custom_call_target="tpu_custom_call" | custom-call | flops 1073741824 | tf_op jit(solution)/shard_map/pallas_call | solution.py:27
  (122 shorter events, 69.0 us)
Async XLA Ops:
  30.5 7.1 %copy-start.8 = (s32[8,16]{1,0:T(8,128)S(1)}, s32[8,16]{1,0:T(8,128)}, u32[]{:S(2)}) copy-start(s32[8,16]{1,0:T(8,128)} %c_ref.1) | copy-start | bytes 1540
  30.5 40.8 %all-to-all-start.1 = ((bf16[16,16,32,128]{3,2,1,0:T(8,128)(2,1)}), bf16[16,16,32,128]{3,2,1,0:T(8,128)(2,1)S(1)}, u32[]{:S(2)}, u32[]{:S(2)}) async-start(bf16[16,16,32,128]{3,2,1,0:T(8,128)(2,1)} %broadcast_in_dim.97), calls=%async_computation.1 | async-start | bytes 4194304 | tf_op jit(solution)/shard_map/all_to_all | solution.py:40
  37.6 17.8 %collective-permute-start.12 = (s32[128]{0:T(128)S(1)}, s32[128]{0:T(128)S(1)}, u32[]{:S(2)}, u32[]{:S(2)}) collective-permute-start(s32[128]{0:T(128)S(1)} %eq.126), channel_id=1, source_target_pairs={{2,0},{4,2},{6,4},{0,6},{3,1},{5,3},{7,5},{1,7},{10,8},{12,10},{14... | collective-permute-start | bytes 1544 | tf_op jit(solution)/shard_map/ppermute | solution.py:47
  41.9 15.6 %collective-permute-start.13 = (s32[128]{0:T(128)S(1)}, s32[128]{0:T(128)S(1)}, u32[]{:S(2)}, u32[]{:S(2)}) collective-permute-start(s32[128]{0:T(128)S(1)} %eq.126), channel_id=1, source_target_pairs={{4,0},{6,2},{0,4},{2,6},{5,1},{7,3},{1,5},{3,7},{12,8},{14,10},{8,... | collective-permute-start | bytes 1544 | tf_op jit(solution)/shard_map/ppermute | solution.py:47
  44.4 17.6 %collective-permute-start.14 = (s32[128]{0:T(128)S(1)}, s32[128]{0:T(128)S(1)}, u32[]{:S(2)}, u32[]{:S(2)}) collective-permute-start(s32[128]{0:T(128)S(1)} %eq.126), channel_id=1, source_target_pairs={{6,0},{0,2},{2,4},{4,6},{7,1},{1,3},{3,5},{5,7},{14,8},{8,10},{10,... | collective-permute-start | bytes 1544 | tf_op jit(solution)/shard_map/ppermute | solution.py:47
  62.0 17.0 %collective-permute-start.15 = (s32[4,128]{1,0:T(4,128)S(1)}, s32[4,128]{1,0:T(4,128)S(1)}, u32[]{:S(2)}, u32[]{:S(2)}) collective-permute-start(s32[4,128]{1,0:T(4,128)S(1)} %get-tuple-element.30), channel_id=1, source_target_pairs={{8,0},{16,8},{24,16},{0,24},{9,1},{17,9},{25,17},{1,25},{10,2},{18... | collective-permute-start | bytes 6152 | tf_op jit(solution)/shard_map/ppermute | solution.py:47
  64.0 15.0 %collective-permute-start.16 = (s32[4,128]{1,0:T(4,128)S(1)}, s32[4,128]{1,0:T(4,128)S(1)}, u32[]{:S(2)}, u32[]{:S(2)}) collective-permute-start(s32[4,128]{1,0:T(4,128)S(1)} %get-tuple-element.30), channel_id=1, source_target_pairs={{16,0},{24,8},{0,16},{8,24},{17,1},{25,9},{1,17},{9,25},{18,2},{26... | collective-permute-start | bytes 6152 | tf_op jit(solution)/shard_map/ppermute | solution.py:47
  69.3 9.7 %collective-permute-start.17 = (s32[4,128]{1,0:T(4,128)S(1)}, s32[4,128]{1,0:T(4,128)S(1)}, u32[]{:S(2)}, u32[]{:S(2)}) collective-permute-start(s32[4,128]{1,0:T(4,128)S(1)} %get-tuple-element.30), channel_id=1, source_target_pairs={{24,0},{0,8},{8,16},{16,24},{25,1},{1,9},{9,17},{17,25},{26,2},{2,... | collective-permute-start | bytes 6152 | tf_op jit(solution)/shard_map/ppermute | solution.py:47
  74.4 32.6 %all-to-all-start.2 = ((bf16[4,8,32,256]{3,2,1,0:T(8,128)(2,1)}), bf16[4,8,32,256]{3,2,1,0:T(8,128)(2,1)S(1)}, u32[]{:S(2)}, u32[]{:S(2)}) async-start(bf16[4,8,32,256]{3,2,1,0:T(8,128)(2,1)} %broadcast_in_dim.99), calls=%async_computation.2 | async-start | bytes 1048576 | tf_op jit(solution)/shard_map/all_to_all | solution.py:40
  109.2 180.5 %all-to-all-start.3 = ((bf16[16,8,32,256]{3,2,1,0:T(8,128)(2,1)}), bf16[16,8,32,256]{3,2,1,0:T(8,128)(2,1)S(1)}, u32[]{:S(2)}, u32[]{:S(2)}) async-start(bf16[16,8,32,256]{3,2,1,0:T(8,128)(2,1)} %shard_map.78), calls=%async_computation.3 | async-start | bytes 4194304 | tf_op jit(solution)/shard_map/all_to_all | solution.py:336
  117.7 52.7 %collective-permute-start = (bf16[128,128]{1,0:T(8,128)(2,1)S(1)}, bf16[128,128]{1,0:T(8,128)(2,1)S(1)}, u32[]{:S(2)}, u32[]{:S(2)}) collective-permute-start(bf16[128,128]{1,0:T(8,128)(2,1)S(1)} %get-tuple-element.9.refs_0_), channel_id=1, source_target_pairs={{32,0},{64,32},{96,64},{0,96},{33,1},{65,33},{97,65},{1,97},{34,2}... | collective-permute-start | bytes 98312 | tf_op jit(solution)/shard_map/ppermute | solution.py:47
  123.8 46.6 %collective-permute-start.1 = (bf16[128,128]{1,0:T(8,128)(2,1)S(1)}, bf16[128,128]{1,0:T(8,128)(2,1)S(1)}, u32[]{:S(2)}, u32[]{:S(2)}) collective-permute-start(bf16[128,128]{1,0:T(8,128)(2,1)S(1)} %get-tuple-element.9.refs_0_), channel_id=1, source_target_pairs={{64,0},{96,32},{0,64},{32,96},{65,1},{97,33},{1,65},{33,97},{66,2}... | collective-permute-start | bytes 98312 | tf_op jit(solution)/shard_map/ppermute | solution.py:47
  128.5 41.9 %collective-permute-start.2 = (bf16[128,128]{1,0:T(8,128)(2,1)S(1)}, bf16[128,128]{1,0:T(8,128)(2,1)S(1)}, u32[]{:S(2)}, u32[]{:S(2)}) collective-permute-start(bf16[128,128]{1,0:T(8,128)(2,1)S(1)} %get-tuple-element.9.refs_0_), channel_id=1, source_target_pairs={{96,0},{0,32},{32,64},{64,96},{97,1},{1,33},{33,65},{65,97},{98,2}... | collective-permute-start | bytes 98312 | tf_op jit(solution)/shard_map/ppermute | solution.py:47
  170.5 12.1 %collective-permute-start.3 = (bf16[4,128,128]{2,1,0:T(8,128)(2,1)S(1)}, bf16[4,128,128]{2,1,0:T(8,128)(2,1)S(1)}, u32[]{:S(2)}, u32[]{:S(2)}) collective-permute-start(bf16[4,128,128]{2,1,0:T(8,128)(2,1)S(1)} %shard_map.74.refs_0_), channel_id=1, source_target_pairs={{8,0},{16,8},{24,16},{0,24},{9,1},{17,9},{25,17},{1,25},{10,2},{18... | collective-permute-start | bytes 393224 | tf_op jit(solution)/shard_map/ppermute | solution.py:47
  177.5 7.4 %collective-permute-start.4 = (bf16[4,128,128]{2,1,0:T(8,128)(2,1)S(1)}, bf16[4,128,128]{2,1,0:T(8,128)(2,1)S(1)}, u32[]{:S(2)}, u32[]{:S(2)}) collective-permute-start(bf16[4,128,128]{2,1,0:T(8,128)(2,1)S(1)} %shard_map.74.refs_0_), channel_id=1, source_target_pairs={{16,0},{24,8},{0,16},{8,24},{17,1},{25,9},{1,17},{9,25},{18,2},{26... | collective-permute-start | bytes 393224 | tf_op jit(solution)/shard_map/ppermute | solution.py:47
  179.4 9.3 %collective-permute-start.5 = (bf16[4,128,128]{2,1,0:T(8,128)(2,1)S(1)}, bf16[4,128,128]{2,1,0:T(8,128)(2,1)S(1)}, u32[]{:S(2)}, u32[]{:S(2)}) collective-permute-start(bf16[4,128,128]{2,1,0:T(8,128)(2,1)S(1)} %shard_map.74.refs_0_), channel_id=1, source_target_pairs={{24,0},{0,8},{8,16},{16,24},{25,1},{1,9},{9,17},{17,25},{26,2},{2,... | collective-permute-start | bytes 393224 | tf_op jit(solution)/shard_map/ppermute | solution.py:47
  188.7 11.4 %collective-permute-start.6 = (bf16[16,64,128]{2,1,0:T(8,128)(2,1)S(1)}, bf16[16,64,128]{2,1,0:T(8,128)(2,1)S(1)}, u32[]{:S(2)}, u32[]{:S(2)}) collective-permute-start(bf16[16,64,128]{2,1,0:T(8,128)(2,1)S(1)} %get-tuple-element.10.refs_0_), channel_id=1, source_target_pairs={{2,0},{4,2},{6,4},{0,6},{3,1},{5,3},{7,5},{1,7},{10,8},{12,10},{14... | collective-permute-start | bytes 786440 | tf_op jit(solution)/shard_map/ppermute | solution.py:47
  193.1 9.5 %collective-permute-start.7 = (bf16[16,64,128]{2,1,0:T(8,128)(2,1)S(1)}, bf16[16,64,128]{2,1,0:T(8,128)(2,1)S(1)}, u32[]{:S(2)}, u32[]{:S(2)}) collective-permute-start(bf16[16,64,128]{2,1,0:T(8,128)(2,1)S(1)} %get-tuple-element.10.refs_0_), channel_id=1, source_target_pairs={{4,0},{6,2},{0,4},{2,6},{5,1},{7,3},{1,5},{3,7},{12,8},{14,10},{8,... | collective-permute-start | bytes 786440 | tf_op jit(solution)/shard_map/ppermute | solution.py:47
  195.5 14.3 %collective-permute-start.8 = (bf16[16,64,128]{2,1,0:T(8,128)(2,1)S(1)}, bf16[16,64,128]{2,1,0:T(8,128)(2,1)}, u32[]{:S(2)}, u32[]{:S(2)}) collective-permute-start(bf16[16,64,128]{2,1,0:T(8,128)(2,1)S(1)} %get-tuple-element.10.refs_0_), channel_id=1, source_target_pairs={{6,0},{0,2},{2,4},{4,6},{7,1},{1,3},{3,5},{5,7},{14,8},{8,10},{10,... | collective-permute-start | bytes 786440 | tf_op jit(solution)/shard_map/ppermute | solution.py:47
  198.8 18.5 %copy-start.17 = (pred[64]{0:T(512)(128)(4,1)}, pred[64]{0:T(512)(128)(4,1)S(1)}, u32[]{:S(2)}) copy-start(pred[64]{0:T(512)(128)(4,1)S(1)} %iota_compare_fusion.1) | copy-start | bytes 196
  213.7 67.2 %collective-permute-start.10 = (bf16[4096,128]{1,0:T(8,128)(2,1)S(1)}, bf16[4096,128]{1,0:T(8,128)(2,1)}, u32[]{:S(2)}, u32[]{:S(2)}) collective-permute-start(bf16[4096,128]{1,0:T(8,128)(2,1)S(1)} %bitcast.35), channel_id=1, source_target_pairs={{256,0},{384,128},{0,256},{128,384},{257,1},{385,129},{1,257},{129... | collective-permute-start | bytes 3145736 | tf_op jit(solution)/shard_map/ppermute | solution.py:47
  221.7 26.2 %collective-permute-start.19 = (bf16[16,64,128]{2,1,0:T(8,128)(2,1)S(1)}, bf16[16,64,128]{2,1,0:T(8,128)(2,1)}, u32[]{:S(2)}, u32[]{:S(2)}) collective-permute-start(bf16[16,64,128]{2,1,0:T(8,128)(2,1)S(1)} %get-tuple-element.12.refs_0_), channel_id=1, source_target_pairs={{128,0},{256,128},{384,256},{0,384},{129,1},{257,129},{385,257},{1... | collective-permute-start | bytes 786440 | tf_op jit(solution)/shard_map/ppermute | solution.py:47
  226.4 60.1 %collective-permute-start.11 = (bf16[4096,128]{1,0:T(8,128)(2,1)S(1)}, bf16[4096,128]{1,0:T(8,128)(2,1)}, u32[]{:S(2)}, u32[]{:S(2)}) collective-permute-start(bf16[4096,128]{1,0:T(8,128)(2,1)S(1)} %bitcast.36), channel_id=1, source_target_pairs={{384,0},{0,128},{128,256},{256,384},{385,1},{1,129},{129,257},{257... | collective-permute-start | bytes 3145736 | tf_op jit(solution)/shard_map/ppermute | solution.py:47
  229.8 56.8 %collective-permute-start.9 = (bf16[4096,128]{1,0:T(8,128)(2,1)S(1)}, bf16[4096,128]{1,0:T(8,128)(2,1)}, u32[]{:S(2)}, u32[]{:S(2)}) collective-permute-start(bf16[4096,128]{1,0:T(8,128)(2,1)S(1)} %bitcast.37), channel_id=1, source_target_pairs={{128,0},{256,128},{384,256},{0,384},{129,1},{257,129},{385,257},{1... | collective-permute-start | bytes 3145736 | tf_op jit(solution)/shard_map/ppermute | solution.py:47
  233.1 41.6 %collective-permute-start.20 = (bf16[16,64,128]{2,1,0:T(8,128)(2,1)S(1)}, bf16[16,64,128]{2,1,0:T(8,128)(2,1)}, u32[]{:S(2)}, u32[]{:S(2)}) collective-permute-start(bf16[16,64,128]{2,1,0:T(8,128)(2,1)S(1)} %get-tuple-element.12.refs_0_), channel_id=1, source_target_pairs={{256,0},{384,128},{0,256},{128,384},{257,1},{385,129},{1,257},{129... | collective-permute-start | bytes 786440 | tf_op jit(solution)/shard_map/ppermute | solution.py:47
  247.9 26.7 %collective-permute-start.21 = (bf16[16,64,128]{2,1,0:T(8,128)(2,1)S(1)}, bf16[16,64,128]{2,1,0:T(8,128)(2,1)}, u32[]{:S(2)}, u32[]{:S(2)}) collective-permute-start(bf16[16,64,128]{2,1,0:T(8,128)(2,1)S(1)} %get-tuple-element.12.refs_0_), channel_id=1, source_target_pairs={{384,0},{0,128},{128,256},{256,384},{385,1},{1,129},{129,257},{257... | collective-permute-start | bytes 786440 | tf_op jit(solution)/shard_map/ppermute | solution.py:47
  251.2 35.3 %copy-start.1 = (bf16[256,4096]{1,0:T(8,128)(2,1)S(1)}, bf16[256,4096]{1,0:T(8,128)(2,1)}, u32[]{:S(2)}) copy-start(bf16[256,4096]{1,0:T(8,128)(2,1)} %t_ref.3) | copy-start | bytes 6291460
  277.1 25.0 %collective-permute-start.22 = (bf16[16,16,2048]{2,1,0:T(8,128)(2,1)}, bf16[16,16,2048]{2,1,0:T(8,128)(2,1)}, u32[]{:S(2)}, u32[]{:S(2)}) collective-permute-start(bf16[16,16,2048]{2,1,0:T(8,128)(2,1)} %shard_map.82.refs_0_), channel_id=1, source_target_pairs={{2,0},{4,2},{6,4},{0,6},{3,1},{5,3},{7,5},{1,7},{10,8},{12,10},{14... | collective-permute-start | bytes 3145736 | tf_op jit(solution)/shard_map/ppermute | solution.py:47
  279.0 26.6 %collective-permute-start.23 = (bf16[16,16,2048]{2,1,0:T(8,128)(2,1)}, bf16[16,16,2048]{2,1,0:T(8,128)(2,1)}, u32[]{:S(2)}, u32[]{:S(2)}) collective-permute-start(bf16[16,16,2048]{2,1,0:T(8,128)(2,1)} %shard_map.82.refs_0_), channel_id=1, source_target_pairs={{4,0},{6,2},{0,4},{2,6},{5,1},{7,3},{1,5},{3,7},{12,8},{14,10},{8,... | collective-permute-start | bytes 3145736 | tf_op jit(solution)/shard_map/ppermute | solution.py:47
  281.0 49.3 %collective-permute-start.24 = (bf16[16,16,2048]{2,1,0:T(8,128)(2,1)}, bf16[16,16,2048]{2,1,0:T(8,128)(2,1)}, u32[]{:S(2)}, u32[]{:S(2)}) collective-permute-start(bf16[16,16,2048]{2,1,0:T(8,128)(2,1)} %shard_map.82.refs_0_), channel_id=1, source_target_pairs={{6,0},{0,2},{2,4},{4,6},{7,1},{1,3},{3,5},{5,7},{14,8},{8,10},{10,... | collective-permute-start | bytes 3145736 | tf_op jit(solution)/shard_map/ppermute | solution.py:47
  286.5 3.2 copy-start.10
  294.1 36.2 %collective-permute-start.18 = (bf16[256,512]{1,0:T(8,128)(2,1)S(1)}, bf16[256,512]{1,0:T(8,128)(2,1)S(1)}, u32[]{:S(2)}, u32[]{:S(2)}) collective-permute-start(bf16[256,512]{1,0:T(8,128)(2,1)S(1)} %shard_map.81.m_ref), channel_id=1, source_target_pairs={{1,0},{0,1},{3,2},{2,3},{5,4},{4,5},{7,6},{6,7},{9,8},{8,9},{11,10... | collective-permute-start | bytes 786440 | tf_op jit(solution)/shard_map/ppermute | solution.py:47
  (14 other events, 11.6 us)

commit v4 on v3

--- a/solution.py
+++ b/solution.py
@@ -12,7 +12,6 @@
 CAP = 2
 NEVER = 1 << 30
 TALL = ("zh", "zl")
-NEAR = ("zl", "y")
 KV = ("zh", "zl", "y")
 DP_KV = ("dp", "zh", "zl", "y")
 F32 = jnp.float32
@@ -72,7 +71,17 @@
     small = rows // planes
     groups = wide_out // planes // HD
 
-    def kernel(x_ref, q_ref, k_ref, v_ref, o_ref, part_ref, cargo_ref):
+    def kernel(x_ref, q_hbm, k_hbm, v_hbm, o_hbm, part_ref, cargo_ref, *scratch):
+        held, sems = scratch[:4], scratch[4]
+        copies = [
+            pltpu.make_async_copy(src, dst, sems.at[i])
+            for i, (src, dst) in enumerate(zip((q_hbm, k_hbm, v_hbm, o_hbm), held, strict=True))
+        ]
+        for copy in copies:
+            copy.start()
+        for copy in copies:
+            copy.wait()
+        q_ref, k_ref, v_ref, o_ref = held
         part_ref[:rows] = q_ref[:, pl.ds(pl.multiple_of(x_ref[0] * HD, HD), HD)]
         for i in range(groups):
             first = pl.multiple_of((x_ref[0] * groups + i) * HD, HD)
@@ -84,11 +93,20 @@
             cargo_ref[z, :small] = keys
             cargo_ref[z, small:] = values
 
+    weights = (query_weight, key_weight, value_weight, out_weight)
     outs = (
         jax.ShapeDtypeStruct((rows + groups * lines, HD), BF16),
         jax.ShapeDtypeStruct((tall, 2 * small, HD), BF16),
     )
-    return call(kernel, outs, x_at[None], query_weight, key_weight, value_weight, out_weight)
+    return pl.pallas_call(
+        kernel,
+        out_shape=outs,
+        in_specs=[pl.BlockSpec(memory_space=pltpu.SMEM)] + [pl.BlockSpec(memory_space=pl.ANY)] * 4,
+        out_specs=(pl.BlockSpec(memory_space=pltpu.VMEM),) * 2,
+        scratch_shapes=[pltpu.VMEM(w.shape, BF16) for w in weights]
+        + [pltpu.SemaphoreType.DMA((4,))],
+        name="pack",
+    )(x_at[None], *weights)
 
 
 def joined(pieces, at):
@@ -201,19 +219,16 @@
     return call(kernel, out, chosen)
 
 
-def pick_blocks(blocks, asked, places):
-    low, wide, count = asked.shape
-
-    def kernel(asked_ref, p_ref, b_ref, o_ref):
-        for t in range(low):
-            for s in range(wide):
-                to = ((p_ref[0] + t) % low) * wide + (p_ref[1] + s) % wide
-                for i in range(count):
-                    o_ref[to, i] = b_ref[asked_ref[t * wide + s, i]]
-
-    out = jax.ShapeDtypeStruct((low * wide, count, *blocks.shape[1:]), BF16)
-    flat = asked.reshape(low * wide, count)
-    return call(kernel, out, flat, places, blocks)
+def pick_blocks(blocks, asked, at):
+    wide, count = asked.shape
+
+    def kernel(asked_ref, at_ref, b_ref, o_ref):
+        for s in range(wide):
+            for i in range(count):
+                o_ref[(at_ref[0] + s) % wide, i] = b_ref[asked_ref[s, i]]
+
+    out = jax.ShapeDtypeStruct((wide, count, *blocks.shape[1:]), BF16)
+    return call(kernel, out, asked, at[None], blocks)
 
 
 def attend(queries, incoming, local_blocks, position, key_pos, facts):
@@ -268,26 +283,32 @@
     )
 
 
-def mix(mine, other, pieces, places):
+def whole_rows(pieces, at):
     n = len(pieces)
     tall, lines, width = pieces[0].shape
-    half = tall // 2
-
-    def kernel(p_ref, m_ref, t_ref, *refs):
-        o_ref, w_s = refs[n], refs[n + 1]
-        for s in range(n):
-            w_s[:, (p_ref[0] + s) % n] = refs[s][...]
-        first = w_s[pl.ds(p_ref[1] * half, half)].reshape(half * n * lines, width)
-        second = w_s[pl.ds((1 - p_ref[1]) * half, half)].reshape(half * n * lines, width)
+
+    def kernel(at_ref, *refs):
+        for s in range(n):
+            refs[-1][:, (at_ref[0] + s) % n] = refs[s][...]
+
+    out = jax.ShapeDtypeStruct((tall, n, lines, width), BF16)
+    return call(kernel, out, at[None], *pieces)
+
+
+def mix(mine, other, weight, core):
+    half = weight.shape[0] // 2
+
+    def kernel(c_ref, m_ref, t_ref, w_ref, o_ref):
+        first = w_ref[pl.ds(c_ref[0] * half, half)]
+        second = w_ref[pl.ds((1 - c_ref[0]) * half, half)]
         o_ref[...] = (
             jnp.dot(m_ref[...], first, preferred_element_type=F32)
             + jnp.dot(t_ref[...], second, preferred_element_type=F32)
         ).astype(BF16)
 
-    out = jax.ShapeDtypeStruct((mine.shape[0], width), BF16)
-    scratch = (pltpu.VMEM((tall, n, lines, width), BF16),)
-    flops = 4 * mine.size * width
-    return call(kernel, out, places, mine, other, *pieces, scratch=scratch, flops=flops)
+    out = jax.ShapeDtypeStruct((mine.shape[0], weight.shape[1]), BF16)
+    flops = 4 * mine.size * weight.shape[1]
+    return call(kernel, out, core[None], mine, other, weight, flops=flops)
 
 
 def body(tokens, query_weight, key_weight, value_weight, out_weight, chosen, live_length):
@@ -298,7 +319,6 @@
     tall = high * low
     owners = tall * wide
     me = lax.axis_index(KV)
-    places = jnp.stack([l_at, y_at])
 
     part, cargo = pack(query_weight, key_weight, value_weight, out_weight, x_at, planes, tall)
     column = lax.all_to_all(cargo, TALL, 0, 0, tiled=True)
@@ -308,7 +328,7 @@
     parts = spread(joined(parts, h_at), "zl")
     paired = project_pair(tokens, every)
     local_blocks = paired.reshape(per_dev, BLOCK, paired.shape[1])
-    class_blocks = copy_for_each(local_blocks, "zh")
+    column_blocks = lax.all_gather(local_blocks, TALL, axis=0, tiled=True)
 
     q_small, o_small = columns_of(parts, l_at, query_weight.shape[0])
     q_pieces = spread(q_small, "y")
@@ -317,23 +337,13 @@
     o_pieces = spread(full_columns(o_pieces, x_at, out_weight.shape[0]), "y")
 
     mates = jnp.stack(spread(chosen.reshape(-1), "y"))
-    mates = jnp.stack(spread(mates, "zl"))
-    ahead = jnp.arange(low, dtype=jnp.int32)[:, None], jnp.arange(wide, dtype=jnp.int32)[None, :]
-    readers = (h_at * low + (l_at + ahead[0]) % low) * wide + (y_at + ahead[1]) % wide
-    highs = jnp.arange(high, dtype=jnp.int32)
-    asked = slots_wanted(
-        mates.reshape(low * wide, -1),
-        (highs * low + l_at) * wide + y_at,
-        per_dev,
-        readers.reshape(-1),
-    )
-    asked = jnp.maximum(asked, 0) + (highs * per_dev)[None, :, None]
-    outgoing = pick_blocks(
-        class_blocks.reshape(high * per_dev, BLOCK, paired.shape[1]),
-        asked.reshape(low, wide, high * CAP),
-        places,
-    )
-    incoming = lax.all_to_all(outgoing, NEAR, split_axis=0, concat_axis=0, tiled=True)
+    mates, chosen = lax.optimization_barrier((mates, chosen))
+    depth = jnp.arange(tall, dtype=jnp.int32)
+    readers = (h_at * low + l_at) * wide + (y_at + jnp.arange(wide, dtype=jnp.int32)) % wide
+    asked = slots_wanted(mates, depth * wide + y_at, per_dev, readers)
+    asked = jnp.maximum(asked, 0) + (depth * per_dev)[None, :, None]
+    outgoing = pick_blocks(column_blocks, asked.reshape(wide, tall * CAP), y_at)
+    incoming = lax.all_to_all(outgoing, "y", split_axis=0, concat_axis=0, tiled=True)
 
     safe = jnp.maximum(chosen, 0)
     wanted = slots_wanted(
@@ -348,7 +358,7 @@
         jnp.where(match, jnp.arange(CAP, dtype=jnp.int32)[None, None, None], 0), axis=(2, 3)
     )
     far = owners * CAP
-    remote_at = ((holder % (low * wide)) * high + holder // (low * wide)) * CAP + slot
+    remote_at = ((holder % wide) * tall + holder // wide) * CAP + slot
     position = jnp.where(holder == me, far + local_of, remote_at)
     key_pos = key_positions(chosen)
     facts = jnp.stack([me * rows, live_length[0], x_at]).astype(jnp.int32)
@@ -363,8 +373,9 @@
         facts,
     )
     other = from_ahead(attended, "tp", 1)
-    cores = jnp.stack([y_at, lax.axis_index("tp")])
-    return mix(attended, other, o_pieces, cores)
+    out_full = whole_rows(o_pieces, y_at)
+    out_full = out_full.reshape(-1, out_full.shape[-1])
+    return mix(attended, other, out_full, lax.axis_index("tp"))
 
 
 def solution(mesh):

time: 337 us -> 273 us (0.81)
  the two profiles are of different devices: /device:TPU:67 before, /device:TPU:85 now
where the time goes in v4:
time: 273 us; the launch traced here: 272 us
  starting transfers between devices  109 us (40%)
  waiting for transfers between devices  64.5 us (24%)
  blocking collectives  54 us (20%)
  Pallas kernels  17.8 us (7%)
  between operations  14.6 us (5%)
  local copies, waits for them, and re-layouts  6.56 us (2%)
  other arithmetic  5.27 us (2%)
    ppermute x22, starting transfers between devices, from_ahead(): return lax.ppermute(x, axis, [((i + step) % n, i) for i in range(n)])  104 us
    ppermute x22, waiting for transfers between devices, from_ahead(): return lax.ppermute(x, axis, [((i + step) % n, i) for i in range(n)])  64.5 us
    all_to_all x1, blocking collectives, copy_for_each(): lax.all_to_all(jnp.broadcast_to(shard[None], (count, *shard.shape)), axis...  28.2 us
    all_to_all x1, blocking collectives, body(): column = lax.all_to_all(cargo, TALL, 0, 0, tiled=True)  25.8 us
    pallas_call x11, Pallas kernels, call(): pl.pallas_call(kernel, out_shape=out_shape, in_specs=spaces, out_specs=ja...  16.2 us
  transfers between devices with their start and end apart: 24, of which 8 were waited for; matrix products, arithmetic and copies ran while one was open for 2% of the time, Pallas kernels for 5%

profile of v4, /device:TPU:85, one launch (start us, length us, event | category | flops | bytes accessed | tf_op | source)
XLA Modules:
  0.0 271.6 jit_solution(9852097913099991238)
XLA Ops:
  8.2 25.8 %all_to_all.15 = bf16[16,32,128]{2,1,0:T(8,128)(2,1)S(1)} all-to-all(bf16[16,32,128]{2,1,0:T(8,128)(2,1)} %get-tuple-element.15), channel_id=1, replica_groups=mesh['dp'=4,'zh'=4,'zl'=4,'y'=4,'tp'=2] {'zh','zl'}, dimensions={0} | all-to-all | bytes 262144 | tf_op jit(solution)/shard_map/all_to_all | solution.py:324
  34.4 28.2 %all_to_all.16 = bf16[16,16,32,128]{3,2,1,0:T(8,128)(2,1)S(1)} all-to-all(bf16[16,16,32,128]{3,2,1,0:T(8,128)(2,1)S(1)} %broadcast_in_dim.99), channel_id=1, replica_groups=mesh['dp'=4,'zh'=4,'zl'=4,'y'=4,'tp'=2] {'dp','y'}, dimensions={0} | all-to-all | bytes 4194304 | tf_op jit(solution)/shard_map/all_to_all | solution.py:39
  64.0 2.5 collective-permute-start.2
  66.5 2.9 %collective-permute-start.1 = (s32[128]{0:T(128)S(1)}, s32[128]{0:T(128)S(1)}, u32[]{:S(2)}, u32[]{:S(2)}) collective-permute-start(s32[128]{0:T(128)S(1)} %reshape.335), channel_id=1, source_target_pairs={{4,0},{6,2},{0,4},{2,6},{5,1},{7,3},{1,5},{3,7},{12,8},{14,10},{8,... | collective-permute-start | bytes 1544 | tf_op jit(solution)/shard_map/ppermute | solution.py:46
  69.4 3.7 %collective-permute-start = (s32[128]{0:T(128)S(1)}, s32[128]{0:T(128)S(1)}, u32[]{:S(2)}, u32[]{:S(2)}) collective-permute-start(s32[128]{0:T(128)S(1)} %reshape.335), channel_id=1, source_target_pairs={{2,0},{4,2},{6,4},{0,6},{3,1},{5,3},{7,5},{1,7},{10,8},{12,10},{14... | collective-permute-start | bytes 1544 | tf_op jit(solution)/shard_map/ppermute | solution.py:46
  73.2 4.8 %collective-permute-start.3 = (bf16[128,128]{1,0:T(8,128)(2,1)S(1)}, bf16[128,128]{1,0:T(8,128)(2,1)S(1)}, u32[]{:S(2)}, u32[]{:S(2)}) collective-permute-start(bf16[128,128]{1,0:T(8,128)(2,1)S(1)} %copy-done.8), channel_id=1, source_target_pairs={{32,0},{64,32},{96,64},{0,96},{33,1},{65,33},{97,65},{1,97},{34,2}... | collective-permute-start | bytes 98312 | tf_op jit(solution)/shard_map/ppermute | solution.py:46
  78.0 7.9 %collective-permute-start.4 = (bf16[128,128]{1,0:T(8,128)(2,1)S(1)}, bf16[128,128]{1,0:T(8,128)(2,1)S(1)}, u32[]{:S(2)}, u32[]{:S(2)}) collective-permute-start(bf16[128,128]{1,0:T(8,128)(2,1)S(1)} %copy-done.8), channel_id=1, source_target_pairs={{64,0},{96,32},{0,64},{32,96},{65,1},{97,33},{1,65},{33,97},{66,2}... | collective-permute-start | bytes 98312 | tf_op jit(solution)/shard_map/ppermute | solution.py:46
  87.2 3.3 %collective-permute-start.5 = (bf16[128,128]{1,0:T(8,128)(2,1)S(1)}, bf16[128,128]{1,0:T(8,128)(2,1)S(1)}, u32[]{:S(2)}, u32[]{:S(2)}) collective-permute-start(bf16[128,128]{1,0:T(8,128)(2,1)S(1)} %copy-done.8), channel_id=1, source_target_pairs={{96,0},{0,32},{32,64},{64,96},{97,1},{1,33},{33,65},{65,97},{98,2}... | collective-permute-start | bytes 98312 | tf_op jit(solution)/shard_map/ppermute | solution.py:46
  94.7 2.2 collective-permute-done.5.refs_3_
  96.9 2.2 collective-permute-start.6
  99.2 5.6 %collective-permute-start.7 = (bf16[4,128,128]{2,1,0:T(8,128)(2,1)S(1)}, bf16[4,128,128]{2,1,0:T(8,128)(2,1)S(1)}, u32[]{:S(2)}, u32[]{:S(2)}) collective-permute-start(bf16[4,128,128]{2,1,0:T(8,128)(2,1)S(1)} %shard_map.73.refs_0_), channel_id=1, source_target_pairs={{16,0},{24,8},{0,16},{8,24},{17,1},{25,9},{1,17},{9,25},{18,2},{26... | collective-permute-start | bytes 393224 | tf_op jit(solution)/shard_map/ppermute | solution.py:46
  106.7 5.9 %collective-permute-done.7.refs_2_ = bf16[4,128,128]{2,1,0:T(8,128)(2,1)S(1)} collective-permute-done((bf16[4,128,128]{2,1,0:T(8,128)(2,1)S(1)}, bf16[4,128,128]{2,1,0:T(8,128)(2,1)S(1)}, u32[]{:S(2)}, u32[]{:S(2)}) %collective-permute-start.7) | collective-permute-done | bytes 131104 | tf_op jit(solution)/shard_map/ppermute | solution.py:46
  112.7 6.7 %collective-permute-done.8.refs_3_ = bf16[4,128,128]{2,1,0:T(8,128)(2,1)S(1)} collective-permute-done((bf16[4,128,128]{2,1,0:T(8,128)(2,1)S(1)}, bf16[4,128,128]{2,1,0:T(8,128)(2,1)S(1)}, u32[]{:S(2)}, u32[]{:S(2)}) %collective-permute-start.8) | collective-permute-done | bytes 131104 | tf_op jit(solution)/shard_map/ppermute | solution.py:46
  121.4 3.3 %collective-permute-start.10 = (bf16[16,64,128]{2,1,0:T(8,128)(2,1)S(1)}, bf16[16,64,128]{2,1,0:T(8,128)(2,1)S(1)}, u32[]{:S(2)}, u32[]{:S(2)}) collective-permute-start(bf16[16,64,128]{2,1,0:T(8,128)(2,1)S(1)} %get-tuple-element.13.refs_0_), channel_id=1, source_target_pairs={{4,0},{6,2},{0,4},{2,6},{5,1},{7,3},{1,5},{3,7},{12,8},{14,10},{8,... | collective-permute-start | bytes 786440 | tf_op jit(solution)/shard_map/ppermute | solution.py:46
  124.7 4.0 %collective-permute-start.11 = (bf16[16,64,128]{2,1,0:T(8,128)(2,1)S(1)}, bf16[16,64,128]{2,1,0:T(8,128)(2,1)S(1)}, u32[]{:S(2)}, u32[]{:S(2)}) collective-permute-start(bf16[16,64,128]{2,1,0:T(8,128)(2,1)S(1)} %get-tuple-element.13.refs_0_), channel_id=1, source_target_pairs={{6,0},{0,2},{2,4},{4,6},{7,1},{1,3},{3,5},{5,7},{14,8},{8,10},{10,... | collective-permute-start | bytes 786440 | tf_op jit(solution)/shard_map/ppermute | solution.py:46
  130.2 7.5 %collective-permute-done.11.refs_3_ = bf16[16,64,128]{2,1,0:T(8,128)(2,1)S(1)} collective-permute-done((bf16[16,64,128]{2,1,0:T(8,128)(2,1)S(1)}, bf16[16,64,128]{2,1,0:T(8,128)(2,1)S(1)}, u32[]{:S(2)}, u32[]{:S(2)}) %collective-permute-start.11) | collective-permute-done | bytes 262176 | tf_op jit(solution)/shard_map/ppermute | solution.py:46
  138.7 3.9 %collective-permute-start.12 = (bf16[4096,128]{1,0:T(8,128)(2,1)}, bf16[4096,128]{1,0:T(8,128)(2,1)}, u32[]{:S(2)}, u32[]{:S(2)}) collective-permute-start(bf16[4096,128]{1,0:T(8,128)(2,1)} %bitcast.12.refs_0_), channel_id=1, source_target_pairs={{128,0},{256,128},{384,256},{0,384},{129,1},{257,129},{385,257},{1... | collective-permute-start | bytes 3145736 | tf_op jit(solution)/shard_map/ppermute | solution.py:46
  142.6 2.1 collective-permute-start.16
  146.4 2.0 shard_map.77
  148.5 5.1 %all-to-all-start.2 = ((bf16[4,32,32,256]{3,2,1,0:T(8,128)(2,1)}), bf16[4,32,32,256]{3,2,1,0:T(8,128)(2,1)S(1)}, u32[]{:S(2)}, u32[]{:S(2)}) async-start(bf16[4,32,32,256]{3,2,1,0:T(8,128)(2,1)} %shard_map.77), calls=%async_computation.2 | async-start | bytes 4194304 | tf_op jit(solution)/shard_map/all_to_all | solution.py:346
  154.0 3.8 %collective-permute-start.17 = (bf16[16,64,128]{2,1,0:T(8,128)(2,1)S(1)}, bf16[16,64,128]{2,1,0:T(8,128)(2,1)S(1)}, u32[]{:S(2)}, u32[]{:S(2)}) collective-permute-start(bf16[16,64,128]{2,1,0:T(8,128)(2,1)S(1)} %get-tuple-element.16.refs_0_), channel_id=1, source_target_pairs={{256,0},{384,128},{0,256},{128,384},{257,1},{385,129},{1,257},{129... | collective-permute-start | bytes 786440 | tf_op jit(solution)/shard_map/ppermute | solution.py:46
  157.7 4.0 %collective-permute-start.18 = (bf16[16,64,128]{2,1,0:T(8,128)(2,1)S(1)}, bf16[16,64,128]{2,1,0:T(8,128)(2,1)S(1)}, u32[]{:S(2)}, u32[]{:S(2)}) collective-permute-start(bf16[16,64,128]{2,1,0:T(8,128)(2,1)S(1)} %get-tuple-element.16.refs_0_), channel_id=1, source_target_pairs={{384,0},{0,128},{128,256},{256,384},{385,1},{1,129},{129,257},{257... | collective-permute-start | bytes 786440 | tf_op jit(solution)/shard_map/ppermute | solution.py:46
  163.6 8.5 %collective-permute-done.16.refs_1_ = bf16[16,64,128]{2,1,0:T(8,128)(2,1)S(1)} collective-permute-done((bf16[16,64,128]{2,1,0:T(8,128)(2,1)S(1)}, bf16[16,64,128]{2,1,0:T(8,128)(2,1)S(1)}, u32[]{:S(2)}, u32[]{:S(2)}) %collective-permute-start.16) | collective-permute-done | bytes 262176 | tf_op jit(solution)/shard_map/ppermute | solution.py:46
  172.8 32.4 %collective-permute-start.14 = (bf16[4096,128]{1,0:T(8,128)(2,1)}, bf16[4096,128]{1,0:T(8,128)(2,1)S(1)}, u32[]{:S(2)}, u32[]{:S(2)}) collective-permute-start(bf16[4096,128]{1,0:T(8,128)(2,1)} %bitcast.12.refs_0_), channel_id=1, source_target_pairs={{384,0},{0,128},{128,256},{256,384},{385,1},{1,129},{129,257},{257... | collective-permute-start | bytes 3145736 | tf_op jit(solution)/shard_map/ppermute | solution.py:46
  211.2 3.4 %collective-permute-start.21 = (bf16[16,16,2048]{2,1,0:T(8,128)(2,1)S(1)}, bf16[16,16,2048]{2,1,0:T(8,128)(2,1)}, u32[]{:S(2)}, u32[]{:S(2)}) collective-permute-start(bf16[16,16,2048]{2,1,0:T(8,128)(2,1)S(1)} %shard_map.81.refs_0_), channel_id=1, source_target_pairs={{6,0},{0,2},{2,4},{4,6},{7,1},{1,3},{3,5},{5,7},{14,8},{8,10},{10,... | collective-permute-start | bytes 3145736 | tf_op jit(solution)/shard_map/ppermute | solution.py:46
  215.6 10.7 %collective-permute-done.14.refs_3_ = bf16[4096,128]{1,0:T(8,128)(2,1)S(1)} collective-permute-done((bf16[4096,128]{1,0:T(8,128)(2,1)}, bf16[4096,128]{1,0:T(8,128)(2,1)S(1)}, u32[]{:S(2)}, u32[]{:S(2)}) %collective-permute-start.14) | collective-permute-done | bytes 1048608 | tf_op jit(solution)/shard_map/ppermute | solution.py:46
  226.3 2.8 %shard_map.78.q_ref = bf16[256,512]{1,0:T(8,128)(2,1)S(1)} custom-call(bf16[256,4096]{1,0:T(8,128)(2,1)S(1)} %copy-done.1, bf16[4096,128]{1,0:T(8,128)(2,1)} %bitcast.12.refs_0_, bf16[4096,128]{1,0:T(8,128)(2,1)} %collective-permute-done.12.refs_1_, bf16[4096,128]{1,0:T(8,128)(2,1)S(1)} %collective-permute-done.13.refs_2_, ...), custom_call_target="tpu_custom_call" | custom-call | flops 1073741824 | tf_op jit(solution)/shard_map/pallas_call | solution.py:26
  230.8 3.4 %shard_map.80.m_ref = bf16[256,512]{1,0:T(8,128)(2,1)S(1)} custom-call(s32[3]{0:T(128)S(1)} %pad_add_fusion.1.f_ref, s32[8,16]{1,0:T(8,128)S(1)} %fusion.4.p_ref, bf16[256,512]{1,0:T(8,128)(2,1)S(1)} %copy-done.4, bf16[128,32,256]{2,1,0:T(8,128)(2,1)S(1)} %bitcast.28, bf16[8,32,256]{2,1,0:T(8,128)(2,1)} %bitcast.17.own_ref, s32[8,1,512]{2,1,0:T(1,128)S(1)} %shard_map.79.kp_ref), custom_call_target="tpu_custom_call" | custom-call | flops 268435456 | tf_op jit(solution)/shard_map/pallas_call | solution.py:26
  234.2 4.5 %collective-permute-start.15 = (bf16[256,512]{1,0:T(8,128)(2,1)S(1)}, bf16[256,512]{1,0:T(8,128)(2,1)S(1)}, u32[]{:S(2)}, u32[]{:S(2)}) collective-permute-start(bf16[256,512]{1,0:T(8,128)(2,1)S(1)} %shard_map.80.m_ref), channel_id=1, source_target_pairs={{1,0},{0,1},{3,2},{2,3},{5,4},{4,5},{7,6},{6,7},{9,8},{8,9},{11,10... | collective-permute-start | bytes 786440 | tf_op jit(solution)/shard_map/ppermute | solution.py:46
  238.7 21.6 %collective-permute-done.21.refs_3_ = bf16[16,16,2048]{2,1,0:T(8,128)(2,1)} collective-permute-done((bf16[16,16,2048]{2,1,0:T(8,128)(2,1)S(1)}, bf16[16,16,2048]{2,1,0:T(8,128)(2,1)}, u32[]{:S(2)}, u32[]{:S(2)}) %collective-permute-start.21) | collective-permute-done | bytes 1048608 | tf_op jit(solution)/shard_map/ppermute | solution.py:46
  260.3 2.1 shard_map.82
  262.5 2.3 shard_map.83
  (90 shorter events, 28.0 us)
Async XLA Ops:
  6.5 138.3 %all-gather.2.cloned.1.call-start = ((), (), s32[]{:S(2)}) async-start(), calls=%async_computation.3 | async-start | bytes 2228224 | tf_op jit(solution)/shard_map/all_gather | solution.py:331
  34.4 28.2 %copy-start = (bf16[256,4096]{1,0:T(8,128)(2,1)S(1)}, bf16[256,4096]{1,0:T(8,128)(2,1)}, u32[]{:S(2)}) copy-start(bf16[256,4096]{1,0:T(8,128)(2,1)} %t_ref.3) | copy-start | bytes 6291460
  62.5 1.4 copy-start.7
  62.5 10.6 %copy-start.8 = (bf16[128,128]{1,0:T(8,128)(2,1)S(1)}, bf16[128,128]{1,0:T(8,128)(2,1)}, u32[]{:S(2)}) copy-start(bf16[128,128]{1,0:T(8,128)(2,1)} %get-tuple-element.12.refs_0_) | copy-start | bytes 98308
  64.0 23.2 %collective-permute-start.2 = (s32[128]{0:T(128)S(1)}, s32[128]{0:T(128)S(1)}, u32[]{:S(2)}, u32[]{:S(2)}) collective-permute-start(s32[128]{0:T(128)S(1)} %reshape.335), channel_id=1, source_target_pairs={{6,0},{0,2},{2,4},{4,6},{7,1},{1,3},{3,5},{5,7},{14,8},{8,10},{10,... | collective-permute-start | bytes 1544 | tf_op jit(solution)/shard_map/ppermute | solution.py:46
  66.5 24.0 %collective-permute-start.1 = (s32[128]{0:T(128)S(1)}, s32[128]{0:T(128)S(1)}, u32[]{:S(2)}, u32[]{:S(2)}) collective-permute-start(s32[128]{0:T(128)S(1)} %reshape.335), channel_id=1, source_target_pairs={{4,0},{6,2},{0,4},{2,6},{5,1},{7,3},{1,5},{3,7},{12,8},{14,10},{8,... | collective-permute-start | bytes 1544 | tf_op jit(solution)/shard_map/ppermute | solution.py:46
  69.4 21.1 %collective-permute-start = (s32[128]{0:T(128)S(1)}, s32[128]{0:T(128)S(1)}, u32[]{:S(2)}, u32[]{:S(2)}) collective-permute-start(s32[128]{0:T(128)S(1)} %reshape.335), channel_id=1, source_target_pairs={{2,0},{4,2},{6,4},{0,6},{3,1},{5,3},{7,5},{1,7},{10,8},{12,10},{14... | collective-permute-start | bytes 1544 | tf_op jit(solution)/shard_map/ppermute | solution.py:46
  73.2 21.5 %collective-permute-start.3 = (bf16[128,128]{1,0:T(8,128)(2,1)S(1)}, bf16[128,128]{1,0:T(8,128)(2,1)S(1)}, u32[]{:S(2)}, u32[]{:S(2)}) collective-permute-start(bf16[128,128]{1,0:T(8,128)(2,1)S(1)} %copy-done.8), channel_id=1, source_target_pairs={{32,0},{64,32},{96,64},{0,96},{33,1},{65,33},{97,65},{1,97},{34,2}... | collective-permute-start | bytes 98312 | tf_op jit(solution)/shard_map/ppermute | solution.py:46
  78.0 16.7 %collective-permute-start.4 = (bf16[128,128]{1,0:T(8,128)(2,1)S(1)}, bf16[128,128]{1,0:T(8,128)(2,1)S(1)}, u32[]{:S(2)}, u32[]{:S(2)}) collective-permute-start(bf16[128,128]{1,0:T(8,128)(2,1)S(1)} %copy-done.8), channel_id=1, source_target_pairs={{64,0},{96,32},{0,64},{32,96},{65,1},{97,33},{1,65},{33,97},{66,2}... | collective-permute-start | bytes 98312 | tf_op jit(solution)/shard_map/ppermute | solution.py:46
  87.2 9.7 %collective-permute-start.5 = (bf16[128,128]{1,0:T(8,128)(2,1)S(1)}, bf16[128,128]{1,0:T(8,128)(2,1)S(1)}, u32[]{:S(2)}, u32[]{:S(2)}) collective-permute-start(bf16[128,128]{1,0:T(8,128)(2,1)S(1)} %copy-done.8), channel_id=1, source_target_pairs={{96,0},{0,32},{32,64},{64,96},{97,1},{1,33},{33,65},{65,97},{98,2}... | collective-permute-start | bytes 98312 | tf_op jit(solution)/shard_map/ppermute | solution.py:46
  96.9 9.8 %collective-permute-start.6 = (bf16[4,128,128]{2,1,0:T(8,128)(2,1)S(1)}, bf16[4,128,128]{2,1,0:T(8,128)(2,1)S(1)}, u32[]{:S(2)}, u32[]{:S(2)}) collective-permute-start(bf16[4,128,128]{2,1,0:T(8,128)(2,1)S(1)} %shard_map.73.refs_0_), channel_id=1, source_target_pairs={{8,0},{16,8},{24,16},{0,24},{9,1},{17,9},{25,17},{1,25},{10,2},{18... | collective-permute-start | bytes 393224 | tf_op jit(solution)/shard_map/ppermute | solution.py:46
  99.2 13.5 %collective-permute-start.7 = (bf16[4,128,128]{2,1,0:T(8,128)(2,1)S(1)}, bf16[4,128,128]{2,1,0:T(8,128)(2,1)S(1)}, u32[]{:S(2)}, u32[]{:S(2)}) collective-permute-start(bf16[4,128,128]{2,1,0:T(8,128)(2,1)S(1)} %shard_map.73.refs_0_), channel_id=1, source_target_pairs={{16,0},{24,8},{0,16},{8,24},{17,1},{25,9},{1,17},{9,25},{18,2},{26... | collective-permute-start | bytes 393224 | tf_op jit(solution)/shard_map/ppermute | solution.py:46
  104.8 14.6 %collective-permute-start.8 = (bf16[4,128,128]{2,1,0:T(8,128)(2,1)S(1)}, bf16[4,128,128]{2,1,0:T(8,128)(2,1)S(1)}, u32[]{:S(2)}, u32[]{:S(2)}) collective-permute-start(bf16[4,128,128]{2,1,0:T(8,128)(2,1)S(1)} %shard_map.73.refs_0_), channel_id=1, source_target_pairs={{24,0},{0,8},{8,16},{16,24},{25,1},{1,9},{9,17},{17,25},{26,2},{2,... | collective-permute-start | bytes 393224 | tf_op jit(solution)/shard_map/ppermute | solution.py:46
  119.4 9.5 %collective-permute-start.9 = (bf16[16,64,128]{2,1,0:T(8,128)(2,1)S(1)}, bf16[16,64,128]{2,1,0:T(8,128)(2,1)S(1)}, u32[]{:S(2)}, u32[]{:S(2)}) collective-permute-start(bf16[16,64,128]{2,1,0:T(8,128)(2,1)S(1)} %get-tuple-element.13.refs_0_), channel_id=1, source_target_pairs={{2,0},{4,2},{6,4},{0,6},{3,1},{5,3},{7,5},{1,7},{10,8},{12,10},{14... | collective-permute-start | bytes 786440 | tf_op jit(solution)/shard_map/ppermute | solution.py:46
  121.4 8.7 %collective-permute-start.10 = (bf16[16,64,128]{2,1,0:T(8,128)(2,1)S(1)}, bf16[16,64,128]{2,1,0:T(8,128)(2,1)S(1)}, u32[]{:S(2)}, u32[]{:S(2)}) collective-permute-start(bf16[16,64,128]{2,1,0:T(8,128)(2,1)S(1)} %get-tuple-element.13.refs_0_), channel_id=1, source_target_pairs={{4,0},{6,2},{0,4},{2,6},{5,1},{7,3},{1,5},{3,7},{12,8},{14,10},{8,... | collective-permute-start | bytes 786440 | tf_op jit(solution)/shard_map/ppermute | solution.py:46
  124.7 13.0 %collective-permute-start.11 = (bf16[16,64,128]{2,1,0:T(8,128)(2,1)S(1)}, bf16[16,64,128]{2,1,0:T(8,128)(2,1)S(1)}, u32[]{:S(2)}, u32[]{:S(2)}) collective-permute-start(bf16[16,64,128]{2,1,0:T(8,128)(2,1)S(1)} %get-tuple-element.13.refs_0_), channel_id=1, source_target_pairs={{6,0},{0,2},{2,4},{4,6},{7,1},{1,3},{3,5},{5,7},{14,8},{8,10},{10,... | collective-permute-start | bytes 786440 | tf_op jit(solution)/shard_map/ppermute | solution.py:46
  138.7 72.5 %collective-permute-start.12 = (bf16[4096,128]{1,0:T(8,128)(2,1)}, bf16[4096,128]{1,0:T(8,128)(2,1)}, u32[]{:S(2)}, u32[]{:S(2)}) collective-permute-start(bf16[4096,128]{1,0:T(8,128)(2,1)} %bitcast.12.refs_0_), channel_id=1, source_target_pairs={{128,0},{256,128},{384,256},{0,384},{129,1},{257,129},{385,257},{1... | collective-permute-start | bytes 3145736 | tf_op jit(solution)/shard_map/ppermute | solution.py:46
  142.6 29.5 %collective-permute-start.16 = (bf16[16,64,128]{2,1,0:T(8,128)(2,1)S(1)}, bf16[16,64,128]{2,1,0:T(8,128)(2,1)S(1)}, u32[]{:S(2)}, u32[]{:S(2)}) collective-permute-start(bf16[16,64,128]{2,1,0:T(8,128)(2,1)S(1)} %get-tuple-element.16.refs_0_), channel_id=1, source_target_pairs={{128,0},{256,128},{384,256},{0,384},{129,1},{257,129},{385,257},{1... | collective-permute-start | bytes 786440 | tf_op jit(solution)/shard_map/ppermute | solution.py:46
  144.8 1.6 copy-start.2
  148.5 81.4 %all-to-all-start.2 = ((bf16[4,32,32,256]{3,2,1,0:T(8,128)(2,1)}), bf16[4,32,32,256]{3,2,1,0:T(8,128)(2,1)S(1)}, u32[]{:S(2)}, u32[]{:S(2)}) async-start(bf16[4,32,32,256]{3,2,1,0:T(8,128)(2,1)} %shard_map.77), calls=%async_computation.2 | async-start | bytes 4194304 | tf_op jit(solution)/shard_map/all_to_all | solution.py:346
  153.9 72.4 %copy-start.1 = (bf16[256,4096]{1,0:T(8,128)(2,1)S(1)}, bf16[256,4096]{1,0:T(8,128)(2,1)}, u32[]{:S(2)}) copy-start(bf16[256,4096]{1,0:T(8,128)(2,1)} %t_ref.3) | copy-start | bytes 6291460
  154.0 52.1 %collective-permute-start.17 = (bf16[16,64,128]{2,1,0:T(8,128)(2,1)S(1)}, bf16[16,64,128]{2,1,0:T(8,128)(2,1)S(1)}, u32[]{:S(2)}, u32[]{:S(2)}) collective-permute-start(bf16[16,64,128]{2,1,0:T(8,128)(2,1)S(1)} %get-tuple-element.16.refs_0_), channel_id=1, source_target_pairs={{256,0},{384,128},{0,256},{128,384},{257,1},{385,129},{1,257},{129... | collective-permute-start | bytes 786440 | tf_op jit(solution)/shard_map/ppermute | solution.py:46
  157.7 48.4 %collective-permute-start.18 = (bf16[16,64,128]{2,1,0:T(8,128)(2,1)S(1)}, bf16[16,64,128]{2,1,0:T(8,128)(2,1)S(1)}, u32[]{:S(2)}, u32[]{:S(2)}) collective-permute-start(bf16[16,64,128]{2,1,0:T(8,128)(2,1)S(1)} %get-tuple-element.16.refs_0_), channel_id=1, source_target_pairs={{384,0},{0,128},{128,256},{256,384},{385,1},{1,129},{129,257},{257... | collective-permute-start | bytes 786440 | tf_op jit(solution)/shard_map/ppermute | solution.py:46
  161.7 53.9 %collective-permute-start.13 = (bf16[4096,128]{1,0:T(8,128)(2,1)}, bf16[4096,128]{1,0:T(8,128)(2,1)S(1)}, u32[]{:S(2)}, u32[]{:S(2)}) collective-permute-start(bf16[4096,128]{1,0:T(8,128)(2,1)} %bitcast.12.refs_0_), channel_id=1, source_target_pairs={{256,0},{384,128},{0,256},{128,384},{257,1},{385,129},{1,257},{129... | collective-permute-start | bytes 3145736 | tf_op jit(solution)/shard_map/ppermute | solution.py:46
  172.8 53.5 %collective-permute-start.14 = (bf16[4096,128]{1,0:T(8,128)(2,1)}, bf16[4096,128]{1,0:T(8,128)(2,1)S(1)}, u32[]{:S(2)}, u32[]{:S(2)}) collective-permute-start(bf16[4096,128]{1,0:T(8,128)(2,1)} %bitcast.12.refs_0_), channel_id=1, source_target_pairs={{384,0},{0,128},{128,256},{256,384},{385,1},{1,129},{129,257},{257... | collective-permute-start | bytes 3145736 | tf_op jit(solution)/shard_map/ppermute | solution.py:46
  206.1 1.0 copy-start.6
  207.3 31.4 %collective-permute-start.19 = (bf16[16,16,2048]{2,1,0:T(8,128)(2,1)S(1)}, bf16[16,16,2048]{2,1,0:T(8,128)(2,1)}, u32[]{:S(2)}, u32[]{:S(2)}) collective-permute-start(bf16[16,16,2048]{2,1,0:T(8,128)(2,1)S(1)} %shard_map.81.refs_0_), channel_id=1, source_target_pairs={{2,0},{4,2},{6,4},{0,6},{3,1},{5,3},{7,5},{1,7},{10,8},{12,10},{14... | collective-permute-start | bytes 3145736 | tf_op jit(solution)/shard_map/ppermute | solution.py:46
  209.3 29.5 %collective-permute-start.20 = (bf16[16,16,2048]{2,1,0:T(8,128)(2,1)S(1)}, bf16[16,16,2048]{2,1,0:T(8,128)(2,1)}, u32[]{:S(2)}, u32[]{:S(2)}) collective-permute-start(bf16[16,16,2048]{2,1,0:T(8,128)(2,1)S(1)} %shard_map.81.refs_0_), channel_id=1, source_target_pairs={{4,0},{6,2},{0,4},{2,6},{5,1},{7,3},{1,5},{3,7},{12,8},{14,10},{8,... | collective-permute-start | bytes 3145736 | tf_op jit(solution)/shard_map/ppermute | solution.py:46
  211.2 49.1 %collective-permute-start.21 = (bf16[16,16,2048]{2,1,0:T(8,128)(2,1)S(1)}, bf16[16,16,2048]{2,1,0:T(8,128)(2,1)}, u32[]{:S(2)}, u32[]{:S(2)}) collective-permute-start(bf16[16,16,2048]{2,1,0:T(8,128)(2,1)S(1)} %shard_map.81.refs_0_), channel_id=1, source_target_pairs={{6,0},{0,2},{2,4},{4,6},{7,1},{1,3},{3,5},{5,7},{14,8},{8,10},{10,... | collective-permute-start | bytes 3145736 | tf_op jit(solution)/shard_map/ppermute | solution.py:46
  229.2 0.7 copy-start.3
  229.9 1.0 copy-start.4
  234.2 28.2 %collective-permute-start.15 = (bf16[256,512]{1,0:T(8,128)(2,1)S(1)}, bf16[256,512]{1,0:T(8,128)(2,1)S(1)}, u32[]{:S(2)}, u32[]{:S(2)}) collective-permute-start(bf16[256,512]{1,0:T(8,128)(2,1)S(1)} %shard_map.80.m_ref), channel_id=1, source_target_pairs={{1,0},{0,1},{3,2},{2,3},{5,4},{4,5},{7,6},{6,7},{9,8},{8,9},{11,10... | collective-permute-start | bytes 786440 | tf_op jit(solution)/shard_map/ppermute | solution.py:46
  (1 other events, 0.7 us)
Sparse Core Ops, SparseCore 0:
  64.1 69.0 all-gather.1

commit v5 on v4

--- a/solution.py
+++ b/solution.py
@@ -143,12 +143,25 @@
     small = both // 2
     deep = planes * wide * small
 
-    def kernel(t_ref, w_ref, o_ref):
+    chunk = 4
+
+    def kernel(t_ref, w_hbm, o_ref, w_ref, sems):
+        copies = [
+            pltpu.make_async_copy(
+                w_hbm.at[:, :, pl.ds(i * chunk, chunk)], w_ref.at[i], sems.at[i]
+            )
+            for i in range(tall // chunk)
+        ]
+        for copy in copies:
+            copy.start()
         total = jnp.zeros(o_ref.shape, F32)
+        lines = [(x, y) for y in range(wide) for x in range(planes)]
         for z in range(tall):
-            lines = [(x, y) for y in range(wide) for x in range(planes)]
-            keys = jnp.concatenate([w_ref[x, y, z, :small] for x, y in lines], axis=0)
-            values = jnp.concatenate([w_ref[x, y, z, small:] for x, y in lines], axis=0)
+            i, j = z // chunk, z % chunk
+            if j == 0:
+                copies[i].wait()
+            keys = jnp.concatenate([w_ref[i, x, y, j, :small] for x, y in lines], axis=0)
+            values = jnp.concatenate([w_ref[i, x, y, j, small:] for x, y in lines], axis=0)
             total += jnp.dot(
                 t_ref[:, z * deep : (z + 1) * deep],
                 jnp.concatenate([keys, values], axis=1),
@@ -156,9 +169,21 @@
             )
         o_ref[...] = total.astype(BF16)
 
-    out = jax.ShapeDtypeStruct((tokens.shape[0], 2 * HD), BF16)
-    flops = 2 * tokens.size * 2 * HD
-    return call(kernel, out, tokens, every, flops=flops)
+    return pl.pallas_call(
+        kernel,
+        out_shape=jax.ShapeDtypeStruct((tokens.shape[0], 2 * HD), BF16),
+        in_specs=[pl.BlockSpec(memory_space=pltpu.VMEM), pl.BlockSpec(memory_space=pl.ANY)],
+        out_specs=pl.BlockSpec(memory_space=pltpu.VMEM),
+        scratch_shapes=[
+            pltpu.VMEM((tall // chunk, planes, wide, chunk, both, HD), BF16),
+            pltpu.SemaphoreType.DMA((tall // chunk,)),
+        ],
+        compiler_params=pltpu.CompilerParams(vmem_limit_bytes=40 << 20),
+        cost_estimate=pl.CostEstimate(
+            flops=4 * tokens.size * HD, bytes_accessed=0, transcendentals=0
+        ),
+        name="project_pair",
+    )(tokens, every)
 
 
 def project_queries(tokens, pieces, tile):
@@ -222,13 +247,25 @@
 def pick_blocks(blocks, asked, at):
     wide, count = asked.shape
 
-    def kernel(asked_ref, at_ref, b_ref, o_ref):
+    def kernel(asked_ref, at_ref, b_hbm, o_ref, sem):
         for s in range(wide):
+            to = (at_ref[0] + s) % wide
             for i in range(count):
-                o_ref[(at_ref[0] + s) % wide, i] = b_ref[asked_ref[s, i]]
-
-    out = jax.ShapeDtypeStruct((wide, count, *blocks.shape[1:]), BF16)
-    return call(kernel, out, asked, at[None], blocks)
+                pltpu.make_async_copy(b_hbm.at[asked_ref[s, i]], o_ref.at[to, i], sem).start()
+        pltpu.make_async_copy(o_ref, o_ref, sem).wait()
+
+    return pl.pallas_call(
+        kernel,
+        out_shape=jax.ShapeDtypeStruct((wide, count, *blocks.shape[1:]), BF16),
+        in_specs=[
+            pl.BlockSpec(memory_space=pltpu.SMEM),
+            pl.BlockSpec(memory_space=pltpu.SMEM),
+            pl.BlockSpec(memory_space=pl.ANY),
+        ],
+        out_specs=pl.BlockSpec(memory_space=pltpu.VMEM),
+        scratch_shapes=[pltpu.SemaphoreType.DMA],
+        name="pick_blocks",
+    )(asked, at[None], blocks)
 
 
 def attend(queries, incoming, local_blocks, position, key_pos, facts):

time: 273 us -> 274 us (level)
  Pallas kernels: 17.8 us -> 20.9 us
    pallas_call x0 -> x2, Pallas kernels: none -> 6.52 us  [the longest x1 4.23 us: pick_blocks(): pl.pallas_call(kernel, out_shape=jax.ShapeDtypeStruct((wide, count, *bloc...]
    pallas_call x11 -> x9, Pallas kernels: 16.2 us -> 12.7 us  [call(): pl.pallas_call(kernel, out_shape=out_shape, in_specs=spaces, out_specs=ja...]
  transfers between devices with their start and end apart: 24 -> 24, of which waited for: 8 -> 8; matrix products, arithmetic and copies ran while one was open for 2% -> 3% of each run, Pallas kernels for 5% -> 5%
where the time goes in v5:
time: 274 us; the launch traced here: 273 us
  starting transfers between devices  108 us (39%)
  waiting for transfers between devices  64.3 us (23%)
  blocking collectives  54 us (20%)
  Pallas kernels  20.9 us (8%)
  between operations  14.6 us (5%)
  other arithmetic  5.83 us (2%)
  local copies, waits for them, and re-layouts  4.96 us (2%)
    ppermute x22, starting transfers between devices, from_ahead(): return lax.ppermute(x, axis, [((i + step) % n, i) for i in range(n)])  102 us
    ppermute x22, waiting for transfers between devices, from_ahead(): return lax.ppermute(x, axis, [((i + step) % n, i) for i in range(n)])  64.3 us
    all_to_all x1, blocking collectives, copy_for_each(): lax.all_to_all(jnp.broadcast_to(shard[None], (count, *shard.shape)), axis...  28.2 us
    all_to_all x1, blocking collectives, body(): column = lax.all_to_all(cargo, TALL, 0, 0, tiled=True)  25.8 us
    pallas_call x9, Pallas kernels, call(): pl.pallas_call(kernel, out_shape=out_shape, in_specs=spaces, out_specs=ja...  12.7 us
    all_to_all x1, starting transfers between devices, body(): lax.all_to_all(outgoing, 'y', split_axis=0, concat_axis=0, tiled=True)  6.01 us
  transfers between devices with their start and end apart: 24, of which 8 were waited for; matrix products, arithmetic and copies ran while one was open for 3% of the time, Pallas kernels for 5%

profile of v5, /device:TPU:85, one launch (start us, length us, event | category | flops | bytes accessed | tf_op | source)
XLA Modules:
  0.0 272.6 jit_solution(18131048078588273890)
XLA Ops:
  8.2 25.8 %all_to_all.15 = bf16[16,32,128]{2,1,0:T(8,128)(2,1)S(1)} all-to-all(bf16[16,32,128]{2,1,0:T(8,128)(2,1)} %get-tuple-element.15), channel_id=1, replica_groups=mesh['dp'=4,'zh'=4,'zl'=4,'y'=4,'tp'=2] {'zh','zl'}, dimensions={0} | all-to-all | bytes 262144 | tf_op jit(solution)/shard_map/all_to_all | solution.py:361
  34.4 28.2 %all_to_all.16 = bf16[16,16,32,128]{3,2,1,0:T(8,128)(2,1)S(1)} all-to-all(bf16[16,16,32,128]{3,2,1,0:T(8,128)(2,1)S(1)} %broadcast_in_dim.99), channel_id=1, replica_groups=mesh['dp'=4,'zh'=4,'zl'=4,'y'=4,'tp'=2] {'dp','y'}, dimensions={0} | all-to-all | bytes 4194304 | tf_op jit(solution)/shard_map/all_to_all | solution.py:39
  62.5 2.3 project_pair.1
  65.0 2.5 collective-permute-start.2
  67.4 2.9 %collective-permute-start.1 = (s32[128]{0:T(128)S(1)}, s32[128]{0:T(128)S(1)}, u32[]{:S(2)}, u32[]{:S(2)}) collective-permute-start(s32[128]{0:T(128)S(1)} %reshape.335), channel_id=1, source_target_pairs={{4,0},{6,2},{0,4},{2,6},{5,1},{7,3},{1,5},{3,7},{12,8},{14,10},{8,... | collective-permute-start | bytes 1544 | tf_op jit(solution)/shard_map/ppermute | solution.py:46
  70.4 3.7 %collective-permute-start = (s32[128]{0:T(128)S(1)}, s32[128]{0:T(128)S(1)}, u32[]{:S(2)}, u32[]{:S(2)}) collective-permute-start(s32[128]{0:T(128)S(1)} %reshape.335), channel_id=1, source_target_pairs={{2,0},{4,2},{6,4},{0,6},{3,1},{5,3},{7,5},{1,7},{10,8},{12,10},{14... | collective-permute-start | bytes 1544 | tf_op jit(solution)/shard_map/ppermute | solution.py:46
  74.1 4.8 %collective-permute-start.3 = (bf16[128,128]{1,0:T(8,128)(2,1)S(1)}, bf16[128,128]{1,0:T(8,128)(2,1)S(1)}, u32[]{:S(2)}, u32[]{:S(2)}) collective-permute-start(bf16[128,128]{1,0:T(8,128)(2,1)S(1)} %copy-done.7), channel_id=1, source_target_pairs={{32,0},{64,32},{96,64},{0,96},{33,1},{65,33},{97,65},{1,97},{34,2}... | collective-permute-start | bytes 98312 | tf_op jit(solution)/shard_map/ppermute | solution.py:46
  78.9 7.9 %collective-permute-start.4 = (bf16[128,128]{1,0:T(8,128)(2,1)S(1)}, bf16[128,128]{1,0:T(8,128)(2,1)S(1)}, u32[]{:S(2)}, u32[]{:S(2)}) collective-permute-start(bf16[128,128]{1,0:T(8,128)(2,1)S(1)} %copy-done.7), channel_id=1, source_target_pairs={{64,0},{96,32},{0,64},{32,96},{65,1},{97,33},{1,65},{33,97},{66,2}... | collective-permute-start | bytes 98312 | tf_op jit(solution)/shard_map/ppermute | solution.py:46
  88.2 3.3 %collective-permute-start.5 = (bf16[128,128]{1,0:T(8,128)(2,1)S(1)}, bf16[128,128]{1,0:T(8,128)(2,1)S(1)}, u32[]{:S(2)}, u32[]{:S(2)}) collective-permute-start(bf16[128,128]{1,0:T(8,128)(2,1)S(1)} %copy-done.7), channel_id=1, source_target_pairs={{96,0},{0,32},{32,64},{64,96},{97,1},{1,33},{33,65},{65,97},{98,2}... | collective-permute-start | bytes 98312 | tf_op jit(solution)/shard_map/ppermute | solution.py:46
  95.7 2.2 collective-permute-done.5.refs_3_
  97.9 2.2 collective-permute-start.6
  100.1 5.6 %collective-permute-start.7 = (bf16[4,128,128]{2,1,0:T(8,128)(2,1)S(1)}, bf16[4,128,128]{2,1,0:T(8,128)(2,1)S(1)}, u32[]{:S(2)}, u32[]{:S(2)}) collective-permute-start(bf16[4,128,128]{2,1,0:T(8,128)(2,1)S(1)} %shard_map.73.refs_0_), channel_id=1, source_target_pairs={{16,0},{24,8},{0,16},{8,24},{17,1},{25,9},{1,17},{9,25},{18,2},{26... | collective-permute-start | bytes 393224 | tf_op jit(solution)/shard_map/ppermute | solution.py:46
  107.7 5.8 %collective-permute-done.7.refs_2_ = bf16[4,128,128]{2,1,0:T(8,128)(2,1)S(1)} collective-permute-done((bf16[4,128,128]{2,1,0:T(8,128)(2,1)S(1)}, bf16[4,128,128]{2,1,0:T(8,128)(2,1)S(1)}, u32[]{:S(2)}, u32[]{:S(2)}) %collective-permute-start.7) | collective-permute-done | bytes 131104 | tf_op jit(solution)/shard_map/ppermute | solution.py:46
  113.5 6.9 %collective-permute-done.8.refs_3_ = bf16[4,128,128]{2,1,0:T(8,128)(2,1)S(1)} collective-permute-done((bf16[4,128,128]{2,1,0:T(8,128)(2,1)S(1)}, bf16[4,128,128]{2,1,0:T(8,128)(2,1)S(1)}, u32[]{:S(2)}, u32[]{:S(2)}) %collective-permute-start.8) | collective-permute-done | bytes 131104 | tf_op jit(solution)/shard_map/ppermute | solution.py:46
  120.4 2.4 collective-permute-start.9
  122.8 2.9 %collective-permute-start.10 = (bf16[16,64,128]{2,1,0:T(8,128)(2,1)S(1)}, bf16[16,64,128]{2,1,0:T(8,128)(2,1)S(1)}, u32[]{:S(2)}, u32[]{:S(2)}) collective-permute-start(bf16[16,64,128]{2,1,0:T(8,128)(2,1)S(1)} %get-tuple-element.13.refs_0_), channel_id=1, source_target_pairs={{4,0},{6,2},{0,4},{2,6},{5,1},{7,3},{1,5},{3,7},{12,8},{14,10},{8,... | collective-permute-start | bytes 786440 | tf_op jit(solution)/shard_map/ppermute | solution.py:46
  125.7 4.0 %collective-permute-start.11 = (bf16[16,64,128]{2,1,0:T(8,128)(2,1)S(1)}, bf16[16,64,128]{2,1,0:T(8,128)(2,1)S(1)}, u32[]{:S(2)}, u32[]{:S(2)}) collective-permute-start(bf16[16,64,128]{2,1,0:T(8,128)(2,1)S(1)} %get-tuple-element.13.refs_0_), channel_id=1, source_target_pairs={{6,0},{0,2},{2,4},{4,6},{7,1},{1,3},{3,5},{5,7},{14,8},{8,10},{10,... | collective-permute-start | bytes 786440 | tf_op jit(solution)/shard_map/ppermute | solution.py:46
  131.8 7.6 %collective-permute-done.11.refs_3_ = bf16[16,64,128]{2,1,0:T(8,128)(2,1)S(1)} collective-permute-done((bf16[16,64,128]{2,1,0:T(8,128)(2,1)S(1)}, bf16[16,64,128]{2,1,0:T(8,128)(2,1)S(1)}, u32[]{:S(2)}, u32[]{:S(2)}) %collective-permute-start.11) | collective-permute-done | bytes 262176 | tf_op jit(solution)/shard_map/ppermute | solution.py:46
  140.5 2.8 %collective-permute-start.12 = (bf16[4096,128]{1,0:T(8,128)(2,1)}, bf16[4096,128]{1,0:T(8,128)(2,1)}, u32[]{:S(2)}, u32[]{:S(2)}) collective-permute-start(bf16[4096,128]{1,0:T(8,128)(2,1)} %bitcast.12.refs_0_), channel_id=1, source_target_pairs={{128,0},{256,128},{384,256},{0,384},{129,1},{257,129},{385,257},{1... | collective-permute-start | bytes 3145736 | tf_op jit(solution)/shard_map/ppermute | solution.py:46
  145.8 4.2 %pick_blocks.1 = bf16[4,32,32,256]{3,2,1,0:T(8,128)(2,1)} custom-call(s32[4,32]{1,0:T(4,128)} %broadcast_add_fusion.asked_ref, s32[1]{0:T(128)} %bitcast.9.at_ref, bf16[128,32,256]{2,1,0:T(8,128)(2,1)} %all-gather.2.cloned.1.call-done.b_hbm), custom_call_target="tpu_custom_call" | custom-call | tf_op jit(solution)/shard_map/pick_blocks/pallas_call | solution.py:257
  150.0 6.0 %all-to-all-start.2 = ((bf16[4,32,32,256]{3,2,1,0:T(8,128)(2,1)}), bf16[4,32,32,256]{3,2,1,0:T(8,128)(2,1)S(1)}, u32[]{:S(2)}, u32[]{:S(2)}) async-start(bf16[4,32,32,256]{3,2,1,0:T(8,128)(2,1)} %pick_blocks.1), calls=%async_computation.2 | async-start | bytes 4194304 | tf_op jit(solution)/shard_map/all_to_all | solution.py:383
  156.5 3.4 %collective-permute-start.17 = (bf16[16,64,128]{2,1,0:T(8,128)(2,1)S(1)}, bf16[16,64,128]{2,1,0:T(8,128)(2,1)S(1)}, u32[]{:S(2)}, u32[]{:S(2)}) collective-permute-start(bf16[16,64,128]{2,1,0:T(8,128)(2,1)S(1)} %get-tuple-element.16.refs_0_), channel_id=1, source_target_pairs={{256,0},{384,128},{0,256},{128,384},{257,1},{385,129},{1,257},{129... | collective-permute-start | bytes 786440 | tf_op jit(solution)/shard_map/ppermute | solution.py:46
  159.9 4.0 %collective-permute-start.18 = (bf16[16,64,128]{2,1,0:T(8,128)(2,1)S(1)}, bf16[16,64,128]{2,1,0:T(8,128)(2,1)S(1)}, u32[]{:S(2)}, u32[]{:S(2)}) collective-permute-start(bf16[16,64,128]{2,1,0:T(8,128)(2,1)S(1)} %get-tuple-element.16.refs_0_), channel_id=1, source_target_pairs={{384,0},{0,128},{128,256},{256,384},{385,1},{1,129},{129,257},{257... | collective-permute-start | bytes 786440 | tf_op jit(solution)/shard_map/ppermute | solution.py:46
  165.8 7.4 %collective-permute-done.16.refs_1_ = bf16[16,64,128]{2,1,0:T(8,128)(2,1)S(1)} collective-permute-done((bf16[16,64,128]{2,1,0:T(8,128)(2,1)S(1)}, bf16[16,64,128]{2,1,0:T(8,128)(2,1)S(1)}, u32[]{:S(2)}, u32[]{:S(2)}) %collective-permute-start.16) | collective-permute-done | bytes 262176 | tf_op jit(solution)/shard_map/ppermute | solution.py:46
  173.9 32.4 %collective-permute-start.14 = (bf16[4096,128]{1,0:T(8,128)(2,1)}, bf16[4096,128]{1,0:T(8,128)(2,1)S(1)}, u32[]{:S(2)}, u32[]{:S(2)}) collective-permute-start(bf16[4096,128]{1,0:T(8,128)(2,1)} %bitcast.12.refs_0_), channel_id=1, source_target_pairs={{384,0},{0,128},{128,256},{256,384},{385,1},{1,129},{129,257},{257... | collective-permute-start | bytes 3145736 | tf_op jit(solution)/shard_map/ppermute | solution.py:46
  212.3 3.4 %collective-permute-start.21 = (bf16[16,16,2048]{2,1,0:T(8,128)(2,1)S(1)}, bf16[16,16,2048]{2,1,0:T(8,128)(2,1)}, u32[]{:S(2)}, u32[]{:S(2)}) collective-permute-start(bf16[16,16,2048]{2,1,0:T(8,128)(2,1)S(1)} %shard_map.79.refs_0_), channel_id=1, source_target_pairs={{6,0},{0,2},{2,4},{4,6},{7,1},{1,3},{3,5},{5,7},{14,8},{8,10},{10,... | collective-permute-start | bytes 3145736 | tf_op jit(solution)/shard_map/ppermute | solution.py:46
  216.7 10.8 %collective-permute-done.14.refs_3_ = bf16[4096,128]{1,0:T(8,128)(2,1)S(1)} collective-permute-done((bf16[4096,128]{1,0:T(8,128)(2,1)}, bf16[4096,128]{1,0:T(8,128)(2,1)S(1)}, u32[]{:S(2)}, u32[]{:S(2)}) %collective-permute-start.14) | collective-permute-done | bytes 1048608 | tf_op jit(solution)/shard_map/ppermute | solution.py:46
  227.5 2.9 %shard_map.76.q_ref = bf16[256,512]{1,0:T(8,128)(2,1)S(1)} custom-call(bf16[256,4096]{1,0:T(8,128)(2,1)S(1)} %copy-done.1, bf16[4096,128]{1,0:T(8,128)(2,1)} %bitcast.12.refs_0_, bf16[4096,128]{1,0:T(8,128)(2,1)} %collective-permute-done.12.refs_1_, bf16[4096,128]{1,0:T(8,128)(2,1)S(1)} %collective-permute-done.13.refs_2_, ...), custom_call_target="tpu_custom_call" | custom-call | flops 1073741824 | tf_op jit(solution)/shard_map/pallas_call | solution.py:26
  232.0 3.4 %shard_map.78.m_ref = bf16[256,512]{1,0:T(8,128)(2,1)S(1)} custom-call(s32[3]{0:T(128)S(1)} %pad_add_fusion.1.f_ref, s32[8,16]{1,0:T(8,128)S(1)} %fusion.4.p_ref, bf16[256,512]{1,0:T(8,128)(2,1)S(1)} %copy-done.3, bf16[128,32,256]{2,1,0:T(8,128)(2,1)S(1)} %bitcast.28, bf16[8,32,256]{2,1,0:T(8,128)(2,1)} %bitcast.17.own_ref, s32[8,1,512]{2,1,0:T(1,128)S(1)} %shard_map.77.kp_ref), custom_call_target="tpu_custom_call" | custom-call | flops 268435456 | tf_op jit(solution)/shard_map/pallas_call | solution.py:26
  235.4 4.4 %collective-permute-start.15 = (bf16[256,512]{1,0:T(8,128)(2,1)S(1)}, bf16[256,512]{1,0:T(8,128)(2,1)S(1)}, u32[]{:S(2)}, u32[]{:S(2)}) collective-permute-start(bf16[256,512]{1,0:T(8,128)(2,1)S(1)} %shard_map.78.m_ref), channel_id=1, source_target_pairs={{1,0},{0,1},{3,2},{2,3},{5,4},{4,5},{7,6},{6,7},{9,8},{8,9},{11,10... | collective-permute-start | bytes 786440 | tf_op jit(solution)/shard_map/ppermute | solution.py:46
  239.9 21.6 %collective-permute-done.21.refs_3_ = bf16[16,16,2048]{2,1,0:T(8,128)(2,1)} collective-permute-done((bf16[16,16,2048]{2,1,0:T(8,128)(2,1)S(1)}, bf16[16,16,2048]{2,1,0:T(8,128)(2,1)}, u32[]{:S(2)}, u32[]{:S(2)}) %collective-permute-start.21) | collective-permute-done | bytes 1048608 | tf_op jit(solution)/shard_map/ppermute | solution.py:46
  263.6 2.2 shard_map.81
  (88 shorter events, 28.2 us)
Async XLA Ops:
  6.5 139.2 %all-gather.2.cloned.1.call-start = ((), (), s32[]{:S(2)}) async-start(), calls=%async_computation.3 | async-start | bytes 2228224 | tf_op jit(solution)/shard_map/all_gather | solution.py:368
  34.4 28.2 %copy-start = (bf16[256,4096]{1,0:T(8,128)(2,1)S(1)}, bf16[256,4096]{1,0:T(8,128)(2,1)}, u32[]{:S(2)}) copy-start(bf16[256,4096]{1,0:T(8,128)(2,1)} %t_ref.3) | copy-start | bytes 6291460
  62.5 2.3 copy-start.6
  62.5 11.6 %copy-start.7 = (bf16[128,128]{1,0:T(8,128)(2,1)S(1)}, bf16[128,128]{1,0:T(8,128)(2,1)}, u32[]{:S(2)}) copy-start(bf16[128,128]{1,0:T(8,128)(2,1)} %get-tuple-element.12.refs_0_) | copy-start | bytes 98308
  65.0 23.2 %collective-permute-start.2 = (s32[128]{0:T(128)S(1)}, s32[128]{0:T(128)S(1)}, u32[]{:S(2)}, u32[]{:S(2)}) collective-permute-start(s32[128]{0:T(128)S(1)} %reshape.335), channel_id=1, source_target_pairs={{6,0},{0,2},{2,4},{4,6},{7,1},{1,3},{3,5},{5,7},{14,8},{8,10},{10,... | collective-permute-start | bytes 1544 | tf_op jit(solution)/shard_map/ppermute | solution.py:46
  67.4 24.0 %collective-permute-start.1 = (s32[128]{0:T(128)S(1)}, s32[128]{0:T(128)S(1)}, u32[]{:S(2)}, u32[]{:S(2)}) collective-permute-start(s32[128]{0:T(128)S(1)} %reshape.335), channel_id=1, source_target_pairs={{4,0},{6,2},{0,4},{2,6},{5,1},{7,3},{1,5},{3,7},{12,8},{14,10},{8,... | collective-permute-start | bytes 1544 | tf_op jit(solution)/shard_map/ppermute | solution.py:46
  70.4 21.1 %collective-permute-start = (s32[128]{0:T(128)S(1)}, s32[128]{0:T(128)S(1)}, u32[]{:S(2)}, u32[]{:S(2)}) collective-permute-start(s32[128]{0:T(128)S(1)} %reshape.335), channel_id=1, source_target_pairs={{2,0},{4,2},{6,4},{0,6},{3,1},{5,3},{7,5},{1,7},{10,8},{12,10},{14... | collective-permute-start | bytes 1544 | tf_op jit(solution)/shard_map/ppermute | solution.py:46
  74.1 21.5 %collective-permute-start.3 = (bf16[128,128]{1,0:T(8,128)(2,1)S(1)}, bf16[128,128]{1,0:T(8,128)(2,1)S(1)}, u32[]{:S(2)}, u32[]{:S(2)}) collective-permute-start(bf16[128,128]{1,0:T(8,128)(2,1)S(1)} %copy-done.7), channel_id=1, source_target_pairs={{32,0},{64,32},{96,64},{0,96},{33,1},{65,33},{97,65},{1,97},{34,2}... | collective-permute-start | bytes 98312 | tf_op jit(solution)/shard_map/ppermute | solution.py:46
  78.9 16.7 %collective-permute-start.4 = (bf16[128,128]{1,0:T(8,128)(2,1)S(1)}, bf16[128,128]{1,0:T(8,128)(2,1)S(1)}, u32[]{:S(2)}, u32[]{:S(2)}) collective-permute-start(bf16[128,128]{1,0:T(8,128)(2,1)S(1)} %copy-done.7), channel_id=1, source_target_pairs={{64,0},{96,32},{0,64},{32,96},{65,1},{97,33},{1,65},{33,97},{66,2}... | collective-permute-start | bytes 98312 | tf_op jit(solution)/shard_map/ppermute | solution.py:46
  88.2 9.7 %collective-permute-start.5 = (bf16[128,128]{1,0:T(8,128)(2,1)S(1)}, bf16[128,128]{1,0:T(8,128)(2,1)S(1)}, u32[]{:S(2)}, u32[]{:S(2)}) collective-permute-start(bf16[128,128]{1,0:T(8,128)(2,1)S(1)} %copy-done.7), channel_id=1, source_target_pairs={{96,0},{0,32},{32,64},{64,96},{97,1},{1,33},{33,65},{65,97},{98,2}... | collective-permute-start | bytes 98312 | tf_op jit(solution)/shard_map/ppermute | solution.py:46
  97.9 9.8 %collective-permute-start.6 = (bf16[4,128,128]{2,1,0:T(8,128)(2,1)S(1)}, bf16[4,128,128]{2,1,0:T(8,128)(2,1)S(1)}, u32[]{:S(2)}, u32[]{:S(2)}) collective-permute-start(bf16[4,128,128]{2,1,0:T(8,128)(2,1)S(1)} %shard_map.73.refs_0_), channel_id=1, source_target_pairs={{8,0},{16,8},{24,16},{0,24},{9,1},{17,9},{25,17},{1,25},{10,2},{18... | collective-permute-start | bytes 393224 | tf_op jit(solution)/shard_map/ppermute | solution.py:46
  100.1 13.4 %collective-permute-start.7 = (bf16[4,128,128]{2,1,0:T(8,128)(2,1)S(1)}, bf16[4,128,128]{2,1,0:T(8,128)(2,1)S(1)}, u32[]{:S(2)}, u32[]{:S(2)}) collective-permute-start(bf16[4,128,128]{2,1,0:T(8,128)(2,1)S(1)} %shard_map.73.refs_0_), channel_id=1, source_target_pairs={{16,0},{24,8},{0,16},{8,24},{17,1},{25,9},{1,17},{9,25},{18,2},{26... | collective-permute-start | bytes 393224 | tf_op jit(solution)/shard_map/ppermute | solution.py:46
  105.7 14.7 %collective-permute-start.8 = (bf16[4,128,128]{2,1,0:T(8,128)(2,1)S(1)}, bf16[4,128,128]{2,1,0:T(8,128)(2,1)S(1)}, u32[]{:S(2)}, u32[]{:S(2)}) collective-permute-start(bf16[4,128,128]{2,1,0:T(8,128)(2,1)S(1)} %shard_map.73.refs_0_), channel_id=1, source_target_pairs={{24,0},{0,8},{8,16},{16,24},{25,1},{1,9},{9,17},{17,25},{26,2},{2,... | collective-permute-start | bytes 393224 | tf_op jit(solution)/shard_map/ppermute | solution.py:46
  120.4 9.5 %collective-permute-start.9 = (bf16[16,64,128]{2,1,0:T(8,128)(2,1)S(1)}, bf16[16,64,128]{2,1,0:T(8,128)(2,1)S(1)}, u32[]{:S(2)}, u32[]{:S(2)}) collective-permute-start(bf16[16,64,128]{2,1,0:T(8,128)(2,1)S(1)} %get-tuple-element.13.refs_0_), channel_id=1, source_target_pairs={{2,0},{4,2},{6,4},{0,6},{3,1},{5,3},{7,5},{1,7},{10,8},{12,10},{14... | collective-permute-start | bytes 786440 | tf_op jit(solution)/shard_map/ppermute | solution.py:46
  122.8 9.0 %collective-permute-start.10 = (bf16[16,64,128]{2,1,0:T(8,128)(2,1)S(1)}, bf16[16,64,128]{2,1,0:T(8,128)(2,1)S(1)}, u32[]{:S(2)}, u32[]{:S(2)}) collective-permute-start(bf16[16,64,128]{2,1,0:T(8,128)(2,1)S(1)} %get-tuple-element.13.refs_0_), channel_id=1, source_target_pairs={{4,0},{6,2},{0,4},{2,6},{5,1},{7,3},{1,5},{3,7},{12,8},{14,10},{8,... | collective-permute-start | bytes 786440 | tf_op jit(solution)/shard_map/ppermute | solution.py:46
  125.7 13.7 %collective-permute-start.11 = (bf16[16,64,128]{2,1,0:T(8,128)(2,1)S(1)}, bf16[16,64,128]{2,1,0:T(8,128)(2,1)S(1)}, u32[]{:S(2)}, u32[]{:S(2)}) collective-permute-start(bf16[16,64,128]{2,1,0:T(8,128)(2,1)S(1)} %get-tuple-element.13.refs_0_), channel_id=1, source_target_pairs={{6,0},{0,2},{2,4},{4,6},{7,1},{1,3},{3,5},{5,7},{14,8},{8,10},{10,... | collective-permute-start | bytes 786440 | tf_op jit(solution)/shard_map/ppermute | solution.py:46
  140.5 71.8 %collective-permute-start.12 = (bf16[4096,128]{1,0:T(8,128)(2,1)}, bf16[4096,128]{1,0:T(8,128)(2,1)}, u32[]{:S(2)}, u32[]{:S(2)}) collective-permute-start(bf16[4096,128]{1,0:T(8,128)(2,1)} %bitcast.12.refs_0_), channel_id=1, source_target_pairs={{128,0},{256,128},{384,256},{0,384},{129,1},{257,129},{385,257},{1... | collective-permute-start | bytes 3145736 | tf_op jit(solution)/shard_map/ppermute | solution.py:46
  143.8 29.4 %collective-permute-start.16 = (bf16[16,64,128]{2,1,0:T(8,128)(2,1)S(1)}, bf16[16,64,128]{2,1,0:T(8,128)(2,1)S(1)}, u32[]{:S(2)}, u32[]{:S(2)}) collective-permute-start(bf16[16,64,128]{2,1,0:T(8,128)(2,1)S(1)} %get-tuple-element.16.refs_0_), channel_id=1, source_target_pairs={{128,0},{256,128},{384,256},{0,384},{129,1},{257,129},{385,257},{1... | collective-permute-start | bytes 786440 | tf_op jit(solution)/shard_map/ppermute | solution.py:46
  150.0 81.0 %all-to-all-start.2 = ((bf16[4,32,32,256]{3,2,1,0:T(8,128)(2,1)}), bf16[4,32,32,256]{3,2,1,0:T(8,128)(2,1)S(1)}, u32[]{:S(2)}, u32[]{:S(2)}) async-start(bf16[4,32,32,256]{3,2,1,0:T(8,128)(2,1)} %pick_blocks.1), calls=%async_computation.2 | async-start | bytes 4194304 | tf_op jit(solution)/shard_map/all_to_all | solution.py:383
  156.4 71.0 %copy-start.1 = (bf16[256,4096]{1,0:T(8,128)(2,1)S(1)}, bf16[256,4096]{1,0:T(8,128)(2,1)}, u32[]{:S(2)}) copy-start(bf16[256,4096]{1,0:T(8,128)(2,1)} %t_ref.3) | copy-start | bytes 6291460
  156.5 50.7 %collective-permute-start.17 = (bf16[16,64,128]{2,1,0:T(8,128)(2,1)S(1)}, bf16[16,64,128]{2,1,0:T(8,128)(2,1)S(1)}, u32[]{:S(2)}, u32[]{:S(2)}) collective-permute-start(bf16[16,64,128]{2,1,0:T(8,128)(2,1)S(1)} %get-tuple-element.16.refs_0_), channel_id=1, source_target_pairs={{256,0},{384,128},{0,256},{128,384},{257,1},{385,129},{1,257},{129... | collective-permute-start | bytes 786440 | tf_op jit(solution)/shard_map/ppermute | solution.py:46
  159.9 47.3 %collective-permute-start.18 = (bf16[16,64,128]{2,1,0:T(8,128)(2,1)S(1)}, bf16[16,64,128]{2,1,0:T(8,128)(2,1)S(1)}, u32[]{:S(2)}, u32[]{:S(2)}) collective-permute-start(bf16[16,64,128]{2,1,0:T(8,128)(2,1)S(1)} %get-tuple-element.16.refs_0_), channel_id=1, source_target_pairs={{384,0},{0,128},{128,256},{256,384},{385,1},{1,129},{129,257},{257... | collective-permute-start | bytes 786440 | tf_op jit(solution)/shard_map/ppermute | solution.py:46
  163.9 52.8 %collective-permute-start.13 = (bf16[4096,128]{1,0:T(8,128)(2,1)}, bf16[4096,128]{1,0:T(8,128)(2,1)S(1)}, u32[]{:S(2)}, u32[]{:S(2)}) collective-permute-start(bf16[4096,128]{1,0:T(8,128)(2,1)} %bitcast.12.refs_0_), channel_id=1, source_target_pairs={{256,0},{384,128},{0,256},{128,384},{257,1},{385,129},{1,257},{129... | collective-permute-start | bytes 3145736 | tf_op jit(solution)/shard_map/ppermute | solution.py:46
  173.2 0.7 copy-start.4
  173.9 53.5 %collective-permute-start.14 = (bf16[4096,128]{1,0:T(8,128)(2,1)}, bf16[4096,128]{1,0:T(8,128)(2,1)S(1)}, u32[]{:S(2)}, u32[]{:S(2)}) collective-permute-start(bf16[4096,128]{1,0:T(8,128)(2,1)} %bitcast.12.refs_0_), channel_id=1, source_target_pairs={{384,0},{0,128},{128,256},{256,384},{385,1},{1,129},{129,257},{257... | collective-permute-start | bytes 3145736 | tf_op jit(solution)/shard_map/ppermute | solution.py:46
  207.2 1.0 copy-start.5
  208.4 31.4 %collective-permute-start.19 = (bf16[16,16,2048]{2,1,0:T(8,128)(2,1)S(1)}, bf16[16,16,2048]{2,1,0:T(8,128)(2,1)}, u32[]{:S(2)}, u32[]{:S(2)}) collective-permute-start(bf16[16,16,2048]{2,1,0:T(8,128)(2,1)S(1)} %shard_map.79.refs_0_), channel_id=1, source_target_pairs={{2,0},{4,2},{6,4},{0,6},{3,1},{5,3},{7,5},{1,7},{10,8},{12,10},{14... | collective-permute-start | bytes 3145736 | tf_op jit(solution)/shard_map/ppermute | solution.py:46
  210.4 29.5 %collective-permute-start.20 = (bf16[16,16,2048]{2,1,0:T(8,128)(2,1)S(1)}, bf16[16,16,2048]{2,1,0:T(8,128)(2,1)}, u32[]{:S(2)}, u32[]{:S(2)}) collective-permute-start(bf16[16,16,2048]{2,1,0:T(8,128)(2,1)S(1)} %shard_map.79.refs_0_), channel_id=1, source_target_pairs={{4,0},{6,2},{0,4},{2,6},{5,1},{7,3},{1,5},{3,7},{12,8},{14,10},{8,... | collective-permute-start | bytes 3145736 | tf_op jit(solution)/shard_map/ppermute | solution.py:46
  212.3 49.1 %collective-permute-start.21 = (bf16[16,16,2048]{2,1,0:T(8,128)(2,1)S(1)}, bf16[16,16,2048]{2,1,0:T(8,128)(2,1)}, u32[]{:S(2)}, u32[]{:S(2)}) collective-permute-start(bf16[16,16,2048]{2,1,0:T(8,128)(2,1)S(1)} %shard_map.79.refs_0_), channel_id=1, source_target_pairs={{6,0},{0,2},{2,4},{4,6},{7,1},{1,3},{3,5},{5,7},{14,8},{8,10},{10,... | collective-permute-start | bytes 3145736 | tf_op jit(solution)/shard_map/ppermute | solution.py:46
  230.4 0.7 copy-start.2
  231.1 1.0 copy-start.3
  235.4 28.1 %collective-permute-start.15 = (bf16[256,512]{1,0:T(8,128)(2,1)S(1)}, bf16[256,512]{1,0:T(8,128)(2,1)S(1)}, u32[]{:S(2)}, u32[]{:S(2)}) collective-permute-start(bf16[256,512]{1,0:T(8,128)(2,1)S(1)} %shard_map.78.m_ref), channel_id=1, source_target_pairs={{1,0},{0,1},{3,2},{2,3},{5,4},{4,5},{7,6},{6,7},{9,8},{8,9},{11,10... | collective-permute-start | bytes 786440 | tf_op jit(solution)/shard_map/ppermute | solution.py:46
Sparse Core Ops, SparseCore 0:
  65.0 69.2 all-gather.1

commit v6 on v4

--- a/solution.py
+++ b/solution.py
@@ -65,27 +65,26 @@
     return jnp.stack(lists, axis=2)
 
 
-def pack(query_weight, key_weight, value_weight, out_weight, x_at, planes, tall):
+def pack(key_weight, value_weight, out_weight, x_at, planes, tall):
     rows = key_weight.shape[0]
     lines, wide_out = out_weight.shape
     small = rows // planes
     groups = wide_out // planes // HD
 
-    def kernel(x_ref, q_hbm, k_hbm, v_hbm, o_hbm, part_ref, cargo_ref, *scratch):
-        held, sems = scratch[:4], scratch[4]
+    def kernel(x_ref, k_hbm, v_hbm, o_hbm, part_ref, cargo_ref, *scratch):
+        held, sems = scratch[:3], scratch[3]
         copies = [
             pltpu.make_async_copy(src, dst, sems.at[i])
-            for i, (src, dst) in enumerate(zip((q_hbm, k_hbm, v_hbm, o_hbm), held, strict=True))
+            for i, (src, dst) in enumerate(zip((k_hbm, v_hbm, o_hbm), held, strict=True))
         ]
         for copy in copies:
             copy.start()
         for copy in copies:
             copy.wait()
-        q_ref, k_ref, v_ref, o_ref = held
-        part_ref[:rows] = q_ref[:, pl.ds(pl.multiple_of(x_ref[0] * HD, HD), HD)]
+        k_ref, v_ref, o_ref = held
         for i in range(groups):
             first = pl.multiple_of((x_ref[0] * groups + i) * HD, HD)
-            part_ref[rows + i * lines : rows + (i + 1) * lines] = o_ref[:, pl.ds(first, HD)]
+            part_ref[i * lines : (i + 1) * lines] = o_ref[:, pl.ds(first, HD)]
         first = pl.multiple_of(x_ref[0] * small, small)
         keys = k_ref[pl.ds(first, small)]
         values = v_ref[pl.ds(first, small)]
@@ -93,18 +92,18 @@
             cargo_ref[z, :small] = keys
             cargo_ref[z, small:] = values
 
-    weights = (query_weight, key_weight, value_weight, out_weight)
+    weights = (key_weight, value_weight, out_weight)
     outs = (
-        jax.ShapeDtypeStruct((rows + groups * lines, HD), BF16),
+        jax.ShapeDtypeStruct((groups * lines, HD), BF16),
         jax.ShapeDtypeStruct((tall, 2 * small, HD), BF16),
     )
     return pl.pallas_call(
         kernel,
         out_shape=outs,
-        in_specs=[pl.BlockSpec(memory_space=pltpu.SMEM)] + [pl.BlockSpec(memory_space=pl.ANY)] * 4,
+        in_specs=[pl.BlockSpec(memory_space=pltpu.SMEM)] + [pl.BlockSpec(memory_space=pl.ANY)] * 3,
         out_specs=(pl.BlockSpec(memory_space=pltpu.VMEM),) * 2,
         scratch_shapes=[pltpu.VMEM(w.shape, BF16) for w in weights]
-        + [pltpu.SemaphoreType.DMA((4,))],
+        + [pltpu.SemaphoreType.DMA((3,))],
         name="pack",
     )(x_at[None], *weights)
 
@@ -120,22 +119,17 @@
     return call(kernel, out, at[None], *pieces)
 
 
-def columns_of(pieces, at, rows):
-    n = len(pieces)
-    high, both, _ = pieces[0].shape
+def columns_of(pieces, at):
+    n = len(pieces)
+    high, rows, _ = pieces[0].shape
 
     def kernel(at_ref, *refs):
         for s in range(n):
             for h in range(high):
-                z = h * n + (at_ref[0] + s) % n
-                refs[n][z] = refs[s][h, :rows]
-                refs[n + 1][z] = refs[s][h, rows:]
-
-    outs = (
-        jax.ShapeDtypeStruct((high * n, rows, HD), BF16),
-        jax.ShapeDtypeStruct((high * n, both - rows, HD), BF16),
-    )
-    return call(kernel, outs, at[None], *pieces)
+                refs[-1][h * n + (at_ref[0] + s) % n] = refs[s][h]
+
+    out = jax.ShapeDtypeStruct((high * n, rows, HD), BF16)
+    return call(kernel, out, at[None], *pieces)
 
 
 def project_pair(tokens, every):
@@ -161,45 +155,42 @@
     return call(kernel, out, tokens, every, flops=flops)
 
 
-def project_queries(tokens, pieces, tile):
-    def kernel(t_ref, *refs):
-        o_ref = refs[-1]
-        for i in range(0, len(pieces), 2):
-            w = jnp.concatenate([refs[i][...], refs[i + 1][...]], axis=1)
-            o_ref[:, i * HD : (i + 2) * HD] = jnp.dot(
-                t_ref[...], w, preferred_element_type=F32
-            ).astype(BF16)
-
-    width = len(pieces) * HD
-    out = jax.ShapeDtypeStruct((tokens.shape[0], width), BF16)
-    flops = 2 * tokens.size * width
-    return call(kernel, out, tokens, *pieces, tile, flops=flops)
-
-
-def turned(pieces, at):
-    n = len(pieces)
-    tall, rows, _ = pieces[0].shape
-
-    def kernel(at_ref, *refs):
-        for s in range(n):
-            refs[-1][:, (at_ref[0] + s) % n] = refs[s][...]
-
-    out = jax.ShapeDtypeStruct((tall, n, rows, HD), BF16)
-    return call(kernel, out, at[None], *pieces)
-
-
-def full_columns(pieces, at, lines):
+def project_queries(tokens, pieces, at, tile):
+    n = len(pieces)
+    tall, lines, width = pieces[0].shape
+
+    def kernel(at_ref, t_ref, *refs):
+        o_ref, w_s = refs[-2], refs[-1]
+        for s in range(n):
+            w_s[:, (at_ref[0] + s) % n] = refs[s][...]
+        o_ref[...] = jnp.dot(
+            t_ref[...], w_s[...].reshape(tall * n * lines, width), preferred_element_type=F32
+        ).astype(BF16)
+
+    return call(
+        kernel,
+        jax.ShapeDtypeStruct((tokens.shape[0], width), BF16),
+        at[None],
+        tokens,
+        *pieces,
+        tile,
+        scratch=(pltpu.VMEM((tall, n, lines, width), BF16),),
+        flops=2 * tokens.size * width,
+    )
+
+
+def full_rows(pieces, at, lines):
     n = len(pieces)
     tall, held, _ = pieces[0].shape
     groups = held // lines
 
     def kernel(at_ref, *refs):
         for s in range(n):
+            y = (at_ref[0] + s) % n
             for i in range(groups):
-                first = pl.multiple_of((((at_ref[0] + s) % n) * groups + i) * HD, HD)
-                refs[n][:, :, pl.ds(first, HD)] = refs[s][:, i * lines : (i + 1) * lines]
-
-    out = jax.ShapeDtypeStruct((tall, lines, n * groups * HD), BF16)
+                refs[-1][:, y, :, i * HD : (i + 1) * HD] = refs[s][:, i * lines : (i + 1) * lines]
+
+    out = jax.ShapeDtypeStruct((tall, n, lines, groups * HD), BF16)
     return call(kernel, out, at[None], *pieces)
 
 
@@ -262,8 +253,7 @@
             summed = jnp.dot(weights.astype(BF16), v_s[j % 2], preferred_element_type=F32)
             result = jnp.where(at < f_ref[1], summed / total, 0.0).astype(BF16)
             for h in range(heads):
-                first = pl.multiple_of(((f_ref[2] + h) % heads) * HD, HD)
-                o_ref[mine, pl.ds(first, HD)] = result[h * BLOCK : (h + 1) * BLOCK]
+                o_ref[mine, h * HD : (h + 1) * HD] = result[h * BLOCK : (h + 1) * BLOCK]
 
     return call(
         kernel,
@@ -283,32 +273,28 @@
     )
 
 
-def whole_rows(pieces, at):
-    n = len(pieces)
-    tall, lines, width = pieces[0].shape
-
-    def kernel(at_ref, *refs):
-        for s in range(n):
-            refs[-1][:, (at_ref[0] + s) % n] = refs[s][...]
-
-    out = jax.ShapeDtypeStruct((tall, n, lines, width), BF16)
-    return call(kernel, out, at[None], *pieces)
-
-
-def mix(mine, other, weight, core):
-    half = weight.shape[0] // 2
-
-    def kernel(c_ref, m_ref, t_ref, w_ref, o_ref):
-        first = w_ref[pl.ds(c_ref[0] * half, half)]
-        second = w_ref[pl.ds((1 - c_ref[0]) * half, half)]
-        o_ref[...] = (
-            jnp.dot(m_ref[...], first, preferred_element_type=F32)
-            + jnp.dot(t_ref[...], second, preferred_element_type=F32)
-        ).astype(BF16)
-
-    out = jax.ShapeDtypeStruct((mine.shape[0], weight.shape[1]), BF16)
-    flops = 4 * mine.size * weight.shape[1]
-    return call(kernel, out, core[None], mine, other, weight, flops=flops)
+def mix(mine, other, pieces, places):
+    n = len(pieces)
+    rows, width = pieces[0].shape
+    half = rows // 2
+
+    def kernel(p_ref, m_ref, t_ref, *refs):
+        for s in range(n):
+            first = pl.multiple_of(((p_ref[0] + s) % n) * width, width)
+            refs[n][:, pl.ds(first, width)] = (
+                jnp.dot(
+                    m_ref[...], refs[s][pl.ds(p_ref[1] * half, half)], preferred_element_type=F32
+                )
+                + jnp.dot(
+                    t_ref[...],
+                    refs[s][pl.ds((1 - p_ref[1]) * half, half)],
+                    preferred_element_type=F32,
+                )
+            ).astype(BF16)
+
+    out = jax.ShapeDtypeStruct((mine.shape[0], n * width), BF16)
+    flops = 4 * mine.size * n * width
+    return call(kernel, out, places, mine, other, *pieces, flops=flops)
 
 
 def body(tokens, query_weight, key_weight, value_weight, out_weight, chosen, live_length):
@@ -320,7 +306,8 @@
     owners = tall * wide
     me = lax.axis_index(KV)
 
-    part, cargo = pack(query_weight, key_weight, value_weight, out_weight, x_at, planes, tall)
+    q_column = lax.all_gather(query_weight, TALL, axis=0, tiled=True)
+    part, cargo = pack(key_weight, value_weight, out_weight, x_at, planes, tall)
     column = lax.all_to_all(cargo, TALL, 0, 0, tiled=True)
     parts = spread(part, "zh")
     every = copy_for_each(column, ("dp", "y"))
@@ -330,11 +317,13 @@
     local_blocks = paired.reshape(per_dev, BLOCK, paired.shape[1])
     column_blocks = lax.all_gather(local_blocks, TALL, axis=0, tiled=True)
 
-    q_small, o_small = columns_of(parts, l_at, query_weight.shape[0])
-    q_pieces = spread(q_small, "y")
-    o_pieces = spread(o_small, "dp")
-    q_pieces = spread(turned(q_pieces, y_at).reshape(-1, HD), "dp")
-    o_pieces = spread(full_columns(o_pieces, x_at, out_weight.shape[0]), "y")
+    q_pieces = spread(q_column, "y")
+    q_pieces = [p.reshape(tall, -1, p.shape[1]) for p in q_pieces]
+    o_pieces = spread(columns_of(parts, l_at), "y")
+    o_tall = full_rows(o_pieces, y_at, out_weight.shape[0])
+    o_pieces = spread(o_tall.reshape(-1, o_tall.shape[-1]), "dp")
+
+    key_pos = key_positions(chosen)
 
     mates = jnp.stack(spread(chosen.reshape(-1), "y"))
     mates, chosen = lax.optimization_barrier((mates, chosen))
@@ -360,10 +349,9 @@
     far = owners * CAP
     remote_at = ((holder % wide) * tall + holder // wide) * CAP + slot
     position = jnp.where(holder == me, far + local_of, remote_at)
-    key_pos = key_positions(chosen)
-    facts = jnp.stack([me * rows, live_length[0], x_at]).astype(jnp.int32)
-
-    queries = project_queries(tokens, q_pieces, outgoing[0, 0, :16, :HD])
+    facts = jnp.stack([me * rows, live_length[0]]).astype(jnp.int32)
+
+    queries = project_queries(tokens, q_pieces, y_at, outgoing[0, 0, :16, :HD])
     attended = attend(
         queries,
         incoming.reshape(far, BLOCK, paired.shape[1]),
@@ -373,9 +361,7 @@
         facts,
     )
     other = from_ahead(attended, "tp", 1)
-    out_full = whole_rows(o_pieces, y_at)
-    out_full = out_full.reshape(-1, out_full.shape[-1])
-    return mix(attended, other, out_full, lax.axis_index("tp"))
+    return mix(attended, other, o_pieces, jnp.stack([x_at, lax.axis_index("tp")]))
 
 
 def solution(mesh):

time: 273 us -> 292 us (1.070)
  the two profiles are of different devices: /device:TPU:85 before, /device:TPU:32 now
where the time goes in v6:
time: 292 us; the launch traced here: 291 us
  waiting for transfers between devices  136 us (47%)
  starting transfers between devices  81 us (28%)
  blocking collectives  29.4 us (10%)
  Pallas kernels  18.8 us (6%)
  between operations  14.5 us (5%)
  local copies, waits for them, and re-layouts  6.21 us (2%)
  other arithmetic  5.34 us (2%)
    ppermute x19, starting transfers between devices, from_ahead(): return lax.ppermute(x, axis, [((i + step) % n, i) for i in range(n)])  69.3 us
    all_gather x1, waiting for transfers between devices, body(): column_blocks = lax.all_gather(local_blocks, TALL, axis=0, tiled=True)  58.3 us
    ppermute x19, waiting for transfers between devices, from_ahead(): return lax.ppermute(x, axis, [((i + step) % n, i) for i in range(n)])  50.5 us
    all_to_all x1, blocking collectives, body(): column = lax.all_to_all(cargo, TALL, 0, 0, tiled=True)  29.4 us
    all_to_all x1, waiting for transfers between devices, copy_for_each(): lax.all_to_all(jnp.broadcast_to(shard[None], (count, *shard.shape)), axis...  26.4 us
    pallas_call x9, Pallas kernels, call(): pl.pallas_call(kernel, out_shape=out_shape, in_specs=spaces, out_specs=ja...  17.2 us
    all_to_all x1, starting transfers between devices, copy_for_each(): lax.all_to_all(jnp.broadcast_to(shard[None], (count, *shard.shape)), axis...  7.22 us
  transfers between devices with their start and end apart: 23, of which 7 were waited for; matrix products, arithmetic and copies ran while one was open for 2% of the time, Pallas kernels for 5%

profile of v6, /device:TPU:32, one launch (start us, length us, event | category | flops | bytes accessed | tf_op | source)
XLA Modules:
  0.0 291.3 jit_solution(1309126408167524776)
XLA Ops:
  8.1 29.4 %all_to_all.15 = bf16[16,32,128]{2,1,0:T(8,128)(2,1)S(1)} all-to-all(bf16[16,32,128]{2,1,0:T(8,128)(2,1)} %get-tuple-element.11), channel_id=1, replica_groups=mesh['dp'=4,'zh'=4,'zl'=4,'y'=4,'tp'=2] {'zh','zl'}, dimensions={0} | all-to-all | bytes 262144 | tf_op jit(solution)/shard_map/all_to_all | solution.py:311
  39.3 7.2 %all-to-all-start.1 = ((bf16[16,16,32,128]{3,2,1,0:T(8,128)(2,1)}), bf16[16,16,32,128]{3,2,1,0:T(8,128)(2,1)}, u32[]{:S(2)}, u32[]{:S(2)}) async-start(bf16[16,16,32,128]{3,2,1,0:T(8,128)(2,1)} %broadcast_in_dim.92), calls=%async_computation.1 | async-start | bytes 4194304 | tf_op jit(solution)/shard_map/all_to_all | solution.py:39
  47.3 26.4 %all-to-all-done.1 = bf16[16,16,32,128]{3,2,1,0:T(8,128)(2,1)} async-done(((bf16[16,16,32,128]{3,2,1,0:T(8,128)(2,1)}), bf16[16,16,32,128]{3,2,1,0:T(8,128)(2,1)}, u32[]{:S(2)}, u32[]{:S(2)}) %all-to-all-start.1) | async-done | bytes 2097184 | tf_op jit(solution)/shard_map/all_to_all | solution.py:39
  73.6 3.0 %shard_map.73 = bf16[256,256]{1,0:T(8,128)(2,1)} custom-call(bf16[256,4096]{1,0:T(8,128)(2,1)S(1)} %copy-done, bf16[4,4,16,32,128]{4,3,2,1,0:T(8,128)(2,1)} %bitcast.17.w_ref), custom_call_target="tpu_custom_call" | custom-call | flops 536870912 | tf_op jit(solution)/shard_map/pallas_call | solution.py:26
  76.8 2.3 collective-permute-start.2
  79.1 4.3 %collective-permute-start.1 = (s32[128]{0:T(128)S(1)}, s32[128]{0:T(128)S(1)}, u32[]{:S(2)}, u32[]{:S(2)}) collective-permute-start(s32[128]{0:T(128)S(1)} %reshape.344), channel_id=1, source_target_pairs={{4,0},{6,2},{0,4},{2,6},{5,1},{7,3},{1,5},{3,7},{12,8},{14,10},{8,... | collective-permute-start | bytes 1544 | tf_op jit(solution)/shard_map/ppermute | solution.py:46
  83.5 3.1 %collective-permute-start = (s32[128]{0:T(128)S(1)}, s32[128]{0:T(128)S(1)}, u32[]{:S(2)}, u32[]{:S(2)}) collective-permute-start(s32[128]{0:T(128)S(1)} %reshape.344), channel_id=1, source_target_pairs={{2,0},{4,2},{6,4},{0,6},{3,1},{5,3},{7,5},{1,7},{10,8},{12,10},{14... | collective-permute-start | bytes 1544 | tf_op jit(solution)/shard_map/ppermute | solution.py:46
  86.6 4.4 %collective-permute-start.7 = (bf16[64,128]{1,0:T(8,128)(2,1)S(1)}, bf16[64,128]{1,0:T(8,128)(2,1)S(1)}, u32[]{:S(2)}, u32[]{:S(2)}) collective-permute-start(bf16[64,128]{1,0:T(8,128)(2,1)S(1)} %copy-done.5), channel_id=1, source_target_pairs={{32,0},{64,32},{96,64},{0,96},{33,1},{65,33},{97,65},{1,97},{34,2}... | collective-permute-start | bytes 49160 | tf_op jit(solution)/shard_map/ppermute | solution.py:46
  91.0 6.8 %collective-permute-start.8 = (bf16[64,128]{1,0:T(8,128)(2,1)S(1)}, bf16[64,128]{1,0:T(8,128)(2,1)S(1)}, u32[]{:S(2)}, u32[]{:S(2)}) collective-permute-start(bf16[64,128]{1,0:T(8,128)(2,1)S(1)} %copy-done.5), channel_id=1, source_target_pairs={{64,0},{96,32},{0,64},{32,96},{65,1},{97,33},{1,65},{33,97},{66,2}... | collective-permute-start | bytes 49160 | tf_op jit(solution)/shard_map/ppermute | solution.py:46
  99.8 3.8 %collective-permute-start.9 = (bf16[64,128]{1,0:T(8,128)(2,1)S(1)}, bf16[64,128]{1,0:T(8,128)(2,1)S(1)}, u32[]{:S(2)}, u32[]{:S(2)}) collective-permute-start(bf16[64,128]{1,0:T(8,128)(2,1)S(1)} %copy-done.5), channel_id=1, source_target_pairs={{96,0},{0,32},{32,64},{64,96},{97,1},{1,33},{33,65},{65,97},{98,2}... | collective-permute-start | bytes 49160 | tf_op jit(solution)/shard_map/ppermute | solution.py:46
  109.3 3.0 %collective-permute-start.10 = (bf16[4,64,128]{2,1,0:T(8,128)(2,1)S(1)}, bf16[4,64,128]{2,1,0:T(8,128)(2,1)S(1)}, u32[]{:S(2)}, u32[]{:S(2)}) collective-permute-start(bf16[4,64,128]{2,1,0:T(8,128)(2,1)S(1)} %shard_map.78.refs_0_), channel_id=1, source_target_pairs={{8,0},{16,8},{24,16},{0,24},{9,1},{17,9},{25,17},{1,25},{10,2},{18... | collective-permute-start | bytes 196616 | tf_op jit(solution)/shard_map/ppermute | solution.py:46
  112.3 3.2 %collective-permute-start.11 = (bf16[4,64,128]{2,1,0:T(8,128)(2,1)S(1)}, bf16[4,64,128]{2,1,0:T(8,128)(2,1)S(1)}, u32[]{:S(2)}, u32[]{:S(2)}) collective-permute-start(bf16[4,64,128]{2,1,0:T(8,128)(2,1)S(1)} %shard_map.78.refs_0_), channel_id=1, source_target_pairs={{16,0},{24,8},{0,16},{8,24},{17,1},{25,9},{1,17},{9,25},{18,2},{26... | collective-permute-start | bytes 196616 | tf_op jit(solution)/shard_map/ppermute | solution.py:46
  115.5 3.7 %collective-permute-start.12 = (bf16[4,64,128]{2,1,0:T(8,128)(2,1)S(1)}, bf16[4,64,128]{2,1,0:T(8,128)(2,1)S(1)}, u32[]{:S(2)}, u32[]{:S(2)}) collective-permute-start(bf16[4,64,128]{2,1,0:T(8,128)(2,1)S(1)} %shard_map.78.refs_0_), channel_id=1, source_target_pairs={{24,0},{0,8},{8,16},{16,24},{25,1},{1,9},{9,17},{17,25},{26,2},{2,... | collective-permute-start | bytes 196616 | tf_op jit(solution)/shard_map/ppermute | solution.py:46
  119.2 3.4 %collective-permute-start.3 = (bf16[1024,512]{1,0:T(8,128)(2,1)}, bf16[1024,512]{1,0:T(8,128)(2,1)}, u32[]{:S(2)}, u32[]{:S(2)}) collective-permute-start(bf16[1024,512]{1,0:T(8,128)(2,1)} %all-gather.3.cloned.1.call-done), channel_id=1, source_target_pairs={{2,0},{4,2},{6,4},{0,6},{3,1},{5,3},{7,5},{1,7},{10,8},{12,10},{14... | collective-permute-start | bytes 3145736 | tf_op jit(solution)/shard_map/ppermute | solution.py:46
  122.8 4.1 %collective-permute-start.13 = (bf16[16,64,128]{2,1,0:T(8,128)(2,1)S(1)}, bf16[16,64,128]{2,1,0:T(8,128)(2,1)S(1)}, u32[]{:S(2)}, u32[]{:S(2)}) collective-permute-start(bf16[16,64,128]{2,1,0:T(8,128)(2,1)S(1)} %shard_map.79.refs_0_), channel_id=1, source_target_pairs={{2,0},{4,2},{6,4},{0,6},{3,1},{5,3},{7,5},{1,7},{10,8},{12,10},{14... | collective-permute-start | bytes 786440 | tf_op jit(solution)/shard_map/ppermute | solution.py:46
  126.9 58.3 %all-gather.5.cloned.1.call-done.b_ref = bf16[128,32,256]{2,1,0:T(8,128)(2,1)} async-done(((bf16[8,32,256]{2,1,0:T(8,128)(2,1)}), bf16[128,32,256]{2,1,0:T(8,128)(2,1)}) %all-gather.5.cloned.1.call-update) | async-done | bytes 2097168 | tf_op jit(solution)/shard_map/all_gather | solution.py:318
  186.8 2.0 shard_map.74
  188.8 4.4 %all-to-all-start.2 = ((bf16[4,32,32,256]{3,2,1,0:T(8,128)(2,1)}), bf16[4,32,32,256]{3,2,1,0:T(8,128)(2,1)}, u32[]{:S(2)}, u32[]{:S(2)}) async-start(bf16[4,32,32,256]{3,2,1,0:T(8,128)(2,1)} %shard_map.74), calls=%async_computation.2 | async-start | bytes 4194304 | tf_op jit(solution)/shard_map/all_to_all | solution.py:335
  193.7 5.4 %collective-permute-start.14 = (bf16[16,64,128]{2,1,0:T(8,128)(2,1)S(1)}, bf16[16,64,128]{2,1,0:T(8,128)(2,1)S(1)}, u32[]{:S(2)}, u32[]{:S(2)}) collective-permute-start(bf16[16,64,128]{2,1,0:T(8,128)(2,1)S(1)} %shard_map.79.refs_0_), channel_id=1, source_target_pairs={{4,0},{6,2},{0,4},{2,6},{5,1},{7,3},{1,5},{3,7},{12,8},{14,10},{8,... | collective-permute-start | bytes 786440 | tf_op jit(solution)/shard_map/ppermute | solution.py:46
  199.1 2.5 collective-permute-start.15
  201.6 4.0 %collective-permute-start.4 = (bf16[1024,512]{1,0:T(8,128)(2,1)}, bf16[1024,512]{1,0:T(8,128)(2,1)S(1)}, u32[]{:S(2)}, u32[]{:S(2)}) collective-permute-start(bf16[1024,512]{1,0:T(8,128)(2,1)} %all-gather.3.cloned.1.call-done), channel_id=1, source_target_pairs={{4,0},{6,2},{0,4},{2,6},{5,1},{7,3},{1,5},{3,7},{12,8},{14,10},{8,... | collective-permute-start | bytes 3145736 | tf_op jit(solution)/shard_map/ppermute | solution.py:46
  206.3 3.4 %collective-permute-start.5 = (bf16[1024,512]{1,0:T(8,128)(2,1)}, bf16[1024,512]{1,0:T(8,128)(2,1)S(1)}, u32[]{:S(2)}, u32[]{:S(2)}) collective-permute-start(bf16[1024,512]{1,0:T(8,128)(2,1)} %all-gather.3.cloned.1.call-done), channel_id=1, source_target_pairs={{6,0},{0,2},{2,4},{4,6},{7,1},{1,3},{3,5},{5,7},{14,8},{8,10},{10,... | collective-permute-start | bytes 3145736 | tf_op jit(solution)/shard_map/ppermute | solution.py:46
  209.8 16.9 %collective-permute-done.14.refs_2_ = bf16[16,64,128]{2,1,0:T(8,128)(2,1)S(1)} collective-permute-done((bf16[16,64,128]{2,1,0:T(8,128)(2,1)S(1)}, bf16[16,64,128]{2,1,0:T(8,128)(2,1)S(1)}, u32[]{:S(2)}, u32[]{:S(2)}) %collective-permute-start.14) | collective-permute-done | bytes 262176 | tf_op jit(solution)/shard_map/ppermute | solution.py:46
  226.7 18.3 %collective-permute-done.15.refs_3_ = bf16[16,64,128]{2,1,0:T(8,128)(2,1)S(1)} collective-permute-done((bf16[16,64,128]{2,1,0:T(8,128)(2,1)S(1)}, bf16[16,64,128]{2,1,0:T(8,128)(2,1)S(1)}, u32[]{:S(2)}, u32[]{:S(2)}) %collective-permute-start.15) | collective-permute-done | bytes 262176 | tf_op jit(solution)/shard_map/ppermute | solution.py:46
  246.2 4.6 %collective-permute-start.16 = (bf16[1024,512]{1,0:T(8,128)(2,1)S(1)}, bf16[1024,512]{1,0:T(8,128)(2,1)}, u32[]{:S(2)}, u32[]{:S(2)}) collective-permute-start(bf16[1024,512]{1,0:T(8,128)(2,1)S(1)} %bitcast.30), channel_id=1, source_target_pairs={{128,0},{256,128},{384,256},{0,384},{129,1},{257,129},{385,257},{1... | collective-permute-start | bytes 3145736 | tf_op jit(solution)/shard_map/ppermute | solution.py:46
  250.8 2.8 collective-permute-start.17
  253.6 2.8 collective-permute-start.18
  257.4 9.3 %collective-permute-done.5 = bf16[1024,512]{1,0:T(8,128)(2,1)S(1)} collective-permute-done((bf16[1024,512]{1,0:T(8,128)(2,1)}, bf16[1024,512]{1,0:T(8,128)(2,1)S(1)}, u32[]{:S(2)}, u32[]{:S(2)}) %collective-permute-start.5) | collective-permute-done | bytes 1048608 | tf_op jit(solution)/shard_map/ppermute | solution.py:46
  266.7 3.1 %shard_map.75.q_ref = bf16[256,512]{1,0:T(8,128)(2,1)S(1)} custom-call(s32[1]{0:T(128)} %bitcast.9.at_ref, bf16[256,4096]{1,0:T(8,128)(2,1)S(1)} %copy-done, bf16[16,64,512]{2,1,0:T(8,128)(2,1)} %bitcast.10.refs_0_, bf16[16,64,512]{2,1,0:T(8,128)(2,1)} %bitcast.11.refs_1_, bf16[16,64,512]{2,1,0:T(8,128)(2,1)S(1)} %bitcast.34, ...), custom_call_target="tpu_custom_call" | custom-call | flops 1073741824 | tf_op jit(solution)/shard_map/pallas_call | solution.py:26
  269.7 4.1 %shard_map.77.m_ref = bf16[256,512]{1,0:T(8,128)(2,1)S(1)} custom-call(s32[2]{0:T(128)S(1)} %pad_add_fusion.2.f_ref, s32[8,16]{1,0:T(8,128)S(1)} %fusion.4.p_ref, bf16[256,512]{1,0:T(8,128)(2,1)S(1)} %shard_map.75.q_ref, bf16[128,32,256]{2,1,0:T(8,128)(2,1)} %bitcast.20.in_ref, bf16[8,32,256]{2,1,0:T(8,128)(2,1)} %bitcast.18.own_ref, ...), custom_call_target="tpu_custom_call" | custom-call | flops 268435456 | tf_op jit(solution)/shard_map/pallas_call | solution.py:26
  275.8 4.5 %collective-permute-done.18.refs_3_ = bf16[1024,512]{1,0:T(8,128)(2,1)} collective-permute-done((bf16[1024,512]{1,0:T(8,128)(2,1)S(1)}, bf16[1024,512]{1,0:T(8,128)(2,1)}, u32[]{:S(2)}, u32[]{:S(2)}) %collective-permute-start.18) | collective-permute-done | bytes 1048608 | tf_op jit(solution)/shard_map/ppermute | solution.py:46
  280.3 4.1 %shard_map.81 = bf16[256,2048]{1,0:T(8,128)(2,1)} custom-call(s32[2]{0:T(128)S(1)} %pad_add_fusion.1.p_ref, bf16[256,512]{1,0:T(8,128)(2,1)S(1)} %shard_map.77.m_ref, bf16[256,512]{1,0:T(8,128)(2,1)S(1)} %collective-permute-done.6.t_ref, bf16[1024,512]{1,0:T(8,128)(2,1)S(1)} %bitcast.33, bf16[1024,512]{1,0:T(8,128)(2,1)} %collective-permute-done.16.refs_1_, ...), custom_call_target="tpu_custom_call" | custom-call | flops 1073741824 | tf_op jit(solution)/shard_map/pallas_call | solution.py:26
  (81 shorter events, 18.3 us)
Async XLA Ops:
  39.3 34.4 %copy-start = (bf16[256,4096]{1,0:T(8,128)(2,1)S(1)}, bf16[256,4096]{1,0:T(8,128)(2,1)}, u32[]{:S(2)}) copy-start(bf16[256,4096]{1,0:T(8,128)(2,1)} %t_ref.3) | copy-start | bytes 6291460
  39.3 34.4 %all-to-all-start.1 = ((bf16[16,16,32,128]{3,2,1,0:T(8,128)(2,1)}), bf16[16,16,32,128]{3,2,1,0:T(8,128)(2,1)}, u32[]{:S(2)}, u32[]{:S(2)}) async-start(bf16[16,16,32,128]{3,2,1,0:T(8,128)(2,1)} %broadcast_in_dim.92), calls=%async_computation.1 | async-start | bytes 4194304 | tf_op jit(solution)/shard_map/all_to_all | solution.py:39
  46.5 72.7 %all-gather.3.cloned.1.call-start = ((), (), s32[]{:S(2)}) async-start(), calls=%async_computation.3 | async-start | bytes 1114112 | tf_op jit(solution)/shard_map/all_gather | solution.py:309
  47.2 138.0 %all-gather.5.cloned.1.call-start = ((), (), s32[]{:S(2)}) async-start(), calls=%async_computation.4 | async-start | bytes 2228224 | tf_op jit(solution)/shard_map/all_gather | solution.py:318
  73.6 3.0 %copy-start.4 = (s32[8,16]{1,0:T(8,128)S(1)}, s32[8,16]{1,0:T(8,128)}, u32[]{:S(2)}) copy-start(s32[8,16]{1,0:T(8,128)} %c_ref.1) | copy-start | bytes 1540
  73.6 12.9 %copy-start.5 = (bf16[64,128]{1,0:T(8,128)(2,1)S(1)}, bf16[64,128]{1,0:T(8,128)(2,1)}, u32[]{:S(2)}) copy-start(bf16[64,128]{1,0:T(8,128)(2,1)} %get-tuple-element.12.refs_0_) | copy-start | bytes 49156
  76.8 23.0 %collective-permute-start.2 = (s32[128]{0:T(128)S(1)}, s32[128]{0:T(128)S(1)}, u32[]{:S(2)}, u32[]{:S(2)}) collective-permute-start(s32[128]{0:T(128)S(1)} %reshape.344), channel_id=1, source_target_pairs={{6,0},{0,2},{2,4},{4,6},{7,1},{1,3},{3,5},{5,7},{14,8},{8,10},{10,... | collective-permute-start | bytes 1544 | tf_op jit(solution)/shard_map/ppermute | solution.py:46
  79.1 24.5 %collective-permute-start.1 = (s32[128]{0:T(128)S(1)}, s32[128]{0:T(128)S(1)}, u32[]{:S(2)}, u32[]{:S(2)}) collective-permute-start(s32[128]{0:T(128)S(1)} %reshape.344), channel_id=1, source_target_pairs={{4,0},{6,2},{0,4},{2,6},{5,1},{7,3},{1,5},{3,7},{12,8},{14,10},{8,... | collective-permute-start | bytes 1544 | tf_op jit(solution)/shard_map/ppermute | solution.py:46
  83.5 20.2 %collective-permute-start = (s32[128]{0:T(128)S(1)}, s32[128]{0:T(128)S(1)}, u32[]{:S(2)}, u32[]{:S(2)}) collective-permute-start(s32[128]{0:T(128)S(1)} %reshape.344), channel_id=1, source_target_pairs={{2,0},{4,2},{6,4},{0,6},{3,1},{5,3},{7,5},{1,7},{10,8},{12,10},{14... | collective-permute-start | bytes 1544 | tf_op jit(solution)/shard_map/ppermute | solution.py:46
  86.6 21.3 %collective-permute-start.7 = (bf16[64,128]{1,0:T(8,128)(2,1)S(1)}, bf16[64,128]{1,0:T(8,128)(2,1)S(1)}, u32[]{:S(2)}, u32[]{:S(2)}) collective-permute-start(bf16[64,128]{1,0:T(8,128)(2,1)S(1)} %copy-done.5), channel_id=1, source_target_pairs={{32,0},{64,32},{96,64},{0,96},{33,1},{65,33},{97,65},{1,97},{34,2}... | collective-permute-start | bytes 49160 | tf_op jit(solution)/shard_map/ppermute | solution.py:46
  91.0 16.9 %collective-permute-start.8 = (bf16[64,128]{1,0:T(8,128)(2,1)S(1)}, bf16[64,128]{1,0:T(8,128)(2,1)S(1)}, u32[]{:S(2)}, u32[]{:S(2)}) collective-permute-start(bf16[64,128]{1,0:T(8,128)(2,1)S(1)} %copy-done.5), channel_id=1, source_target_pairs={{64,0},{96,32},{0,64},{32,96},{65,1},{97,33},{1,65},{33,97},{66,2}... | collective-permute-start | bytes 49160 | tf_op jit(solution)/shard_map/ppermute | solution.py:46
  99.8 9.5 %collective-permute-start.9 = (bf16[64,128]{1,0:T(8,128)(2,1)S(1)}, bf16[64,128]{1,0:T(8,128)(2,1)S(1)}, u32[]{:S(2)}, u32[]{:S(2)}) collective-permute-start(bf16[64,128]{1,0:T(8,128)(2,1)S(1)} %copy-done.5), channel_id=1, source_target_pairs={{96,0},{0,32},{32,64},{64,96},{97,1},{1,33},{33,65},{65,97},{98,2}... | collective-permute-start | bytes 49160 | tf_op jit(solution)/shard_map/ppermute | solution.py:46
  109.3 13.4 %collective-permute-start.10 = (bf16[4,64,128]{2,1,0:T(8,128)(2,1)S(1)}, bf16[4,64,128]{2,1,0:T(8,128)(2,1)S(1)}, u32[]{:S(2)}, u32[]{:S(2)}) collective-permute-start(bf16[4,64,128]{2,1,0:T(8,128)(2,1)S(1)} %shard_map.78.refs_0_), channel_id=1, source_target_pairs={{8,0},{16,8},{24,16},{0,24},{9,1},{17,9},{25,17},{1,25},{10,2},{18... | collective-permute-start | bytes 196616 | tf_op jit(solution)/shard_map/ppermute | solution.py:46
  112.3 10.4 %collective-permute-start.11 = (bf16[4,64,128]{2,1,0:T(8,128)(2,1)S(1)}, bf16[4,64,128]{2,1,0:T(8,128)(2,1)S(1)}, u32[]{:S(2)}, u32[]{:S(2)}) collective-permute-start(bf16[4,64,128]{2,1,0:T(8,128)(2,1)S(1)} %shard_map.78.refs_0_), channel_id=1, source_target_pairs={{16,0},{24,8},{0,16},{8,24},{17,1},{25,9},{1,17},{9,25},{18,2},{26... | collective-permute-start | bytes 196616 | tf_op jit(solution)/shard_map/ppermute | solution.py:46
  115.5 7.3 %collective-permute-start.12 = (bf16[4,64,128]{2,1,0:T(8,128)(2,1)S(1)}, bf16[4,64,128]{2,1,0:T(8,128)(2,1)S(1)}, u32[]{:S(2)}, u32[]{:S(2)}) collective-permute-start(bf16[4,64,128]{2,1,0:T(8,128)(2,1)S(1)} %shard_map.78.refs_0_), channel_id=1, source_target_pairs={{24,0},{0,8},{8,16},{16,24},{25,1},{1,9},{9,17},{17,25},{26,2},{2,... | collective-permute-start | bytes 196616 | tf_op jit(solution)/shard_map/ppermute | solution.py:46
  119.2 134.3 %collective-permute-start.3 = (bf16[1024,512]{1,0:T(8,128)(2,1)}, bf16[1024,512]{1,0:T(8,128)(2,1)}, u32[]{:S(2)}, u32[]{:S(2)}) collective-permute-start(bf16[1024,512]{1,0:T(8,128)(2,1)} %all-gather.3.cloned.1.call-done), channel_id=1, source_target_pairs={{2,0},{4,2},{6,4},{0,6},{3,1},{5,3},{7,5},{1,7},{10,8},{12,10},{14... | collective-permute-start | bytes 3145736 | tf_op jit(solution)/shard_map/ppermute | solution.py:46
  122.8 82.8 %collective-permute-start.13 = (bf16[16,64,128]{2,1,0:T(8,128)(2,1)S(1)}, bf16[16,64,128]{2,1,0:T(8,128)(2,1)S(1)}, u32[]{:S(2)}, u32[]{:S(2)}) collective-permute-start(bf16[16,64,128]{2,1,0:T(8,128)(2,1)S(1)} %shard_map.79.refs_0_), channel_id=1, source_target_pairs={{2,0},{4,2},{6,4},{0,6},{3,1},{5,3},{7,5},{1,7},{10,8},{12,10},{14... | collective-permute-start | bytes 786440 | tf_op jit(solution)/shard_map/ppermute | solution.py:46
  185.2 1.6 copy-start.1
  188.8 80.9 %all-to-all-start.2 = ((bf16[4,32,32,256]{3,2,1,0:T(8,128)(2,1)}), bf16[4,32,32,256]{3,2,1,0:T(8,128)(2,1)}, u32[]{:S(2)}, u32[]{:S(2)}) async-start(bf16[4,32,32,256]{3,2,1,0:T(8,128)(2,1)} %shard_map.74), calls=%async_computation.2 | async-start | bytes 4194304 | tf_op jit(solution)/shard_map/all_to_all | solution.py:335
  193.7 33.0 %collective-permute-start.14 = (bf16[16,64,128]{2,1,0:T(8,128)(2,1)S(1)}, bf16[16,64,128]{2,1,0:T(8,128)(2,1)S(1)}, u32[]{:S(2)}, u32[]{:S(2)}) collective-permute-start(bf16[16,64,128]{2,1,0:T(8,128)(2,1)S(1)} %shard_map.79.refs_0_), channel_id=1, source_target_pairs={{4,0},{6,2},{0,4},{2,6},{5,1},{7,3},{1,5},{3,7},{12,8},{14,10},{8,... | collective-permute-start | bytes 786440 | tf_op jit(solution)/shard_map/ppermute | solution.py:46
  199.1 45.9 %collective-permute-start.15 = (bf16[16,64,128]{2,1,0:T(8,128)(2,1)S(1)}, bf16[16,64,128]{2,1,0:T(8,128)(2,1)S(1)}, u32[]{:S(2)}, u32[]{:S(2)}) collective-permute-start(bf16[16,64,128]{2,1,0:T(8,128)(2,1)S(1)} %shard_map.79.refs_0_), channel_id=1, source_target_pairs={{6,0},{0,2},{2,4},{4,6},{7,1},{1,3},{3,5},{5,7},{14,8},{8,10},{10,... | collective-permute-start | bytes 786440 | tf_op jit(solution)/shard_map/ppermute | solution.py:46
  201.6 55.7 %collective-permute-start.4 = (bf16[1024,512]{1,0:T(8,128)(2,1)}, bf16[1024,512]{1,0:T(8,128)(2,1)S(1)}, u32[]{:S(2)}, u32[]{:S(2)}) collective-permute-start(bf16[1024,512]{1,0:T(8,128)(2,1)} %all-gather.3.cloned.1.call-done), channel_id=1, source_target_pairs={{4,0},{6,2},{0,4},{2,6},{5,1},{7,3},{1,5},{3,7},{12,8},{14,10},{8,... | collective-permute-start | bytes 3145736 | tf_op jit(solution)/shard_map/ppermute | solution.py:46
  205.6 0.7 copy-start.2
  206.3 60.3 %collective-permute-start.5 = (bf16[1024,512]{1,0:T(8,128)(2,1)}, bf16[1024,512]{1,0:T(8,128)(2,1)S(1)}, u32[]{:S(2)}, u32[]{:S(2)}) collective-permute-start(bf16[1024,512]{1,0:T(8,128)(2,1)} %all-gather.3.cloned.1.call-done), channel_id=1, source_target_pairs={{6,0},{0,2},{2,4},{4,6},{7,1},{1,3},{3,5},{5,7},{14,8},{8,10},{10,... | collective-permute-start | bytes 3145736 | tf_op jit(solution)/shard_map/ppermute | solution.py:46
  245.0 1.0 copy-start.3
  246.2 29.7 %collective-permute-start.16 = (bf16[1024,512]{1,0:T(8,128)(2,1)S(1)}, bf16[1024,512]{1,0:T(8,128)(2,1)}, u32[]{:S(2)}, u32[]{:S(2)}) collective-permute-start(bf16[1024,512]{1,0:T(8,128)(2,1)S(1)} %bitcast.30), channel_id=1, source_target_pairs={{128,0},{256,128},{384,256},{0,384},{129,1},{257,129},{385,257},{1... | collective-permute-start | bytes 3145736 | tf_op jit(solution)/shard_map/ppermute | solution.py:46
  250.8 25.0 %collective-permute-start.17 = (bf16[1024,512]{1,0:T(8,128)(2,1)S(1)}, bf16[1024,512]{1,0:T(8,128)(2,1)}, u32[]{:S(2)}, u32[]{:S(2)}) collective-permute-start(bf16[1024,512]{1,0:T(8,128)(2,1)S(1)} %bitcast.31), channel_id=1, source_target_pairs={{256,0},{384,128},{0,256},{128,384},{257,1},{385,129},{1,257},{129... | collective-permute-start | bytes 3145736 | tf_op jit(solution)/shard_map/ppermute | solution.py:46
  253.6 26.8 %collective-permute-start.18 = (bf16[1024,512]{1,0:T(8,128)(2,1)S(1)}, bf16[1024,512]{1,0:T(8,128)(2,1)}, u32[]{:S(2)}, u32[]{:S(2)}) collective-permute-start(bf16[1024,512]{1,0:T(8,128)(2,1)S(1)} %bitcast.32), channel_id=1, source_target_pairs={{384,0},{0,128},{128,256},{256,384},{385,1},{1,129},{129,257},{257... | collective-permute-start | bytes 3145736 | tf_op jit(solution)/shard_map/ppermute | solution.py:46
  273.8 6.5 %collective-permute-start.6 = (bf16[256,512]{1,0:T(8,128)(2,1)S(1)}, bf16[256,512]{1,0:T(8,128)(2,1)S(1)}, u32[]{:S(2)}, u32[]{:S(2)}) collective-permute-start(bf16[256,512]{1,0:T(8,128)(2,1)S(1)} %shard_map.77.m_ref), channel_id=1, source_target_pairs={{1,0},{0,1},{3,2},{2,3},{5,4},{4,5},{7,6},{6,7},{9,8},{8,9},{11,10... | collective-permute-start | bytes 786440 | tf_op jit(solution)/shard_map/ppermute | solution.py:46
Sparse Core Ops, SparseCore 0:
  49.4 64.0 all-gather.2
  115.6 69.5 all-gather.4

commit v7 on v2

--- a/solution.py
+++ b/solution.py
@@ -75,7 +75,17 @@
     q_groups = query_weight.shape[1] // 2 // HD
     o_groups = wide_out // 2 // HD
 
-    def kernel(x_ref, q_ref, k_ref, v_ref, o_ref, half_ref, cargo_ref):
+    def kernel(x_ref, q_hbm, k_hbm, v_hbm, o_hbm, half_ref, cargo_ref, *scratch):
+        held, sems = scratch[:4], scratch[4]
+        copies = [
+            pltpu.make_async_copy(src, dst, sems.at[i])
+            for i, (src, dst) in enumerate(zip((q_hbm, k_hbm, v_hbm, o_hbm), held, strict=True))
+        ]
+        for copy in copies:
+            copy.start()
+        for copy in copies:
+            copy.wait()
+        q_ref, k_ref, v_ref, o_ref = held
         parity = x_ref[0] % 2
         for i in range(q_groups):
             first = pl.multiple_of((parity * q_groups + i) * HD, HD)
@@ -95,7 +105,16 @@
         jax.ShapeDtypeStruct((q_groups * rows + o_groups * lines, HD), BF16),
         jax.ShapeDtypeStruct((tall, 2 * small, HD), BF16),
     )
-    return call(kernel, outs, x_at[None], query_weight, key_weight, value_weight, out_weight)
+    weights = (query_weight, key_weight, value_weight, out_weight)
+    return pl.pallas_call(
+        kernel,
+        out_shape=outs,
+        in_specs=[pl.BlockSpec(memory_space=pltpu.SMEM)] + [pl.BlockSpec(memory_space=pl.ANY)] * 4,
+        out_specs=(pl.BlockSpec(memory_space=pltpu.VMEM),) * 2,
+        scratch_shapes=[pltpu.VMEM(w.shape, BF16) for w in weights]
+        + [pltpu.SemaphoreType.DMA((4,))],
+        name="pack",
+    )(x_at[None], *weights)
 
 
 def project_pair(tokens, every):
@@ -188,16 +207,35 @@
     return call(kernel, out, chosen)
 
 
-def pick_blocks(blocks, asked):
+def pick_blocks(blocks, asked, per_dev):
     wide, count = asked.shape
-
-    def kernel(asked_ref, b_ref, o_ref):
-        for y in range(wide):
-            for i in range(count):
-                o_ref[y, i] = b_ref[asked_ref[y, i]]
-
-    out = jax.ShapeDtypeStruct((wide, count, *blocks.shape[1:]), BF16)
-    return call(kernel, out, asked, blocks)
+    tall = count // CAP
+    chunk = 4
+    held = chunk * per_dev
+
+    def kernel(asked_ref, b_hbm, o_ref, b_ref, sems):
+        copies = [
+            pltpu.make_async_copy(
+                b_hbm.at[pl.ds(c * held, held)], b_ref.at[pl.ds(c * held, held)], sems.at[c]
+            )
+            for c in range(tall // chunk)
+        ]
+        for copy in copies:
+            copy.start()
+        for c, copy in enumerate(copies):
+            copy.wait()
+            for i in range(c * chunk * CAP, (c + 1) * chunk * CAP):
+                for y in range(wide):
+                    o_ref[y, i] = b_ref[asked_ref[y, i]]
+
+    return pl.pallas_call(
+        kernel,
+        out_shape=jax.ShapeDtypeStruct((wide, count, *blocks.shape[1:]), BF16),
+        in_specs=[pl.BlockSpec(memory_space=pltpu.SMEM), pl.BlockSpec(memory_space=pl.ANY)],
+        out_specs=pl.BlockSpec(memory_space=pltpu.VMEM),
+        scratch_shapes=[pltpu.VMEM(blocks.shape, BF16), pltpu.SemaphoreType.DMA((tall // chunk,))],
+        name="pick_blocks",
+    )(asked, blocks)
 
 
 def attend(queries, incoming, local_blocks, position, key_pos, facts):
@@ -252,26 +290,32 @@
     )
 
 
-def mix(mine, other, pieces, places):
+def whole_rows(pieces, at, tile):
     n = len(pieces)
     tall, lines, width = pieces[0].shape
-    half = tall // 2
-
-    def kernel(p_ref, m_ref, t_ref, *refs):
-        o_ref, w_s = refs[n], refs[n + 1]
+
+    def kernel(at_ref, *refs):
         for s in range(n):
-            w_s[:, (p_ref[0] + s) % n] = refs[s][...]
-        first = w_s[pl.ds(p_ref[1] * half, half)].reshape(half * n * lines, width)
-        second = w_s[pl.ds((1 - p_ref[1]) * half, half)].reshape(half * n * lines, width)
+            refs[-1][:, (at_ref[0] + s) % n] = refs[s][...]
+
+    out = jax.ShapeDtypeStruct((tall, n, lines, width), BF16)
+    return call(kernel, out, at[None], *pieces, tile)
+
+
+def mix(mine, other, weight, core):
+    half = weight.shape[0] // 2
+
+    def kernel(c_ref, m_ref, t_ref, w_ref, o_ref):
+        first = w_ref[pl.ds(c_ref[0] * half, half)]
+        second = w_ref[pl.ds((1 - c_ref[0]) * half, half)]
         o_ref[...] = (
             jnp.dot(m_ref[...], first, preferred_element_type=F32)
             + jnp.dot(t_ref[...], second, preferred_element_type=F32)
         ).astype(BF16)
 
-    out = jax.ShapeDtypeStruct((mine.shape[0], width), BF16)
-    scratch = (pltpu.VMEM((tall, n, lines, width), BF16),)
-    flops = 4 * mine.size * width
-    return call(kernel, out, places, mine, other, *pieces, scratch=scratch, flops=flops)
+    out = jax.ShapeDtypeStruct((mine.shape[0], weight.shape[1]), BF16)
+    flops = 4 * mine.size * weight.shape[1]
+    return call(kernel, out, core[None], mine, other, weight, flops=flops)
 
 
 def body(tokens, query_weight, key_weight, value_weight, out_weight, chosen, live_length):
@@ -334,7 +378,7 @@
     key_pos = key_positions(late_chosen)
     facts = jnp.stack([me * rows, live_length[0], 2 * parity]).astype(jnp.int32)
 
-    outgoing = pick_blocks(column_blocks, asked)
+    outgoing = pick_blocks(column_blocks, asked, per_dev)
     incoming = lax.all_to_all(outgoing, "kv_1", split_axis=0, concat_axis=0, tiled=True)
     queries = project_queries(tokens, q_pieces, outgoing[0, 0, :16, :HD])
     attended = attend(
@@ -346,8 +390,9 @@
         facts,
     )
     other = from_ahead(attended, "tp", 1)
-    places = jnp.stack([y_at, lax.axis_index("tp")]).astype(jnp.int32)
-    return mix(attended, other, o_pieces, places)
+    out_full = whole_rows(o_pieces, y_at, queries[:16, :HD])
+    out_full = out_full.reshape(-1, out_full.shape[-1])
+    return mix(attended, other, out_full, lax.axis_index("tp"))
 
 
 def solution(mesh):

time: 288 us -> 287 us (level)
  local copies, waits for them, and re-layouts: 15.8 us -> 10 us
  Pallas kernels: 15.4 us -> 19.7 us
    unnamed x22 -> x8, local copies, waits for them, and re-layouts: 7.96 us -> 1.61 us
    pallas_call x0 -> x2, Pallas kernels: none -> 5.25 us  [the longest x1 3.62 us: pick_blocks(): pl.pallas_call(kernel, out_shape=jax.ShapeDtypeStruct((wide, count, *bloc...]
    pallas_call x9 -> x8, Pallas kernels: 15.4 us -> 14.4 us  [call(): pl.pallas_call(kernel, out_shape=out_shape, in_specs=spaces, out_specs=ja...]
  transfers between devices with their start and end apart: 18 -> 18, of which waited for: 7 -> 7; matrix products, arithmetic and copies ran while one was open for 4% -> 5% of each run, Pallas kernels for 4% -> 5%
where the time goes in v7:
time: 287 us; the launch traced here: 286 us
  waiting for transfers between devices  148 us (52%)
  starting transfers between devices  57.8 us (20%)
  blocking collectives  30 us (10%)
  Pallas kernels  19.7 us (7%)
  between operations  14.6 us (5%)
  local copies, waits for them, and re-layouts  10 us (3%)
  other arithmetic  6.6 us (2%)
    all_gather x1, waiting for transfers between devices, body(): column_blocks = lax.all_gather(local_blocks, 'kv_0', axis=0, tiled=True)  58.5 us
    ppermute x14, starting transfers between devices, from_ahead(): return lax.ppermute(x, axis, [((i + step) % n, i) for i in range(n)])  46 us
    all_gather x1, waiting for transfers between devices, body(): halves = lax.all_gather(halves, 'kv_0', axis=0, tiled=False)  38.6 us
    all_to_all x1, blocking collectives, body(): column = lax.all_to_all(cargo, 'kv_0', 0, 0, tiled=True)  30 us
    ppermute x14, waiting for transfers between devices, from_ahead(): return lax.ppermute(x, axis, [((i + step) % n, i) for i in range(n)])  27.1 us
    all_to_all x1, waiting for transfers between devices, copy_for_each(): lax.all_to_all(jnp.broadcast_to(shard[None], (count, *shard.shape)), axis...  22.9 us
    pallas_call x8, Pallas kernels, call(): pl.pallas_call(kernel, out_shape=out_shape, in_specs=spaces, out_specs=ja...  14.4 us
    all_to_all x1, starting transfers between devices, copy_for_each(): lax.all_to_all(jnp.broadcast_to(shard[None], (count, *shard.shape)), axis...  7.48 us
  transfers between devices with their start and end apart: 18, of which 7 were waited for; matrix products, arithmetic and copies ran while one was open for 5% of the time, Pallas kernels for 5%

profile of v7, /device:TPU:2, one launch (start us, length us, event | category | flops | bytes accessed | tf_op | source)
XLA Modules:
  0.0 286.5 jit_solution(4733121002761865207)
XLA Ops:
  6.5 1.6 pack.1
  8.2 30.0 %all_to_all.15 = bf16[16,32,128]{2,1,0:T(8,128)(2,1)S(1)} all-to-all(bf16[16,32,128]{2,1,0:T(8,128)(2,1)} %get-tuple-element.10), channel_id=1, replica_groups=mesh['dp'=4,'kv_0'=16,'kv_1'=4,'tp'=2] {'kv_0'}, dimensions={0} | all-to-all | bytes 262144 | tf_op jit(solution)/shard_map/all_to_all | solution.py:335
  38.2 1.8 broadcast_in_dim.132
  39.9 7.5 %all-to-all-start.1 = ((bf16[16,16,32,128]{3,2,1,0:T(8,128)(2,1)}), bf16[16,16,32,128]{3,2,1,0:T(8,128)(2,1)S(1)}, u32[]{:S(2)}, u32[]{:S(2)}) async-start(bf16[16,16,32,128]{3,2,1,0:T(8,128)(2,1)} %broadcast_in_dim.132), calls=%async_computation.1 | async-start | bytes 4194304 | tf_op jit(solution)/shard_map/all_to_all | solution.py:38
  49.3 22.9 %all-to-all-done.1 = bf16[16,16,32,128]{3,2,1,0:T(8,128)(2,1)S(1)} async-done(((bf16[16,16,32,128]{3,2,1,0:T(8,128)(2,1)}), bf16[16,16,32,128]{3,2,1,0:T(8,128)(2,1)S(1)}, u32[]{:S(2)}, u32[]{:S(2)}) %all-to-all-start.1) | async-done | bytes 2097184 | tf_op jit(solution)/shard_map/all_to_all | solution.py:38
  72.3 1.6 copy-done
  75.2 38.6 %all-gather.6.cloned.1.call-done = bf16[4096,128]{1,0:T(8,128)(2,1)} async-done(((bf16[256,128]{1,0:T(8,128)(2,1)}), bf16[4096,128]{1,0:T(8,128)(2,1)}) %all-gather.6.cloned.1.call-update) | async-done | bytes 1048592 | tf_op jit(solution)/shard_map/all_gather | solution.py:332
  113.9 3.4 %collective-permute-start.7 = (s32[8,16]{1,0:T(8,128)S(1)}, s32[8,16]{1,0:T(8,128)S(1)}, u32[]{:S(2)}, u32[]{:S(2)}) collective-permute-start(s32[8,16]{1,0:T(8,128)S(1)} %copy-done.3), channel_id=1, source_target_pairs={{6,0},{0,2},{2,4},{4,6},{7,1},{1,3},{3,5},{5,7},{14,8},{8,10},{10,... | collective-permute-start | bytes 1544 | tf_op jit(solution)/shard_map/ppermute | solution.py:45
  117.3 4.6 %collective-permute-start.6 = (s32[8,16]{1,0:T(8,128)S(1)}, s32[8,16]{1,0:T(8,128)S(1)}, u32[]{:S(2)}, u32[]{:S(2)}) collective-permute-start(s32[8,16]{1,0:T(8,128)S(1)} %copy-done.3), channel_id=1, source_target_pairs={{4,0},{6,2},{0,4},{2,6},{5,1},{7,3},{1,5},{3,7},{12,8},{14,10},{8,... | collective-permute-start | bytes 1544 | tf_op jit(solution)/shard_map/ppermute | solution.py:45
  122.0 3.3 %collective-permute-start.5 = (s32[8,16]{1,0:T(8,128)S(1)}, s32[8,16]{1,0:T(8,128)S(1)}, u32[]{:S(2)}, u32[]{:S(2)}) collective-permute-start(s32[8,16]{1,0:T(8,128)S(1)} %copy-done.3), channel_id=1, source_target_pairs={{2,0},{4,2},{6,4},{0,6},{3,1},{5,3},{7,5},{1,7},{10,8},{12,10},{14... | collective-permute-start | bytes 1544 | tf_op jit(solution)/shard_map/ppermute | solution.py:45
  125.3 1.9 fusion.12
  127.2 2.1 fusion.13
  129.3 2.5 collective-permute-start.2
  131.8 2.8 collective-permute-start.1
  136.3 3.7 %collective-permute-start = (bf16[16,128,128]{2,1,0:T(8,128)(2,1)S(1)}, bf16[16,128,128]{2,1,0:T(8,128)(2,1)}, u32[]{:S(2)}, u32[]{:S(2)}) collective-permute-start(bf16[16,128,128]{2,1,0:T(8,128)(2,1)S(1)} %get-tuple-element.44.refs_0_), channel_id=1, source_target_pairs={{2,0},{4,2},{6,4},{0,6},{3,1},{5,3},{7,5},{1,7},{10,8},{12,10},{14... | collective-permute-start | bytes 1572872 | tf_op jit(solution)/shard_map/ppermute | solution.py:45
  145.7 58.5 %all-gather.4.cloned.1.call-done.b_hbm = bf16[128,32,256]{2,1,0:T(8,128)(2,1)} async-done(((bf16[8,32,256]{2,1,0:T(8,128)(2,1)}), bf16[128,32,256]{2,1,0:T(8,128)(2,1)}) %all-gather.4.cloned.1.call-update) | async-done | bytes 2097168 | tf_op jit(solution)/shard_map/all_gather | solution.py:341
  204.2 3.6 %pick_blocks.1 = bf16[4,32,32,256]{3,2,1,0:T(8,128)(2,1)} custom-call(s32[4,32]{1,0:T(4,128)} %constant_dynamic-slice_fusion.asked_ref, bf16[128,32,256]{2,1,0:T(8,128)(2,1)} %all-gather.4.cloned.1.call-done.b_hbm), custom_call_target="tpu_custom_call" | custom-call | tf_op jit(solution)/shard_map/pick_blocks/pallas_call | solution.py:231
  207.8 4.3 %all-to-all-start.2 = ((bf16[4,32,32,256]{3,2,1,0:T(8,128)(2,1)}), bf16[4,32,32,256]{3,2,1,0:T(8,128)(2,1)S(1)}, u32[]{:S(2)}, u32[]{:S(2)}) async-start(bf16[4,32,32,256]{3,2,1,0:T(8,128)(2,1)} %pick_blocks.1), calls=%async_computation.2 | async-start | bytes 4194304 | tf_op jit(solution)/shard_map/all_to_all | solution.py:382
  212.3 3.4 %collective-permute-start.10 = (bf16[16,64,128]{2,1,0:T(8,128)(2,1)}, bf16[16,64,128]{2,1,0:T(8,128)(2,1)S(1)}, u32[]{:S(2)}, u32[]{:S(2)}) collective-permute-start(bf16[16,64,128]{2,1,0:T(8,128)(2,1)} %get-tuple-element.41), channel_id=1, source_target_pairs={{384,0},{0,128},{128,256},{256,384},{385,1},{1,129},{129,257},{257... | collective-permute-start | bytes 786440 | tf_op jit(solution)/shard_map/ppermute | solution.py:45
  215.7 2.5 collective-permute-start.9
  219.9 3.8 %collective-permute-start.3 = (bf16[4096,128]{1,0:T(8,128)(2,1)S(1)}, bf16[4096,128]{1,0:T(8,128)(2,1)S(1)}, u32[]{:S(2)}, u32[]{:S(2)}) collective-permute-start(bf16[4096,128]{1,0:T(8,128)(2,1)S(1)} %bitcast.40), channel_id=1, source_target_pairs={{128,0},{256,128},{384,256},{0,384},{129,1},{257,129},{385,257},{1... | collective-permute-start | bytes 3145736 | tf_op jit(solution)/shard_map/ppermute | solution.py:45
  223.7 2.2 collective-permute-start.4
  227.3 3.9 %collective-permute-start.13 = (bf16[16,16,2048]{2,1,0:T(8,128)(2,1)S(1)}, bf16[16,16,2048]{2,1,0:T(8,128)(2,1)}, u32[]{:S(2)}, u32[]{:S(2)}) collective-permute-start(bf16[16,16,2048]{2,1,0:T(8,128)(2,1)S(1)} %shard_map.78.refs_0_), channel_id=1, source_target_pairs={{6,0},{0,2},{2,4},{4,6},{7,1},{1,3},{3,5},{5,7},{14,8},{8,10},{10,... | collective-permute-start | bytes 3145736 | tf_op jit(solution)/shard_map/ppermute | solution.py:45
  231.2 4.6 %collective-permute-start.12 = (bf16[16,16,2048]{2,1,0:T(8,128)(2,1)S(1)}, bf16[16,16,2048]{2,1,0:T(8,128)(2,1)}, u32[]{:S(2)}, u32[]{:S(2)}) collective-permute-start(bf16[16,16,2048]{2,1,0:T(8,128)(2,1)S(1)} %shard_map.78.refs_0_), channel_id=1, source_target_pairs={{4,0},{6,2},{0,4},{2,6},{5,1},{7,3},{1,5},{3,7},{12,8},{14,10},{8,... | collective-permute-start | bytes 3145736 | tf_op jit(solution)/shard_map/ppermute | solution.py:45
  235.8 3.4 %collective-permute-start.11 = (bf16[16,16,2048]{2,1,0:T(8,128)(2,1)S(1)}, bf16[16,16,2048]{2,1,0:T(8,128)(2,1)}, u32[]{:S(2)}, u32[]{:S(2)}) collective-permute-start(bf16[16,16,2048]{2,1,0:T(8,128)(2,1)S(1)} %shard_map.78.refs_0_), channel_id=1, source_target_pairs={{2,0},{4,2},{6,4},{0,6},{3,1},{5,3},{7,5},{1,7},{10,8},{12,10},{14... | collective-permute-start | bytes 3145736 | tf_op jit(solution)/shard_map/ppermute | solution.py:45
  240.2 2.7 collective-permute-done.4.refs_3_
  244.2 4.1 %shard_map.77.m_ref = bf16[256,512]{1,0:T(8,128)(2,1)} custom-call(s32[3]{0:T(128)S(1)} %pad_add_fusion.6.f_ref, s32[8,16]{1,0:T(8,128)S(1)} %fusion.4.p_ref, bf16[256,512]{1,0:T(8,128)(2,1)S(1)} %shard_map.75.q_ref, bf16[128,32,256]{2,1,0:T(8,128)(2,1)S(1)} %bitcast.37, bf16[8,32,256]{2,1,0:T(8,128)(2,1)} %bitcast.19.own_ref, s32[8,1,512]{2,1,0:T(1,128)S(1)} %shard_map.76.kp_ref), custom_call_target="tpu_custom_call" | custom-call | flops 268435456 | tf_op jit(solution)/shard_map/pallas_call | solution.py:25
  248.3 1.9 collective-permute-start.8
  250.2 7.7 %collective-permute-done.13.refs_3_ = bf16[16,16,2048]{2,1,0:T(8,128)(2,1)} collective-permute-done((bf16[16,16,2048]{2,1,0:T(8,128)(2,1)S(1)}, bf16[16,16,2048]{2,1,0:T(8,128)(2,1)}, u32[]{:S(2)}, u32[]{:S(2)}) %collective-permute-start.13) | collective-permute-done | bytes 1048608 | tf_op jit(solution)/shard_map/ppermute | solution.py:45
  258.0 16.3 %collective-permute-done.12.refs_2_ = bf16[16,16,2048]{2,1,0:T(8,128)(2,1)} collective-permute-done((bf16[16,16,2048]{2,1,0:T(8,128)(2,1)S(1)}, bf16[16,16,2048]{2,1,0:T(8,128)(2,1)}, u32[]{:S(2)}, u32[]{:S(2)}) %collective-permute-start.12) | collective-permute-done | bytes 1048608 | tf_op jit(solution)/shard_map/ppermute | solution.py:45
  274.3 2.1 shard_map.79
  276.4 3.2 %shard_map.80 = bf16[256,2048]{1,0:T(8,128)(2,1)} custom-call(s32[1]{0:T(128)} %bitcast.c_ref, bf16[256,512]{1,0:T(8,128)(2,1)} %shard_map.77.m_ref, bf16[256,512]{1,0:T(8,128)(2,1)S(1)} %collective-permute-done.8.t_ref, bf16[1024,2048]{1,0:T(8,128)(2,1)S(1)} %bitcast.35), custom_call_target="tpu_custom_call" | custom-call | flops 1073741824 | tf_op jit(solution)/shard_map/pallas_call | solution.py:25
  (102 shorter events, 15.4 us)
Async XLA Ops:
  39.9 32.3 %all-to-all-start.1 = ((bf16[16,16,32,128]{3,2,1,0:T(8,128)(2,1)}), bf16[16,16,32,128]{3,2,1,0:T(8,128)(2,1)S(1)}, u32[]{:S(2)}, u32[]{:S(2)}) async-start(bf16[16,16,32,128]{3,2,1,0:T(8,128)(2,1)} %broadcast_in_dim.132), calls=%async_computation.1 | async-start | bytes 4194304 | tf_op jit(solution)/shard_map/all_to_all | solution.py:38
  47.4 66.5 %all-gather.6.cloned.1.call-start = ((), (), s32[]{:S(2)}) async-start(), calls=%async_computation.4 | async-start | bytes 1114112 | tf_op jit(solution)/shard_map/all_gather | solution.py:332
  48.1 156.0 %all-gather.4.cloned.1.call-start = ((), (), s32[]{:S(2)}) async-start(), calls=%async_computation.3 | async-start | bytes 2228224 | tf_op jit(solution)/shard_map/all_gather | solution.py:341
  72.3 1.6 copy-start
  73.8 40.0 %copy-start.3 = (s32[8,16]{1,0:T(8,128)S(1)}, s32[8,16]{1,0:T(8,128)}, u32[]{:S(2)}) copy-start(s32[8,16]{1,0:T(8,128)} %c_ref) | copy-start | bytes 1540
  113.9 22.4 %collective-permute-start.7 = (s32[8,16]{1,0:T(8,128)S(1)}, s32[8,16]{1,0:T(8,128)S(1)}, u32[]{:S(2)}, u32[]{:S(2)}) collective-permute-start(s32[8,16]{1,0:T(8,128)S(1)} %copy-done.3), channel_id=1, source_target_pairs={{6,0},{0,2},{2,4},{4,6},{7,1},{1,3},{3,5},{5,7},{14,8},{8,10},{10,... | collective-permute-start | bytes 1544 | tf_op jit(solution)/shard_map/ppermute | solution.py:45
  117.3 22.8 %collective-permute-start.6 = (s32[8,16]{1,0:T(8,128)S(1)}, s32[8,16]{1,0:T(8,128)S(1)}, u32[]{:S(2)}, u32[]{:S(2)}) collective-permute-start(s32[8,16]{1,0:T(8,128)S(1)} %copy-done.3), channel_id=1, source_target_pairs={{4,0},{6,2},{0,4},{2,6},{5,1},{7,3},{1,5},{3,7},{12,8},{14,10},{8,... | collective-permute-start | bytes 1544 | tf_op jit(solution)/shard_map/ppermute | solution.py:45
  122.0 18.2 %collective-permute-start.5 = (s32[8,16]{1,0:T(8,128)S(1)}, s32[8,16]{1,0:T(8,128)S(1)}, u32[]{:S(2)}, u32[]{:S(2)}) collective-permute-start(s32[8,16]{1,0:T(8,128)S(1)} %copy-done.3), channel_id=1, source_target_pairs={{2,0},{4,2},{6,4},{0,6},{3,1},{5,3},{7,5},{1,7},{10,8},{12,10},{14... | collective-permute-start | bytes 1544 | tf_op jit(solution)/shard_map/ppermute | solution.py:45
  129.3 88.9 %collective-permute-start.2 = (bf16[16,128,128]{2,1,0:T(8,128)(2,1)S(1)}, bf16[16,128,128]{2,1,0:T(8,128)(2,1)S(1)}, u32[]{:S(2)}, u32[]{:S(2)}) collective-permute-start(bf16[16,128,128]{2,1,0:T(8,128)(2,1)S(1)} %get-tuple-element.44.refs_0_), channel_id=1, source_target_pairs={{6,0},{0,2},{2,4},{4,6},{7,1},{1,3},{3,5},{5,7},{14,8},{8,10},{10,... | collective-permute-start | bytes 1572872 | tf_op jit(solution)/shard_map/ppermute | solution.py:45
  131.8 86.4 %collective-permute-start.1 = (bf16[16,128,128]{2,1,0:T(8,128)(2,1)S(1)}, bf16[16,128,128]{2,1,0:T(8,128)(2,1)}, u32[]{:S(2)}, u32[]{:S(2)}) collective-permute-start(bf16[16,128,128]{2,1,0:T(8,128)(2,1)S(1)} %get-tuple-element.44.refs_0_), channel_id=1, source_target_pairs={{4,0},{6,2},{0,4},{2,6},{5,1},{7,3},{1,5},{3,7},{12,8},{14,10},{8,... | collective-permute-start | bytes 1572872 | tf_op jit(solution)/shard_map/ppermute | solution.py:45
  136.3 81.9 %collective-permute-start = (bf16[16,128,128]{2,1,0:T(8,128)(2,1)S(1)}, bf16[16,128,128]{2,1,0:T(8,128)(2,1)}, u32[]{:S(2)}, u32[]{:S(2)}) collective-permute-start(bf16[16,128,128]{2,1,0:T(8,128)(2,1)S(1)} %get-tuple-element.44.refs_0_), channel_id=1, source_target_pairs={{2,0},{4,2},{6,4},{0,6},{3,1},{5,3},{7,5},{1,7},{10,8},{12,10},{14... | collective-permute-start | bytes 1572872 | tf_op jit(solution)/shard_map/ppermute | solution.py:45
  207.8 36.4 %all-to-all-start.2 = ((bf16[4,32,32,256]{3,2,1,0:T(8,128)(2,1)}), bf16[4,32,32,256]{3,2,1,0:T(8,128)(2,1)S(1)}, u32[]{:S(2)}, u32[]{:S(2)}) async-start(bf16[4,32,32,256]{3,2,1,0:T(8,128)(2,1)} %pick_blocks.1), calls=%async_computation.2 | async-start | bytes 4194304 | tf_op jit(solution)/shard_map/all_to_all | solution.py:382
  212.3 14.4 %collective-permute-start.10 = (bf16[16,64,128]{2,1,0:T(8,128)(2,1)}, bf16[16,64,128]{2,1,0:T(8,128)(2,1)S(1)}, u32[]{:S(2)}, u32[]{:S(2)}) collective-permute-start(bf16[16,64,128]{2,1,0:T(8,128)(2,1)} %get-tuple-element.41), channel_id=1, source_target_pairs={{384,0},{0,128},{128,256},{256,384},{385,1},{1,129},{129,257},{257... | collective-permute-start | bytes 786440 | tf_op jit(solution)/shard_map/ppermute | solution.py:45
  215.7 11.3 %collective-permute-start.9 = (bf16[16,64,128]{2,1,0:T(8,128)(2,1)}, bf16[16,64,128]{2,1,0:T(8,128)(2,1)S(1)}, u32[]{:S(2)}, u32[]{:S(2)}) collective-permute-start(bf16[16,64,128]{2,1,0:T(8,128)(2,1)} %get-tuple-element.42), channel_id=1, source_target_pairs={{128,0},{256,128},{384,256},{0,384},{129,1},{257,129},{385,257},{1... | collective-permute-start | bytes 786440 | tf_op jit(solution)/shard_map/ppermute | solution.py:45
  219.6 7.4 %copy-start.2 = (bf16[16,128,128]{2,1,0:T(8,128)(2,1)S(1)}, bf16[16,128,128]{2,1,0:T(8,128)(2,1)}, u32[]{:S(2)}) copy-start(bf16[16,128,128]{2,1,0:T(8,128)(2,1)} %get-tuple-element.43.own_ref) | copy-start | bytes 1572868
  219.8 23.1 %copy-start.1 = (bf16[256,4096]{1,0:T(8,128)(2,1)S(1)}, bf16[256,4096]{1,0:T(8,128)(2,1)}, u32[]{:S(2)}) copy-start(bf16[256,4096]{1,0:T(8,128)(2,1)} %t_ref.3) | copy-start | bytes 6291460
  219.9 20.4 %collective-permute-start.3 = (bf16[4096,128]{1,0:T(8,128)(2,1)S(1)}, bf16[4096,128]{1,0:T(8,128)(2,1)S(1)}, u32[]{:S(2)}, u32[]{:S(2)}) collective-permute-start(bf16[4096,128]{1,0:T(8,128)(2,1)S(1)} %bitcast.40), channel_id=1, source_target_pairs={{128,0},{256,128},{384,256},{0,384},{129,1},{257,129},{385,257},{1... | collective-permute-start | bytes 3145736 | tf_op jit(solution)/shard_map/ppermute | solution.py:45
  223.7 19.3 %collective-permute-start.4 = (bf16[4096,128]{1,0:T(8,128)(2,1)S(1)}, bf16[4096,128]{1,0:T(8,128)(2,1)S(1)}, u32[]{:S(2)}, u32[]{:S(2)}) collective-permute-start(bf16[4096,128]{1,0:T(8,128)(2,1)S(1)} %bitcast.38), channel_id=1, source_target_pairs={{384,0},{0,128},{128,256},{256,384},{385,1},{1,129},{129,257},{257... | collective-permute-start | bytes 3145736 | tf_op jit(solution)/shard_map/ppermute | solution.py:45
  227.3 30.7 %collective-permute-start.13 = (bf16[16,16,2048]{2,1,0:T(8,128)(2,1)S(1)}, bf16[16,16,2048]{2,1,0:T(8,128)(2,1)}, u32[]{:S(2)}, u32[]{:S(2)}) collective-permute-start(bf16[16,16,2048]{2,1,0:T(8,128)(2,1)S(1)} %shard_map.78.refs_0_), channel_id=1, source_target_pairs={{6,0},{0,2},{2,4},{4,6},{7,1},{1,3},{3,5},{5,7},{14,8},{8,10},{10,... | collective-permute-start | bytes 3145736 | tf_op jit(solution)/shard_map/ppermute | solution.py:45
  231.2 43.0 %collective-permute-start.12 = (bf16[16,16,2048]{2,1,0:T(8,128)(2,1)S(1)}, bf16[16,16,2048]{2,1,0:T(8,128)(2,1)}, u32[]{:S(2)}, u32[]{:S(2)}) collective-permute-start(bf16[16,16,2048]{2,1,0:T(8,128)(2,1)S(1)} %shard_map.78.refs_0_), channel_id=1, source_target_pairs={{4,0},{6,2},{0,4},{2,6},{5,1},{7,3},{1,5},{3,7},{12,8},{14,10},{8,... | collective-permute-start | bytes 3145736 | tf_op jit(solution)/shard_map/ppermute | solution.py:45
  235.8 38.5 %collective-permute-start.11 = (bf16[16,16,2048]{2,1,0:T(8,128)(2,1)S(1)}, bf16[16,16,2048]{2,1,0:T(8,128)(2,1)}, u32[]{:S(2)}, u32[]{:S(2)}) collective-permute-start(bf16[16,16,2048]{2,1,0:T(8,128)(2,1)S(1)} %shard_map.78.refs_0_), channel_id=1, source_target_pairs={{2,0},{4,2},{6,4},{0,6},{3,1},{5,3},{7,5},{1,7},{10,8},{12,10},{14... | collective-permute-start | bytes 3145736 | tf_op jit(solution)/shard_map/ppermute | solution.py:45
  248.3 28.1 %collective-permute-start.8 = (bf16[256,512]{1,0:T(8,128)(2,1)}, bf16[256,512]{1,0:T(8,128)(2,1)S(1)}, u32[]{:S(2)}, u32[]{:S(2)}) collective-permute-start(bf16[256,512]{1,0:T(8,128)(2,1)} %shard_map.77.m_ref), channel_id=1, source_target_pairs={{1,0},{0,1},{3,2},{2,3},{5,4},{4,5},{7,6},{6,7},{9,8},{8,9},{11,10... | collective-permute-start | bytes 786440 | tf_op jit(solution)/shard_map/ppermute | solution.py:45
Sparse Core Ops, SparseCore 0:
  50.3 63.5 all-gather.5
  134.7 69.3 all-gather.3

commit v8 on v6

--- a/solution.py
+++ b/solution.py
@@ -65,26 +65,27 @@
     return jnp.stack(lists, axis=2)
 
 
-def pack(key_weight, value_weight, out_weight, x_at, planes, tall):
+def pack(query_weight, key_weight, value_weight, out_weight, x_at, planes, tall):
     rows = key_weight.shape[0]
     lines, wide_out = out_weight.shape
     small = rows // planes
     groups = wide_out // planes // HD
 
-    def kernel(x_ref, k_hbm, v_hbm, o_hbm, part_ref, cargo_ref, *scratch):
-        held, sems = scratch[:3], scratch[3]
+    def kernel(x_ref, q_hbm, k_hbm, v_hbm, o_hbm, part_ref, cargo_ref, *scratch):
+        held, sems = scratch[:4], scratch[4]
         copies = [
             pltpu.make_async_copy(src, dst, sems.at[i])
-            for i, (src, dst) in enumerate(zip((k_hbm, v_hbm, o_hbm), held, strict=True))
+            for i, (src, dst) in enumerate(zip((q_hbm, k_hbm, v_hbm, o_hbm), held, strict=True))
         ]
         for copy in copies:
             copy.start()
         for copy in copies:
             copy.wait()
-        k_ref, v_ref, o_ref = held
+        q_ref, k_ref, v_ref, o_ref = held
+        part_ref[:rows] = q_ref[:, pl.ds(pl.multiple_of(x_ref[0] * HD, HD), HD)]
         for i in range(groups):
             first = pl.multiple_of((x_ref[0] * groups + i) * HD, HD)
-            part_ref[i * lines : (i + 1) * lines] = o_ref[:, pl.ds(first, HD)]
+            part_ref[rows + i * lines : rows + (i + 1) * lines] = o_ref[:, pl.ds(first, HD)]
         first = pl.multiple_of(x_ref[0] * small, small)
         keys = k_ref[pl.ds(first, small)]
         values = v_ref[pl.ds(first, small)]
@@ -92,18 +93,18 @@
             cargo_ref[z, :small] = keys
             cargo_ref[z, small:] = values
 
-    weights = (key_weight, value_weight, out_weight)
+    weights = (query_weight, key_weight, value_weight, out_weight)
     outs = (
-        jax.ShapeDtypeStruct((groups * lines, HD), BF16),
+        jax.ShapeDtypeStruct((rows + groups * lines, HD), BF16),
         jax.ShapeDtypeStruct((tall, 2 * small, HD), BF16),
     )
     return pl.pallas_call(
         kernel,
         out_shape=outs,
-        in_specs=[pl.BlockSpec(memory_space=pltpu.SMEM)] + [pl.BlockSpec(memory_space=pl.ANY)] * 3,
+        in_specs=[pl.BlockSpec(memory_space=pltpu.SMEM)] + [pl.BlockSpec(memory_space=pl.ANY)] * 4,
         out_specs=(pl.BlockSpec(memory_space=pltpu.VMEM),) * 2,
         scratch_shapes=[pltpu.VMEM(w.shape, BF16) for w in weights]
-        + [pltpu.SemaphoreType.DMA((3,))],
+        + [pltpu.SemaphoreType.DMA((4,))],
         name="pack",
     )(x_at[None], *weights)
 
@@ -119,17 +120,26 @@
     return call(kernel, out, at[None], *pieces)
 
 
-def columns_of(pieces, at):
-    n = len(pieces)
-    high, rows, _ = pieces[0].shape
-
-    def kernel(at_ref, *refs):
+def columns_of(pieces, at, rows, notes):
+    n = len(pieces)
+    high, both, _ = pieces[0].shape
+    tall = high * n
+
+    def kernel(at_ref, n_ref, *refs):
+        q_ref, o_ref = refs[n], refs[n + 1]
         for s in range(n):
             for h in range(high):
-                refs[-1][h * n + (at_ref[0] + s) % n] = refs[s][h]
-
-    out = jax.ShapeDtypeStruct((high * n, rows, HD), BF16)
-    return call(kernel, out, at[None], *pieces)
+                z = h * n + (at_ref[0] + s) % n
+                q_ref[z] = refs[s][h, :rows]
+                o_ref[z] = refs[s][h, rows:]
+        o_ref[tall] = jnp.zeros((both - rows, HD), BF16)
+        o_ref[tall, : n_ref.shape[0]] = n_ref[...]
+
+    outs = (
+        jax.ShapeDtypeStruct((tall, rows, HD), BF16),
+        jax.ShapeDtypeStruct((tall + 1, both - rows, HD), BF16),
+    )
+    return call(kernel, outs, at[None], notes, *pieces)
 
 
 def project_pair(tokens, every):
@@ -179,16 +189,32 @@
     )
 
 
-def full_rows(pieces, at, lines):
+def full_columns(pieces, at, lines):
     n = len(pieces)
     tall, held, _ = pieces[0].shape
     groups = held // lines
 
     def kernel(at_ref, *refs):
         for s in range(n):
+            for i in range(groups):
+                first = pl.multiple_of((((at_ref[0] + s) % n) * groups + i) * HD, HD)
+                refs[n][:, :, pl.ds(first, HD)] = refs[s][:, i * lines : (i + 1) * lines]
+
+    out = jax.ShapeDtypeStruct((tall, lines, n * groups * HD), BF16)
+    return call(kernel, out, at[None], *pieces)
+
+
+def full_rows(pieces, at, lines):
+    n = len(pieces)
+    tall, held = pieces[0].shape[0] - 1, pieces[0].shape[1]
+    groups = held // lines
+
+    def kernel(at_ref, *refs):
+        for s in range(n):
             y = (at_ref[0] + s) % n
             for i in range(groups):
-                refs[-1][:, y, :, i * HD : (i + 1) * HD] = refs[s][:, i * lines : (i + 1) * lines]
+                cut = refs[s][:tall, i * lines : (i + 1) * lines]
+                refs[-1][:, y, :, i * HD : (i + 1) * HD] = cut
 
     out = jax.ShapeDtypeStruct((tall, n, lines, groups * HD), BF16)
     return call(kernel, out, at[None], *pieces)
@@ -306,8 +332,7 @@
     owners = tall * wide
     me = lax.axis_index(KV)
 
-    q_column = lax.all_gather(query_weight, TALL, axis=0, tiled=True)
-    part, cargo = pack(key_weight, value_weight, out_weight, x_at, planes, tall)
+    part, cargo = pack(query_weight, key_weight, value_weight, out_weight, x_at, planes, tall)
     column = lax.all_to_all(cargo, TALL, 0, 0, tiled=True)
     parts = spread(part, "zh")
     every = copy_for_each(column, ("dp", "y"))
@@ -317,15 +342,20 @@
     local_blocks = paired.reshape(per_dev, BLOCK, paired.shape[1])
     column_blocks = lax.all_gather(local_blocks, TALL, axis=0, tiled=True)
 
-    q_pieces = spread(q_column, "y")
-    q_pieces = [p.reshape(tall, -1, p.shape[1]) for p in q_pieces]
-    o_pieces = spread(columns_of(parts, l_at), "y")
+    notes = jnp.stack([chosen // per_dev, chosen % per_dev]).reshape(2, -1)
+    notes = jnp.pad(notes.astype(BF16), ((0, 14), (0, 0)))
+    lines = query_weight.shape[0]
+    q_small, o_small = columns_of(parts, l_at, lines, notes)
+    q_pieces = spread(q_small, "dp")
+    o_pieces = spread(o_small, "y")
+    q_pieces = spread(full_columns(q_pieces, x_at, lines), "y")
+    heard = jnp.stack([p[tall, :2] for p in o_pieces]).astype(jnp.int32)
+    mates = heard[:, 0] * per_dev + heard[:, 1]
     o_tall = full_rows(o_pieces, y_at, out_weight.shape[0])
     o_pieces = spread(o_tall.reshape(-1, o_tall.shape[-1]), "dp")
 
     key_pos = key_positions(chosen)
 
-    mates = jnp.stack(spread(chosen.reshape(-1), "y"))
     mates, chosen = lax.optimization_barrier((mates, chosen))
     depth = jnp.arange(tall, dtype=jnp.int32)
     readers = (h_at * low + l_at) * wide + (y_at + jnp.arange(wide, dtype=jnp.int32)) % wide

time: 292 us -> 236 us (0.81)
  the two profiles are of different devices: /device:TPU:32 before, /device:TPU:65 now
where the time goes in v8:
time: 236 us; the launch traced here: 235 us
  starting transfers between devices  71.5 us (30%)
  waiting for transfers between devices  57.6 us (24%)
  blocking collectives  57.1 us (24%)
  Pallas kernels  20.9 us (9%)
  between operations  14.5 us (6%)
  local copies, waits for them, and re-layouts  8.25 us (3%)
  other arithmetic  5.39 us (2%)
    ppermute x19, starting transfers between devices, from_ahead(): return lax.ppermute(x, axis, [((i + step) % n, i) for i in range(n)])  67 us
    ppermute x19, waiting for transfers between devices, from_ahead(): return lax.ppermute(x, axis, [((i + step) % n, i) for i in range(n)])  43.4 us
    all_to_all x1, blocking collectives, copy_for_each(): lax.all_to_all(jnp.broadcast_to(shard[None], (count, *shard.shape)), axis...  31.3 us
    all_to_all x1, blocking collectives, body(): column = lax.all_to_all(cargo, TALL, 0, 0, tiled=True)  25.8 us
    pallas_call x10, Pallas kernels, call(): pl.pallas_call(kernel, out_shape=out_shape, in_specs=spaces, out_specs=ja...  19.3 us
    all_to_all x1, waiting for transfers between devices, body(): lax.all_to_all(outgoing, 'y', split_axis=0, concat_axis=0, tiled=True)  14.2 us
    unnamed x20, local copies, waits for them, and re-layouts  6.58 us
  transfers between devices with their start and end apart: 21, of which 9 were waited for; matrix products, arithmetic and copies ran while one was open for 3% of the time, Pallas kernels for 6%

profile of v8, /device:TPU:65, one launch (start us, length us, event | category | flops | bytes accessed | tf_op | source)
XLA Modules:
  0.0 235.3 jit_solution(7987218218053040866)
XLA Ops:
  8.2 25.8 %all_to_all.15 = bf16[16,32,128]{2,1,0:T(8,128)(2,1)S(1)} all-to-all(bf16[16,32,128]{2,1,0:T(8,128)(2,1)} %get-tuple-element.16), channel_id=1, replica_groups=mesh['dp'=4,'zh'=4,'zl'=4,'y'=4,'tp'=2] {'zh','zl'}, dimensions={0} | all-to-all | bytes 262144 | tf_op jit(solution)/shard_map/all_to_all | solution.py:336
  34.4 31.3 %all_to_all.16 = bf16[16,16,32,128]{3,2,1,0:T(8,128)(2,1)S(1)} all-to-all(bf16[16,16,32,128]{3,2,1,0:T(8,128)(2,1)S(1)} %broadcast_in_dim.95), channel_id=1, replica_groups=mesh['dp'=4,'zh'=4,'zl'=4,'y'=4,'tp'=2] {'dp','y'}, dimensions={0} | all-to-all | bytes 4194304 | tf_op jit(solution)/shard_map/all_to_all | solution.py:39
  67.1 4.2 %collective-permute-start = (bf16[128,128]{1,0:T(8,128)(2,1)S(1)}, bf16[128,128]{1,0:T(8,128)(2,1)S(1)}, u32[]{:S(2)}, u32[]{:S(2)}) collective-permute-start(bf16[128,128]{1,0:T(8,128)(2,1)S(1)} %copy-done.9), channel_id=1, source_target_pairs={{32,0},{64,32},{96,64},{0,96},{33,1},{65,33},{97,65},{1,97},{34,2}... | collective-permute-start | bytes 98312 | tf_op jit(solution)/shard_map/ppermute | solution.py:46
  71.4 8.7 %collective-permute-start.1 = (bf16[128,128]{1,0:T(8,128)(2,1)S(1)}, bf16[128,128]{1,0:T(8,128)(2,1)S(1)}, u32[]{:S(2)}, u32[]{:S(2)}) collective-permute-start(bf16[128,128]{1,0:T(8,128)(2,1)S(1)} %copy-done.9), channel_id=1, source_target_pairs={{64,0},{96,32},{0,64},{32,96},{65,1},{97,33},{1,65},{33,97},{66,2}... | collective-permute-start | bytes 98312 | tf_op jit(solution)/shard_map/ppermute | solution.py:46
  80.0 3.3 %collective-permute-start.2 = (bf16[128,128]{1,0:T(8,128)(2,1)S(1)}, bf16[128,128]{1,0:T(8,128)(2,1)S(1)}, u32[]{:S(2)}, u32[]{:S(2)}) collective-permute-start(bf16[128,128]{1,0:T(8,128)(2,1)S(1)} %copy-done.9), channel_id=1, source_target_pairs={{96,0},{0,32},{32,64},{64,96},{97,1},{1,33},{33,65},{65,97},{98,2}... | collective-permute-start | bytes 98312 | tf_op jit(solution)/shard_map/ppermute | solution.py:46
  84.8 5.7 %collective-permute-done.2.refs_3_ = bf16[128,128]{1,0:T(8,128)(2,1)S(1)} collective-permute-done((bf16[128,128]{1,0:T(8,128)(2,1)S(1)}, bf16[128,128]{1,0:T(8,128)(2,1)S(1)}, u32[]{:S(2)}, u32[]{:S(2)}) %collective-permute-start.2) | collective-permute-done | bytes 32800 | tf_op jit(solution)/shard_map/ppermute | solution.py:46
  90.5 1.9 collective-permute-start.3
  92.5 5.2 %collective-permute-start.4 = (bf16[4,128,128]{2,1,0:T(8,128)(2,1)S(1)}, bf16[4,128,128]{2,1,0:T(8,128)(2,1)S(1)}, u32[]{:S(2)}, u32[]{:S(2)}) collective-permute-start(bf16[4,128,128]{2,1,0:T(8,128)(2,1)S(1)} %shard_map.73.refs_0_), channel_id=1, source_target_pairs={{16,0},{24,8},{0,16},{8,24},{17,1},{25,9},{1,17},{9,25},{18,2},{26... | collective-permute-start | bytes 393224 | tf_op jit(solution)/shard_map/ppermute | solution.py:46
  97.7 1.9 collective-permute-start.5
  99.8 7.9 %collective-permute-done.4.refs_2_ = bf16[4,128,128]{2,1,0:T(8,128)(2,1)S(1)} collective-permute-done((bf16[4,128,128]{2,1,0:T(8,128)(2,1)S(1)}, bf16[4,128,128]{2,1,0:T(8,128)(2,1)S(1)}, u32[]{:S(2)}, u32[]{:S(2)}) %collective-permute-start.4) | collective-permute-done | bytes 131104 | tf_op jit(solution)/shard_map/ppermute | solution.py:46
  107.7 5.6 %collective-permute-done.5.refs_3_ = bf16[4,128,128]{2,1,0:T(8,128)(2,1)S(1)} collective-permute-done((bf16[4,128,128]{2,1,0:T(8,128)(2,1)S(1)}, bf16[4,128,128]{2,1,0:T(8,128)(2,1)S(1)}, u32[]{:S(2)}, u32[]{:S(2)}) %collective-permute-start.5) | collective-permute-done | bytes 131104 | tf_op jit(solution)/shard_map/ppermute | solution.py:46
  114.1 2.1 collective-permute-start.10
  116.9 3.1 %collective-permute-start.6 = (bf16[17,64,128]{2,1,0:T(8,128)(2,1)S(1)}, bf16[17,64,128]{2,1,0:T(8,128)(2,1)S(1)}, u32[]{:S(2)}, u32[]{:S(2)}) collective-permute-start(bf16[17,64,128]{2,1,0:T(8,128)(2,1)S(1)} %get-tuple-element.12.refs_0_), channel_id=1, source_target_pairs={{2,0},{4,2},{6,4},{0,6},{3,1},{5,3},{7,5},{1,7},{10,8},{12,10},{14... | collective-permute-start | bytes 835592 | tf_op jit(solution)/shard_map/ppermute | solution.py:46
  120.0 3.0 %collective-permute-start.7 = (bf16[17,64,128]{2,1,0:T(8,128)(2,1)S(1)}, bf16[17,64,128]{2,1,0:T(8,128)(2,1)S(1)}, u32[]{:S(2)}, u32[]{:S(2)}) collective-permute-start(bf16[17,64,128]{2,1,0:T(8,128)(2,1)S(1)} %get-tuple-element.12.refs_0_), channel_id=1, source_target_pairs={{4,0},{6,2},{0,4},{2,6},{5,1},{7,3},{1,5},{3,7},{12,8},{14,10},{8,... | collective-permute-start | bytes 835592 | tf_op jit(solution)/shard_map/ppermute | solution.py:46
  123.0 2.4 collective-permute-start.8
  125.4 2.9 %collective-permute-start.11 = (bf16[16,64,128]{2,1,0:T(8,128)(2,1)}, bf16[16,64,128]{2,1,0:T(8,128)(2,1)}, u32[]{:S(2)}, u32[]{:S(2)}) collective-permute-start(bf16[16,64,128]{2,1,0:T(8,128)(2,1)} %get-tuple-element.14.refs_0_), channel_id=1, source_target_pairs={{384,0},{0,128},{128,256},{256,384},{385,1},{1,129},{129,257},{257... | collective-permute-start | bytes 786440 | tf_op jit(solution)/shard_map/ppermute | solution.py:46
  128.3 3.6 %collective-permute-start.9 = (bf16[16,64,128]{2,1,0:T(8,128)(2,1)}, bf16[16,64,128]{2,1,0:T(8,128)(2,1)}, u32[]{:S(2)}, u32[]{:S(2)}) collective-permute-start(bf16[16,64,128]{2,1,0:T(8,128)(2,1)} %get-tuple-element.14.refs_0_), channel_id=1, source_target_pairs={{128,0},{256,128},{384,256},{0,384},{129,1},{257,129},{385,257},{1... | collective-permute-start | bytes 786440 | tf_op jit(solution)/shard_map/ppermute | solution.py:46
  136.1 2.3 shard_map.75.refs_0_
  138.4 4.6 %collective-permute-start.12 = (bf16[16,64,512]{2,1,0:T(8,128)(2,1)}, bf16[16,64,512]{2,1,0:T(8,128)(2,1)}, u32[]{:S(2)}, u32[]{:S(2)}) collective-permute-start(bf16[16,64,512]{2,1,0:T(8,128)(2,1)} %shard_map.75.refs_0_), channel_id=1, source_target_pairs={{2,0},{4,2},{6,4},{0,6},{3,1},{5,3},{7,5},{1,7},{10,8},{12,10},{14... | collective-permute-start | bytes 3145736 | tf_op jit(solution)/shard_map/ppermute | solution.py:46
  143.0 1.9 collective-permute-start.13
  145.6 2.5 %collective-permute-start.14 = (bf16[16,64,512]{2,1,0:T(8,128)(2,1)}, bf16[16,64,512]{2,1,0:T(8,128)(2,1)}, u32[]{:S(2)}, u32[]{:S(2)}) collective-permute-start(bf16[16,64,512]{2,1,0:T(8,128)(2,1)} %shard_map.75.refs_0_), channel_id=1, source_target_pairs={{6,0},{0,2},{2,4},{4,6},{7,1},{1,3},{3,5},{5,7},{14,8},{8,10},{10,... | collective-permute-start | bytes 3145736 | tf_op jit(solution)/shard_map/ppermute | solution.py:46
  152.6 4.4 %collective-permute-start.16 = (bf16[1024,512]{1,0:T(8,128)(2,1)S(1)}, bf16[1024,512]{1,0:T(8,128)(2,1)}, u32[]{:S(2)}, u32[]{:S(2)}) collective-permute-start(bf16[1024,512]{1,0:T(8,128)(2,1)S(1)} %bitcast.25), channel_id=1, source_target_pairs={{128,0},{256,128},{384,256},{0,384},{129,1},{257,129},{385,257},{1... | collective-permute-start | bytes 3145736 | tf_op jit(solution)/shard_map/ppermute | solution.py:46
  157.0 2.5 %collective-permute-start.17 = (bf16[1024,512]{1,0:T(8,128)(2,1)S(1)}, bf16[1024,512]{1,0:T(8,128)(2,1)}, u32[]{:S(2)}, u32[]{:S(2)}) collective-permute-start(bf16[1024,512]{1,0:T(8,128)(2,1)S(1)} %bitcast.26), channel_id=1, source_target_pairs={{256,0},{384,128},{0,256},{128,384},{257,1},{385,129},{1,257},{129... | collective-permute-start | bytes 3145736 | tf_op jit(solution)/shard_map/ppermute | solution.py:46
  165.5 2.0 shard_map.77
  167.5 4.4 %all-to-all-start.2 = ((bf16[4,32,32,256]{3,2,1,0:T(8,128)(2,1)}), bf16[4,32,32,256]{3,2,1,0:T(8,128)(2,1)}, u32[]{:S(2)}, u32[]{:S(2)}) async-start(bf16[4,32,32,256]{3,2,1,0:T(8,128)(2,1)} %shard_map.77), calls=%async_computation.2 | async-start | bytes 4194304 | tf_op jit(solution)/shard_map/all_to_all | solution.py:365
  172.6 1.9 collective-permute-start.18
  175.5 18.7 %collective-permute-done.14.refs_3_ = bf16[16,64,512]{2,1,0:T(8,128)(2,1)} collective-permute-done((bf16[16,64,512]{2,1,0:T(8,128)(2,1)}, bf16[16,64,512]{2,1,0:T(8,128)(2,1)}, u32[]{:S(2)}, u32[]{:S(2)}) %collective-permute-start.14) | collective-permute-done | bytes 1048608 | tf_op jit(solution)/shard_map/ppermute | solution.py:46
  194.2 3.7 %shard_map.78.q_ref = bf16[256,512]{1,0:T(8,128)(2,1)S(1)} custom-call(s32[1]{0:T(128)} %bitcast.9.at_ref, bf16[256,4096]{1,0:T(8,128)(2,1)S(1)} %copy-done, bf16[16,64,512]{2,1,0:T(8,128)(2,1)} %shard_map.75.refs_0_, bf16[16,64,512]{2,1,0:T(8,128)(2,1)} %collective-permute-done.12.refs_1_, bf16[16,64,512]{2,1,0:T(8,128)(2,1)} %collective-permute-done.13.refs_2_, ...), custom_call_target="tpu_custom_call" | custom-call | flops 1073741824 | tf_op jit(solution)/shard_map/pallas_call | solution.py:26
  197.9 14.2 %all-to-all-done.2 = bf16[4,32,32,256]{3,2,1,0:T(8,128)(2,1)} async-done(((bf16[4,32,32,256]{3,2,1,0:T(8,128)(2,1)}), bf16[4,32,32,256]{3,2,1,0:T(8,128)(2,1)}, u32[]{:S(2)}, u32[]{:S(2)}) %all-to-all-start.2) | async-done | bytes 2097184 | tf_op jit(solution)/shard_map/all_to_all | solution.py:365
  212.2 4.1 %shard_map.80.m_ref = bf16[256,512]{1,0:T(8,128)(2,1)S(1)} custom-call(s32[2]{0:T(128)S(1)} %pad_add_fusion.1.f_ref, s32[8,16]{1,0:T(8,128)S(1)} %fusion.8.p_ref, bf16[256,512]{1,0:T(8,128)(2,1)S(1)} %shard_map.78.q_ref, bf16[128,32,256]{2,1,0:T(8,128)(2,1)} %bitcast.16.in_ref, bf16[8,32,256]{2,1,0:T(8,128)(2,1)} %bitcast.14.own_ref, ...), custom_call_target="tpu_custom_call" | custom-call | flops 268435456 | tf_op jit(solution)/shard_map/pallas_call | solution.py:26
  216.2 7.0 %collective-permute-start.15 = (bf16[256,512]{1,0:T(8,128)(2,1)S(1)}, bf16[256,512]{1,0:T(8,128)(2,1)S(1)}, u32[]{:S(2)}, u32[]{:S(2)}) collective-permute-start(bf16[256,512]{1,0:T(8,128)(2,1)S(1)} %shard_map.80.m_ref), channel_id=1, source_target_pairs={{1,0},{0,1},{3,2},{2,3},{5,4},{4,5},{7,6},{6,7},{9,8},{8,9},{11,10... | collective-permute-start | bytes 786440 | tf_op jit(solution)/shard_map/ppermute | solution.py:46
  224.4 4.1 %shard_map.82 = bf16[256,2048]{1,0:T(8,128)(2,1)} custom-call(s32[2]{0:T(128)S(1)} %pad_add_fusion.p_ref, bf16[256,512]{1,0:T(8,128)(2,1)S(1)} %shard_map.80.m_ref, bf16[256,512]{1,0:T(8,128)(2,1)S(1)} %collective-permute-done.15.t_ref, bf16[1024,512]{1,0:T(8,128)(2,1)S(1)} %bitcast.28, bf16[1024,512]{1,0:T(8,128)(2,1)} %collective-permute-done.16.refs_1_, ...), custom_call_target="tpu_custom_call" | custom-call | flops 1073741824 | tf_op jit(solution)/shard_map/pallas_call | solution.py:26
  (93 shorter events, 23.8 us)
Async XLA Ops:
  6.5 157.4 %all-gather.2.cloned.1.call-start = ((), (), s32[]{:S(2)}) async-start(), calls=%async_computation.3 | async-start | bytes 2228224 | tf_op jit(solution)/shard_map/all_gather | solution.py:343
  34.4 31.3 %copy-start = (bf16[256,4096]{1,0:T(8,128)(2,1)S(1)}, bf16[256,4096]{1,0:T(8,128)(2,1)}, u32[]{:S(2)}) copy-start(bf16[256,4096]{1,0:T(8,128)(2,1)} %t_ref.3) | copy-start | bytes 6291460
  65.7 1.4 copy-start.9
  65.7 17.8 %copy-start.8 = (s32[8,16]{1,0:T(8,128)S(1)}, s32[8,16]{1,0:T(8,128)}, u32[]{:S(2)}) copy-start(s32[8,16]{1,0:T(8,128)} %c_ref.1) | copy-start | bytes 1540
  67.1 16.4 %collective-permute-start = (bf16[128,128]{1,0:T(8,128)(2,1)S(1)}, bf16[128,128]{1,0:T(8,128)(2,1)S(1)}, u32[]{:S(2)}, u32[]{:S(2)}) collective-permute-start(bf16[128,128]{1,0:T(8,128)(2,1)S(1)} %copy-done.9), channel_id=1, source_target_pairs={{32,0},{64,32},{96,64},{0,96},{33,1},{65,33},{97,65},{1,97},{34,2}... | collective-permute-start | bytes 98312 | tf_op jit(solution)/shard_map/ppermute | solution.py:46
  71.4 13.5 %collective-permute-start.1 = (bf16[128,128]{1,0:T(8,128)(2,1)S(1)}, bf16[128,128]{1,0:T(8,128)(2,1)S(1)}, u32[]{:S(2)}, u32[]{:S(2)}) collective-permute-start(bf16[128,128]{1,0:T(8,128)(2,1)S(1)} %copy-done.9), channel_id=1, source_target_pairs={{64,0},{96,32},{0,64},{32,96},{65,1},{97,33},{1,65},{33,97},{66,2}... | collective-permute-start | bytes 98312 | tf_op jit(solution)/shard_map/ppermute | solution.py:46
  80.0 10.5 %collective-permute-start.2 = (bf16[128,128]{1,0:T(8,128)(2,1)S(1)}, bf16[128,128]{1,0:T(8,128)(2,1)S(1)}, u32[]{:S(2)}, u32[]{:S(2)}) collective-permute-start(bf16[128,128]{1,0:T(8,128)(2,1)S(1)} %copy-done.9), channel_id=1, source_target_pairs={{96,0},{0,32},{32,64},{64,96},{97,1},{1,33},{33,65},{65,97},{98,2}... | collective-permute-start | bytes 98312 | tf_op jit(solution)/shard_map/ppermute | solution.py:46
  90.5 9.3 %collective-permute-start.3 = (bf16[4,128,128]{2,1,0:T(8,128)(2,1)S(1)}, bf16[4,128,128]{2,1,0:T(8,128)(2,1)S(1)}, u32[]{:S(2)}, u32[]{:S(2)}) collective-permute-start(bf16[4,128,128]{2,1,0:T(8,128)(2,1)S(1)} %shard_map.73.refs_0_), channel_id=1, source_target_pairs={{8,0},{16,8},{24,16},{0,24},{9,1},{17,9},{25,17},{1,25},{10,2},{18... | collective-permute-start | bytes 393224 | tf_op jit(solution)/shard_map/ppermute | solution.py:46
  92.5 15.2 %collective-permute-start.4 = (bf16[4,128,128]{2,1,0:T(8,128)(2,1)S(1)}, bf16[4,128,128]{2,1,0:T(8,128)(2,1)S(1)}, u32[]{:S(2)}, u32[]{:S(2)}) collective-permute-start(bf16[4,128,128]{2,1,0:T(8,128)(2,1)S(1)} %shard_map.73.refs_0_), channel_id=1, source_target_pairs={{16,0},{24,8},{0,16},{8,24},{17,1},{25,9},{1,17},{9,25},{18,2},{26... | collective-permute-start | bytes 393224 | tf_op jit(solution)/shard_map/ppermute | solution.py:46
  97.7 15.7 %collective-permute-start.5 = (bf16[4,128,128]{2,1,0:T(8,128)(2,1)S(1)}, bf16[4,128,128]{2,1,0:T(8,128)(2,1)S(1)}, u32[]{:S(2)}, u32[]{:S(2)}) collective-permute-start(bf16[4,128,128]{2,1,0:T(8,128)(2,1)S(1)} %shard_map.73.refs_0_), channel_id=1, source_target_pairs={{24,0},{0,8},{8,16},{16,24},{25,1},{1,9},{9,17},{17,25},{26,2},{2,... | collective-permute-start | bytes 393224 | tf_op jit(solution)/shard_map/ppermute | solution.py:46
  114.1 14.3 %collective-permute-start.10 = (bf16[16,64,128]{2,1,0:T(8,128)(2,1)}, bf16[16,64,128]{2,1,0:T(8,128)(2,1)}, u32[]{:S(2)}, u32[]{:S(2)}) collective-permute-start(bf16[16,64,128]{2,1,0:T(8,128)(2,1)} %get-tuple-element.14.refs_0_), channel_id=1, source_target_pairs={{256,0},{384,128},{0,256},{128,384},{257,1},{385,129},{1,257},{129... | collective-permute-start | bytes 786440 | tf_op jit(solution)/shard_map/ppermute | solution.py:46
  116.9 28.0 %collective-permute-start.6 = (bf16[17,64,128]{2,1,0:T(8,128)(2,1)S(1)}, bf16[17,64,128]{2,1,0:T(8,128)(2,1)S(1)}, u32[]{:S(2)}, u32[]{:S(2)}) collective-permute-start(bf16[17,64,128]{2,1,0:T(8,128)(2,1)S(1)} %get-tuple-element.12.refs_0_), channel_id=1, source_target_pairs={{2,0},{4,2},{6,4},{0,6},{3,1},{5,3},{7,5},{1,7},{10,8},{12,10},{14... | collective-permute-start | bytes 835592 | tf_op jit(solution)/shard_map/ppermute | solution.py:46
  120.0 28.1 %collective-permute-start.7 = (bf16[17,64,128]{2,1,0:T(8,128)(2,1)S(1)}, bf16[17,64,128]{2,1,0:T(8,128)(2,1)S(1)}, u32[]{:S(2)}, u32[]{:S(2)}) collective-permute-start(bf16[17,64,128]{2,1,0:T(8,128)(2,1)S(1)} %get-tuple-element.12.refs_0_), channel_id=1, source_target_pairs={{4,0},{6,2},{0,4},{2,6},{5,1},{7,3},{1,5},{3,7},{12,8},{14,10},{8,... | collective-permute-start | bytes 835592 | tf_op jit(solution)/shard_map/ppermute | solution.py:46
  123.0 25.8 %collective-permute-start.8 = (bf16[17,64,128]{2,1,0:T(8,128)(2,1)S(1)}, bf16[17,64,128]{2,1,0:T(8,128)(2,1)S(1)}, u32[]{:S(2)}, u32[]{:S(2)}) collective-permute-start(bf16[17,64,128]{2,1,0:T(8,128)(2,1)S(1)} %get-tuple-element.12.refs_0_), channel_id=1, source_target_pairs={{6,0},{0,2},{2,4},{4,6},{7,1},{1,3},{3,5},{5,7},{14,8},{8,10},{10,... | collective-permute-start | bytes 835592 | tf_op jit(solution)/shard_map/ppermute | solution.py:46
  125.4 8.8 %collective-permute-start.11 = (bf16[16,64,128]{2,1,0:T(8,128)(2,1)}, bf16[16,64,128]{2,1,0:T(8,128)(2,1)}, u32[]{:S(2)}, u32[]{:S(2)}) collective-permute-start(bf16[16,64,128]{2,1,0:T(8,128)(2,1)} %get-tuple-element.14.refs_0_), channel_id=1, source_target_pairs={{384,0},{0,128},{128,256},{256,384},{385,1},{1,129},{129,257},{257... | collective-permute-start | bytes 786440 | tf_op jit(solution)/shard_map/ppermute | solution.py:46
  128.3 7.7 %collective-permute-start.9 = (bf16[16,64,128]{2,1,0:T(8,128)(2,1)}, bf16[16,64,128]{2,1,0:T(8,128)(2,1)}, u32[]{:S(2)}, u32[]{:S(2)}) collective-permute-start(bf16[16,64,128]{2,1,0:T(8,128)(2,1)} %get-tuple-element.14.refs_0_), channel_id=1, source_target_pairs={{128,0},{256,128},{384,256},{0,384},{129,1},{257,129},{385,257},{1... | collective-permute-start | bytes 786440 | tf_op jit(solution)/shard_map/ppermute | solution.py:46
  138.4 34.1 %collective-permute-start.12 = (bf16[16,64,512]{2,1,0:T(8,128)(2,1)}, bf16[16,64,512]{2,1,0:T(8,128)(2,1)}, u32[]{:S(2)}, u32[]{:S(2)}) collective-permute-start(bf16[16,64,512]{2,1,0:T(8,128)(2,1)} %shard_map.75.refs_0_), channel_id=1, source_target_pairs={{2,0},{4,2},{6,4},{0,6},{3,1},{5,3},{7,5},{1,7},{10,8},{12,10},{14... | collective-permute-start | bytes 3145736 | tf_op jit(solution)/shard_map/ppermute | solution.py:46
  143.0 32.5 %collective-permute-start.13 = (bf16[16,64,512]{2,1,0:T(8,128)(2,1)}, bf16[16,64,512]{2,1,0:T(8,128)(2,1)}, u32[]{:S(2)}, u32[]{:S(2)}) collective-permute-start(bf16[16,64,512]{2,1,0:T(8,128)(2,1)} %shard_map.75.refs_0_), channel_id=1, source_target_pairs={{4,0},{6,2},{0,4},{2,6},{5,1},{7,3},{1,5},{3,7},{12,8},{14,10},{8,... | collective-permute-start | bytes 3145736 | tf_op jit(solution)/shard_map/ppermute | solution.py:46
  144.9 0.7 copy-start.2
  145.6 48.6 %collective-permute-start.14 = (bf16[16,64,512]{2,1,0:T(8,128)(2,1)}, bf16[16,64,512]{2,1,0:T(8,128)(2,1)}, u32[]{:S(2)}, u32[]{:S(2)}) collective-permute-start(bf16[16,64,512]{2,1,0:T(8,128)(2,1)} %shard_map.75.refs_0_), channel_id=1, source_target_pairs={{6,0},{0,2},{2,4},{4,6},{7,1},{1,3},{3,5},{5,7},{14,8},{8,10},{10,... | collective-permute-start | bytes 3145736 | tf_op jit(solution)/shard_map/ppermute | solution.py:46
  148.1 0.7 copy-start.4
  148.8 0.7 copy-start.6
  149.5 1.0 copy-start.3
  150.5 1.0 copy-start.5
  151.5 1.0 copy-start.7
  152.6 70.7 %collective-permute-start.16 = (bf16[1024,512]{1,0:T(8,128)(2,1)S(1)}, bf16[1024,512]{1,0:T(8,128)(2,1)}, u32[]{:S(2)}, u32[]{:S(2)}) collective-permute-start(bf16[1024,512]{1,0:T(8,128)(2,1)S(1)} %bitcast.25), channel_id=1, source_target_pairs={{128,0},{256,128},{384,256},{0,384},{129,1},{257,129},{385,257},{1... | collective-permute-start | bytes 3145736 | tf_op jit(solution)/shard_map/ppermute | solution.py:46
  157.0 66.4 %collective-permute-start.17 = (bf16[1024,512]{1,0:T(8,128)(2,1)S(1)}, bf16[1024,512]{1,0:T(8,128)(2,1)}, u32[]{:S(2)}, u32[]{:S(2)}) collective-permute-start(bf16[1024,512]{1,0:T(8,128)(2,1)S(1)} %bitcast.26), channel_id=1, source_target_pairs={{256,0},{384,128},{0,256},{128,384},{257,1},{385,129},{1,257},{129... | collective-permute-start | bytes 3145736 | tf_op jit(solution)/shard_map/ppermute | solution.py:46
  163.9 1.6 copy-start.1
  167.5 44.6 %all-to-all-start.2 = ((bf16[4,32,32,256]{3,2,1,0:T(8,128)(2,1)}), bf16[4,32,32,256]{3,2,1,0:T(8,128)(2,1)}, u32[]{:S(2)}, u32[]{:S(2)}) async-start(bf16[4,32,32,256]{3,2,1,0:T(8,128)(2,1)} %shard_map.77), calls=%async_computation.2 | async-start | bytes 4194304 | tf_op jit(solution)/shard_map/all_to_all | solution.py:365
  172.6 50.8 %collective-permute-start.18 = (bf16[1024,512]{1,0:T(8,128)(2,1)S(1)}, bf16[1024,512]{1,0:T(8,128)(2,1)}, u32[]{:S(2)}, u32[]{:S(2)}) collective-permute-start(bf16[1024,512]{1,0:T(8,128)(2,1)S(1)} %bitcast.27), channel_id=1, source_target_pairs={{384,0},{0,128},{128,256},{256,384},{385,1},{1,129},{129,257},{257... | collective-permute-start | bytes 3145736 | tf_op jit(solution)/shard_map/ppermute | solution.py:46
  216.2 8.2 %collective-permute-start.15 = (bf16[256,512]{1,0:T(8,128)(2,1)S(1)}, bf16[256,512]{1,0:T(8,128)(2,1)S(1)}, u32[]{:S(2)}, u32[]{:S(2)}) collective-permute-start(bf16[256,512]{1,0:T(8,128)(2,1)S(1)} %shard_map.80.m_ref), channel_id=1, source_target_pairs={{1,0},{0,1},{3,2},{2,3},{5,4},{4,5},{7,6},{6,7},{9,8},{8,9},{11,10... | collective-permute-start | bytes 786440 | tf_op jit(solution)/shard_map/ppermute | solution.py:46
Sparse Core Ops, SparseCore 0:
  67.2 67.1 all-gather.1

commit v9 on v8

--- a/solution.py
+++ b/solution.py
@@ -147,12 +147,25 @@
     small = both // 2
     deep = planes * wide * small
 
-    def kernel(t_ref, w_ref, o_ref):
+    chunk = 4
+
+    def kernel(t_ref, w_hbm, o_ref, w_ref, sems):
+        copies = [
+            pltpu.make_async_copy(
+                w_hbm.at[:, :, pl.ds(i * chunk, chunk)], w_ref.at[i], sems.at[i]
+            )
+            for i in range(tall // chunk)
+        ]
+        for copy in copies:
+            copy.start()
         total = jnp.zeros(o_ref.shape, F32)
+        lines = [(x, y) for y in range(wide) for x in range(planes)]
         for z in range(tall):
-            lines = [(x, y) for y in range(wide) for x in range(planes)]
-            keys = jnp.concatenate([w_ref[x, y, z, :small] for x, y in lines], axis=0)
-            values = jnp.concatenate([w_ref[x, y, z, small:] for x, y in lines], axis=0)
+            i, j = z // chunk, z % chunk
+            if j == 0:
+                copies[i].wait()
+            keys = jnp.concatenate([w_ref[i, x, y, j, :small] for x, y in lines], axis=0)
+            values = jnp.concatenate([w_ref[i, x, y, j, small:] for x, y in lines], axis=0)
             total += jnp.dot(
                 t_ref[:, z * deep : (z + 1) * deep],
                 jnp.concatenate([keys, values], axis=1),
@@ -160,9 +173,21 @@
             )
         o_ref[...] = total.astype(BF16)
 
-    out = jax.ShapeDtypeStruct((tokens.shape[0], 2 * HD), BF16)
-    flops = 2 * tokens.size * 2 * HD
-    return call(kernel, out, tokens, every, flops=flops)
+    return pl.pallas_call(
+        kernel,
+        out_shape=jax.ShapeDtypeStruct((tokens.shape[0], 2 * HD), BF16),
+        in_specs=[pl.BlockSpec(memory_space=pltpu.VMEM), pl.BlockSpec(memory_space=pl.ANY)],
+        out_specs=pl.BlockSpec(memory_space=pltpu.VMEM),
+        scratch_shapes=[
+            pltpu.VMEM((tall // chunk, planes, wide, chunk, both, HD), BF16),
+            pltpu.SemaphoreType.DMA((tall // chunk,)),
+        ],
+        compiler_params=pltpu.CompilerParams(vmem_limit_bytes=40 << 20),
+        cost_estimate=pl.CostEstimate(
+            flops=4 * tokens.size * HD, bytes_accessed=0, transcendentals=0
+        ),
+        name="project_pair",
+    )(tokens, every)
 
 
 def project_queries(tokens, pieces, at, tile):
@@ -305,22 +330,38 @@
     half = rows // 2
 
     def kernel(p_ref, m_ref, t_ref, *refs):
-        for s in range(n):
+        o_ref, w_s, sems = refs[n:]
+        copies = [pltpu.make_async_copy(refs[s], w_s.at[s], sems.at[s]) for s in range(n)]
+        for copy in copies:
+            copy.start()
+        for s, copy in enumerate(copies):
+            copy.wait()
             first = pl.multiple_of(((p_ref[0] + s) % n) * width, width)
-            refs[n][:, pl.ds(first, width)] = (
+            o_ref[:, pl.ds(first, width)] = (
                 jnp.dot(
-                    m_ref[...], refs[s][pl.ds(p_ref[1] * half, half)], preferred_element_type=F32
+                    m_ref[...], w_s[s, pl.ds(p_ref[1] * half, half)], preferred_element_type=F32
                 )
                 + jnp.dot(
                     t_ref[...],
-                    refs[s][pl.ds((1 - p_ref[1]) * half, half)],
+                    w_s[s, pl.ds((1 - p_ref[1]) * half, half)],
                     preferred_element_type=F32,
                 )
             ).astype(BF16)
 
-    out = jax.ShapeDtypeStruct((mine.shape[0], n * width), BF16)
-    flops = 4 * mine.size * n * width
-    return call(kernel, out, places, mine, other, *pieces, flops=flops)
+    vmem = pl.BlockSpec(memory_space=pltpu.VMEM)
+    return pl.pallas_call(
+        kernel,
+        out_shape=jax.ShapeDtypeStruct((mine.shape[0], n * width), BF16),
+        in_specs=[pl.BlockSpec(memory_space=pltpu.SMEM), vmem, vmem]
+        + [pl.BlockSpec(memory_space=pl.ANY)] * n,
+        out_specs=vmem,
+        scratch_shapes=[pltpu.VMEM((n, rows, width), BF16), pltpu.SemaphoreType.DMA((n,))],
+        compiler_params=pltpu.CompilerParams(vmem_limit_bytes=40 << 20),
+        cost_estimate=pl.CostEstimate(
+            flops=4 * mine.size * n * width, bytes_accessed=0, transcendentals=0
+        ),
+        name="mix",
+    )(places, mine, other, *pieces)
 
 
 def body(tokens, query_weight, key_weight, value_weight, out_weight, chosen, live_length):

time: 236 us -> 237 us (level)
    pallas_call x0 -> x2, Pallas kernels: none -> 6.43 us  [the longest x1 4.16 us: mix(): pl.pallas_call(kernel, out_shape=jax.ShapeDtypeStruct((mine.shape[0], n *...]
    pallas_call x10 -> x8, Pallas kernels: 19.3 us -> 13.8 us  [call(): pl.pallas_call(kernel, out_shape=out_shape, in_specs=spaces, out_specs=ja...]
where the time goes in v9:
time: 237 us; the launch traced here: 236 us
  starting transfers between devices  71.3 us (30%)
  waiting for transfers between devices  57.8 us (24%)
  blocking collectives  57.1 us (24%)
  Pallas kernels  21.9 us (9%)
  between operations  14.6 us (6%)
  local copies, waits for them, and re-layouts  8.25 us (3%)
  other arithmetic  5.39 us (2%)
    ppermute x19, starting transfers between devices, from_ahead(): return lax.ppermute(x, axis, [((i + step) % n, i) for i in range(n)])  66.9 us
    ppermute x19, waiting for transfers between devices, from_ahead(): return lax.ppermute(x, axis, [((i + step) % n, i) for i in range(n)])  43.4 us
    all_to_all x1, blocking collectives, copy_for_each(): lax.all_to_all(jnp.broadcast_to(shard[None], (count, *shard.shape)), axis...  31.3 us
    all_to_all x1, blocking collectives, body(): column = lax.all_to_all(cargo, TALL, 0, 0, tiled=True)  25.8 us
    all_to_all x1, waiting for transfers between devices, body(): lax.all_to_all(outgoing, 'y', split_axis=0, concat_axis=0, tiled=True)  14.4 us
    pallas_call x8, Pallas kernels, call(): pl.pallas_call(kernel, out_shape=out_shape, in_specs=spaces, out_specs=ja...  13.8 us
    unnamed x20, local copies, waits for them, and re-layouts  6.58 us
  transfers between devices with their start and end apart: 21, of which 9 were waited for; matrix products, arithmetic and copies ran while one was open for 3% of the time, Pallas kernels for 6%

profile of v9, /device:TPU:65, one launch (start us, length us, event | category | flops | bytes accessed | tf_op | source)
XLA Modules:
  0.0 236.4 jit_solution(10833445764494582601)
XLA Ops:
  8.2 25.8 %all_to_all.15 = bf16[16,32,128]{2,1,0:T(8,128)(2,1)S(1)} all-to-all(bf16[16,32,128]{2,1,0:T(8,128)(2,1)} %get-tuple-element.16), channel_id=1, replica_groups=mesh['dp'=4,'zh'=4,'zl'=4,'y'=4,'tp'=2] {'zh','zl'}, dimensions={0} | all-to-all | bytes 262144 | tf_op jit(solution)/shard_map/all_to_all | solution.py:377
  34.4 31.3 %all_to_all.16 = bf16[16,16,32,128]{3,2,1,0:T(8,128)(2,1)S(1)} all-to-all(bf16[16,16,32,128]{3,2,1,0:T(8,128)(2,1)S(1)} %broadcast_in_dim.95), channel_id=1, replica_groups=mesh['dp'=4,'zh'=4,'zl'=4,'y'=4,'tp'=2] {'dp','y'}, dimensions={0} | all-to-all | bytes 4194304 | tf_op jit(solution)/shard_map/all_to_all | solution.py:39
  65.7 2.3 project_pair.1
  68.0 4.2 %collective-permute-start = (bf16[128,128]{1,0:T(8,128)(2,1)S(1)}, bf16[128,128]{1,0:T(8,128)(2,1)S(1)}, u32[]{:S(2)}, u32[]{:S(2)}) collective-permute-start(bf16[128,128]{1,0:T(8,128)(2,1)S(1)} %copy-done.9), channel_id=1, source_target_pairs={{32,0},{64,32},{96,64},{0,96},{33,1},{65,33},{97,65},{1,97},{34,2}... | collective-permute-start | bytes 98312 | tf_op jit(solution)/shard_map/ppermute | solution.py:46
  72.3 8.7 %collective-permute-start.1 = (bf16[128,128]{1,0:T(8,128)(2,1)S(1)}, bf16[128,128]{1,0:T(8,128)(2,1)S(1)}, u32[]{:S(2)}, u32[]{:S(2)}) collective-permute-start(bf16[128,128]{1,0:T(8,128)(2,1)S(1)} %copy-done.9), channel_id=1, source_target_pairs={{64,0},{96,32},{0,64},{32,96},{65,1},{97,33},{1,65},{33,97},{66,2}... | collective-permute-start | bytes 98312 | tf_op jit(solution)/shard_map/ppermute | solution.py:46
  81.0 3.3 %collective-permute-start.2 = (bf16[128,128]{1,0:T(8,128)(2,1)S(1)}, bf16[128,128]{1,0:T(8,128)(2,1)S(1)}, u32[]{:S(2)}, u32[]{:S(2)}) collective-permute-start(bf16[128,128]{1,0:T(8,128)(2,1)S(1)} %copy-done.9), channel_id=1, source_target_pairs={{96,0},{0,32},{32,64},{64,96},{97,1},{1,33},{33,65},{65,97},{98,2}... | collective-permute-start | bytes 98312 | tf_op jit(solution)/shard_map/ppermute | solution.py:46
  85.8 5.6 %collective-permute-done.2.refs_3_ = bf16[128,128]{1,0:T(8,128)(2,1)S(1)} collective-permute-done((bf16[128,128]{1,0:T(8,128)(2,1)S(1)}, bf16[128,128]{1,0:T(8,128)(2,1)S(1)}, u32[]{:S(2)}, u32[]{:S(2)}) %collective-permute-start.2) | collective-permute-done | bytes 32800 | tf_op jit(solution)/shard_map/ppermute | solution.py:46
  93.4 5.2 %collective-permute-start.4 = (bf16[4,128,128]{2,1,0:T(8,128)(2,1)S(1)}, bf16[4,128,128]{2,1,0:T(8,128)(2,1)S(1)}, u32[]{:S(2)}, u32[]{:S(2)}) collective-permute-start(bf16[4,128,128]{2,1,0:T(8,128)(2,1)S(1)} %shard_map.73.refs_0_), channel_id=1, source_target_pairs={{16,0},{24,8},{0,16},{8,24},{17,1},{25,9},{1,17},{9,25},{18,2},{26... | collective-permute-start | bytes 393224 | tf_op jit(solution)/shard_map/ppermute | solution.py:46
  98.6 1.9 collective-permute-start.5
  100.7 7.8 %collective-permute-done.4.refs_2_ = bf16[4,128,128]{2,1,0:T(8,128)(2,1)S(1)} collective-permute-done((bf16[4,128,128]{2,1,0:T(8,128)(2,1)S(1)}, bf16[4,128,128]{2,1,0:T(8,128)(2,1)S(1)}, u32[]{:S(2)}, u32[]{:S(2)}) %collective-permute-start.4) | collective-permute-done | bytes 131104 | tf_op jit(solution)/shard_map/ppermute | solution.py:46
  108.5 5.7 %collective-permute-done.5.refs_3_ = bf16[4,128,128]{2,1,0:T(8,128)(2,1)S(1)} collective-permute-done((bf16[4,128,128]{2,1,0:T(8,128)(2,1)S(1)}, bf16[4,128,128]{2,1,0:T(8,128)(2,1)S(1)}, u32[]{:S(2)}, u32[]{:S(2)}) %collective-permute-start.5) | collective-permute-done | bytes 131104 | tf_op jit(solution)/shard_map/ppermute | solution.py:46
  115.0 2.1 collective-permute-start.10
  117.8 3.1 %collective-permute-start.6 = (bf16[17,64,128]{2,1,0:T(8,128)(2,1)S(1)}, bf16[17,64,128]{2,1,0:T(8,128)(2,1)S(1)}, u32[]{:S(2)}, u32[]{:S(2)}) collective-permute-start(bf16[17,64,128]{2,1,0:T(8,128)(2,1)S(1)} %get-tuple-element.12.refs_0_), channel_id=1, source_target_pairs={{2,0},{4,2},{6,4},{0,6},{3,1},{5,3},{7,5},{1,7},{10,8},{12,10},{14... | collective-permute-start | bytes 835592 | tf_op jit(solution)/shard_map/ppermute | solution.py:46
  120.9 3.0 %collective-permute-start.7 = (bf16[17,64,128]{2,1,0:T(8,128)(2,1)S(1)}, bf16[17,64,128]{2,1,0:T(8,128)(2,1)S(1)}, u32[]{:S(2)}, u32[]{:S(2)}) collective-permute-start(bf16[17,64,128]{2,1,0:T(8,128)(2,1)S(1)} %get-tuple-element.12.refs_0_), channel_id=1, source_target_pairs={{4,0},{6,2},{0,4},{2,6},{5,1},{7,3},{1,5},{3,7},{12,8},{14,10},{8,... | collective-permute-start | bytes 835592 | tf_op jit(solution)/shard_map/ppermute | solution.py:46
  124.0 2.3 collective-permute-start.8
  126.3 3.0 %collective-permute-start.11 = (bf16[16,64,128]{2,1,0:T(8,128)(2,1)}, bf16[16,64,128]{2,1,0:T(8,128)(2,1)}, u32[]{:S(2)}, u32[]{:S(2)}) collective-permute-start(bf16[16,64,128]{2,1,0:T(8,128)(2,1)} %get-tuple-element.14.refs_0_), channel_id=1, source_target_pairs={{384,0},{0,128},{128,256},{256,384},{385,1},{1,129},{129,257},{257... | collective-permute-start | bytes 786440 | tf_op jit(solution)/shard_map/ppermute | solution.py:46
  129.3 3.5 %collective-permute-start.9 = (bf16[16,64,128]{2,1,0:T(8,128)(2,1)}, bf16[16,64,128]{2,1,0:T(8,128)(2,1)}, u32[]{:S(2)}, u32[]{:S(2)}) collective-permute-start(bf16[16,64,128]{2,1,0:T(8,128)(2,1)} %get-tuple-element.14.refs_0_), channel_id=1, source_target_pairs={{128,0},{256,128},{384,256},{0,384},{129,1},{257,129},{385,257},{1... | collective-permute-start | bytes 786440 | tf_op jit(solution)/shard_map/ppermute | solution.py:46
  137.0 2.3 shard_map.75.refs_0_
  139.4 4.6 %collective-permute-start.12 = (bf16[16,64,512]{2,1,0:T(8,128)(2,1)}, bf16[16,64,512]{2,1,0:T(8,128)(2,1)}, u32[]{:S(2)}, u32[]{:S(2)}) collective-permute-start(bf16[16,64,512]{2,1,0:T(8,128)(2,1)} %shard_map.75.refs_0_), channel_id=1, source_target_pairs={{2,0},{4,2},{6,4},{0,6},{3,1},{5,3},{7,5},{1,7},{10,8},{12,10},{14... | collective-permute-start | bytes 3145736 | tf_op jit(solution)/shard_map/ppermute | solution.py:46
  143.9 1.9 collective-permute-start.13
  146.6 2.5 %collective-permute-start.14 = (bf16[16,64,512]{2,1,0:T(8,128)(2,1)}, bf16[16,64,512]{2,1,0:T(8,128)(2,1)}, u32[]{:S(2)}, u32[]{:S(2)}) collective-permute-start(bf16[16,64,512]{2,1,0:T(8,128)(2,1)} %shard_map.75.refs_0_), channel_id=1, source_target_pairs={{6,0},{0,2},{2,4},{4,6},{7,1},{1,3},{3,5},{5,7},{14,8},{8,10},{10,... | collective-permute-start | bytes 3145736 | tf_op jit(solution)/shard_map/ppermute | solution.py:46
  153.6 4.3 %collective-permute-start.16 = (bf16[1024,512]{1,0:T(8,128)(2,1)S(1)}, bf16[1024,512]{1,0:T(8,128)(2,1)}, u32[]{:S(2)}, u32[]{:S(2)}) collective-permute-start(bf16[1024,512]{1,0:T(8,128)(2,1)S(1)} %bitcast.25), channel_id=1, source_target_pairs={{128,0},{256,128},{384,256},{0,384},{129,1},{257,129},{385,257},{1... | collective-permute-start | bytes 3145736 | tf_op jit(solution)/shard_map/ppermute | solution.py:46
  157.9 2.6 %collective-permute-start.17 = (bf16[1024,512]{1,0:T(8,128)(2,1)S(1)}, bf16[1024,512]{1,0:T(8,128)(2,1)}, u32[]{:S(2)}, u32[]{:S(2)}) collective-permute-start(bf16[1024,512]{1,0:T(8,128)(2,1)S(1)} %bitcast.26), channel_id=1, source_target_pairs={{256,0},{384,128},{0,256},{128,384},{257,1},{385,129},{1,257},{129... | collective-permute-start | bytes 3145736 | tf_op jit(solution)/shard_map/ppermute | solution.py:46
  166.6 2.0 shard_map.76
  168.6 4.4 %all-to-all-start.2 = ((bf16[4,32,32,256]{3,2,1,0:T(8,128)(2,1)}), bf16[4,32,32,256]{3,2,1,0:T(8,128)(2,1)}, u32[]{:S(2)}, u32[]{:S(2)}) async-start(bf16[4,32,32,256]{3,2,1,0:T(8,128)(2,1)} %shard_map.76), calls=%async_computation.2 | async-start | bytes 4194304 | tf_op jit(solution)/shard_map/all_to_all | solution.py:406
  173.6 1.9 collective-permute-start.18
  176.5 18.7 %collective-permute-done.14.refs_3_ = bf16[16,64,512]{2,1,0:T(8,128)(2,1)} collective-permute-done((bf16[16,64,512]{2,1,0:T(8,128)(2,1)}, bf16[16,64,512]{2,1,0:T(8,128)(2,1)}, u32[]{:S(2)}, u32[]{:S(2)}) %collective-permute-start.14) | collective-permute-done | bytes 1048608 | tf_op jit(solution)/shard_map/ppermute | solution.py:46
  195.2 3.7 %shard_map.77.q_ref = bf16[256,512]{1,0:T(8,128)(2,1)S(1)} custom-call(s32[1]{0:T(128)} %bitcast.9.at_ref, bf16[256,4096]{1,0:T(8,128)(2,1)S(1)} %copy-done, bf16[16,64,512]{2,1,0:T(8,128)(2,1)} %shard_map.75.refs_0_, bf16[16,64,512]{2,1,0:T(8,128)(2,1)} %collective-permute-done.12.refs_1_, bf16[16,64,512]{2,1,0:T(8,128)(2,1)} %collective-permute-done.13.refs_2_, ...), custom_call_target="tpu_custom_call" | custom-call | flops 1073741824 | tf_op jit(solution)/shard_map/pallas_call | solution.py:26
  198.9 14.4 %all-to-all-done.2 = bf16[4,32,32,256]{3,2,1,0:T(8,128)(2,1)} async-done(((bf16[4,32,32,256]{3,2,1,0:T(8,128)(2,1)}), bf16[4,32,32,256]{3,2,1,0:T(8,128)(2,1)}, u32[]{:S(2)}, u32[]{:S(2)}) %all-to-all-start.2) | async-done | bytes 2097184 | tf_op jit(solution)/shard_map/all_to_all | solution.py:406
  213.3 4.1 %shard_map.79.m_ref = bf16[256,512]{1,0:T(8,128)(2,1)S(1)} custom-call(s32[2]{0:T(128)S(1)} %pad_add_fusion.1.f_ref, s32[8,16]{1,0:T(8,128)S(1)} %fusion.8.p_ref, bf16[256,512]{1,0:T(8,128)(2,1)S(1)} %shard_map.77.q_ref, bf16[128,32,256]{2,1,0:T(8,128)(2,1)} %bitcast.16.in_ref, bf16[8,32,256]{2,1,0:T(8,128)(2,1)} %bitcast.14.own_ref, ...), custom_call_target="tpu_custom_call" | custom-call | flops 268435456 | tf_op jit(solution)/shard_map/pallas_call | solution.py:26
  217.4 6.8 %collective-permute-start.15 = (bf16[256,512]{1,0:T(8,128)(2,1)S(1)}, bf16[256,512]{1,0:T(8,128)(2,1)S(1)}, u32[]{:S(2)}, u32[]{:S(2)}) collective-permute-start(bf16[256,512]{1,0:T(8,128)(2,1)S(1)} %shard_map.79.m_ref), channel_id=1, source_target_pairs={{1,0},{0,1},{3,2},{2,3},{5,4},{4,5},{7,6},{6,7},{9,8},{8,9},{11,10... | collective-permute-start | bytes 786440 | tf_op jit(solution)/shard_map/ppermute | solution.py:46
  225.3 4.2 %mix.1 = bf16[256,2048]{1,0:T(8,128)(2,1)} custom-call(s32[2]{0:T(128)S(1)} %pad_add_fusion.p_ref, bf16[256,512]{1,0:T(8,128)(2,1)S(1)} %shard_map.79.m_ref, bf16[256,512]{1,0:T(8,128)(2,1)S(1)} %collective-permute-done.15.t_ref, bf16[1024,512]{1,0:T(8,128)(2,1)S(1)} %bitcast.28, bf16[1024,512]{1,0:T(8,128)(2,1)} %collective-permute-done.16.refs_1_, ...), custom_call_target="tpu_custom_call" | custom-call | flops 1073741824 | tf_op jit(solution)/shard_map/mix/pallas_call | solution.py:352
  (93 shorter events, 24.5 us)
Async XLA Ops:
  6.5 158.4 %all-gather.2.cloned.1.call-start = ((), (), s32[]{:S(2)}) async-start(), calls=%async_computation.3 | async-start | bytes 2228224 | tf_op jit(solution)/shard_map/all_gather | solution.py:384
  34.4 31.3 %copy-start = (bf16[256,4096]{1,0:T(8,128)(2,1)S(1)}, bf16[256,4096]{1,0:T(8,128)(2,1)}, u32[]{:S(2)}) copy-start(bf16[256,4096]{1,0:T(8,128)(2,1)} %t_ref.3) | copy-start | bytes 6291460
  65.7 2.3 copy-start.9
  65.7 18.7 %copy-start.8 = (s32[8,16]{1,0:T(8,128)S(1)}, s32[8,16]{1,0:T(8,128)}, u32[]{:S(2)}) copy-start(s32[8,16]{1,0:T(8,128)} %c_ref.1) | copy-start | bytes 1540
  68.0 16.4 %collective-permute-start = (bf16[128,128]{1,0:T(8,128)(2,1)S(1)}, bf16[128,128]{1,0:T(8,128)(2,1)S(1)}, u32[]{:S(2)}, u32[]{:S(2)}) collective-permute-start(bf16[128,128]{1,0:T(8,128)(2,1)S(1)} %copy-done.9), channel_id=1, source_target_pairs={{32,0},{64,32},{96,64},{0,96},{33,1},{65,33},{97,65},{1,97},{34,2}... | collective-permute-start | bytes 98312 | tf_op jit(solution)/shard_map/ppermute | solution.py:46
  72.3 13.5 %collective-permute-start.1 = (bf16[128,128]{1,0:T(8,128)(2,1)S(1)}, bf16[128,128]{1,0:T(8,128)(2,1)S(1)}, u32[]{:S(2)}, u32[]{:S(2)}) collective-permute-start(bf16[128,128]{1,0:T(8,128)(2,1)S(1)} %copy-done.9), channel_id=1, source_target_pairs={{64,0},{96,32},{0,64},{32,96},{65,1},{97,33},{1,65},{33,97},{66,2}... | collective-permute-start | bytes 98312 | tf_op jit(solution)/shard_map/ppermute | solution.py:46
  81.0 10.5 %collective-permute-start.2 = (bf16[128,128]{1,0:T(8,128)(2,1)S(1)}, bf16[128,128]{1,0:T(8,128)(2,1)S(1)}, u32[]{:S(2)}, u32[]{:S(2)}) collective-permute-start(bf16[128,128]{1,0:T(8,128)(2,1)S(1)} %copy-done.9), channel_id=1, source_target_pairs={{96,0},{0,32},{32,64},{64,96},{97,1},{1,33},{33,65},{65,97},{98,2}... | collective-permute-start | bytes 98312 | tf_op jit(solution)/shard_map/ppermute | solution.py:46
  91.4 9.3 %collective-permute-start.3 = (bf16[4,128,128]{2,1,0:T(8,128)(2,1)S(1)}, bf16[4,128,128]{2,1,0:T(8,128)(2,1)S(1)}, u32[]{:S(2)}, u32[]{:S(2)}) collective-permute-start(bf16[4,128,128]{2,1,0:T(8,128)(2,1)S(1)} %shard_map.73.refs_0_), channel_id=1, source_target_pairs={{8,0},{16,8},{24,16},{0,24},{9,1},{17,9},{25,17},{1,25},{10,2},{18... | collective-permute-start | bytes 393224 | tf_op jit(solution)/shard_map/ppermute | solution.py:46
  93.4 15.2 %collective-permute-start.4 = (bf16[4,128,128]{2,1,0:T(8,128)(2,1)S(1)}, bf16[4,128,128]{2,1,0:T(8,128)(2,1)S(1)}, u32[]{:S(2)}, u32[]{:S(2)}) collective-permute-start(bf16[4,128,128]{2,1,0:T(8,128)(2,1)S(1)} %shard_map.73.refs_0_), channel_id=1, source_target_pairs={{16,0},{24,8},{0,16},{8,24},{17,1},{25,9},{1,17},{9,25},{18,2},{26... | collective-permute-start | bytes 393224 | tf_op jit(solution)/shard_map/ppermute | solution.py:46
  98.6 15.7 %collective-permute-start.5 = (bf16[4,128,128]{2,1,0:T(8,128)(2,1)S(1)}, bf16[4,128,128]{2,1,0:T(8,128)(2,1)S(1)}, u32[]{:S(2)}, u32[]{:S(2)}) collective-permute-start(bf16[4,128,128]{2,1,0:T(8,128)(2,1)S(1)} %shard_map.73.refs_0_), channel_id=1, source_target_pairs={{24,0},{0,8},{8,16},{16,24},{25,1},{1,9},{9,17},{17,25},{26,2},{2,... | collective-permute-start | bytes 393224 | tf_op jit(solution)/shard_map/ppermute | solution.py:46
  115.0 14.3 %collective-permute-start.10 = (bf16[16,64,128]{2,1,0:T(8,128)(2,1)}, bf16[16,64,128]{2,1,0:T(8,128)(2,1)}, u32[]{:S(2)}, u32[]{:S(2)}) collective-permute-start(bf16[16,64,128]{2,1,0:T(8,128)(2,1)} %get-tuple-element.14.refs_0_), channel_id=1, source_target_pairs={{256,0},{384,128},{0,256},{128,384},{257,1},{385,129},{1,257},{129... | collective-permute-start | bytes 786440 | tf_op jit(solution)/shard_map/ppermute | solution.py:46
  117.8 28.0 %collective-permute-start.6 = (bf16[17,64,128]{2,1,0:T(8,128)(2,1)S(1)}, bf16[17,64,128]{2,1,0:T(8,128)(2,1)S(1)}, u32[]{:S(2)}, u32[]{:S(2)}) collective-permute-start(bf16[17,64,128]{2,1,0:T(8,128)(2,1)S(1)} %get-tuple-element.12.refs_0_), channel_id=1, source_target_pairs={{2,0},{4,2},{6,4},{0,6},{3,1},{5,3},{7,5},{1,7},{10,8},{12,10},{14... | collective-permute-start | bytes 835592 | tf_op jit(solution)/shard_map/ppermute | solution.py:46
  120.9 28.2 %collective-permute-start.7 = (bf16[17,64,128]{2,1,0:T(8,128)(2,1)S(1)}, bf16[17,64,128]{2,1,0:T(8,128)(2,1)S(1)}, u32[]{:S(2)}, u32[]{:S(2)}) collective-permute-start(bf16[17,64,128]{2,1,0:T(8,128)(2,1)S(1)} %get-tuple-element.12.refs_0_), channel_id=1, source_target_pairs={{4,0},{6,2},{0,4},{2,6},{5,1},{7,3},{1,5},{3,7},{12,8},{14,10},{8,... | collective-permute-start | bytes 835592 | tf_op jit(solution)/shard_map/ppermute | solution.py:46
  124.0 25.8 %collective-permute-start.8 = (bf16[17,64,128]{2,1,0:T(8,128)(2,1)S(1)}, bf16[17,64,128]{2,1,0:T(8,128)(2,1)S(1)}, u32[]{:S(2)}, u32[]{:S(2)}) collective-permute-start(bf16[17,64,128]{2,1,0:T(8,128)(2,1)S(1)} %get-tuple-element.12.refs_0_), channel_id=1, source_target_pairs={{6,0},{0,2},{2,4},{4,6},{7,1},{1,3},{3,5},{5,7},{14,8},{8,10},{10,... | collective-permute-start | bytes 835592 | tf_op jit(solution)/shard_map/ppermute | solution.py:46
  126.3 8.8 %collective-permute-start.11 = (bf16[16,64,128]{2,1,0:T(8,128)(2,1)}, bf16[16,64,128]{2,1,0:T(8,128)(2,1)}, u32[]{:S(2)}, u32[]{:S(2)}) collective-permute-start(bf16[16,64,128]{2,1,0:T(8,128)(2,1)} %get-tuple-element.14.refs_0_), channel_id=1, source_target_pairs={{384,0},{0,128},{128,256},{256,384},{385,1},{1,129},{129,257},{257... | collective-permute-start | bytes 786440 | tf_op jit(solution)/shard_map/ppermute | solution.py:46
  129.3 7.7 %collective-permute-start.9 = (bf16[16,64,128]{2,1,0:T(8,128)(2,1)}, bf16[16,64,128]{2,1,0:T(8,128)(2,1)}, u32[]{:S(2)}, u32[]{:S(2)}) collective-permute-start(bf16[16,64,128]{2,1,0:T(8,128)(2,1)} %get-tuple-element.14.refs_0_), channel_id=1, source_target_pairs={{128,0},{256,128},{384,256},{0,384},{129,1},{257,129},{385,257},{1... | collective-permute-start | bytes 786440 | tf_op jit(solution)/shard_map/ppermute | solution.py:46
  139.4 34.2 %collective-permute-start.12 = (bf16[16,64,512]{2,1,0:T(8,128)(2,1)}, bf16[16,64,512]{2,1,0:T(8,128)(2,1)}, u32[]{:S(2)}, u32[]{:S(2)}) collective-permute-start(bf16[16,64,512]{2,1,0:T(8,128)(2,1)} %shard_map.75.refs_0_), channel_id=1, source_target_pairs={{2,0},{4,2},{6,4},{0,6},{3,1},{5,3},{7,5},{1,7},{10,8},{12,10},{14... | collective-permute-start | bytes 3145736 | tf_op jit(solution)/shard_map/ppermute | solution.py:46
  143.9 32.6 %collective-permute-start.13 = (bf16[16,64,512]{2,1,0:T(8,128)(2,1)}, bf16[16,64,512]{2,1,0:T(8,128)(2,1)}, u32[]{:S(2)}, u32[]{:S(2)}) collective-permute-start(bf16[16,64,512]{2,1,0:T(8,128)(2,1)} %shard_map.75.refs_0_), channel_id=1, source_target_pairs={{4,0},{6,2},{0,4},{2,6},{5,1},{7,3},{1,5},{3,7},{12,8},{14,10},{8,... | collective-permute-start | bytes 3145736 | tf_op jit(solution)/shard_map/ppermute | solution.py:46
  145.9 0.7 copy-start.2
  146.6 48.6 %collective-permute-start.14 = (bf16[16,64,512]{2,1,0:T(8,128)(2,1)}, bf16[16,64,512]{2,1,0:T(8,128)(2,1)}, u32[]{:S(2)}, u32[]{:S(2)}) collective-permute-start(bf16[16,64,512]{2,1,0:T(8,128)(2,1)} %shard_map.75.refs_0_), channel_id=1, source_target_pairs={{6,0},{0,2},{2,4},{4,6},{7,1},{1,3},{3,5},{5,7},{14,8},{8,10},{10,... | collective-permute-start | bytes 3145736 | tf_op jit(solution)/shard_map/ppermute | solution.py:46
  149.1 0.7 copy-start.4
  149.8 0.7 copy-start.6
  150.5 1.0 copy-start.3
  151.5 1.0 copy-start.5
  152.4 1.0 copy-start.7
  153.6 70.7 %collective-permute-start.16 = (bf16[1024,512]{1,0:T(8,128)(2,1)S(1)}, bf16[1024,512]{1,0:T(8,128)(2,1)}, u32[]{:S(2)}, u32[]{:S(2)}) collective-permute-start(bf16[1024,512]{1,0:T(8,128)(2,1)S(1)} %bitcast.25), channel_id=1, source_target_pairs={{128,0},{256,128},{384,256},{0,384},{129,1},{257,129},{385,257},{1... | collective-permute-start | bytes 3145736 | tf_op jit(solution)/shard_map/ppermute | solution.py:46
  157.9 66.4 %collective-permute-start.17 = (bf16[1024,512]{1,0:T(8,128)(2,1)S(1)}, bf16[1024,512]{1,0:T(8,128)(2,1)}, u32[]{:S(2)}, u32[]{:S(2)}) collective-permute-start(bf16[1024,512]{1,0:T(8,128)(2,1)S(1)} %bitcast.26), channel_id=1, source_target_pairs={{256,0},{384,128},{0,256},{128,384},{257,1},{385,129},{1,257},{129... | collective-permute-start | bytes 3145736 | tf_op jit(solution)/shard_map/ppermute | solution.py:46
  165.0 1.6 copy-start.1
  168.6 44.7 %all-to-all-start.2 = ((bf16[4,32,32,256]{3,2,1,0:T(8,128)(2,1)}), bf16[4,32,32,256]{3,2,1,0:T(8,128)(2,1)}, u32[]{:S(2)}, u32[]{:S(2)}) async-start(bf16[4,32,32,256]{3,2,1,0:T(8,128)(2,1)} %shard_map.76), calls=%async_computation.2 | async-start | bytes 4194304 | tf_op jit(solution)/shard_map/all_to_all | solution.py:406
  173.6 50.7 %collective-permute-start.18 = (bf16[1024,512]{1,0:T(8,128)(2,1)S(1)}, bf16[1024,512]{1,0:T(8,128)(2,1)}, u32[]{:S(2)}, u32[]{:S(2)}) collective-permute-start(bf16[1024,512]{1,0:T(8,128)(2,1)S(1)} %bitcast.27), channel_id=1, source_target_pairs={{384,0},{0,128},{128,256},{256,384},{385,1},{1,129},{129,257},{257... | collective-permute-start | bytes 3145736 | tf_op jit(solution)/shard_map/ppermute | solution.py:46
  217.4 8.0 %collective-permute-start.15 = (bf16[256,512]{1,0:T(8,128)(2,1)S(1)}, bf16[256,512]{1,0:T(8,128)(2,1)S(1)}, u32[]{:S(2)}, u32[]{:S(2)}) collective-permute-start(bf16[256,512]{1,0:T(8,128)(2,1)S(1)} %shard_map.79.m_ref), channel_id=1, source_target_pairs={{1,0},{0,1},{3,2},{2,3},{5,4},{4,5},{7,6},{6,7},{9,8},{8,9},{11,10... | collective-permute-start | bytes 786440 | tf_op jit(solution)/shard_map/ppermute | solution.py:46
Sparse Core Ops, SparseCore 0:
  68.2 67.2 all-gather.1

commit v10 on v9

--- a/solution.py
+++ b/solution.py
@@ -273,14 +273,14 @@
     return call(kernel, out, asked, at[None], blocks)
 
 
-def attend(queries, incoming, local_blocks, position, key_pos, facts):
+def attend(queries, incoming, local_blocks, position, key_pos, facts, tile):
     rows, width = queries.shape
     heads = width // HD
     far = incoming.shape[0]
     per_dev, nsel = position.shape
     keys = nsel * BLOCK
 
-    def kernel(f_ref, p_ref, q_ref, in_ref, own_ref, kp_ref, o_ref, tab, k_s, v_s):
+    def kernel(f_ref, p_ref, q_ref, in_ref, own_ref, kp_ref, tile_ref, o_ref, tab, k_s, v_s):
         tab[:far] = in_ref[...]
         tab[far:] = own_ref[...]
         for j in range(per_dev):
@@ -315,6 +315,7 @@
         incoming,
         local_blocks,
         key_pos,
+        tile,
         scratch=(
             pltpu.VMEM((far + per_dev, BLOCK, 2 * HD), BF16),
             pltpu.VMEM((2, keys, HD), BF16),
@@ -324,44 +325,47 @@
     )
 
 
-def mix(mine, other, pieces, places):
-    n = len(pieces)
-    rows, width = pieces[0].shape
+def staged(pieces, tile):
+    n = len(pieces)
+
+    def kernel(*refs):
+        for s in range(n):
+            refs[-1][s] = refs[s][...]
+
+    out = jax.ShapeDtypeStruct((n, *pieces[0].shape), BF16)
+    return call(kernel, out, *pieces, tile)
+
+
+def mix(mine, other, weight, places):
+    n, rows, width = weight.shape
     half = rows // 2
 
-    def kernel(p_ref, m_ref, t_ref, *refs):
-        o_ref, w_s, sems = refs[n:]
-        copies = [pltpu.make_async_copy(refs[s], w_s.at[s], sems.at[s]) for s in range(n)]
-        for copy in copies:
-            copy.start()
-        for s, copy in enumerate(copies):
-            copy.wait()
+    def kernel(p_ref, m_ref, t_ref, w_ref, o_ref):
+        for s in range(n):
             first = pl.multiple_of(((p_ref[0] + s) % n) * width, width)
             o_ref[:, pl.ds(first, width)] = (
                 jnp.dot(
-                    m_ref[...], w_s[s, pl.ds(p_ref[1] * half, half)], preferred_element_type=F32
+                    m_ref[...], w_ref[s, pl.ds(p_ref[1] * half, half)], preferred_element_type=F32
                 )
                 + jnp.dot(
                     t_ref[...],
-                    w_s[s, pl.ds((1 - p_ref[1]) * half, half)],
+                    w_ref[s, pl.ds((1 - p_ref[1]) * half, half)],
                     preferred_element_type=F32,
                 )
             ).astype(BF16)
 
-    vmem = pl.BlockSpec(memory_space=pltpu.VMEM)
+    out = jax.ShapeDtypeStruct((mine.shape[0], n * width), BF16)
+    flops = 4 * mine.size * n * width
     return pl.pallas_call(
         kernel,
-        out_shape=jax.ShapeDtypeStruct((mine.shape[0], n * width), BF16),
-        in_specs=[pl.BlockSpec(memory_space=pltpu.SMEM), vmem, vmem]
-        + [pl.BlockSpec(memory_space=pl.ANY)] * n,
-        out_specs=vmem,
-        scratch_shapes=[pltpu.VMEM((n, rows, width), BF16), pltpu.SemaphoreType.DMA((n,))],
+        out_shape=out,
+        in_specs=[pl.BlockSpec(memory_space=pltpu.SMEM)]
+        + [pl.BlockSpec(memory_space=pltpu.VMEM)] * 3,
+        out_specs=pl.BlockSpec(memory_space=pltpu.VMEM),
         compiler_params=pltpu.CompilerParams(vmem_limit_bytes=40 << 20),
-        cost_estimate=pl.CostEstimate(
-            flops=4 * mine.size * n * width, bytes_accessed=0, transcendentals=0
-        ),
+        cost_estimate=pl.CostEstimate(flops=flops, bytes_accessed=0, transcendentals=0),
         name="mix",
-    )(places, mine, other, *pieces)
+    )(places, mine, other, weight)
 
 
 def body(tokens, query_weight, key_weight, value_weight, out_weight, chosen, live_length):
@@ -423,6 +427,7 @@
     facts = jnp.stack([me * rows, live_length[0]]).astype(jnp.int32)
 
     queries = project_queries(tokens, q_pieces, y_at, outgoing[0, 0, :16, :HD])
+    out_full = staged(o_pieces, queries[:16, :HD])
     attended = attend(
         queries,
         incoming.reshape(far, BLOCK, paired.shape[1]),
@@ -430,9 +435,10 @@
         position,
         key_pos,
         facts,
+        out_full[0, :16, :HD],
     )
     other = from_ahead(attended, "tp", 1)
-    return mix(attended, other, o_pieces, jnp.stack([x_at, lax.axis_index("tp")]))
+    return mix(attended, other, out_full, jnp.stack([x_at, lax.axis_index("tp")]))
 
 
 def solution(mesh):

time: 237 us -> 219 us (0.924)
  the two profiles are of different devices: /device:TPU:65 before, /device:TPU:71 now
where the time goes in v10:
time: 219 us; the launch traced here: 218 us
  starting transfers between devices  79.1 us (36%)
  waiting for transfers between devices  53.4 us (24%)
  blocking collectives  25.8 us (12%)
  Pallas kernels  22.5 us (10%)
  local copies, waits for them, and re-layouts  17.4 us (8%)
  between operations  14.6 us (7%)
  other arithmetic  5.39 us (2%)
    ppermute x19, starting transfers between devices, from_ahead(): return lax.ppermute(x, axis, [((i + step) % n, i) for i in range(n)])  67.6 us
    ppermute x19, waiting for transfers between devices, from_ahead(): return lax.ppermute(x, axis, [((i + step) % n, i) for i in range(n)])  32.5 us
    all_to_all x1, blocking collectives, body(): column = lax.all_to_all(cargo, TALL, 0, 0, tiled=True)  25.8 us
    pallas_call x9, Pallas kernels, call(): pl.pallas_call(kernel, out_shape=out_shape, in_specs=spaces, out_specs=ja...  14.9 us
    unnamed x28, local copies, waits for them, and re-layouts  12.4 us
    all_to_all x1, waiting for transfers between devices, body(): lax.all_to_all(outgoing, 'y', split_axis=0, concat_axis=0, tiled=True)  11.2 us
    all_to_all x1, waiting for transfers between devices, copy_for_each(): lax.all_to_all(jnp.broadcast_to(shard[None], (count, *shard.shape)), axis...  9.59 us
    all_to_all x1, starting transfers between devices, copy_for_each(): lax.all_to_all(jnp.broadcast_to(shard[None], (count, *shard.shape)), axis...  7 us
  transfers between devices with their start and end apart: 22, of which 7 were waited for; matrix products, arithmetic and copies ran while one was open for 4% of the time, Pallas kernels for 6%

profile of v10, /device:TPU:71, one launch (start us, length us, event | category | flops | bytes accessed | tf_op | source)
XLA Modules:
  0.0 218.2 jit_solution(17552925153196016236)
XLA Ops:
  8.2 25.8 %all_to_all.15 = bf16[16,32,128]{2,1,0:T(8,128)(2,1)S(1)} all-to-all(bf16[16,32,128]{2,1,0:T(8,128)(2,1)} %get-tuple-element.16), channel_id=1, replica_groups=mesh['dp'=4,'zh'=4,'zl'=4,'y'=4,'tp'=2] {'zh','zl'}, dimensions={0} | all-to-all | bytes 262144 | tf_op jit(solution)/shard_map/all_to_all | solution.py:381
  35.7 7.0 %all-to-all-start.1 = ((bf16[16,16,32,128]{3,2,1,0:T(8,128)(2,1)}), bf16[16,16,32,128]{3,2,1,0:T(8,128)(2,1)}, u32[]{:S(2)}, u32[]{:S(2)}) async-start(bf16[16,16,32,128]{3,2,1,0:T(8,128)(2,1)} %broadcast_in_dim.95), calls=%async_computation.1 | async-start | bytes 4194304 | tf_op jit(solution)/shard_map/all_to_all | solution.py:39
  42.7 4.6 %collective-permute-start = (bf16[128,128]{1,0:T(8,128)(2,1)S(1)}, bf16[128,128]{1,0:T(8,128)(2,1)S(1)}, u32[]{:S(2)}, u32[]{:S(2)}) collective-permute-start(bf16[128,128]{1,0:T(8,128)(2,1)S(1)} %copy-done.13), channel_id=1, source_target_pairs={{32,0},{64,32},{96,64},{0,96},{33,1},{65,33},{97,65},{1,97},{34,2}... | collective-permute-start | bytes 98312 | tf_op jit(solution)/shard_map/ppermute | solution.py:46
  47.4 6.7 %collective-permute-start.1 = (bf16[128,128]{1,0:T(8,128)(2,1)S(1)}, bf16[128,128]{1,0:T(8,128)(2,1)S(1)}, u32[]{:S(2)}, u32[]{:S(2)}) collective-permute-start(bf16[128,128]{1,0:T(8,128)(2,1)S(1)} %copy-done.13), channel_id=1, source_target_pairs={{64,0},{96,32},{0,64},{32,96},{65,1},{97,33},{1,65},{33,97},{66,2}... | collective-permute-start | bytes 98312 | tf_op jit(solution)/shard_map/ppermute | solution.py:46
  54.1 3.6 %collective-permute-start.2 = (bf16[128,128]{1,0:T(8,128)(2,1)S(1)}, bf16[128,128]{1,0:T(8,128)(2,1)S(1)}, u32[]{:S(2)}, u32[]{:S(2)}) collective-permute-start(bf16[128,128]{1,0:T(8,128)(2,1)S(1)} %copy-done.13), channel_id=1, source_target_pairs={{96,0},{0,32},{32,64},{64,96},{97,1},{1,33},{33,65},{65,97},{98,2}... | collective-permute-start | bytes 98312 | tf_op jit(solution)/shard_map/ppermute | solution.py:46
  57.7 9.6 %all-to-all-done.1 = bf16[16,16,32,128]{3,2,1,0:T(8,128)(2,1)} async-done(((bf16[16,16,32,128]{3,2,1,0:T(8,128)(2,1)}), bf16[16,16,32,128]{3,2,1,0:T(8,128)(2,1)}, u32[]{:S(2)}, u32[]{:S(2)}) %all-to-all-start.1) | async-done | bytes 2097184 | tf_op jit(solution)/shard_map/all_to_all | solution.py:39
  67.3 3.2 %project_pair.1 = bf16[256,256]{1,0:T(8,128)(2,1)} custom-call(bf16[256,4096]{1,0:T(8,128)(2,1)S(1)} %copy-done.2, bf16[4,4,16,32,128]{4,3,2,1,0:T(8,128)(2,1)} %bitcast.13.w_hbm), custom_call_target="tpu_custom_call" | custom-call | flops 536870912 | tf_op jit(solution)/shard_map/project_pair/pallas_call | solution.py:176
  70.7 2.3 %collective-permute-start.3 = (bf16[4,128,128]{2,1,0:T(8,128)(2,1)S(1)}, bf16[4,128,128]{2,1,0:T(8,128)(2,1)S(1)}, u32[]{:S(2)}, u32[]{:S(2)}) collective-permute-start(bf16[4,128,128]{2,1,0:T(8,128)(2,1)S(1)} %shard_map.73.refs_0_), channel_id=1, source_target_pairs={{8,0},{16,8},{24,16},{0,24},{9,1},{17,9},{25,17},{1,25},{10,2},{18... | collective-permute-start | bytes 393224 | tf_op jit(solution)/shard_map/ppermute | solution.py:46
  73.1 5.0 %collective-permute-start.4 = (bf16[4,128,128]{2,1,0:T(8,128)(2,1)S(1)}, bf16[4,128,128]{2,1,0:T(8,128)(2,1)S(1)}, u32[]{:S(2)}, u32[]{:S(2)}) collective-permute-start(bf16[4,128,128]{2,1,0:T(8,128)(2,1)S(1)} %shard_map.73.refs_0_), channel_id=1, source_target_pairs={{16,0},{24,8},{0,16},{8,24},{17,1},{25,9},{1,17},{9,25},{18,2},{26... | collective-permute-start | bytes 393224 | tf_op jit(solution)/shard_map/ppermute | solution.py:46
  80.9 8.2 %collective-permute-done.5.refs_3_ = bf16[4,128,128]{2,1,0:T(8,128)(2,1)S(1)} collective-permute-done((bf16[4,128,128]{2,1,0:T(8,128)(2,1)S(1)}, bf16[4,128,128]{2,1,0:T(8,128)(2,1)S(1)}, u32[]{:S(2)}, u32[]{:S(2)}) %collective-permute-start.5) | collective-permute-done | bytes 131104 | tf_op jit(solution)/shard_map/ppermute | solution.py:46
  89.1 2.6 %collective-permute-start.10 = (bf16[16,64,128]{2,1,0:T(8,128)(2,1)S(1)}, bf16[16,64,128]{2,1,0:T(8,128)(2,1)S(1)}, u32[]{:S(2)}, u32[]{:S(2)}) collective-permute-start(bf16[16,64,128]{2,1,0:T(8,128)(2,1)S(1)} %get-tuple-element.14.refs_0_), channel_id=1, source_target_pairs={{256,0},{384,128},{0,256},{128,384},{257,1},{385,129},{1,257},{129... | collective-permute-start | bytes 786440 | tf_op jit(solution)/shard_map/ppermute | solution.py:46
  92.5 6.6 %collective-permute-start.6 = (bf16[17,64,128]{2,1,0:T(8,128)(2,1)S(1)}, bf16[17,64,128]{2,1,0:T(8,128)(2,1)}, u32[]{:S(2)}, u32[]{:S(2)}) collective-permute-start(bf16[17,64,128]{2,1,0:T(8,128)(2,1)S(1)} %get-tuple-element.12.refs_0_), channel_id=1, source_target_pairs={{2,0},{4,2},{6,4},{0,6},{3,1},{5,3},{7,5},{1,7},{10,8},{12,10},{14... | collective-permute-start | bytes 835592 | tf_op jit(solution)/shard_map/ppermute | solution.py:46
  99.2 3.4 %collective-permute-start.7 = (bf16[17,64,128]{2,1,0:T(8,128)(2,1)S(1)}, bf16[17,64,128]{2,1,0:T(8,128)(2,1)}, u32[]{:S(2)}, u32[]{:S(2)}) collective-permute-start(bf16[17,64,128]{2,1,0:T(8,128)(2,1)S(1)} %get-tuple-element.12.refs_0_), channel_id=1, source_target_pairs={{4,0},{6,2},{0,4},{2,6},{5,1},{7,3},{1,5},{3,7},{12,8},{14,10},{8,... | collective-permute-start | bytes 835592 | tf_op jit(solution)/shard_map/ppermute | solution.py:46
  102.6 2.8 %collective-permute-start.8 = (bf16[17,64,128]{2,1,0:T(8,128)(2,1)S(1)}, bf16[17,64,128]{2,1,0:T(8,128)(2,1)}, u32[]{:S(2)}, u32[]{:S(2)}) collective-permute-start(bf16[17,64,128]{2,1,0:T(8,128)(2,1)S(1)} %get-tuple-element.12.refs_0_), channel_id=1, source_target_pairs={{6,0},{0,2},{2,4},{4,6},{7,1},{1,3},{3,5},{5,7},{14,8},{8,10},{10,... | collective-permute-start | bytes 835592 | tf_op jit(solution)/shard_map/ppermute | solution.py:46
  108.0 3.4 %collective-permute-start.9 = (bf16[16,64,128]{2,1,0:T(8,128)(2,1)S(1)}, bf16[16,64,128]{2,1,0:T(8,128)(2,1)S(1)}, u32[]{:S(2)}, u32[]{:S(2)}) collective-permute-start(bf16[16,64,128]{2,1,0:T(8,128)(2,1)S(1)} %get-tuple-element.14.refs_0_), channel_id=1, source_target_pairs={{128,0},{256,128},{384,256},{0,384},{129,1},{257,129},{385,257},{1... | collective-permute-start | bytes 786440 | tf_op jit(solution)/shard_map/ppermute | solution.py:46
  113.8 2.9 %collective-permute-done.9.refs_1_ = bf16[16,64,128]{2,1,0:T(8,128)(2,1)S(1)} collective-permute-done((bf16[16,64,128]{2,1,0:T(8,128)(2,1)S(1)}, bf16[16,64,128]{2,1,0:T(8,128)(2,1)S(1)}, u32[]{:S(2)}, u32[]{:S(2)}) %collective-permute-start.9) | collective-permute-done | bytes 262176 | tf_op jit(solution)/shard_map/ppermute | solution.py:46
  121.4 3.8 %collective-permute-start.12 = (bf16[16,64,512]{2,1,0:T(8,128)(2,1)S(1)}, bf16[16,64,512]{2,1,0:T(8,128)(2,1)}, u32[]{:S(2)}, u32[]{:S(2)}) collective-permute-start(bf16[16,64,512]{2,1,0:T(8,128)(2,1)S(1)} %shard_map.75.refs_0_), channel_id=1, source_target_pairs={{2,0},{4,2},{6,4},{0,6},{3,1},{5,3},{7,5},{1,7},{10,8},{12,10},{14... | collective-permute-start | bytes 3145736 | tf_op jit(solution)/shard_map/ppermute | solution.py:46
  127.1 2.5 %collective-permute-start.14 = (bf16[16,64,512]{2,1,0:T(8,128)(2,1)S(1)}, bf16[16,64,512]{2,1,0:T(8,128)(2,1)}, u32[]{:S(2)}, u32[]{:S(2)}) collective-permute-start(bf16[16,64,512]{2,1,0:T(8,128)(2,1)S(1)} %shard_map.75.refs_0_), channel_id=1, source_target_pairs={{6,0},{0,2},{2,4},{4,6},{7,1},{1,3},{3,5},{5,7},{14,8},{8,10},{10,... | collective-permute-start | bytes 3145736 | tf_op jit(solution)/shard_map/ppermute | solution.py:46
  129.6 2.3 %shard_map.79 = bf16[16,4,16,512]{3,2,1,0:T(8,128)(2,1)} custom-call(s32[1]{0:T(128)} %bitcast.9.at_ref, bf16[17,64,128]{2,1,0:T(8,128)(2,1)S(1)} %get-tuple-element.12.refs_0_, bf16[17,64,128]{2,1,0:T(8,128)(2,1)} %collective-permute-done.6.refs_1_, bf16[17,64,128]{2,1,0:T(8,128)(2,1)} %collective-permute-done.7.refs_2_, ...), custom_call_target="tpu_custom_call" | custom-call | tf_op jit(solution)/shard_map/pallas_call | solution.py:26
  131.9 2.1 collective-permute-start.15
  134.0 2.7 %collective-permute-start.16 = (bf16[1024,512]{1,0:T(8,128)(2,1)}, bf16[1024,512]{1,0:T(8,128)(2,1)}, u32[]{:S(2)}, u32[]{:S(2)}) collective-permute-start(bf16[1024,512]{1,0:T(8,128)(2,1)} %bitcast.17.refs_0_), channel_id=1, source_target_pairs={{256,0},{384,128},{0,256},{128,384},{257,1},{385,129},{1,257},{129... | collective-permute-start | bytes 3145736 | tf_op jit(solution)/shard_map/ppermute | solution.py:46
  145.2 2.1 shard_map.76
  147.2 4.5 %all-to-all-start.2 = ((bf16[4,32,32,256]{3,2,1,0:T(8,128)(2,1)}), bf16[4,32,32,256]{3,2,1,0:T(8,128)(2,1)}, u32[]{:S(2)}, u32[]{:S(2)}) async-start(bf16[4,32,32,256]{3,2,1,0:T(8,128)(2,1)} %shard_map.76), calls=%async_computation.2 | async-start | bytes 4194304 | tf_op jit(solution)/shard_map/all_to_all | solution.py:410
  151.7 3.6 %collective-permute-start.17 = (bf16[1024,512]{1,0:T(8,128)(2,1)}, bf16[1024,512]{1,0:T(8,128)(2,1)S(1)}, u32[]{:S(2)}, u32[]{:S(2)}) collective-permute-start(bf16[1024,512]{1,0:T(8,128)(2,1)} %bitcast.17.refs_0_), channel_id=1, source_target_pairs={{384,0},{0,128},{128,256},{256,384},{385,1},{1,129},{129,257},{257... | collective-permute-start | bytes 3145736 | tf_op jit(solution)/shard_map/ppermute | solution.py:46
  156.5 19.7 %collective-permute-done.14.refs_3_ = bf16[16,64,512]{2,1,0:T(8,128)(2,1)} collective-permute-done((bf16[16,64,512]{2,1,0:T(8,128)(2,1)S(1)}, bf16[16,64,512]{2,1,0:T(8,128)(2,1)}, u32[]{:S(2)}, u32[]{:S(2)}) %collective-permute-start.14) | collective-permute-done | bytes 1048608 | tf_op jit(solution)/shard_map/ppermute | solution.py:46
  176.2 3.4 %shard_map.77.q_ref = bf16[256,512]{1,0:T(8,128)(2,1)S(1)} custom-call(s32[1]{0:T(128)} %bitcast.9.at_ref, bf16[256,4096]{1,0:T(8,128)(2,1)S(1)} %copy-done.2, bf16[16,64,512]{2,1,0:T(8,128)(2,1)S(1)} %shard_map.75.refs_0_, bf16[16,64,512]{2,1,0:T(8,128)(2,1)} %collective-permute-done.12.refs_1_, bf16[16,64,512]{2,1,0:T(8,128)(2,1)} %collective-permute-done.13.refs_2_, ...), custom_call_target="tpu_custom_call" | custom-call | flops 1073741824 | tf_op jit(solution)/shard_map/pallas_call | solution.py:26
  179.6 2.1 shard_map.80.w_ref
  183.8 11.2 %all-to-all-done.2 = bf16[4,32,32,256]{3,2,1,0:T(8,128)(2,1)} async-done(((bf16[4,32,32,256]{3,2,1,0:T(8,128)(2,1)}), bf16[4,32,32,256]{3,2,1,0:T(8,128)(2,1)}, u32[]{:S(2)}, u32[]{:S(2)}) %all-to-all-start.2) | async-done | bytes 2097184 | tf_op jit(solution)/shard_map/all_to_all | solution.py:410
  195.1 4.1 %shard_map.81.m_ref = bf16[256,512]{1,0:T(8,128)(2,1)S(1)} custom-call(s32[2]{0:T(128)S(1)} %pad_add_fusion.1.f_ref, s32[8,16]{1,0:T(8,128)S(1)} %fusion.8.p_ref, bf16[256,512]{1,0:T(8,128)(2,1)S(1)} %shard_map.77.q_ref, bf16[128,32,256]{2,1,0:T(8,128)(2,1)} %bitcast.16.in_ref, bf16[8,32,256]{2,1,0:T(8,128)(2,1)} %bitcast.14.own_ref, ...), custom_call_target="tpu_custom_call" | custom-call | flops 268435456 | tf_op jit(solution)/shard_map/pallas_call | solution.py:26
  199.1 6.1 %collective-permute-start.18 = (bf16[256,512]{1,0:T(8,128)(2,1)S(1)}, bf16[256,512]{1,0:T(8,128)(2,1)S(1)}, u32[]{:S(2)}, u32[]{:S(2)}) collective-permute-start(bf16[256,512]{1,0:T(8,128)(2,1)S(1)} %shard_map.81.m_ref), channel_id=1, source_target_pairs={{1,0},{0,1},{3,2},{2,3},{5,4},{4,5},{7,6},{6,7},{9,8},{8,9},{11,10... | collective-permute-start | bytes 786440 | tf_op jit(solution)/shard_map/ppermute | solution.py:46
  206.4 2.2 %copy-done.1 = bf16[4,1024,512]{2,1,0:T(8,128)(2,1)S(1)} copy-done((bf16[4,1024,512]{2,1,0:T(8,128)(2,1)S(1)}, bf16[4,1024,512]{2,1,0:T(8,128)(2,1)}, u32[]{:S(2)}) %copy-start.1) | copy-done | bytes 4194328
  208.5 2.8 %mix.1 = bf16[256,2048]{1,0:T(8,128)(2,1)} custom-call(s32[2]{0:T(128)S(1)} %pad_add_fusion.p_ref, bf16[256,512]{1,0:T(8,128)(2,1)S(1)} %shard_map.81.m_ref, bf16[256,512]{1,0:T(8,128)(2,1)S(1)} %collective-permute-done.18.t_ref, bf16[4,1024,512]{2,1,0:T(8,128)(2,1)S(1)} %copy-done.1), custom_call_target="tpu_custom_call" | custom-call | flops 1073741824 | tf_op jit(solution)/shard_map/mix/pallas_call | solution.py:359
  (105 shorter events, 30.8 us)
Async XLA Ops:
  35.7 7.0 %copy-start.13 = (bf16[128,128]{1,0:T(8,128)(2,1)S(1)}, bf16[128,128]{1,0:T(8,128)(2,1)}, u32[]{:S(2)}) copy-start(bf16[128,128]{1,0:T(8,128)(2,1)} %get-tuple-element.11.refs_0_) | copy-start | bytes 98308
  35.7 31.6 %copy-start.2 = (bf16[256,4096]{1,0:T(8,128)(2,1)S(1)}, bf16[256,4096]{1,0:T(8,128)(2,1)}, u32[]{:S(2)}) copy-start(bf16[256,4096]{1,0:T(8,128)(2,1)} %t_ref.3) | copy-start | bytes 6291460
  35.7 31.6 %all-to-all-start.1 = ((bf16[16,16,32,128]{3,2,1,0:T(8,128)(2,1)}), bf16[16,16,32,128]{3,2,1,0:T(8,128)(2,1)}, u32[]{:S(2)}, u32[]{:S(2)}) async-start(bf16[16,16,32,128]{3,2,1,0:T(8,128)(2,1)} %broadcast_in_dim.95), calls=%async_computation.1 | async-start | bytes 4194304 | tf_op jit(solution)/shard_map/all_to_all | solution.py:39
  42.7 100.9 %all-gather.2.cloned.1.call-start = ((), (), s32[]{:S(2)}) async-start(), calls=%async_computation.3 | async-start | bytes 2228224 | tf_op jit(solution)/shard_map/all_gather | solution.py:388
  42.7 27.9 %collective-permute-start = (bf16[128,128]{1,0:T(8,128)(2,1)S(1)}, bf16[128,128]{1,0:T(8,128)(2,1)S(1)}, u32[]{:S(2)}, u32[]{:S(2)}) collective-permute-start(bf16[128,128]{1,0:T(8,128)(2,1)S(1)} %copy-done.13), channel_id=1, source_target_pairs={{32,0},{64,32},{96,64},{0,96},{33,1},{65,33},{97,65},{1,97},{34,2}... | collective-permute-start | bytes 98312 | tf_op jit(solution)/shard_map/ppermute | solution.py:46
  47.4 23.3 %collective-permute-start.1 = (bf16[128,128]{1,0:T(8,128)(2,1)S(1)}, bf16[128,128]{1,0:T(8,128)(2,1)S(1)}, u32[]{:S(2)}, u32[]{:S(2)}) collective-permute-start(bf16[128,128]{1,0:T(8,128)(2,1)S(1)} %copy-done.13), channel_id=1, source_target_pairs={{64,0},{96,32},{0,64},{32,96},{65,1},{97,33},{1,65},{33,97},{66,2}... | collective-permute-start | bytes 98312 | tf_op jit(solution)/shard_map/ppermute | solution.py:46
  54.1 16.6 %collective-permute-start.2 = (bf16[128,128]{1,0:T(8,128)(2,1)S(1)}, bf16[128,128]{1,0:T(8,128)(2,1)S(1)}, u32[]{:S(2)}, u32[]{:S(2)}) collective-permute-start(bf16[128,128]{1,0:T(8,128)(2,1)S(1)} %copy-done.13), channel_id=1, source_target_pairs={{96,0},{0,32},{32,64},{64,96},{97,1},{1,33},{33,65},{65,97},{98,2}... | collective-permute-start | bytes 98312 | tf_op jit(solution)/shard_map/ppermute | solution.py:46
  67.3 3.3 %copy-start.12 = (s32[8,16]{1,0:T(8,128)S(1)}, s32[8,16]{1,0:T(8,128)}, u32[]{:S(2)}) copy-start(s32[8,16]{1,0:T(8,128)} %c_ref.1) | copy-start | bytes 1540
  70.7 9.5 %collective-permute-start.3 = (bf16[4,128,128]{2,1,0:T(8,128)(2,1)S(1)}, bf16[4,128,128]{2,1,0:T(8,128)(2,1)S(1)}, u32[]{:S(2)}, u32[]{:S(2)}) collective-permute-start(bf16[4,128,128]{2,1,0:T(8,128)(2,1)S(1)} %shard_map.73.refs_0_), channel_id=1, source_target_pairs={{8,0},{16,8},{24,16},{0,24},{9,1},{17,9},{25,17},{1,25},{10,2},{18... | collective-permute-start | bytes 393224 | tf_op jit(solution)/shard_map/ppermute | solution.py:46
  73.1 7.8 %collective-permute-start.4 = (bf16[4,128,128]{2,1,0:T(8,128)(2,1)S(1)}, bf16[4,128,128]{2,1,0:T(8,128)(2,1)S(1)}, u32[]{:S(2)}, u32[]{:S(2)}) collective-permute-start(bf16[4,128,128]{2,1,0:T(8,128)(2,1)S(1)} %shard_map.73.refs_0_), channel_id=1, source_target_pairs={{16,0},{24,8},{0,16},{8,24},{17,1},{25,9},{1,17},{9,25},{18,2},{26... | collective-permute-start | bytes 393224 | tf_op jit(solution)/shard_map/ppermute | solution.py:46
  78.1 10.9 %collective-permute-start.5 = (bf16[4,128,128]{2,1,0:T(8,128)(2,1)S(1)}, bf16[4,128,128]{2,1,0:T(8,128)(2,1)S(1)}, u32[]{:S(2)}, u32[]{:S(2)}) collective-permute-start(bf16[4,128,128]{2,1,0:T(8,128)(2,1)S(1)} %shard_map.73.refs_0_), channel_id=1, source_target_pairs={{24,0},{0,8},{8,16},{16,24},{25,1},{1,9},{9,17},{17,25},{26,2},{2,... | collective-permute-start | bytes 393224 | tf_op jit(solution)/shard_map/ppermute | solution.py:46
  89.1 18.2 %collective-permute-start.10 = (bf16[16,64,128]{2,1,0:T(8,128)(2,1)S(1)}, bf16[16,64,128]{2,1,0:T(8,128)(2,1)S(1)}, u32[]{:S(2)}, u32[]{:S(2)}) collective-permute-start(bf16[16,64,128]{2,1,0:T(8,128)(2,1)S(1)} %get-tuple-element.14.refs_0_), channel_id=1, source_target_pairs={{256,0},{384,128},{0,256},{128,384},{257,1},{385,129},{1,257},{129... | collective-permute-start | bytes 786440 | tf_op jit(solution)/shard_map/ppermute | solution.py:46
  92.5 34.6 %collective-permute-start.6 = (bf16[17,64,128]{2,1,0:T(8,128)(2,1)S(1)}, bf16[17,64,128]{2,1,0:T(8,128)(2,1)}, u32[]{:S(2)}, u32[]{:S(2)}) collective-permute-start(bf16[17,64,128]{2,1,0:T(8,128)(2,1)S(1)} %get-tuple-element.12.refs_0_), channel_id=1, source_target_pairs={{2,0},{4,2},{6,4},{0,6},{3,1},{5,3},{7,5},{1,7},{10,8},{12,10},{14... | collective-permute-start | bytes 835592 | tf_op jit(solution)/shard_map/ppermute | solution.py:46
  99.2 30.4 %collective-permute-start.7 = (bf16[17,64,128]{2,1,0:T(8,128)(2,1)S(1)}, bf16[17,64,128]{2,1,0:T(8,128)(2,1)}, u32[]{:S(2)}, u32[]{:S(2)}) collective-permute-start(bf16[17,64,128]{2,1,0:T(8,128)(2,1)S(1)} %get-tuple-element.12.refs_0_), channel_id=1, source_target_pairs={{4,0},{6,2},{0,4},{2,6},{5,1},{7,3},{1,5},{3,7},{12,8},{14,10},{8,... | collective-permute-start | bytes 835592 | tf_op jit(solution)/shard_map/ppermute | solution.py:46
  102.6 27.0 %collective-permute-start.8 = (bf16[17,64,128]{2,1,0:T(8,128)(2,1)S(1)}, bf16[17,64,128]{2,1,0:T(8,128)(2,1)}, u32[]{:S(2)}, u32[]{:S(2)}) collective-permute-start(bf16[17,64,128]{2,1,0:T(8,128)(2,1)S(1)} %get-tuple-element.12.refs_0_), channel_id=1, source_target_pairs={{6,0},{0,2},{2,4},{4,6},{7,1},{1,3},{3,5},{5,7},{14,8},{8,10},{10,... | collective-permute-start | bytes 835592 | tf_op jit(solution)/shard_map/ppermute | solution.py:46
  105.3 7.8 %collective-permute-start.11 = (bf16[16,64,128]{2,1,0:T(8,128)(2,1)S(1)}, bf16[16,64,128]{2,1,0:T(8,128)(2,1)S(1)}, u32[]{:S(2)}, u32[]{:S(2)}) collective-permute-start(bf16[16,64,128]{2,1,0:T(8,128)(2,1)S(1)} %get-tuple-element.14.refs_0_), channel_id=1, source_target_pairs={{384,0},{0,128},{128,256},{256,384},{385,1},{1,129},{129,257},{257... | collective-permute-start | bytes 786440 | tf_op jit(solution)/shard_map/ppermute | solution.py:46
  108.0 8.7 %collective-permute-start.9 = (bf16[16,64,128]{2,1,0:T(8,128)(2,1)S(1)}, bf16[16,64,128]{2,1,0:T(8,128)(2,1)S(1)}, u32[]{:S(2)}, u32[]{:S(2)}) collective-permute-start(bf16[16,64,128]{2,1,0:T(8,128)(2,1)S(1)} %get-tuple-element.14.refs_0_), channel_id=1, source_target_pairs={{128,0},{256,128},{384,256},{0,384},{129,1},{257,129},{385,257},{1... | collective-permute-start | bytes 786440 | tf_op jit(solution)/shard_map/ppermute | solution.py:46
  117.4 1.0 copy-start.5
  118.3 0.9 copy-start.7
  119.3 0.9 copy-start.9
  120.2 1.0 copy-start.11
  121.4 30.4 %collective-permute-start.12 = (bf16[16,64,512]{2,1,0:T(8,128)(2,1)S(1)}, bf16[16,64,512]{2,1,0:T(8,128)(2,1)}, u32[]{:S(2)}, u32[]{:S(2)}) collective-permute-start(bf16[16,64,512]{2,1,0:T(8,128)(2,1)S(1)} %shard_map.75.refs_0_), channel_id=1, source_target_pairs={{2,0},{4,2},{6,4},{0,6},{3,1},{5,3},{7,5},{1,7},{10,8},{12,10},{14... | collective-permute-start | bytes 3145736 | tf_op jit(solution)/shard_map/ppermute | solution.py:46
  125.2 31.3 %collective-permute-start.13 = (bf16[16,64,512]{2,1,0:T(8,128)(2,1)S(1)}, bf16[16,64,512]{2,1,0:T(8,128)(2,1)}, u32[]{:S(2)}, u32[]{:S(2)}) collective-permute-start(bf16[16,64,512]{2,1,0:T(8,128)(2,1)S(1)} %shard_map.75.refs_0_), channel_id=1, source_target_pairs={{4,0},{6,2},{0,4},{2,6},{5,1},{7,3},{1,5},{3,7},{12,8},{14,10},{8,... | collective-permute-start | bytes 3145736 | tf_op jit(solution)/shard_map/ppermute | solution.py:46
  127.1 49.1 %collective-permute-start.14 = (bf16[16,64,512]{2,1,0:T(8,128)(2,1)S(1)}, bf16[16,64,512]{2,1,0:T(8,128)(2,1)}, u32[]{:S(2)}, u32[]{:S(2)}) collective-permute-start(bf16[16,64,512]{2,1,0:T(8,128)(2,1)S(1)} %shard_map.75.refs_0_), channel_id=1, source_target_pairs={{6,0},{0,2},{2,4},{4,6},{7,1},{1,3},{3,5},{5,7},{14,8},{8,10},{10,... | collective-permute-start | bytes 3145736 | tf_op jit(solution)/shard_map/ppermute | solution.py:46
  131.9 47.7 %collective-permute-start.15 = (bf16[1024,512]{1,0:T(8,128)(2,1)}, bf16[1024,512]{1,0:T(8,128)(2,1)}, u32[]{:S(2)}, u32[]{:S(2)}) collective-permute-start(bf16[1024,512]{1,0:T(8,128)(2,1)} %bitcast.17.refs_0_), channel_id=1, source_target_pairs={{128,0},{256,128},{384,256},{0,384},{129,1},{257,129},{385,257},{1... | collective-permute-start | bytes 3145736 | tf_op jit(solution)/shard_map/ppermute | solution.py:46
  134.0 45.6 %collective-permute-start.16 = (bf16[1024,512]{1,0:T(8,128)(2,1)}, bf16[1024,512]{1,0:T(8,128)(2,1)}, u32[]{:S(2)}, u32[]{:S(2)}) collective-permute-start(bf16[1024,512]{1,0:T(8,128)(2,1)} %bitcast.17.refs_0_), channel_id=1, source_target_pairs={{256,0},{384,128},{0,256},{128,384},{257,1},{385,129},{1,257},{129... | collective-permute-start | bytes 3145736 | tf_op jit(solution)/shard_map/ppermute | solution.py:46
  143.6 1.6 copy-start.3
  147.2 47.8 %all-to-all-start.2 = ((bf16[4,32,32,256]{3,2,1,0:T(8,128)(2,1)}), bf16[4,32,32,256]{3,2,1,0:T(8,128)(2,1)}, u32[]{:S(2)}, u32[]{:S(2)}) async-start(bf16[4,32,32,256]{3,2,1,0:T(8,128)(2,1)} %shard_map.76), calls=%async_computation.2 | async-start | bytes 4194304 | tf_op jit(solution)/shard_map/all_to_all | solution.py:410
  151.7 27.9 %collective-permute-start.17 = (bf16[1024,512]{1,0:T(8,128)(2,1)}, bf16[1024,512]{1,0:T(8,128)(2,1)S(1)}, u32[]{:S(2)}, u32[]{:S(2)}) collective-permute-start(bf16[1024,512]{1,0:T(8,128)(2,1)} %bitcast.17.refs_0_), channel_id=1, source_target_pairs={{384,0},{0,128},{128,256},{256,384},{385,1},{1,129},{129,257},{257... | collective-permute-start | bytes 3145736 | tf_op jit(solution)/shard_map/ppermute | solution.py:46
  181.8 2.0 copy-start
  199.1 7.2 %collective-permute-start.18 = (bf16[256,512]{1,0:T(8,128)(2,1)S(1)}, bf16[256,512]{1,0:T(8,128)(2,1)S(1)}, u32[]{:S(2)}, u32[]{:S(2)}) collective-permute-start(bf16[256,512]{1,0:T(8,128)(2,1)S(1)} %shard_map.81.m_ref), channel_id=1, source_target_pairs={{1,0},{0,1},{3,2},{2,3},{5,4},{4,5},{7,6},{6,7},{9,8},{8,9},{11,10... | collective-permute-start | bytes 786440 | tf_op jit(solution)/shard_map/ppermute | solution.py:46
  206.4 2.2 %copy-start.1 = (bf16[4,1024,512]{2,1,0:T(8,128)(2,1)S(1)}, bf16[4,1024,512]{2,1,0:T(8,128)(2,1)}, u32[]{:S(2)}) copy-start(bf16[4,1024,512]{2,1,0:T(8,128)(2,1)} %copy-done) | copy-start | bytes 12582916
  (4 other events, 2.8 us)
Sparse Core Ops, SparseCore 0:
  70.7 60.8 all-gather.1
